TPU v7x, 512 devices: a whole 4x4x16 slice. The times are simulated.
512 devices in a mesh: rep: 2 (over z_hi), fs: 32 (over z_lo, y), tp: 8 (over x, core).
Axes of the slice: x: 4, y: 4, z: 16 (z_hi: 2, z_lo: 8; z = z_hi * 8 + z_lo), core: 2. Of those that a mesh axis runs over, the one named last changes fastest.
Arguments:
- inputs: bfloat16 [24576, 2048], P(('rep', 'fs')), may hold values from -16 to 16
- w_up: bfloat16 [2048, 4096], P('fs', 'tp'), may hold values from -0.125 to 0.125
- w_down: bfloat16 [4096, 2048], P('tp', 'fs'), may hold values from -0.09375 to 0.09375
- cotangent: bfloat16 [24576, 2048], P(('rep', 'fs')), may hold values from -16 to 16
Outputs:
- d_inputs: bfloat16 [24576, 2048], P(('rep', 'fs'))
- d_w_up: float32 [2048, 4096], P('fs', 'tp')
All inputs are finite; a program needn't handle non-finite values.
Results may differ from a plain program's by a relative error of at most 0.014.
Values may be sent and summed in bfloat16 or wider, within the bound.
No kernel may reach another device: no remote copies, remote signals or barrier semaphores. Data moves between devices by JAX's collectives and lax.ppermute only.
A program may use at most 64 MiB of HBM per device.

v0:
```python
import jax
import jax.numpy as jnp
from jax import lax
from jax.experimental import pallas as pl
from jax.experimental.pallas import tpu as pltpu
from jax.sharding import Mesh
from jax.sharding import PartitionSpec as P


FS = ("zh", "zl", "y")
REP_FS = ("rep", "zh", "zl", "y")
Z = ("rep", "zh", "zl")
TP = ("x", "core")
N_Z = 8
N_Y = 4

BF = jnp.bfloat16
F32 = jnp.float32
NEAR = (0, 1, -1, 2, -2)
FAR = (3, -3, 4)


def exchange(parts, axes):
    return lax.all_to_all(parts, axes, split_axis=0, concat_axis=0, tiled=True)


def copies_over(value, axes):
    n = lax.axis_size(axes)
    copies = jnp.broadcast_to(value, (n, *value.shape))
    return exchange(copies, axes)


def shifted(value, axes, step):
    n = lax.axis_size(axes)
    return lax.ppermute(value, axes, [(i, (i + step) % n) for i in range(n)])


def swapped(value, axes, partner):
    n = lax.axis_size(axes)
    return lax.ppermute(value, axes, [(i, partner(i)) for i in range(n)])


def z_blocks(*groups):
    me = lax.axis_index("zh") * 4 + lax.axis_index("zl")
    for ref, shifts in groups:
        for k, shift in enumerate(shifts):
            yield ref, k, lax.rem(me - shift + 2 * N_Z, N_Z)


def rows_of(ref, k, part):
    rows = ref.shape[2] // 2
    at = slice(part * rows, (part + 1) * rows)
    return jnp.concatenate([ref[y, k, at] for y in range(N_Y)], axis=0)


def add_products(x_ref, c_ref, ref, shifts, pre_acc, hid_acc, fresh):
    width = N_Y * ref.shape[2] // 2
    for ref, k, z in z_blocks((ref, shifts)):
        at = pl.ds(pl.multiple_of(z * width, width), width)
        pre = jnp.dot(x_ref[:, at], rows_of(ref, k, 0), preferred_element_type=F32)
        hid = jnp.dot(c_ref[:, at], rows_of(ref, k, 1), preferred_element_type=F32)
        if fresh and k == 0:
            pre_acc[...] = pre
            hid_acc[...] = hid
        else:
            pre_acc[...] += pre
            hid_acc[...] += hid


def near_kernel(x_ref, c_ref, near_ref, pre_ref, hid_ref):
    add_products(x_ref, c_ref, near_ref, NEAR, pre_ref, hid_ref, True)


def weight_kernel(
    x_ref, c_ref, far_ref, pre_ref, hid_ref, grad_ref, dw_ref, pre_acc, hid_acc
):
    rows = far_ref.shape[2] // 2
    width = N_Y * rows
    pre_acc[...] = pre_ref[...]
    hid_acc[...] = hid_ref[...]
    add_products(x_ref, c_ref, far_ref, FAR, pre_acc, hid_acc, False)
    grad_ref[...] = (2.0 * jnp.maximum(pre_acc[...], 0.0) * hid_acc[...]).astype(BF)
    for z in range(N_Z):
        dw = lax.dot_general(
            x_ref[:, z * width : (z + 1) * width], grad_ref[...],
            (((0,), (0,)), ((), ())), preferred_element_type=F32,
        ).astype(BF)
        for y in range(N_Y):
            dw_ref[y, z % 4, z // 4] = dw[y * rows : (y + 1) * rows]


def input_kernel(grad_ref, near_ref, far_ref, keep_ref, give_ref):
    core = lax.axis_index("core")
    tokens = keep_ref.shape[0]
    width = N_Y * near_ref.shape[2] // 2
    for out, which in ((give_ref, 1 - core), (keep_ref, core)):
        mine = grad_ref[pl.ds(pl.multiple_of(which * tokens, tokens), tokens), :]
        for ref, k, z in z_blocks((near_ref, NEAR), (far_ref, FAR)):
            out[:, pl.ds(pl.multiple_of(z * width, width), width)] = lax.dot_general(
                mine, rows_of(ref, k, 0), (((1,), (1,)), ((), ())),
                preferred_element_type=F32,
            ).astype(BF)


def call(kernel, outs, args, flops, scratch=(), dtype=BF):
    vm = pl.BlockSpec(memory_space=pltpu.VMEM)
    return pl.pallas_call(
        kernel,
        out_shape=tuple(jax.ShapeDtypeStruct(s, dtype) for s in outs),
        in_specs=[vm] * len(args),
        out_specs=(vm,) * len(outs),
        scratch_shapes=scratch,
        cost_estimate=pl.CostEstimate(
            flops=flops,
            bytes_accessed=2 * sum(a.size for a in args),
            transcendentals=0,
        ),
    )(*args)


def total(a, b):
    return (a.astype(F32) + b.astype(F32)).astype(BF)


def per_device(inputs, w_up, w_down, cotangent):
    rows, h = w_up.shape
    tokens, width = inputs.shape
    own = jnp.concatenate([w_up, w_down.T], axis=0)
    back = [shifted(own, Z, 1)]
    ahead = [shifted(own, Z, -1)]
    back.append(shifted(own, Z, 2))
    ahead.append(shifted(own, Z, -2))
    near = jnp.stack([own, back[0], ahead[0], back[1], ahead[1]])
    near = copies_over(near, "y")
    back = shifted(jnp.concatenate([back[0], back[1][:rows]], axis=0), Z, 2)
    ahead = shifted(jnp.concatenate([ahead[0], ahead[1][rows:]], axis=0), Z, -2)
    last = jnp.concatenate([back[2 * rows :], ahead[2 * rows :]], axis=0)
    far = jnp.stack([back[: 2 * rows], ahead[: 2 * rows], last])
    far = copies_over(far, "y")
    unit = tokens * width * h // 2
    pre, hid = call(
        near_kernel, [(tokens, h)] * 2, (inputs, cotangent, near), 5 * unit, dtype=F32
    )
    grad, dw = call(
        weight_kernel,
        [(tokens, h), (N_Y, 4, 2, rows, h)],
        (inputs, cotangent, far, pre, hid),
        7 * unit,
        [pltpu.VMEM((tokens, h), F32)] * 2,
    )
    keep, give = call(
        input_kernel, [(tokens // 2, width)] * 2, (grad, near, far), 4 * unit
    )

    over_core = total(keep, swapped(give, "core", lambda i: 1 - i))
    over_pair = total(over_core, swapped(over_core, "x", lambda i: i ^ 1))
    mine = total(over_pair, swapped(over_pair, "x", lambda i: 3 - i))
    other = swapped(mine, "core", lambda i: 1 - i)
    first = lax.axis_index("core") == 0
    d_inputs = jnp.concatenate(
        [jnp.where(first, mine, other), jnp.where(first, other, mine)], axis=0
    )

    by_y = exchange(dw, "y")
    over_y = by_y.astype(F32).sum(0).astype(BF)
    over_near = exchange(over_y, "zl").astype(F32).sum(0).astype(BF)
    to_far = jnp.broadcast_to(over_near, (2, *over_near.shape))
    d_w_up = exchange(to_far.reshape(4, rows, h), ("rep", "zh")).astype(F32).sum(0)
    return (d_inputs, d_w_up)


def solution(mesh):
    split = Mesh(
        mesh.devices.reshape(2, 2, 4, N_Y, 4, 2),
        ("rep", "zh", "zl", "y", "x", "core"),
    )
    placed = (P(REP_FS, None), P(FS, TP), P(TP, FS), P(REP_FS, None))
    return jax.shard_map(
        per_device,
        mesh=split,
        in_specs=placed,
        out_specs=(P(REP_FS, None), P(FS, TP)),
        check_vma=False,
    )
```

profile of v0, /device:TPU:4, one launch (start us, length us, event | category | flops | bytes accessed | tf_op | source)
XLA Modules:
  0.0 189.0 jit_solution(1491376398317810928)
XLA Ops:
  0.6 0.9 pad_maximum_fusion.4
  1.5 3.8 %collective-permute-start = (bf16[128,512]{1,0:T(8,128)(2,1)S(1)}, bf16[128,512]{1,0:T(8,128)(2,1)S(1)}, u32[]{:S(2)}, u32[]{:S(2)}) collective-permute-start(bf16[128,512]{1,0:T(8,128)(2,1)S(1)} %pad_maximum_fusion.4), channel_id=1, source_target_pairs={{0,32},{32,64},{64,96},{96,128},{128,160},{160,192},{192,224},{224... | collective-permute-start | bytes 393224 | tf_op jit(solution)/shard_map/ppermute | solution.py:35
  5.3 5.2 %collective-permute-start.1 = (bf16[128,512]{1,0:T(8,128)(2,1)S(1)}, bf16[128,512]{1,0:T(8,128)(2,1)S(1)}, u32[]{:S(2)}, u32[]{:S(2)}) collective-permute-start(bf16[128,512]{1,0:T(8,128)(2,1)S(1)} %pad_maximum_fusion.4), channel_id=1, source_target_pairs={{0,64},{32,96},{64,128},{96,160},{128,192},{160,224},{192,256},{22... | collective-permute-start | bytes 393224 | tf_op jit(solution)/shard_map/ppermute | solution.py:35
  10.5 7.7 %collective-permute-start.4 = (bf16[128,512]{1,0:T(8,128)(2,1)S(1)}, bf16[128,512]{1,0:T(8,128)(2,1)S(1)}, u32[]{:S(2)}, u32[]{:S(2)}) collective-permute-start(bf16[128,512]{1,0:T(8,128)(2,1)S(1)} %pad_maximum_fusion.4), channel_id=1, source_target_pairs={{0,448},{32,480},{64,0},{96,32},{128,64},{160,96},{192,128},{224,1... | collective-permute-start | bytes 393224 | tf_op jit(solution)/shard_map/ppermute | solution.py:35
  18.2 3.4 %collective-permute-start.3 = (bf16[128,512]{1,0:T(8,128)(2,1)S(1)}, bf16[128,512]{1,0:T(8,128)(2,1)S(1)}, u32[]{:S(2)}, u32[]{:S(2)}) collective-permute-start(bf16[128,512]{1,0:T(8,128)(2,1)S(1)} %pad_maximum_fusion.4), channel_id=1, source_target_pairs={{0,480},{32,0},{64,32},{96,64},{128,96},{160,128},{192,160},{224,1... | collective-permute-start | bytes 393224 | tf_op jit(solution)/shard_map/ppermute | solution.py:35
  21.6 0.9 bitcast_dynamic-update-slice_fusion.4
  22.5 0.0 collective-permute-done
  22.5 3.5 %collective-permute-done.3 = bf16[128,512]{1,0:T(8,128)(2,1)S(1)} collective-permute-done((bf16[128,512]{1,0:T(8,128)(2,1)S(1)}, bf16[128,512]{1,0:T(8,128)(2,1)S(1)}, u32[]{:S(2)}, u32[]{:S(2)}) %collective-permute-start.3) | collective-permute-done | bytes 131104 | tf_op jit(solution)/shard_map/ppermute | solution.py:35
  26.1 0.0 collective-permute-done.1
  26.1 0.0 collective-permute-done.4
  26.1 1.8 broadcast_in_dim.10
  27.9 4.5 %all-to-all-start.1 = ((bf16[4,5,128,512]{3,2,1,0:T(8,128)(2,1)}), bf16[4,5,128,512]{3,2,1,0:T(8,128)(2,1)S(1)}, u32[]{:S(2)}, u32[]{:S(2)}) async-start(bf16[4,5,128,512]{3,2,1,0:T(8,128)(2,1)} %broadcast_in_dim.10), calls=%async_computation.1 | async-start | bytes 5242880 | tf_op jit(solution)/shard_map/all_to_all | solution.py:24
  32.4 3.3 %collective-permute-start.2 = (bf16[192,512]{1,0:T(8,128)(2,1)S(1)}, bf16[192,512]{1,0:T(8,128)(2,1)S(1)}, u32[]{:S(2)}, u32[]{:S(2)}) collective-permute-start(bf16[192,512]{1,0:T(8,128)(2,1)S(1)} %pad_maximum_fusion.2), channel_id=1, source_target_pairs={{0,64},{32,96},{64,128},{96,160},{128,192},{160,224},{192,256},{22... | collective-permute-start | bytes 589832 | tf_op jit(solution)/shard_map/ppermute | solution.py:35
  35.7 4.7 %collective-permute-start.5 = (bf16[192,512]{1,0:T(8,128)(2,1)S(1)}, bf16[192,512]{1,0:T(8,128)(2,1)S(1)}, u32[]{:S(2)}, u32[]{:S(2)}) collective-permute-start(bf16[192,512]{1,0:T(8,128)(2,1)S(1)} %pad_maximum_fusion.3), channel_id=1, source_target_pairs={{0,448},{32,480},{64,0},{96,32},{128,64},{160,96},{192,128},{224,1... | collective-permute-start | bytes 589832 | tf_op jit(solution)/shard_map/ppermute | solution.py:35
  40.4 4.1 %collective-permute-done.2 = bf16[192,512]{1,0:T(8,128)(2,1)S(1)} collective-permute-done((bf16[192,512]{1,0:T(8,128)(2,1)S(1)}, bf16[192,512]{1,0:T(8,128)(2,1)S(1)}, u32[]{:S(2)}, u32[]{:S(2)}) %collective-permute-start.2) | collective-permute-done | bytes 196640 | tf_op jit(solution)/shard_map/ppermute | solution.py:35
  44.5 5.5 %collective-permute-done.5 = bf16[192,512]{1,0:T(8,128)(2,1)S(1)} collective-permute-done((bf16[192,512]{1,0:T(8,128)(2,1)S(1)}, bf16[192,512]{1,0:T(8,128)(2,1)S(1)}, u32[]{:S(2)}, u32[]{:S(2)}) %collective-permute-start.5) | collective-permute-done | bytes 196640 | tf_op jit(solution)/shard_map/ppermute | solution.py:35
  50.1 14.4 %all-to-all-done.1.near_ref = bf16[4,5,128,512]{3,2,1,0:T(8,128)(2,1)S(1)} async-done(((bf16[4,5,128,512]{3,2,1,0:T(8,128)(2,1)}), bf16[4,5,128,512]{3,2,1,0:T(8,128)(2,1)S(1)}, u32[]{:S(2)}, u32[]{:S(2)}) %all-to-all-start.1) | async-done | bytes 2621472 | tf_op jit(solution)/shard_map/all_to_all | solution.py:24
  64.5 0.0 copy-start
  64.5 1.4 broadcast_in_dim.9
  65.9 0.7 copy-done
  66.6 4.3 %all-to-all-start = ((bf16[4,3,128,512]{3,2,1,0:T(8,128)(2,1)}), bf16[4,3,128,512]{3,2,1,0:T(8,128)(2,1)}, u32[]{:S(2)}, u32[]{:S(2)}) async-start(bf16[4,3,128,512]{3,2,1,0:T(8,128)(2,1)} %broadcast_in_dim.9), calls=%async_computation | async-start | bytes 3145728 | tf_op jit(solution)/shard_map/all_to_all | solution.py:24
  71.0 4.9 %shard_map.59 = (f32[384,512]{1,0:T(8,128)}, f32[384,512]{1,0:T(8,128)}) custom-call(bf16[384,2048]{1,0:T(8,128)(2,1)} %x_ref.3, bf16[384,2048]{1,0:T(8,128)(2,1)} %c_ref.3, bf16[4,5,128,512]{3,2,1,0:T(8,128)(2,1)} %copy-done), custom_call_target="tpu_custom_call" | custom-call | flops 1006632960 | bytes 5767168 | tf_op jit(solution)/shard_map/pallas_call | solution.py:107
  75.9 15.2 %all-to-all-done.far_ref = bf16[4,3,128,512]{3,2,1,0:T(8,128)(2,1)} async-done(((bf16[4,3,128,512]{3,2,1,0:T(8,128)(2,1)}), bf16[4,3,128,512]{3,2,1,0:T(8,128)(2,1)}, u32[]{:S(2)}, u32[]{:S(2)}) %all-to-all-start) | async-done | bytes 1572896 | tf_op jit(solution)/shard_map/all_to_all | solution.py:24
  91.0 6.1 %shard_map.60 = (bf16[384,512]{1,0:T(8,128)(2,1)}, bf16[4,4,2,64,512]{4,3,2,1,0:T(8,128)(2,1)}) custom-call(bf16[384,2048]{1,0:T(8,128)(2,1)} %x_ref.3, bf16[384,2048]{1,0:T(8,128)(2,1)} %c_ref.3, bf16[4,3,128,512]{3,2,1,0:T(8,128)(2,1)} %all-to-all-done.far_ref, f32[384,512]{1,0:T(8,128)} %get-tuple-element.8.pre_ref, f32[384,512]{1,0:T(8,128)} %get-tuple-element.9.hid_ref), custom_call_target="tpu_custom_call" | custom-call | flops 1409286144 | bytes 5505024 | tf_op jit(solution)/shard_map/pallas_call | solution.py:107
  97.2 4.8 %shard_map.61 = (bf16[192,2048]{1,0:T(8,128)(2,1)}, bf16[192,2048]{1,0:T(8,128)(2,1)}) custom-call(bf16[384,512]{1,0:T(8,128)(2,1)} %get-tuple-element.10.grad_ref, bf16[4,5,128,512]{3,2,1,0:T(8,128)(2,1)} %copy-done, bf16[4,3,128,512]{3,2,1,0:T(8,128)(2,1)} %all-to-all-done.far_ref), custom_call_target="tpu_custom_call" | custom-call | flops 805306368 | bytes 4587520 | tf_op jit(solution)/shard_map/pallas_call | solution.py:107
  102.0 1.9 %collective-permute-start.6 = (bf16[192,2048]{1,0:T(8,128)(2,1)}, bf16[192,2048]{1,0:T(8,128)(2,1)S(1)}, u32[]{:S(2)}, u32[]{:S(2)}) collective-permute-start(bf16[192,2048]{1,0:T(8,128)(2,1)} %get-tuple-element.12), channel_id=1, source_target_pairs={{0,1},{1,0},{2,3},{3,2},{4,5},{5,4},{6,7},{7,6},{8,9},{9,8},{10,11... | collective-permute-start | bytes 2359304 | tf_op jit(solution)/shard_map/ppermute | solution.py:40
  103.9 2.5 %collective-permute-done.6 = bf16[192,2048]{1,0:T(8,128)(2,1)S(1)} collective-permute-done((bf16[192,2048]{1,0:T(8,128)(2,1)}, bf16[192,2048]{1,0:T(8,128)(2,1)S(1)}, u32[]{:S(2)}, u32[]{:S(2)}) %collective-permute-start.6) | collective-permute-done | bytes 786464 | tf_op jit(solution)/shard_map/ppermute | solution.py:40
  106.4 1.4 add_convert_fusion.2
  107.8 0.0 copy-start.1
  107.8 3.1 %collective-permute-start.7 = (bf16[192,2048]{1,0:T(8,128)(2,1)S(1)}, bf16[192,2048]{1,0:T(8,128)(2,1)}, u32[]{:S(2)}, u32[]{:S(2)}) collective-permute-start(bf16[192,2048]{1,0:T(8,128)(2,1)S(1)} %add_convert_fusion.2), channel_id=1, source_target_pairs={{0,2},{2,0},{4,6},{6,4},{1,3},{3,1},{5,7},{7,5},{8,10},{10,8},{12,... | collective-permute-start | bytes 2359304 | tf_op jit(solution)/shard_map/ppermute | solution.py:40
  110.9 0.0 copy-done.1
  110.9 3.6 %all-to-all-start.2 = ((bf16[4,4,2,64,512]{4,3,2,1,0:T(8,128)(2,1)}), bf16[4,4,2,64,512]{4,3,2,1,0:T(8,128)(2,1)S(1)}, u32[]{:S(2)}, u32[]{:S(2)}) async-start(bf16[4,4,2,64,512]{4,3,2,1,0:T(8,128)(2,1)} %get-tuple-element.13), calls=%async_computation.2 | async-start | bytes 4194304 | tf_op jit(solution)/shard_map/all_to_all | solution.py:24
  114.6 14.8 %collective-permute-done.7 = bf16[192,2048]{1,0:T(8,128)(2,1)} collective-permute-done((bf16[192,2048]{1,0:T(8,128)(2,1)S(1)}, bf16[192,2048]{1,0:T(8,128)(2,1)}, u32[]{:S(2)}, u32[]{:S(2)}) %collective-permute-start.7) | collective-permute-done | bytes 786464 | tf_op jit(solution)/shard_map/ppermute | solution.py:40
  129.4 1.6 add_convert_fusion.1
  131.0 2.4 %collective-permute-start.8 = (bf16[192,2048]{1,0:T(8,128)(2,1)S(1)}, bf16[192,2048]{1,0:T(8,128)(2,1)}, u32[]{:S(2)}, u32[]{:S(2)}) collective-permute-start(bf16[192,2048]{1,0:T(8,128)(2,1)S(1)} %add_convert_fusion.1), channel_id=1, source_target_pairs={{0,6},{2,4},{4,2},{6,0},{1,7},{3,5},{5,3},{7,1},{8,14},{10,12},{12... | collective-permute-start | bytes 2359304 | tf_op jit(solution)/shard_map/ppermute | solution.py:40
  133.5 7.7 %all-to-all-done.2 = bf16[4,4,2,64,512]{4,3,2,1,0:T(8,128)(2,1)S(1)} async-done(((bf16[4,4,2,64,512]{4,3,2,1,0:T(8,128)(2,1)}), bf16[4,4,2,64,512]{4,3,2,1,0:T(8,128)(2,1)S(1)}, u32[]{:S(2)}, u32[]{:S(2)}) %all-to-all-start.2) | async-done | bytes 2097184 | tf_op jit(solution)/shard_map/all_to_all | solution.py:24
  141.2 1.3 reduce_sum.33
  142.4 3.5 %all-to-all-start.3 = ((bf16[4,2,64,512]{3,2,1,0:T(8,128)(2,1)}), bf16[4,2,64,512]{3,2,1,0:T(8,128)(2,1)S(1)}, u32[]{:S(2)}, u32[]{:S(2)}) async-start(bf16[4,2,64,512]{3,2,1,0:T(8,128)(2,1)} %reduce_sum.33), calls=%async_computation.3 | async-start | bytes 1048576 | tf_op jit(solution)/shard_map/all_to_all | solution.py:24
  145.9 5.9 %collective-permute-done.8 = bf16[192,2048]{1,0:T(8,128)(2,1)} collective-permute-done((bf16[192,2048]{1,0:T(8,128)(2,1)S(1)}, bf16[192,2048]{1,0:T(8,128)(2,1)}, u32[]{:S(2)}, u32[]{:S(2)}) %collective-permute-start.8) | collective-permute-done | bytes 786464 | tf_op jit(solution)/shard_map/ppermute | solution.py:40
  151.8 1.4 add_convert_fusion
  153.2 1.9 %collective-permute-start.9 = (bf16[192,2048]{1,0:T(8,128)(2,1)S(1)}, bf16[192,2048]{1,0:T(8,128)(2,1)S(1)}, u32[]{:S(2)}, u32[]{:S(2)}) collective-permute-start(bf16[192,2048]{1,0:T(8,128)(2,1)S(1)} %add_convert_fusion), channel_id=1, source_target_pairs={{0,1},{1,0},{2,3},{3,2},{4,5},{5,4},{6,7},{7,6},{8,9},{9,8},{10,11... | collective-permute-start | bytes 2359304 | tf_op jit(solution)/shard_map/ppermute | solution.py:40
  155.1 4.7 %all-to-all-done.3 = bf16[4,2,64,512]{3,2,1,0:T(8,128)(2,1)S(1)} async-done(((bf16[4,2,64,512]{3,2,1,0:T(8,128)(2,1)}), bf16[4,2,64,512]{3,2,1,0:T(8,128)(2,1)S(1)}, u32[]{:S(2)}, u32[]{:S(2)}) %all-to-all-start.3) | async-done | bytes 524320 | tf_op jit(solution)/shard_map/all_to_all | solution.py:24
  159.8 0.1 reduce_sum.34
  159.9 0.7 broadcast_in_dim.11
  160.6 9.3 %all-to-all-start.4 = ((bf16[4,64,512]{2,1,0:T(8,128)(2,1)}), bf16[4,64,512]{2,1,0:T(8,128)(2,1)S(1)}, u32[]{:S(2)}, u32[]{:S(2)}) async-start(bf16[4,64,512]{2,1,0:T(8,128)(2,1)} %bitcast.9), calls=%async_computation.4 | async-start | bytes 524288 | tf_op jit(solution)/shard_map/all_to_all | solution.py:24
  169.9 0.0 collective-permute-done.9
  169.9 0.1 broadcast_select_fusion.1
  170.0 1.2 pad_maximum_fusion
  171.2 17.1 %all-to-all-done.4 = bf16[4,64,512]{2,1,0:T(8,128)(2,1)S(1)} async-done(((bf16[4,64,512]{2,1,0:T(8,128)(2,1)}), bf16[4,64,512]{2,1,0:T(8,128)(2,1)S(1)}, u32[]{:S(2)}, u32[]{:S(2)}) %all-to-all-start.4) | async-done | bytes 262176 | tf_op jit(solution)/shard_map/all_to_all | solution.py:24
  188.4 0.7 convert_reduce_fusion
  (14 shorter events, 0.2 us)
Async XLA Ops:
  1.5 21.0 %collective-permute-start = (bf16[128,512]{1,0:T(8,128)(2,1)S(1)}, bf16[128,512]{1,0:T(8,128)(2,1)S(1)}, u32[]{:S(2)}, u32[]{:S(2)}) collective-permute-start(bf16[128,512]{1,0:T(8,128)(2,1)S(1)} %pad_maximum_fusion.4), channel_id=1, source_target_pairs={{0,32},{32,64},{64,96},{96,128},{128,160},{160,192},{192,224},{224... | collective-permute-start | bytes 393224 | tf_op jit(solution)/shard_map/ppermute | solution.py:35
  5.3 20.7 %collective-permute-start.1 = (bf16[128,512]{1,0:T(8,128)(2,1)S(1)}, bf16[128,512]{1,0:T(8,128)(2,1)S(1)}, u32[]{:S(2)}, u32[]{:S(2)}) collective-permute-start(bf16[128,512]{1,0:T(8,128)(2,1)S(1)} %pad_maximum_fusion.4), channel_id=1, source_target_pairs={{0,64},{32,96},{64,128},{96,160},{128,192},{160,224},{192,256},{22... | collective-permute-start | bytes 393224 | tf_op jit(solution)/shard_map/ppermute | solution.py:35
  10.5 15.6 %collective-permute-start.4 = (bf16[128,512]{1,0:T(8,128)(2,1)S(1)}, bf16[128,512]{1,0:T(8,128)(2,1)S(1)}, u32[]{:S(2)}, u32[]{:S(2)}) collective-permute-start(bf16[128,512]{1,0:T(8,128)(2,1)S(1)} %pad_maximum_fusion.4), channel_id=1, source_target_pairs={{0,448},{32,480},{64,0},{96,32},{128,64},{160,96},{192,128},{224,1... | collective-permute-start | bytes 393224 | tf_op jit(solution)/shard_map/ppermute | solution.py:35
  18.2 7.8 %collective-permute-start.3 = (bf16[128,512]{1,0:T(8,128)(2,1)S(1)}, bf16[128,512]{1,0:T(8,128)(2,1)S(1)}, u32[]{:S(2)}, u32[]{:S(2)}) collective-permute-start(bf16[128,512]{1,0:T(8,128)(2,1)S(1)} %pad_maximum_fusion.4), channel_id=1, source_target_pairs={{0,480},{32,0},{64,32},{96,64},{128,96},{160,128},{192,160},{224,1... | collective-permute-start | bytes 393224 | tf_op jit(solution)/shard_map/ppermute | solution.py:35
  27.9 36.6 %all-to-all-start.1 = ((bf16[4,5,128,512]{3,2,1,0:T(8,128)(2,1)}), bf16[4,5,128,512]{3,2,1,0:T(8,128)(2,1)S(1)}, u32[]{:S(2)}, u32[]{:S(2)}) async-start(bf16[4,5,128,512]{3,2,1,0:T(8,128)(2,1)} %broadcast_in_dim.10), calls=%async_computation.1 | async-start | bytes 5242880 | tf_op jit(solution)/shard_map/all_to_all | solution.py:24
  32.4 12.1 %collective-permute-start.2 = (bf16[192,512]{1,0:T(8,128)(2,1)S(1)}, bf16[192,512]{1,0:T(8,128)(2,1)S(1)}, u32[]{:S(2)}, u32[]{:S(2)}) collective-permute-start(bf16[192,512]{1,0:T(8,128)(2,1)S(1)} %pad_maximum_fusion.2), channel_id=1, source_target_pairs={{0,64},{32,96},{64,128},{96,160},{128,192},{160,224},{192,256},{22... | collective-permute-start | bytes 589832 | tf_op jit(solution)/shard_map/ppermute | solution.py:35
  35.7 14.3 %collective-permute-start.5 = (bf16[192,512]{1,0:T(8,128)(2,1)S(1)}, bf16[192,512]{1,0:T(8,128)(2,1)S(1)}, u32[]{:S(2)}, u32[]{:S(2)}) collective-permute-start(bf16[192,512]{1,0:T(8,128)(2,1)S(1)} %pad_maximum_fusion.3), channel_id=1, source_target_pairs={{0,448},{32,480},{64,0},{96,32},{128,64},{160,96},{192,128},{224,1... | collective-permute-start | bytes 589832 | tf_op jit(solution)/shard_map/ppermute | solution.py:35
  64.5 2.1 %copy-start = (bf16[4,5,128,512]{3,2,1,0:T(8,128)(2,1)}, bf16[4,5,128,512]{3,2,1,0:T(8,128)(2,1)S(1)}, u32[]{:S(2)}) copy-start(bf16[4,5,128,512]{3,2,1,0:T(8,128)(2,1)S(1)} %all-to-all-done.1.near_ref) | copy-start | bytes 7864324
  66.6 24.4 %all-to-all-start = ((bf16[4,3,128,512]{3,2,1,0:T(8,128)(2,1)}), bf16[4,3,128,512]{3,2,1,0:T(8,128)(2,1)}, u32[]{:S(2)}, u32[]{:S(2)}) async-start(bf16[4,3,128,512]{3,2,1,0:T(8,128)(2,1)} %broadcast_in_dim.9), calls=%async_computation | async-start | bytes 3145728 | tf_op jit(solution)/shard_map/all_to_all | solution.py:24
  102.0 4.4 %collective-permute-start.6 = (bf16[192,2048]{1,0:T(8,128)(2,1)}, bf16[192,2048]{1,0:T(8,128)(2,1)S(1)}, u32[]{:S(2)}, u32[]{:S(2)}) collective-permute-start(bf16[192,2048]{1,0:T(8,128)(2,1)} %get-tuple-element.12), channel_id=1, source_target_pairs={{0,1},{1,0},{2,3},{3,2},{4,5},{5,4},{6,7},{7,6},{8,9},{9,8},{10,11... | collective-permute-start | bytes 2359304 | tf_op jit(solution)/shard_map/ppermute | solution.py:40
  107.8 3.1 %copy-start.1 = (bf16[192,2048]{1,0:T(8,128)(2,1)}, bf16[192,2048]{1,0:T(8,128)(2,1)S(1)}, u32[]{:S(2)}) copy-start(bf16[192,2048]{1,0:T(8,128)(2,1)S(1)} %add_convert_fusion.2) | copy-start | bytes 2359300
  107.8 21.6 %collective-permute-start.7 = (bf16[192,2048]{1,0:T(8,128)(2,1)S(1)}, bf16[192,2048]{1,0:T(8,128)(2,1)}, u32[]{:S(2)}, u32[]{:S(2)}) collective-permute-start(bf16[192,2048]{1,0:T(8,128)(2,1)S(1)} %add_convert_fusion.2), channel_id=1, source_target_pairs={{0,2},{2,0},{4,6},{6,4},{1,3},{3,1},{5,7},{7,5},{8,10},{10,8},{12,... | collective-permute-start | bytes 2359304 | tf_op jit(solution)/shard_map/ppermute | solution.py:40
  110.9 30.2 %all-to-all-start.2 = ((bf16[4,4,2,64,512]{4,3,2,1,0:T(8,128)(2,1)}), bf16[4,4,2,64,512]{4,3,2,1,0:T(8,128)(2,1)S(1)}, u32[]{:S(2)}, u32[]{:S(2)}) async-start(bf16[4,4,2,64,512]{4,3,2,1,0:T(8,128)(2,1)} %get-tuple-element.13), calls=%async_computation.2 | async-start | bytes 4194304 | tf_op jit(solution)/shard_map/all_to_all | solution.py:24
  131.0 20.7 %collective-permute-start.8 = (bf16[192,2048]{1,0:T(8,128)(2,1)S(1)}, bf16[192,2048]{1,0:T(8,128)(2,1)}, u32[]{:S(2)}, u32[]{:S(2)}) collective-permute-start(bf16[192,2048]{1,0:T(8,128)(2,1)S(1)} %add_convert_fusion.1), channel_id=1, source_target_pairs={{0,6},{2,4},{4,2},{6,0},{1,7},{3,5},{5,3},{7,1},{8,14},{10,12},{12... | collective-permute-start | bytes 2359304 | tf_op jit(solution)/shard_map/ppermute | solution.py:40
  142.4 17.4 %all-to-all-start.3 = ((bf16[4,2,64,512]{3,2,1,0:T(8,128)(2,1)}), bf16[4,2,64,512]{3,2,1,0:T(8,128)(2,1)S(1)}, u32[]{:S(2)}, u32[]{:S(2)}) async-start(bf16[4,2,64,512]{3,2,1,0:T(8,128)(2,1)} %reduce_sum.33), calls=%async_computation.3 | async-start | bytes 1048576 | tf_op jit(solution)/shard_map/all_to_all | solution.py:24
  153.2 16.7 %collective-permute-start.9 = (bf16[192,2048]{1,0:T(8,128)(2,1)S(1)}, bf16[192,2048]{1,0:T(8,128)(2,1)S(1)}, u32[]{:S(2)}, u32[]{:S(2)}) collective-permute-start(bf16[192,2048]{1,0:T(8,128)(2,1)S(1)} %add_convert_fusion), channel_id=1, source_target_pairs={{0,1},{1,0},{2,3},{3,2},{4,5},{5,4},{6,7},{7,6},{8,9},{9,8},{10,11... | collective-permute-start | bytes 2359304 | tf_op jit(solution)/shard_map/ppermute | solution.py:40
  160.6 27.8 %all-to-all-start.4 = ((bf16[4,64,512]{2,1,0:T(8,128)(2,1)}), bf16[4,64,512]{2,1,0:T(8,128)(2,1)S(1)}, u32[]{:S(2)}, u32[]{:S(2)}) async-start(bf16[4,64,512]{2,1,0:T(8,128)(2,1)} %bitcast.9), calls=%async_computation.4 | async-start | bytes 524288 | tf_op jit(solution)/shard_map/all_to_all | solution.py:24
where the time goes:
time: 190 us; the launch traced here: 189 us
  waiting for transfers between devices  95.3 us (50%)
  starting transfers between devices  62.5 us (33%)
  Pallas kernels  15.9 us (8%)
  other arithmetic  9.66 us (5%)
  local copies, waits for them, and re-layouts  4.69 us (2%)
    all_to_all x5, waiting for transfers between devices, exchange(): return lax.all_to_all(parts, axes, split_axis=0, concat_axis=0, tiled=True)  59 us
    ppermute x6, starting transfers between devices, shifted(): return lax.ppermute(value, axes, [(i, (i + step) % n) for i in range(n)])  28 us
    all_to_all x5, starting transfers between devices, exchange(): return lax.all_to_all(parts, axes, split_axis=0, concat_axis=0, tiled=True)  25.1 us
    ppermute x4, waiting for transfers between devices, swapped(): return lax.ppermute(value, axes, [(i, partner(i)) for i in range(n)])  23.2 us
    pallas_call x3, Pallas kernels, call(): pl.pallas_call(kernel, out_shape=tuple((jax.ShapeDtypeStruct(s, dtype) fo...  15.9 us
    ppermute x6, waiting for transfers between devices, shifted(): return lax.ppermute(value, axes, [(i, (i + step) % n) for i in range(n)])  13.1 us
    ppermute x4, starting transfers between devices, swapped(): return lax.ppermute(value, axes, [(i, partner(i)) for i in range(n)])  9.38 us
    convert_element_type x3, other arithmetic, total(): return (a.astype(F32) + b.astype(F32)).astype(BF)  4.42 us
  transfers between devices with their start and end apart: 15, of which 11 were waited for; matrix products, arithmetic and copies ran while one was open for 4% of the time, Pallas kernels for 3%

commit v1 on v0

--- a/solution.py
+++ b/solution.py
@@ -16,8 +16,8 @@
 
 BF = jnp.bfloat16
 F32 = jnp.float32
-NEAR = (0, 1, -1, 2, -2)
-FAR = (3, -3, 4)
+NEAR = (0, 1, -1)
+FAR = (2, -2, 3, -3, 4)
 
 
 def exchange(parts, axes):
@@ -126,26 +126,25 @@
     rows, h = w_up.shape
     tokens, width = inputs.shape
     own = jnp.concatenate([w_up, w_down.T], axis=0)
-    back = [shifted(own, Z, 1)]
-    ahead = [shifted(own, Z, -1)]
-    back.append(shifted(own, Z, 2))
-    ahead.append(shifted(own, Z, -2))
-    near = jnp.stack([own, back[0], ahead[0], back[1], ahead[1]])
-    near = copies_over(near, "y")
-    back = shifted(jnp.concatenate([back[0], back[1][:rows]], axis=0), Z, 2)
-    ahead = shifted(jnp.concatenate([ahead[0], ahead[1][rows:]], axis=0), Z, -2)
-    last = jnp.concatenate([back[2 * rows :], ahead[2 * rows :]], axis=0)
-    far = jnp.stack([back[: 2 * rows], ahead[: 2 * rows], last])
-    far = copies_over(far, "y")
+    back = [own]
+    ahead = [own]
+    for _ in range(3):
+        back.append(shifted(back[-1], Z, 1))
+        ahead.append(shifted(ahead[-1], Z, -1))
+    last = jnp.concatenate(
+        [shifted(back[3][:rows], Z, 1), shifted(ahead[3][rows:], Z, -1)], axis=0
+    )
+    near = copies_over(jnp.stack([own, back[1], ahead[1]]), "y")
+    far = copies_over(jnp.stack([back[2], ahead[2], back[3], ahead[3], last]), "y")
     unit = tokens * width * h // 2
     pre, hid = call(
-        near_kernel, [(tokens, h)] * 2, (inputs, cotangent, near), 5 * unit, dtype=F32
+        near_kernel, [(tokens, h)] * 2, (inputs, cotangent, near), 3 * unit, dtype=F32
     )
     grad, dw = call(
         weight_kernel,
         [(tokens, h), (N_Y, 4, 2, rows, h)],
         (inputs, cotangent, far, pre, hid),
-        7 * unit,
+        9 * unit,
         [pltpu.VMEM((tokens, h), F32)] * 2,
     )
     keep, give = call(
@@ -153,8 +152,10 @@
     )
 
     over_core = total(keep, swapped(give, "core", lambda i: 1 - i))
-    over_pair = total(over_core, swapped(over_core, "x", lambda i: i ^ 1))
-    mine = total(over_pair, swapped(over_pair, "x", lambda i: 3 - i))
+    step = swapped(over_core, "x", lambda i: i ^ 1)
+    over_pair = total(over_core, step)
+    step = swapped(over_pair, "x", lambda i: 3 - i)
+    mine = total(over_pair, step)
     other = swapped(mine, "core", lambda i: 1 - i)
     first = lax.axis_index("core") == 0
     d_inputs = jnp.concatenate(
@@ -163,10 +164,11 @@
 
     by_y = exchange(dw, "y")
     over_y = by_y.astype(F32).sum(0).astype(BF)
-    over_near = exchange(over_y, "zl").astype(F32).sum(0).astype(BF)
-    to_far = jnp.broadcast_to(over_near, (2, *over_near.shape))
-    d_w_up = exchange(to_far.reshape(4, rows, h), ("rep", "zh")).astype(F32).sum(0)
-    return (d_inputs, d_w_up)
+    by_near = exchange(over_y, "zl")
+    over_near = by_near.astype(F32).sum(0).astype(BF)
+    to_far = jnp.broadcast_to(over_near, (2, *over_near.shape)).reshape(4, rows, h)
+    by_far = exchange(to_far, ("rep", "zh"))
+    return (d_inputs, by_far.astype(F32).sum(0))
 
 
 def solution(mesh):

time: 190 us -> 184 us (0.968)
  waiting for transfers between devices: 95.3 us -> 82.7 us
  starting transfers between devices: 62.5 us -> 69.1 us
    ppermute x6 -> x8, starting transfers between devices: 28 us -> 34.9 us  [shifted(): return lax.ppermute(value, axes, [(i, (i + step) % n) for i in range(n)])]
    ppermute x6 -> x8, waiting for transfers between devices: 13.1 us -> 6.54 us  [shifted(): return lax.ppermute(value, axes, [(i, (i + step) % n) for i in range(n)])]
    all_to_all x5, waiting for transfers between devices: 59 us -> 53 us  [exchange(): return lax.all_to_all(parts, axes, split_axis=0, concat_axis=0, tiled=True)]
  transfers between devices with their start and end apart: 15 -> 17, of which waited for: 11 -> 13; matrix products, arithmetic and copies ran while one was open for 4% -> 4% of each run, Pallas kernels for 3% -> 2%
where the time goes in v1:
time: 184 us; the launch traced here: 183 us
  waiting for transfers between devices  82.7 us (45%)
  starting transfers between devices  69.1 us (38%)
  Pallas kernels  16 us (9%)
  other arithmetic  8.75 us (5%)
  local copies, waits for them, and re-layouts  5.56 us (3%)
    all_to_all x5, waiting for transfers between devices, exchange(): return lax.all_to_all(parts, axes, split_axis=0, concat_axis=0, tiled=True)  53 us
    ppermute x8, starting transfers between devices, shifted(): return lax.ppermute(value, axes, [(i, (i + step) % n) for i in range(n)])  34.9 us
    all_to_all x5, starting transfers between devices, exchange(): return lax.all_to_all(parts, axes, split_axis=0, concat_axis=0, tiled=True)  24.8 us
    ppermute x4, waiting for transfers between devices, swapped(): return lax.ppermute(value, axes, [(i, partner(i)) for i in range(n)])  23.2 us
    pallas_call x3, Pallas kernels, call(): pl.pallas_call(kernel, out_shape=tuple((jax.ShapeDtypeStruct(s, dtype) fo...  16 us
    ppermute x4, starting transfers between devices, swapped(): return lax.ppermute(value, axes, [(i, partner(i)) for i in range(n)])  9.38 us
    ppermute x8, waiting for transfers between devices, shifted(): return lax.ppermute(value, axes, [(i, (i + step) % n) for i in range(n)])  6.54 us
    convert_element_type x3, other arithmetic, total(): return (a.astype(F32) + b.astype(F32)).astype(BF)  4.42 us
  transfers between devices with their start and end apart: 17, of which 13 were waited for; matrix products, arithmetic and copies ran while one was open for 4% of the time, Pallas kernels for 2%

profile of v1, /device:TPU:4, one launch (start us, length us, event | category | flops | bytes accessed | tf_op | source)
XLA Modules:
  0.0 183.0 jit_solution(5744247106784725820)
XLA Ops:
  0.6 0.9 fusion.1
  1.5 3.8 %collective-permute-start = (bf16[128,512]{1,0:T(8,128)(2,1)S(1)}, bf16[128,512]{1,0:T(8,128)(2,1)S(1)}, u32[]{:S(2)}, u32[]{:S(2)}) collective-permute-start(bf16[128,512]{1,0:T(8,128)(2,1)S(1)} %get-tuple-element.17), channel_id=1, source_target_pairs={{0,32},{32,64},{64,96},{96,128},{128,160},{160,192},{192,224},{224... | collective-permute-start | bytes 393224 | tf_op jit(solution)/shard_map/ppermute | solution.py:35
  5.4 9.5 %collective-permute-start.2 = (bf16[128,512]{1,0:T(8,128)(2,1)S(1)}, bf16[128,512]{1,0:T(8,128)(2,1)S(1)}, u32[]{:S(2)}, u32[]{:S(2)}) collective-permute-start(bf16[128,512]{1,0:T(8,128)(2,1)S(1)} %get-tuple-element.17), channel_id=1, source_target_pairs={{0,480},{32,0},{64,32},{96,64},{128,96},{160,128},{192,160},{224,1... | collective-permute-start | bytes 393224 | tf_op jit(solution)/shard_map/ppermute | solution.py:35
  14.9 1.6 collective-permute-done
  16.4 1.2 collective-permute-done.2
  17.6 1.3 broadcast_in_dim.10
  18.9 4.5 %all-to-all-start.1 = ((bf16[4,3,128,512]{3,2,1,0:T(8,128)(2,1)}), bf16[4,3,128,512]{3,2,1,0:T(8,128)(2,1)S(1)}, u32[]{:S(2)}, u32[]{:S(2)}) async-start(bf16[4,3,128,512]{3,2,1,0:T(8,128)(2,1)} %broadcast_in_dim.10), calls=%async_computation.1 | async-start | bytes 3145728 | tf_op jit(solution)/shard_map/all_to_all | solution.py:24
  23.4 1.9 %collective-permute-start.1 = (bf16[128,512]{1,0:T(8,128)(2,1)S(1)}, bf16[128,512]{1,0:T(8,128)(2,1)S(1)}, u32[]{:S(2)}, u32[]{:S(2)}) collective-permute-start(bf16[128,512]{1,0:T(8,128)(2,1)S(1)} %collective-permute-done), channel_id=1, source_target_pairs={{0,32},{32,64},{64,96},{96,128},{128,160},{160,192},{192,224},{224... | collective-permute-start | bytes 393224 | tf_op jit(solution)/shard_map/ppermute | solution.py:35
  25.3 5.6 %collective-permute-start.3 = (bf16[128,512]{1,0:T(8,128)(2,1)S(1)}, bf16[128,512]{1,0:T(8,128)(2,1)S(1)}, u32[]{:S(2)}, u32[]{:S(2)}) collective-permute-start(bf16[128,512]{1,0:T(8,128)(2,1)S(1)} %collective-permute-done.2), channel_id=1, source_target_pairs={{0,480},{32,0},{64,32},{96,64},{128,96},{160,128},{192,160},{224,1... | collective-permute-start | bytes 393224 | tf_op jit(solution)/shard_map/ppermute | solution.py:35
  30.9 1.0 collective-permute-done.1
  31.9 1.9 %collective-permute-start.4 = (bf16[128,512]{1,0:T(8,128)(2,1)S(1)}, bf16[128,512]{1,0:T(8,128)(2,1)S(1)}, u32[]{:S(2)}, u32[]{:S(2)}) collective-permute-start(bf16[128,512]{1,0:T(8,128)(2,1)S(1)} %collective-permute-done.1), channel_id=1, source_target_pairs={{0,32},{32,64},{64,96},{96,128},{128,160},{160,192},{192,224},{224... | collective-permute-start | bytes 393224 | tf_op jit(solution)/shard_map/ppermute | solution.py:35
  33.8 0.0 collective-permute-done.3
  33.8 5.1 %collective-permute-start.5 = (bf16[128,512]{1,0:T(8,128)(2,1)S(1)}, bf16[128,512]{1,0:T(8,128)(2,1)S(1)}, u32[]{:S(2)}, u32[]{:S(2)}) collective-permute-start(bf16[128,512]{1,0:T(8,128)(2,1)S(1)} %collective-permute-done.3), channel_id=1, source_target_pairs={{0,480},{32,0},{64,32},{96,64},{128,96},{160,128},{192,160},{224,1... | collective-permute-start | bytes 393224 | tf_op jit(solution)/shard_map/ppermute | solution.py:35
  39.0 1.0 collective-permute-done.4
  40.0 1.9 %collective-permute-start.6 = (bf16[64,512]{1,0:T(8,128)(2,1)S(1)}, bf16[64,512]{1,0:T(8,128)(2,1)S(1)}, u32[]{:S(2)}, u32[]{:S(2)}) collective-permute-start(bf16[64,512]{1,0:T(8,128)(2,1)S(1)} %slice.8), channel_id=1, source_target_pairs={{0,32},{32,64},{64,96},{96,128},{128,160},{160,192},{192,224},{224... | collective-permute-start | bytes 196616 | tf_op jit(solution)/shard_map/ppermute | solution.py:35
  41.9 0.0 collective-permute-done.5
  41.9 5.1 %collective-permute-start.7 = (bf16[64,512]{1,0:T(8,128)(2,1)S(1)}, bf16[64,512]{1,0:T(8,128)(2,1)S(1)}, u32[]{:S(2)}, u32[]{:S(2)}) collective-permute-start(bf16[64,512]{1,0:T(8,128)(2,1)S(1)} %slice.9), channel_id=1, source_target_pairs={{0,480},{32,0},{64,32},{96,64},{128,96},{160,128},{192,160},{224,1... | collective-permute-start | bytes 196616 | tf_op jit(solution)/shard_map/ppermute | solution.py:35
  47.1 0.2 collective-permute-done.6
  47.3 1.6 collective-permute-done.7
  49.0 0.0 all-to-all-done.1.near_ref
  49.0 0.0 copy-start.1
  49.0 2.0 %broadcast_in_dim.9 = bf16[4,5,128,512]{3,2,1,0:T(8,128)(2,1)} broadcast(bf16[5,128,512]{2,1,0:T(8,128)(2,1)S(1)} %fusion), dimensions={1,2,3} | broadcast | bytes 3276800 | tf_op jit(solution)/shard_map/broadcast_in_dim | solution.py:29
  51.0 0.0 copy-done.1
  51.0 4.8 %all-to-all-start = ((bf16[4,5,128,512]{3,2,1,0:T(8,128)(2,1)}), bf16[4,5,128,512]{3,2,1,0:T(8,128)(2,1)S(1)}, u32[]{:S(2)}, u32[]{:S(2)}) async-start(bf16[4,5,128,512]{3,2,1,0:T(8,128)(2,1)} %broadcast_in_dim.9), calls=%async_computation | async-start | bytes 5242880 | tf_op jit(solution)/shard_map/all_to_all | solution.py:24
  55.8 4.2 %shard_map.59 = (f32[384,512]{1,0:T(8,128)}, f32[384,512]{1,0:T(8,128)}) custom-call(bf16[384,2048]{1,0:T(8,128)(2,1)} %x_ref.3, bf16[384,2048]{1,0:T(8,128)(2,1)} %c_ref.3, bf16[4,3,128,512]{3,2,1,0:T(8,128)(2,1)} %copy-done.1), custom_call_target="tpu_custom_call" | custom-call | flops 603979776 | bytes 4718592 | tf_op jit(solution)/shard_map/pallas_call | solution.py:107
  60.0 23.4 %all-to-all-done.far_ref = bf16[4,5,128,512]{3,2,1,0:T(8,128)(2,1)S(1)} async-done(((bf16[4,5,128,512]{3,2,1,0:T(8,128)(2,1)}), bf16[4,5,128,512]{3,2,1,0:T(8,128)(2,1)S(1)}, u32[]{:S(2)}, u32[]{:S(2)}) %all-to-all-start) | async-done | bytes 2621472 | tf_op jit(solution)/shard_map/all_to_all | solution.py:24
  83.5 0.0 copy-start
  83.5 1.5 copy-done
  85.0 6.9 %shard_map.60 = (bf16[384,512]{1,0:T(8,128)(2,1)}, bf16[4,4,2,64,512]{4,3,2,1,0:T(8,128)(2,1)}) custom-call(bf16[384,2048]{1,0:T(8,128)(2,1)} %x_ref.3, bf16[384,2048]{1,0:T(8,128)(2,1)} %c_ref.3, bf16[4,5,128,512]{3,2,1,0:T(8,128)(2,1)} %copy-done, f32[384,512]{1,0:T(8,128)} %get-tuple-element.8.pre_ref, f32[384,512]{1,0:T(8,128)} %get-tuple-element.9.hid_ref), custom_call_target="tpu_custom_call" | custom-call | flops 1811939328 | bytes 6553600 | tf_op jit(solution)/shard_map/pallas_call | solution.py:107
  91.8 4.9 %shard_map.61 = (bf16[192,2048]{1,0:T(8,128)(2,1)}, bf16[192,2048]{1,0:T(8,128)(2,1)}) custom-call(bf16[384,512]{1,0:T(8,128)(2,1)} %get-tuple-element.10.grad_ref, bf16[4,3,128,512]{3,2,1,0:T(8,128)(2,1)} %copy-done.1, bf16[4,5,128,512]{3,2,1,0:T(8,128)(2,1)} %copy-done), custom_call_target="tpu_custom_call" | custom-call | flops 805306368 | bytes 4587520 | tf_op jit(solution)/shard_map/pallas_call | solution.py:107
  96.7 1.9 %collective-permute-start.8 = (bf16[192,2048]{1,0:T(8,128)(2,1)}, bf16[192,2048]{1,0:T(8,128)(2,1)S(1)}, u32[]{:S(2)}, u32[]{:S(2)}) collective-permute-start(bf16[192,2048]{1,0:T(8,128)(2,1)} %get-tuple-element.12), channel_id=1, source_target_pairs={{0,1},{1,0},{2,3},{3,2},{4,5},{5,4},{6,7},{7,6},{8,9},{9,8},{10,11... | collective-permute-start | bytes 2359304 | tf_op jit(solution)/shard_map/ppermute | solution.py:40
  98.6 2.5 %collective-permute-done.8 = bf16[192,2048]{1,0:T(8,128)(2,1)S(1)} collective-permute-done((bf16[192,2048]{1,0:T(8,128)(2,1)}, bf16[192,2048]{1,0:T(8,128)(2,1)S(1)}, u32[]{:S(2)}, u32[]{:S(2)}) %collective-permute-start.8) | collective-permute-done | bytes 786464 | tf_op jit(solution)/shard_map/ppermute | solution.py:40
  101.1 1.4 add_convert_fusion.2
  102.5 0.0 copy-start.2
  102.5 3.1 %collective-permute-start.9 = (bf16[192,2048]{1,0:T(8,128)(2,1)S(1)}, bf16[192,2048]{1,0:T(8,128)(2,1)}, u32[]{:S(2)}, u32[]{:S(2)}) collective-permute-start(bf16[192,2048]{1,0:T(8,128)(2,1)S(1)} %add_convert_fusion.2), channel_id=1, source_target_pairs={{0,2},{2,0},{4,6},{6,4},{1,3},{3,1},{5,7},{7,5},{8,10},{10,8},{12,... | collective-permute-start | bytes 2359304 | tf_op jit(solution)/shard_map/ppermute | solution.py:40
  105.6 0.0 copy-done.2
  105.6 3.6 %all-to-all-start.2 = ((bf16[4,4,2,64,512]{4,3,2,1,0:T(8,128)(2,1)}), bf16[4,4,2,64,512]{4,3,2,1,0:T(8,128)(2,1)S(1)}, u32[]{:S(2)}, u32[]{:S(2)}) async-start(bf16[4,4,2,64,512]{4,3,2,1,0:T(8,128)(2,1)} %get-tuple-element.13), calls=%async_computation.2 | async-start | bytes 4194304 | tf_op jit(solution)/shard_map/all_to_all | solution.py:24
  109.2 14.8 %collective-permute-done.9 = bf16[192,2048]{1,0:T(8,128)(2,1)} collective-permute-done((bf16[192,2048]{1,0:T(8,128)(2,1)S(1)}, bf16[192,2048]{1,0:T(8,128)(2,1)}, u32[]{:S(2)}, u32[]{:S(2)}) %collective-permute-start.9) | collective-permute-done | bytes 786464 | tf_op jit(solution)/shard_map/ppermute | solution.py:40
  124.1 1.6 add_convert_fusion.1
  125.7 2.4 %collective-permute-start.10 = (bf16[192,2048]{1,0:T(8,128)(2,1)S(1)}, bf16[192,2048]{1,0:T(8,128)(2,1)}, u32[]{:S(2)}, u32[]{:S(2)}) collective-permute-start(bf16[192,2048]{1,0:T(8,128)(2,1)S(1)} %add_convert_fusion.1), channel_id=1, source_target_pairs={{0,6},{2,4},{4,2},{6,0},{1,7},{3,5},{5,3},{7,1},{8,14},{10,12},{12... | collective-permute-start | bytes 2359304 | tf_op jit(solution)/shard_map/ppermute | solution.py:40
  128.2 7.7 %all-to-all-done.2 = bf16[4,4,2,64,512]{4,3,2,1,0:T(8,128)(2,1)S(1)} async-done(((bf16[4,4,2,64,512]{4,3,2,1,0:T(8,128)(2,1)}), bf16[4,4,2,64,512]{4,3,2,1,0:T(8,128)(2,1)S(1)}, u32[]{:S(2)}, u32[]{:S(2)}) %all-to-all-start.2) | async-done | bytes 2097184 | tf_op jit(solution)/shard_map/all_to_all | solution.py:24
  135.8 1.3 reduce_sum.33
  137.1 3.5 %all-to-all-start.3 = ((bf16[4,2,64,512]{3,2,1,0:T(8,128)(2,1)}), bf16[4,2,64,512]{3,2,1,0:T(8,128)(2,1)S(1)}, u32[]{:S(2)}, u32[]{:S(2)}) async-start(bf16[4,2,64,512]{3,2,1,0:T(8,128)(2,1)} %reduce_sum.33), calls=%async_computation.3 | async-start | bytes 1048576 | tf_op jit(solution)/shard_map/all_to_all | solution.py:24
  140.6 5.9 %collective-permute-done.10 = bf16[192,2048]{1,0:T(8,128)(2,1)} collective-permute-done((bf16[192,2048]{1,0:T(8,128)(2,1)S(1)}, bf16[192,2048]{1,0:T(8,128)(2,1)}, u32[]{:S(2)}, u32[]{:S(2)}) %collective-permute-start.10) | collective-permute-done | bytes 786464 | tf_op jit(solution)/shard_map/ppermute | solution.py:40
  146.4 1.4 add_convert_fusion
  147.8 1.9 %collective-permute-start.11 = (bf16[192,2048]{1,0:T(8,128)(2,1)S(1)}, bf16[192,2048]{1,0:T(8,128)(2,1)S(1)}, u32[]{:S(2)}, u32[]{:S(2)}) collective-permute-start(bf16[192,2048]{1,0:T(8,128)(2,1)S(1)} %add_convert_fusion), channel_id=1, source_target_pairs={{0,1},{1,0},{2,3},{3,2},{4,5},{5,4},{6,7},{7,6},{8,9},{9,8},{10,11... | collective-permute-start | bytes 2359304 | tf_op jit(solution)/shard_map/ppermute | solution.py:40
  149.8 4.7 %all-to-all-done.3 = bf16[4,2,64,512]{3,2,1,0:T(8,128)(2,1)S(1)} async-done(((bf16[4,2,64,512]{3,2,1,0:T(8,128)(2,1)}), bf16[4,2,64,512]{3,2,1,0:T(8,128)(2,1)S(1)}, u32[]{:S(2)}, u32[]{:S(2)}) %all-to-all-start.3) | async-done | bytes 524320 | tf_op jit(solution)/shard_map/all_to_all | solution.py:24
  154.5 0.1 reduce_sum.34
  154.6 0.7 broadcast_in_dim.11
  155.3 8.5 %all-to-all-start.4 = ((bf16[4,64,512]{2,1,0:T(8,128)(2,1)}), bf16[4,64,512]{2,1,0:T(8,128)(2,1)S(1)}, u32[]{:S(2)}, u32[]{:S(2)}) async-start(bf16[4,64,512]{2,1,0:T(8,128)(2,1)} %bitcast.9), calls=%async_computation.4 | async-start | bytes 524288 | tf_op jit(solution)/shard_map/all_to_all | solution.py:24
  163.8 0.0 collective-permute-done.11
  163.8 0.1 broadcast_select_fusion.1
  163.9 1.2 pad_maximum_fusion
  165.1 17.1 %all-to-all-done.4 = bf16[4,64,512]{2,1,0:T(8,128)(2,1)S(1)} async-done(((bf16[4,64,512]{2,1,0:T(8,128)(2,1)}), bf16[4,64,512]{2,1,0:T(8,128)(2,1)S(1)}, u32[]{:S(2)}, u32[]{:S(2)}) %all-to-all-start.4) | async-done | bytes 262176 | tf_op jit(solution)/shard_map/all_to_all | solution.py:24
  182.3 0.7 convert_reduce_fusion
  (8 shorter events, 0.1 us)
Async XLA Ops:
  1.5 14.9 %collective-permute-start = (bf16[128,512]{1,0:T(8,128)(2,1)S(1)}, bf16[128,512]{1,0:T(8,128)(2,1)S(1)}, u32[]{:S(2)}, u32[]{:S(2)}) collective-permute-start(bf16[128,512]{1,0:T(8,128)(2,1)S(1)} %get-tuple-element.17), channel_id=1, source_target_pairs={{0,32},{32,64},{64,96},{96,128},{128,160},{160,192},{192,224},{224... | collective-permute-start | bytes 393224 | tf_op jit(solution)/shard_map/ppermute | solution.py:35
  5.4 12.2 %collective-permute-start.2 = (bf16[128,512]{1,0:T(8,128)(2,1)S(1)}, bf16[128,512]{1,0:T(8,128)(2,1)S(1)}, u32[]{:S(2)}, u32[]{:S(2)}) collective-permute-start(bf16[128,512]{1,0:T(8,128)(2,1)S(1)} %get-tuple-element.17), channel_id=1, source_target_pairs={{0,480},{32,0},{64,32},{96,64},{128,96},{160,128},{192,160},{224,1... | collective-permute-start | bytes 393224 | tf_op jit(solution)/shard_map/ppermute | solution.py:35
  18.9 30.0 %all-to-all-start.1 = ((bf16[4,3,128,512]{3,2,1,0:T(8,128)(2,1)}), bf16[4,3,128,512]{3,2,1,0:T(8,128)(2,1)S(1)}, u32[]{:S(2)}, u32[]{:S(2)}) async-start(bf16[4,3,128,512]{3,2,1,0:T(8,128)(2,1)} %broadcast_in_dim.10), calls=%async_computation.1 | async-start | bytes 3145728 | tf_op jit(solution)/shard_map/all_to_all | solution.py:24
  23.4 8.5 %collective-permute-start.1 = (bf16[128,512]{1,0:T(8,128)(2,1)S(1)}, bf16[128,512]{1,0:T(8,128)(2,1)S(1)}, u32[]{:S(2)}, u32[]{:S(2)}) collective-permute-start(bf16[128,512]{1,0:T(8,128)(2,1)S(1)} %collective-permute-done), channel_id=1, source_target_pairs={{0,32},{32,64},{64,96},{96,128},{128,160},{160,192},{192,224},{224... | collective-permute-start | bytes 393224 | tf_op jit(solution)/shard_map/ppermute | solution.py:35
  25.3 8.5 %collective-permute-start.3 = (bf16[128,512]{1,0:T(8,128)(2,1)S(1)}, bf16[128,512]{1,0:T(8,128)(2,1)S(1)}, u32[]{:S(2)}, u32[]{:S(2)}) collective-permute-start(bf16[128,512]{1,0:T(8,128)(2,1)S(1)} %collective-permute-done.2), channel_id=1, source_target_pairs={{0,480},{32,0},{64,32},{96,64},{128,96},{160,128},{192,160},{224,1... | collective-permute-start | bytes 393224 | tf_op jit(solution)/shard_map/ppermute | solution.py:35
  31.9 8.1 %collective-permute-start.4 = (bf16[128,512]{1,0:T(8,128)(2,1)S(1)}, bf16[128,512]{1,0:T(8,128)(2,1)S(1)}, u32[]{:S(2)}, u32[]{:S(2)}) collective-permute-start(bf16[128,512]{1,0:T(8,128)(2,1)S(1)} %collective-permute-done.1), channel_id=1, source_target_pairs={{0,32},{32,64},{64,96},{96,128},{128,160},{160,192},{192,224},{224... | collective-permute-start | bytes 393224 | tf_op jit(solution)/shard_map/ppermute | solution.py:35
  33.8 8.1 %collective-permute-start.5 = (bf16[128,512]{1,0:T(8,128)(2,1)S(1)}, bf16[128,512]{1,0:T(8,128)(2,1)S(1)}, u32[]{:S(2)}, u32[]{:S(2)}) collective-permute-start(bf16[128,512]{1,0:T(8,128)(2,1)S(1)} %collective-permute-done.3), channel_id=1, source_target_pairs={{0,480},{32,0},{64,32},{96,64},{128,96},{160,128},{192,160},{224,1... | collective-permute-start | bytes 393224 | tf_op jit(solution)/shard_map/ppermute | solution.py:35
  40.0 7.4 %collective-permute-start.6 = (bf16[64,512]{1,0:T(8,128)(2,1)S(1)}, bf16[64,512]{1,0:T(8,128)(2,1)S(1)}, u32[]{:S(2)}, u32[]{:S(2)}) collective-permute-start(bf16[64,512]{1,0:T(8,128)(2,1)S(1)} %slice.8), channel_id=1, source_target_pairs={{0,32},{32,64},{64,96},{96,128},{128,160},{160,192},{192,224},{224... | collective-permute-start | bytes 196616 | tf_op jit(solution)/shard_map/ppermute | solution.py:35
  41.9 7.0 %collective-permute-start.7 = (bf16[64,512]{1,0:T(8,128)(2,1)S(1)}, bf16[64,512]{1,0:T(8,128)(2,1)S(1)}, u32[]{:S(2)}, u32[]{:S(2)}) collective-permute-start(bf16[64,512]{1,0:T(8,128)(2,1)S(1)} %slice.9), channel_id=1, source_target_pairs={{0,480},{32,0},{64,32},{96,64},{128,96},{160,128},{192,160},{224,1... | collective-permute-start | bytes 196616 | tf_op jit(solution)/shard_map/ppermute | solution.py:35
  49.0 2.0 %copy-start.1 = (bf16[4,3,128,512]{3,2,1,0:T(8,128)(2,1)}, bf16[4,3,128,512]{3,2,1,0:T(8,128)(2,1)S(1)}, u32[]{:S(2)}) copy-start(bf16[4,3,128,512]{3,2,1,0:T(8,128)(2,1)S(1)} %all-to-all-done.1.near_ref) | copy-start | bytes 4718596
  51.0 32.5 %all-to-all-start = ((bf16[4,5,128,512]{3,2,1,0:T(8,128)(2,1)}), bf16[4,5,128,512]{3,2,1,0:T(8,128)(2,1)S(1)}, u32[]{:S(2)}, u32[]{:S(2)}) async-start(bf16[4,5,128,512]{3,2,1,0:T(8,128)(2,1)} %broadcast_in_dim.9), calls=%async_computation | async-start | bytes 5242880 | tf_op jit(solution)/shard_map/all_to_all | solution.py:24
  83.5 1.5 copy-start
  96.7 4.4 %collective-permute-start.8 = (bf16[192,2048]{1,0:T(8,128)(2,1)}, bf16[192,2048]{1,0:T(8,128)(2,1)S(1)}, u32[]{:S(2)}, u32[]{:S(2)}) collective-permute-start(bf16[192,2048]{1,0:T(8,128)(2,1)} %get-tuple-element.12), channel_id=1, source_target_pairs={{0,1},{1,0},{2,3},{3,2},{4,5},{5,4},{6,7},{7,6},{8,9},{9,8},{10,11... | collective-permute-start | bytes 2359304 | tf_op jit(solution)/shard_map/ppermute | solution.py:40
  102.5 3.1 %copy-start.2 = (bf16[192,2048]{1,0:T(8,128)(2,1)}, bf16[192,2048]{1,0:T(8,128)(2,1)S(1)}, u32[]{:S(2)}) copy-start(bf16[192,2048]{1,0:T(8,128)(2,1)S(1)} %add_convert_fusion.2) | copy-start | bytes 2359300
  102.5 21.6 %collective-permute-start.9 = (bf16[192,2048]{1,0:T(8,128)(2,1)S(1)}, bf16[192,2048]{1,0:T(8,128)(2,1)}, u32[]{:S(2)}, u32[]{:S(2)}) collective-permute-start(bf16[192,2048]{1,0:T(8,128)(2,1)S(1)} %add_convert_fusion.2), channel_id=1, source_target_pairs={{0,2},{2,0},{4,6},{6,4},{1,3},{3,1},{5,7},{7,5},{8,10},{10,8},{12,... | collective-permute-start | bytes 2359304 | tf_op jit(solution)/shard_map/ppermute | solution.py:40
  105.6 30.2 %all-to-all-start.2 = ((bf16[4,4,2,64,512]{4,3,2,1,0:T(8,128)(2,1)}), bf16[4,4,2,64,512]{4,3,2,1,0:T(8,128)(2,1)S(1)}, u32[]{:S(2)}, u32[]{:S(2)}) async-start(bf16[4,4,2,64,512]{4,3,2,1,0:T(8,128)(2,1)} %get-tuple-element.13), calls=%async_computation.2 | async-start | bytes 4194304 | tf_op jit(solution)/shard_map/all_to_all | solution.py:24
  125.7 20.7 %collective-permute-start.10 = (bf16[192,2048]{1,0:T(8,128)(2,1)S(1)}, bf16[192,2048]{1,0:T(8,128)(2,1)}, u32[]{:S(2)}, u32[]{:S(2)}) collective-permute-start(bf16[192,2048]{1,0:T(8,128)(2,1)S(1)} %add_convert_fusion.1), channel_id=1, source_target_pairs={{0,6},{2,4},{4,2},{6,0},{1,7},{3,5},{5,3},{7,1},{8,14},{10,12},{12... | collective-permute-start | bytes 2359304 | tf_op jit(solution)/shard_map/ppermute | solution.py:40
  137.1 17.4 %all-to-all-start.3 = ((bf16[4,2,64,512]{3,2,1,0:T(8,128)(2,1)}), bf16[4,2,64,512]{3,2,1,0:T(8,128)(2,1)S(1)}, u32[]{:S(2)}, u32[]{:S(2)}) async-start(bf16[4,2,64,512]{3,2,1,0:T(8,128)(2,1)} %reduce_sum.33), calls=%async_computation.3 | async-start | bytes 1048576 | tf_op jit(solution)/shard_map/all_to_all | solution.py:24
  147.8 15.9 %collective-permute-start.11 = (bf16[192,2048]{1,0:T(8,128)(2,1)S(1)}, bf16[192,2048]{1,0:T(8,128)(2,1)S(1)}, u32[]{:S(2)}, u32[]{:S(2)}) collective-permute-start(bf16[192,2048]{1,0:T(8,128)(2,1)S(1)} %add_convert_fusion), channel_id=1, source_target_pairs={{0,1},{1,0},{2,3},{3,2},{4,5},{5,4},{6,7},{7,6},{8,9},{9,8},{10,11... | collective-permute-start | bytes 2359304 | tf_op jit(solution)/shard_map/ppermute | solution.py:40
  155.3 27.0 %all-to-all-start.4 = ((bf16[4,64,512]{2,1,0:T(8,128)(2,1)}), bf16[4,64,512]{2,1,0:T(8,128)(2,1)S(1)}, u32[]{:S(2)}, u32[]{:S(2)}) async-start(bf16[4,64,512]{2,1,0:T(8,128)(2,1)} %bitcast.9), calls=%async_computation.4 | async-start | bytes 524288 | tf_op jit(solution)/shard_map/all_to_all | solution.py:24

commit v2 on v1

--- a/solution.py
+++ b/solution.py
@@ -71,44 +71,110 @@
     add_products(x_ref, c_ref, near_ref, NEAR, pre_ref, hid_ref, True)
 
 
-def weight_kernel(
-    x_ref, c_ref, far_ref, pre_ref, hid_ref, grad_ref, dw_ref, pre_acc, hid_acc
-):
-    rows = far_ref.shape[2] // 2
+def far_copies(plus, minus, dsts, sems):
+    me = lax.axis_index("y")
+    rows = plus[0].shape[0] // 5
     width = N_Y * rows
-    pre_acc[...] = pre_ref[...]
-    hid_acc[...] = hid_ref[...]
-    add_products(x_ref, c_ref, far_ref, FAR, pre_acc, hid_acc, False)
+    copies = []
+    for n in range(len(FAR)):
+        group = []
+        for part, dst in enumerate(dsts):
+            if n < 4:
+                refs, piece = (plus, minus)[n % 2], n // 2 * 2 + part
+            else:
+                refs, piece = (plus, minus)[part], 4
+            for k, dist in enumerate((0, 1, -1, 2)):
+                y = lax.rem(me - dist + 2 * N_Y, N_Y)
+                at = pl.multiple_of(n * width + y * rows, rows)
+                copy = pltpu.make_async_copy(
+                    refs[k].at[pl.ds(piece * rows, rows)],
+                    dst.at[pl.ds(at, rows)],
+                    sems.at[n, part, k],
+                )
+                copy.start()
+                group.append(copy)
+        copies.append(group)
+    return copies
+
+
+def weight_kernel(x_hbm, c_hbm, pre_hbm, hid_hbm, *refs):
+    plus, minus = refs[0:4], refs[4:8]
+    grad_ref, dw_hbm, x, c, up, down, pre_acc, hid_acc, dw, sems, far_sems, out_sems = (
+        refs[8:]
+    )
+    width = dw.shape[1] * dw.shape[2]
+    first = [
+        pltpu.make_async_copy(src, dst, sems.at[k])
+        for k, (src, dst) in enumerate(
+            ((x_hbm, x), (pre_hbm, pre_acc), (hid_hbm, hid_acc))
+        )
+    ]
+    for copy in first:
+        copy.start()
+    places = []
+    c_copies = []
+    for n, (_, _, z) in enumerate(z_blocks((None, FAR))):
+        at = pl.ds(pl.multiple_of(z * width, width), width)
+        copy = pltpu.make_async_copy(c_hbm.at[:, at], c.at[n], sems.at[3 + n])
+        copy.start()
+        places.append(at)
+        c_copies.append(copy)
+    blocks = far_copies(plus, minus, (up, down), far_sems)
+    for copy in first:
+        copy.wait()
+    for n, at in enumerate(places):
+        for copy in (c_copies[n], *blocks[n]):
+            copy.wait()
+        mine = slice(n * width, (n + 1) * width)
+        pre_acc[...] += jnp.dot(x[:, at], up[mine], preferred_element_type=F32)
+        hid_acc[...] += jnp.dot(c[n], down[mine], preferred_element_type=F32)
     grad_ref[...] = (2.0 * jnp.maximum(pre_acc[...], 0.0) * hid_acc[...]).astype(BF)
+    out = []
     for z in range(N_Z):
-        dw = lax.dot_general(
-            x_ref[:, z * width : (z + 1) * width], grad_ref[...],
+        product = lax.dot_general(
+            x[:, z * width : (z + 1) * width], grad_ref[...],
             (((0,), (0,)), ((), ())), preferred_element_type=F32,
         ).astype(BF)
-        for y in range(N_Y):
-            dw_ref[y, z % 4, z // 4] = dw[y * rows : (y + 1) * rows]
-
-
-def input_kernel(grad_ref, near_ref, far_ref, keep_ref, give_ref):
+        dw[z] = product.reshape(dw.shape[1:])
+        copy = pltpu.make_async_copy(
+            dw.at[z], dw_hbm.at[:, z % 4, z // 4], out_sems.at[z]
+        )
+        copy.start()
+        out.append(copy)
+    for copy in out:
+        copy.wait()
+
+
+def input_kernel(grad_ref, near_ref, *refs):
+    plus, minus = refs[0:4], refs[4:8]
+    keep_ref, give_ref, up, sems = refs[8:]
     core = lax.axis_index("core")
     tokens = keep_ref.shape[0]
     width = N_Y * near_ref.shape[2] // 2
+    copies = far_copies(plus, minus, (up,), sems)
+    for group in copies:
+        for copy in group:
+            copy.wait()
     for out, which in ((give_ref, 1 - core), (keep_ref, core)):
         mine = grad_ref[pl.ds(pl.multiple_of(which * tokens, tokens), tokens), :]
-        for ref, k, z in z_blocks((near_ref, NEAR), (far_ref, FAR)):
+        for ref, k, z in z_blocks((near_ref, NEAR), (None, FAR)):
+            if ref is None:
+                block = up[k * width : (k + 1) * width]
+            else:
+                block = rows_of(ref, k, 0)
             out[:, pl.ds(pl.multiple_of(z * width, width), width)] = lax.dot_general(
-                mine, rows_of(ref, k, 0), (((1,), (1,)), ((), ())),
-                preferred_element_type=F32,
+                mine, block, (((1,), (1,)), ((), ())), preferred_element_type=F32
             ).astype(BF)
 
 
-def call(kernel, outs, args, flops, scratch=(), dtype=BF):
+def call(kernel, outs, args, flops, in_hbm, scratch=(), dtype=BF, out_hbm=()):
     vm = pl.BlockSpec(memory_space=pltpu.VMEM)
+    hbm = pl.BlockSpec(memory_space=pl.ANY)
     return pl.pallas_call(
         kernel,
         out_shape=tuple(jax.ShapeDtypeStruct(s, dtype) for s in outs),
-        in_specs=[vm] * len(args),
-        out_specs=(vm,) * len(outs),
+        in_specs=[hbm if k in in_hbm else vm for k in range(len(args))],
+        out_specs=tuple(hbm if k in out_hbm else vm for k in range(len(outs))),
         scratch_shapes=scratch,
         cost_estimate=pl.CostEstimate(
             flops=flops,
@@ -131,24 +197,58 @@
     for _ in range(3):
         back.append(shifted(back[-1], Z, 1))
         ahead.append(shifted(ahead[-1], Z, -1))
-    last = jnp.concatenate(
-        [shifted(back[3][:rows], Z, 1), shifted(ahead[3][rows:], Z, -1)], axis=0
-    )
+    plus_last = shifted(back[3][:rows], Z, 1)
+    minus_last = shifted(ahead[3][rows:], Z, -1)
     near = copies_over(jnp.stack([own, back[1], ahead[1]]), "y")
-    far = copies_over(jnp.stack([back[2], ahead[2], back[3], ahead[3], last]), "y")
+    plus = [jnp.concatenate([back[2], back[3], plus_last], axis=0)]
+    minus = [jnp.concatenate([ahead[2], ahead[3], minus_last], axis=0)]
+    plus.append(shifted(plus[0], "y", 1))
+    minus_after = shifted(minus[0], "y", -1)
+    minus.append(shifted(minus[0], "y", 1))
+    plus.append(shifted(plus[0], "y", -1))
+    minus.append(minus_after)
+    plus.append(shifted(plus[1], "y", 1))
+    minus.append(shifted(minus_after, "y", -1))
     unit = tokens * width * h // 2
+    part = N_Y * rows
     pre, hid = call(
-        near_kernel, [(tokens, h)] * 2, (inputs, cotangent, near), 3 * unit, dtype=F32
+        near_kernel,
+        [(tokens, h)] * 2,
+        (inputs, cotangent, near),
+        3 * unit,
+        (),
+        dtype=F32,
     )
     grad, dw = call(
         weight_kernel,
         [(tokens, h), (N_Y, 4, 2, rows, h)],
-        (inputs, cotangent, far, pre, hid),
+        (inputs, cotangent, pre, hid, *plus, *minus),
         9 * unit,
-        [pltpu.VMEM((tokens, h), F32)] * 2,
+        range(12),
+        [
+            pltpu.VMEM((tokens, width), BF),
+            pltpu.VMEM((len(FAR), tokens, part), BF),
+            pltpu.VMEM((len(FAR) * part, h), BF),
+            pltpu.VMEM((len(FAR) * part, h), BF),
+            pltpu.VMEM((tokens, h), F32),
+            pltpu.VMEM((tokens, h), F32),
+            pltpu.VMEM((N_Z, N_Y, rows, h), BF),
+            pltpu.SemaphoreType.DMA((3 + len(FAR),)),
+            pltpu.SemaphoreType.DMA((len(FAR), 2, N_Y)),
+            pltpu.SemaphoreType.DMA((N_Z,)),
+        ],
+        out_hbm=(1,),
     )
     keep, give = call(
-        input_kernel, [(tokens // 2, width)] * 2, (grad, near, far), 4 * unit
+        input_kernel,
+        [(tokens // 2, width)] * 2,
+        (grad, near, *plus, *minus),
+        4 * unit,
+        range(2, 10),
+        [
+            pltpu.VMEM((len(FAR) * part, h), BF),
+            pltpu.SemaphoreType.DMA((len(FAR), 1, N_Y)),
+        ],
     )
 
     over_core = total(keep, swapped(give, "core", lambda i: 1 - i))

time: 184 us -> 173 us (0.940)
  waiting for transfers between devices: 82.7 us -> 55.3 us
  starting transfers between devices: 69.1 us -> 86.6 us
  local copies, waits for them, and re-layouts: 5.56 us -> 3.24 us
    all_to_all x5 -> x4, waiting for transfers between devices: 53 us -> 29.5 us  [exchange(): return lax.all_to_all(parts, axes, split_axis=0, concat_axis=0, tiled=True)]
    ppermute x8 -> x14, starting transfers between devices: 34.9 us -> 57.3 us  [shifted(): return lax.ppermute(value, axes, [(i, (i + step) % n) for i in range(n)])]
    all_to_all x5 -> x4, starting transfers between devices: 24.8 us -> 19.8 us  [exchange(): return lax.all_to_all(parts, axes, split_axis=0, concat_axis=0, tiled=True)]
    ppermute x8 -> x14, waiting for transfers between devices: 6.54 us -> 2.58 us  [shifted(): return lax.ppermute(value, axes, [(i, (i + step) % n) for i in range(n)])]
    broadcast_in_dim x2 -> x1, local copies, waits for them, and re-layouts: 3.28 us -> 1.28 us  [copies_over(): copies = jnp.broadcast_to(value, (n, *value.shape))]
  transfers between devices with their start and end apart: 17 -> 22, of which waited for: 13 -> 10; matrix products, arithmetic and copies ran while one was open for 4% -> 5% of each run, Pallas kernels for 2% -> 2%
where the time goes in v2:
time: 173 us; the launch traced here: 172 us
  starting transfers between devices  86.6 us (50%)
  waiting for transfers between devices  55.3 us (32%)
  Pallas kernels  17.1 us (10%)
  other arithmetic  8.75 us (5%)
  local copies, waits for them, and re-layouts  3.24 us (2%)
    ppermute x14, starting transfers between devices, shifted(): return lax.ppermute(value, axes, [(i, (i + step) % n) for i in range(n)])  57.3 us
    all_to_all x4, waiting for transfers between devices, exchange(): return lax.all_to_all(parts, axes, split_axis=0, concat_axis=0, tiled=True)  29.5 us
    ppermute x4, waiting for transfers between devices, swapped(): return lax.ppermute(value, axes, [(i, partner(i)) for i in range(n)])  23.1 us
    all_to_all x4, starting transfers between devices, exchange(): return lax.all_to_all(parts, axes, split_axis=0, concat_axis=0, tiled=True)  19.8 us
    pallas_call x3, Pallas kernels, call(): pl.pallas_call(kernel, out_shape=tuple((jax.ShapeDtypeStruct(s, dtype) fo...  17.1 us
    ppermute x4, starting transfers between devices, swapped(): return lax.ppermute(value, axes, [(i, partner(i)) for i in range(n)])  9.41 us
    convert_element_type x3, other arithmetic, total(): return (a.astype(F32) + b.astype(F32)).astype(BF)  4.42 us
  transfers between devices with their start and end apart: 22, of which 10 were waited for; matrix products, arithmetic and copies ran while one was open for 5% of the time, Pallas kernels for 2%

profile of v2, /device:TPU:4, one launch (start us, length us, event | category | flops | bytes accessed | tf_op | source)
XLA Modules:
  0.0 172.0 jit_solution(12517627665045347641)
XLA Ops:
  0.6 0.9 fusion
  1.5 11.4 %collective-permute-start.1 = (bf16[128,512]{1,0:T(8,128)(2,1)S(1)}, bf16[128,512]{1,0:T(8,128)(2,1)S(1)}, u32[]{:S(2)}, u32[]{:S(2)}) collective-permute-start(bf16[128,512]{1,0:T(8,128)(2,1)S(1)} %get-tuple-element.17), channel_id=1, source_target_pairs={{0,480},{32,0},{64,32},{96,64},{128,96},{160,128},{192,160},{224,1... | collective-permute-start | bytes 393224 | tf_op jit(solution)/shard_map/ppermute | solution.py:35
  12.9 1.9 %collective-permute-start = (bf16[128,512]{1,0:T(8,128)(2,1)S(1)}, bf16[128,512]{1,0:T(8,128)(2,1)S(1)}, u32[]{:S(2)}, u32[]{:S(2)}) collective-permute-start(bf16[128,512]{1,0:T(8,128)(2,1)S(1)} %get-tuple-element.17), channel_id=1, source_target_pairs={{0,32},{32,64},{64,96},{96,128},{128,160},{160,192},{192,224},{224... | collective-permute-start | bytes 393224 | tf_op jit(solution)/shard_map/ppermute | solution.py:35
  14.9 0.8 collective-permute-done.1
  15.7 5.6 %collective-permute-start.8 = (bf16[128,512]{1,0:T(8,128)(2,1)S(1)}, bf16[128,512]{1,0:T(8,128)(2,1)S(1)}, u32[]{:S(2)}, u32[]{:S(2)}) collective-permute-start(bf16[128,512]{1,0:T(8,128)(2,1)S(1)} %collective-permute-done.1), channel_id=1, source_target_pairs={{0,480},{32,0},{64,32},{96,64},{128,96},{160,128},{192,160},{224,1... | collective-permute-start | bytes 393224 | tf_op jit(solution)/shard_map/ppermute | solution.py:35
  21.3 0.0 collective-permute-done
  21.3 1.9 %collective-permute-start.2 = (bf16[128,512]{1,0:T(8,128)(2,1)S(1)}, bf16[128,512]{1,0:T(8,128)(2,1)S(1)}, u32[]{:S(2)}, u32[]{:S(2)}) collective-permute-start(bf16[128,512]{1,0:T(8,128)(2,1)S(1)} %collective-permute-done), channel_id=1, source_target_pairs={{0,32},{32,64},{64,96},{96,128},{128,160},{160,192},{192,224},{224... | collective-permute-start | bytes 393224 | tf_op jit(solution)/shard_map/ppermute | solution.py:35
  23.3 1.3 broadcast_in_dim.6
  24.5 4.5 %all-to-all-start = ((bf16[4,3,128,512]{3,2,1,0:T(8,128)(2,1)}), bf16[4,3,128,512]{3,2,1,0:T(8,128)(2,1)S(1)}, u32[]{:S(2)}, u32[]{:S(2)}) async-start(bf16[4,3,128,512]{3,2,1,0:T(8,128)(2,1)} %broadcast_in_dim.6), calls=%async_computation | async-start | bytes 3145728 | tf_op jit(solution)/shard_map/all_to_all | solution.py:24
  29.0 0.0 collective-permute-done.8
  29.0 5.1 %collective-permute-start.9 = (bf16[128,512]{1,0:T(8,128)(2,1)S(1)}, bf16[128,512]{1,0:T(8,128)(2,1)S(1)}, u32[]{:S(2)}, u32[]{:S(2)}) collective-permute-start(bf16[128,512]{1,0:T(8,128)(2,1)S(1)} %collective-permute-done.8), channel_id=1, source_target_pairs={{0,480},{32,0},{64,32},{96,64},{128,96},{160,128},{192,160},{224,1... | collective-permute-start | bytes 393224 | tf_op jit(solution)/shard_map/ppermute | solution.py:35
  34.1 0.0 collective-permute-done.2
  34.1 1.9 %collective-permute-start.3 = (bf16[128,512]{1,0:T(8,128)(2,1)S(1)}, bf16[128,512]{1,0:T(8,128)(2,1)S(1)}, u32[]{:S(2)}, u32[]{:S(2)}) collective-permute-start(bf16[128,512]{1,0:T(8,128)(2,1)S(1)} %collective-permute-done.2), channel_id=1, source_target_pairs={{0,32},{32,64},{64,96},{96,128},{128,160},{160,192},{192,224},{224... | collective-permute-start | bytes 393224 | tf_op jit(solution)/shard_map/ppermute | solution.py:35
  36.1 0.5 collective-permute-done.9
  36.6 5.6 %collective-permute-start.10 = (bf16[64,512]{1,0:T(8,128)(2,1)S(1)}, bf16[64,512]{1,0:T(8,128)(2,1)S(1)}, u32[]{:S(2)}, u32[]{:S(2)}) collective-permute-start(bf16[64,512]{1,0:T(8,128)(2,1)S(1)} %slice.9), channel_id=1, source_target_pairs={{0,480},{32,0},{64,32},{96,64},{128,96},{160,128},{192,160},{224,1... | collective-permute-start | bytes 196616 | tf_op jit(solution)/shard_map/ppermute | solution.py:35
  42.2 0.0 collective-permute-done.3
  42.2 1.9 %collective-permute-start.4 = (bf16[64,512]{1,0:T(8,128)(2,1)S(1)}, bf16[64,512]{1,0:T(8,128)(2,1)S(1)}, u32[]{:S(2)}, u32[]{:S(2)}) collective-permute-start(bf16[64,512]{1,0:T(8,128)(2,1)S(1)} %slice.8), channel_id=1, source_target_pairs={{0,32},{32,64},{64,96},{96,128},{128,160},{160,192},{192,224},{224... | collective-permute-start | bytes 196616 | tf_op jit(solution)/shard_map/ppermute | solution.py:35
  44.2 0.0 collective-permute-done.10
  44.2 0.0 copy-start.3
  44.2 5.1 %collective-permute-start.12 = (bf16[320,512]{1,0:T(8,128)(2,1)S(1)}, bf16[320,512]{1,0:T(8,128)(2,1)S(1)}, u32[]{:S(2)}, u32[]{:S(2)}) collective-permute-start(bf16[320,512]{1,0:T(8,128)(2,1)S(1)} %constant_dynamic-update-slice_fusion.3.refs_4_), channel_id=1, source_target_pairs={{0,24},{8,0},{16,8},{24,16},{1,25},{9,1},{17,9},{25,17},{2,26},{10... | collective-permute-start | bytes 983048 | tf_op jit(solution)/shard_map/ppermute | solution.py:35
  49.4 0.2 collective-permute-done.4
  49.6 3.9 %collective-permute-start.5 = (bf16[320,512]{1,0:T(8,128)(2,1)S(1)}, bf16[320,512]{1,0:T(8,128)(2,1)S(1)}, u32[]{:S(2)}, u32[]{:S(2)}) collective-permute-start(bf16[320,512]{1,0:T(8,128)(2,1)S(1)} %constant_dynamic-update-slice_fusion.refs_0_), channel_id=1, source_target_pairs={{0,8},{8,16},{16,24},{24,0},{1,9},{9,17},{17,25},{25,1},{2,10},{10... | collective-permute-start | bytes 983048 | tf_op jit(solution)/shard_map/ppermute | solution.py:35
  53.5 3.4 %collective-permute-start.11 = (bf16[320,512]{1,0:T(8,128)(2,1)S(1)}, bf16[320,512]{1,0:T(8,128)(2,1)S(1)}, u32[]{:S(2)}, u32[]{:S(2)}) collective-permute-start(bf16[320,512]{1,0:T(8,128)(2,1)S(1)} %constant_dynamic-update-slice_fusion.3.refs_4_), channel_id=1, source_target_pairs={{0,8},{8,16},{16,24},{24,0},{1,9},{9,17},{17,25},{25,1},{2,10},{10... | collective-permute-start | bytes 983048 | tf_op jit(solution)/shard_map/ppermute | solution.py:35
  56.9 3.7 %collective-permute-start.6 = (bf16[320,512]{1,0:T(8,128)(2,1)S(1)}, bf16[320,512]{1,0:T(8,128)(2,1)S(1)}, u32[]{:S(2)}, u32[]{:S(2)}) collective-permute-start(bf16[320,512]{1,0:T(8,128)(2,1)S(1)} %constant_dynamic-update-slice_fusion.refs_0_), channel_id=1, source_target_pairs={{0,24},{8,0},{16,8},{24,16},{1,25},{9,1},{17,9},{25,17},{2,26},{10... | collective-permute-start | bytes 983048 | tf_op jit(solution)/shard_map/ppermute | solution.py:35
  60.6 0.0 collective-permute-done.12.refs_6_
  60.6 0.0 copy-start.4
  60.6 1.9 %collective-permute-start.13 = (bf16[320,512]{1,0:T(8,128)(2,1)S(1)}, bf16[320,512]{1,0:T(8,128)(2,1)}, u32[]{:S(2)}, u32[]{:S(2)}) collective-permute-start(bf16[320,512]{1,0:T(8,128)(2,1)S(1)} %collective-permute-done.12.refs_6_), channel_id=1, source_target_pairs={{0,24},{8,0},{16,8},{24,16},{1,25},{9,1},{17,9},{25,17},{2,26},{10... | collective-permute-start | bytes 983048 | tf_op jit(solution)/shard_map/ppermute | solution.py:35
  62.6 0.0 collective-permute-done.5.refs_1_
  62.6 3.9 %collective-permute-start.7 = (bf16[320,512]{1,0:T(8,128)(2,1)S(1)}, bf16[320,512]{1,0:T(8,128)(2,1)}, u32[]{:S(2)}, u32[]{:S(2)}) collective-permute-start(bf16[320,512]{1,0:T(8,128)(2,1)S(1)} %collective-permute-done.5.refs_1_), channel_id=1, source_target_pairs={{0,8},{8,16},{16,24},{24,0},{1,9},{9,17},{17,25},{25,1},{2,10},{10... | collective-permute-start | bytes 983048 | tf_op jit(solution)/shard_map/ppermute | solution.py:35
  66.5 0.0 all-to-all-done.near_ref
  66.5 0.0 copy-start
  66.5 1.1 copy-done
  67.7 4.2 %shard_map.59 = (f32[384,512]{1,0:T(8,128)}, f32[384,512]{1,0:T(8,128)}) custom-call(bf16[384,2048]{1,0:T(8,128)(2,1)} %x_hbm.1, bf16[384,2048]{1,0:T(8,128)(2,1)} %c_hbm.1, bf16[4,3,128,512]{3,2,1,0:T(8,128)(2,1)} %copy-done), custom_call_target="tpu_custom_call" | custom-call | flops 603979776 | bytes 4718592 | tf_op jit(solution)/shard_map/pallas_call | solution.py:173
  71.8 0.0 collective-permute-done.11.refs_5_
  71.8 0.0 collective-permute-done.6.refs_2_
  71.9 0.0 copy-start.7
  71.9 0.0 collective-permute-done.13.refs_7_
  71.9 1.0 collective-permute-done.7.refs_3_
  72.9 7.4 %shard_map.60 = (bf16[384,512]{1,0:T(8,128)(2,1)}, bf16[4,4,2,64,512]{4,3,2,1,0:T(8,128)(2,1)}) custom-call(bf16[384,2048]{1,0:T(8,128)(2,1)} %x_hbm.1, bf16[384,2048]{1,0:T(8,128)(2,1)} %c_hbm.1, f32[384,512]{1,0:T(8,128)} %get-tuple-element.8.pre_hbm, f32[384,512]{1,0:T(8,128)} %get-tuple-element.9.hid_hbm, bf16[320,512]{1,0:T(8,128)(2,1)} %copy-done.2, ...), custom_call_target="tpu_custom_call" | custom-call | flops 1811939328 | bytes 6553600 | tf_op jit(solution)/shard_map/pallas_call | solution.py:173
  80.4 5.5 %shard_map.61 = (bf16[192,2048]{1,0:T(8,128)(2,1)}, bf16[192,2048]{1,0:T(8,128)(2,1)}) custom-call(bf16[384,512]{1,0:T(8,128)(2,1)} %get-tuple-element.10.grad_ref, bf16[4,3,128,512]{3,2,1,0:T(8,128)(2,1)} %copy-done, bf16[320,512]{1,0:T(8,128)(2,1)} %copy-done.2, bf16[320,512]{1,0:T(8,128)(2,1)} %copy-done.5, bf16[320,512]{1,0:T(8,128)(2,1)} %copy-done.7, ...), custom_call_target="tpu_custom_call" | custom-call | flops 805306368 | bytes 4587520 | tf_op jit(solution)/shard_map/pallas_call | solution.py:173
  85.9 1.9 %collective-permute-start.14 = (bf16[192,2048]{1,0:T(8,128)(2,1)}, bf16[192,2048]{1,0:T(8,128)(2,1)S(1)}, u32[]{:S(2)}, u32[]{:S(2)}) collective-permute-start(bf16[192,2048]{1,0:T(8,128)(2,1)} %get-tuple-element.12), channel_id=1, source_target_pairs={{0,1},{1,0},{2,3},{3,2},{4,5},{5,4},{6,7},{7,6},{8,9},{9,8},{10,11... | collective-permute-start | bytes 2359304 | tf_op jit(solution)/shard_map/ppermute | solution.py:40
  87.8 2.5 %collective-permute-done.14 = bf16[192,2048]{1,0:T(8,128)(2,1)S(1)} collective-permute-done((bf16[192,2048]{1,0:T(8,128)(2,1)}, bf16[192,2048]{1,0:T(8,128)(2,1)S(1)}, u32[]{:S(2)}, u32[]{:S(2)}) %collective-permute-start.14) | collective-permute-done | bytes 786464 | tf_op jit(solution)/shard_map/ppermute | solution.py:40
  90.3 1.4 add_convert_fusion.2
  91.7 0.0 copy-start.1
  91.7 3.1 %collective-permute-start.15 = (bf16[192,2048]{1,0:T(8,128)(2,1)S(1)}, bf16[192,2048]{1,0:T(8,128)(2,1)}, u32[]{:S(2)}, u32[]{:S(2)}) collective-permute-start(bf16[192,2048]{1,0:T(8,128)(2,1)S(1)} %add_convert_fusion.2), channel_id=1, source_target_pairs={{0,2},{2,0},{4,6},{6,4},{1,3},{3,1},{5,7},{7,5},{8,10},{10,8},{12,... | collective-permute-start | bytes 2359304 | tf_op jit(solution)/shard_map/ppermute | solution.py:40
  94.9 3.6 %all-to-all-start.1 = ((bf16[4,4,2,64,512]{4,3,2,1,0:T(8,128)(2,1)}), bf16[4,4,2,64,512]{4,3,2,1,0:T(8,128)(2,1)S(1)}, u32[]{:S(2)}, u32[]{:S(2)}) async-start(bf16[4,4,2,64,512]{4,3,2,1,0:T(8,128)(2,1)} %get-tuple-element.13), calls=%async_computation.1 | async-start | bytes 4194304 | tf_op jit(solution)/shard_map/all_to_all | solution.py:24
  98.5 14.8 %collective-permute-done.15 = bf16[192,2048]{1,0:T(8,128)(2,1)} collective-permute-done((bf16[192,2048]{1,0:T(8,128)(2,1)S(1)}, bf16[192,2048]{1,0:T(8,128)(2,1)}, u32[]{:S(2)}, u32[]{:S(2)}) %collective-permute-start.15) | collective-permute-done | bytes 786464 | tf_op jit(solution)/shard_map/ppermute | solution.py:40
  113.3 1.6 add_convert_fusion.1
  114.9 2.4 %collective-permute-start.16 = (bf16[192,2048]{1,0:T(8,128)(2,1)S(1)}, bf16[192,2048]{1,0:T(8,128)(2,1)}, u32[]{:S(2)}, u32[]{:S(2)}) collective-permute-start(bf16[192,2048]{1,0:T(8,128)(2,1)S(1)} %add_convert_fusion.1), channel_id=1, source_target_pairs={{0,6},{2,4},{4,2},{6,0},{1,7},{3,5},{5,3},{7,1},{8,14},{10,12},{12... | collective-permute-start | bytes 2359304 | tf_op jit(solution)/shard_map/ppermute | solution.py:40
  117.4 7.7 %all-to-all-done.1 = bf16[4,4,2,64,512]{4,3,2,1,0:T(8,128)(2,1)S(1)} async-done(((bf16[4,4,2,64,512]{4,3,2,1,0:T(8,128)(2,1)}), bf16[4,4,2,64,512]{4,3,2,1,0:T(8,128)(2,1)S(1)}, u32[]{:S(2)}, u32[]{:S(2)}) %all-to-all-start.1) | async-done | bytes 2097184 | tf_op jit(solution)/shard_map/all_to_all | solution.py:24
  125.1 1.3 reduce_sum.33
  126.3 3.5 %all-to-all-start.2 = ((bf16[4,2,64,512]{3,2,1,0:T(8,128)(2,1)}), bf16[4,2,64,512]{3,2,1,0:T(8,128)(2,1)S(1)}, u32[]{:S(2)}, u32[]{:S(2)}) async-start(bf16[4,2,64,512]{3,2,1,0:T(8,128)(2,1)} %reduce_sum.33), calls=%async_computation.2 | async-start | bytes 1048576 | tf_op jit(solution)/shard_map/all_to_all | solution.py:24
  129.8 5.8 %collective-permute-done.16 = bf16[192,2048]{1,0:T(8,128)(2,1)} collective-permute-done((bf16[192,2048]{1,0:T(8,128)(2,1)S(1)}, bf16[192,2048]{1,0:T(8,128)(2,1)}, u32[]{:S(2)}, u32[]{:S(2)}) %collective-permute-start.16) | collective-permute-done | bytes 786464 | tf_op jit(solution)/shard_map/ppermute | solution.py:40
  135.7 1.4 add_convert_fusion
  137.1 1.9 %collective-permute-start.17 = (bf16[192,2048]{1,0:T(8,128)(2,1)S(1)}, bf16[192,2048]{1,0:T(8,128)(2,1)S(1)}, u32[]{:S(2)}, u32[]{:S(2)}) collective-permute-start(bf16[192,2048]{1,0:T(8,128)(2,1)S(1)} %add_convert_fusion), channel_id=1, source_target_pairs={{0,1},{1,0},{2,3},{3,2},{4,5},{5,4},{6,7},{7,6},{8,9},{9,8},{10,11... | collective-permute-start | bytes 2359304 | tf_op jit(solution)/shard_map/ppermute | solution.py:40
  139.0 4.7 %all-to-all-done.2 = bf16[4,2,64,512]{3,2,1,0:T(8,128)(2,1)S(1)} async-done(((bf16[4,2,64,512]{3,2,1,0:T(8,128)(2,1)}), bf16[4,2,64,512]{3,2,1,0:T(8,128)(2,1)S(1)}, u32[]{:S(2)}, u32[]{:S(2)}) %all-to-all-start.2) | async-done | bytes 524320 | tf_op jit(solution)/shard_map/all_to_all | solution.py:24
  143.7 0.1 reduce_sum.34
  143.8 0.7 broadcast_in_dim.7
  144.5 8.3 %all-to-all-start.3 = ((bf16[4,64,512]{2,1,0:T(8,128)(2,1)}), bf16[4,64,512]{2,1,0:T(8,128)(2,1)S(1)}, u32[]{:S(2)}, u32[]{:S(2)}) async-start(bf16[4,64,512]{2,1,0:T(8,128)(2,1)} %bitcast.4), calls=%async_computation.3 | async-start | bytes 524288 | tf_op jit(solution)/shard_map/all_to_all | solution.py:24
  152.8 0.0 collective-permute-done.17
  152.8 0.1 broadcast_select_fusion.1
  152.9 1.2 pad_maximum_fusion
  154.2 17.1 %all-to-all-done.3 = bf16[4,64,512]{2,1,0:T(8,128)(2,1)S(1)} async-done(((bf16[4,64,512]{2,1,0:T(8,128)(2,1)}), bf16[4,64,512]{2,1,0:T(8,128)(2,1)S(1)}, u32[]{:S(2)}, u32[]{:S(2)}) %all-to-all-start.3) | async-done | bytes 262176 | tf_op jit(solution)/shard_map/all_to_all | solution.py:24
  171.3 0.7 convert_reduce_fusion
  (19 shorter events, 0.1 us)
Async XLA Ops:
  1.5 14.1 %collective-permute-start.1 = (bf16[128,512]{1,0:T(8,128)(2,1)S(1)}, bf16[128,512]{1,0:T(8,128)(2,1)S(1)}, u32[]{:S(2)}, u32[]{:S(2)}) collective-permute-start(bf16[128,512]{1,0:T(8,128)(2,1)S(1)} %get-tuple-element.17), channel_id=1, source_target_pairs={{0,480},{32,0},{64,32},{96,64},{128,96},{160,128},{192,160},{224,1... | collective-permute-start | bytes 393224 | tf_op jit(solution)/shard_map/ppermute | solution.py:35
  12.9 8.3 %collective-permute-start = (bf16[128,512]{1,0:T(8,128)(2,1)S(1)}, bf16[128,512]{1,0:T(8,128)(2,1)S(1)}, u32[]{:S(2)}, u32[]{:S(2)}) collective-permute-start(bf16[128,512]{1,0:T(8,128)(2,1)S(1)} %get-tuple-element.17), channel_id=1, source_target_pairs={{0,32},{32,64},{64,96},{96,128},{128,160},{160,192},{192,224},{224... | collective-permute-start | bytes 393224 | tf_op jit(solution)/shard_map/ppermute | solution.py:35
  15.7 13.3 %collective-permute-start.8 = (bf16[128,512]{1,0:T(8,128)(2,1)S(1)}, bf16[128,512]{1,0:T(8,128)(2,1)S(1)}, u32[]{:S(2)}, u32[]{:S(2)}) collective-permute-start(bf16[128,512]{1,0:T(8,128)(2,1)S(1)} %collective-permute-done.1), channel_id=1, source_target_pairs={{0,480},{32,0},{64,32},{96,64},{128,96},{160,128},{192,160},{224,1... | collective-permute-start | bytes 393224 | tf_op jit(solution)/shard_map/ppermute | solution.py:35
  21.3 12.9 %collective-permute-start.2 = (bf16[128,512]{1,0:T(8,128)(2,1)S(1)}, bf16[128,512]{1,0:T(8,128)(2,1)S(1)}, u32[]{:S(2)}, u32[]{:S(2)}) collective-permute-start(bf16[128,512]{1,0:T(8,128)(2,1)S(1)} %collective-permute-done), channel_id=1, source_target_pairs={{0,32},{32,64},{64,96},{96,128},{128,160},{160,192},{192,224},{224... | collective-permute-start | bytes 393224 | tf_op jit(solution)/shard_map/ppermute | solution.py:35
  24.5 42.0 %all-to-all-start = ((bf16[4,3,128,512]{3,2,1,0:T(8,128)(2,1)}), bf16[4,3,128,512]{3,2,1,0:T(8,128)(2,1)S(1)}, u32[]{:S(2)}, u32[]{:S(2)}) async-start(bf16[4,3,128,512]{3,2,1,0:T(8,128)(2,1)} %broadcast_in_dim.6), calls=%async_computation | async-start | bytes 3145728 | tf_op jit(solution)/shard_map/all_to_all | solution.py:24
  29.0 7.6 %collective-permute-start.9 = (bf16[128,512]{1,0:T(8,128)(2,1)S(1)}, bf16[128,512]{1,0:T(8,128)(2,1)S(1)}, u32[]{:S(2)}, u32[]{:S(2)}) collective-permute-start(bf16[128,512]{1,0:T(8,128)(2,1)S(1)} %collective-permute-done.8), channel_id=1, source_target_pairs={{0,480},{32,0},{64,32},{96,64},{128,96},{160,128},{192,160},{224,1... | collective-permute-start | bytes 393224 | tf_op jit(solution)/shard_map/ppermute | solution.py:35
  34.1 8.1 %collective-permute-start.3 = (bf16[128,512]{1,0:T(8,128)(2,1)S(1)}, bf16[128,512]{1,0:T(8,128)(2,1)S(1)}, u32[]{:S(2)}, u32[]{:S(2)}) collective-permute-start(bf16[128,512]{1,0:T(8,128)(2,1)S(1)} %collective-permute-done.2), channel_id=1, source_target_pairs={{0,32},{32,64},{64,96},{96,128},{128,160},{160,192},{192,224},{224... | collective-permute-start | bytes 393224 | tf_op jit(solution)/shard_map/ppermute | solution.py:35
  36.6 7.6 %collective-permute-start.10 = (bf16[64,512]{1,0:T(8,128)(2,1)S(1)}, bf16[64,512]{1,0:T(8,128)(2,1)S(1)}, u32[]{:S(2)}, u32[]{:S(2)}) collective-permute-start(bf16[64,512]{1,0:T(8,128)(2,1)S(1)} %slice.9), channel_id=1, source_target_pairs={{0,480},{32,0},{64,32},{96,64},{128,96},{160,128},{192,160},{224,1... | collective-permute-start | bytes 196616 | tf_op jit(solution)/shard_map/ppermute | solution.py:35
  42.2 7.4 %collective-permute-start.4 = (bf16[64,512]{1,0:T(8,128)(2,1)S(1)}, bf16[64,512]{1,0:T(8,128)(2,1)S(1)}, u32[]{:S(2)}, u32[]{:S(2)}) collective-permute-start(bf16[64,512]{1,0:T(8,128)(2,1)S(1)} %slice.8), channel_id=1, source_target_pairs={{0,32},{32,64},{64,96},{96,128},{128,160},{160,192},{192,224},{224... | collective-permute-start | bytes 196616 | tf_op jit(solution)/shard_map/ppermute | solution.py:35
  44.2 28.7 %copy-start.3 = (bf16[320,512]{1,0:T(8,128)(2,1)}, bf16[320,512]{1,0:T(8,128)(2,1)S(1)}, u32[]{:S(2)}) copy-start(bf16[320,512]{1,0:T(8,128)(2,1)S(1)} %constant_dynamic-update-slice_fusion.3.refs_4_) | copy-start | bytes 983044
  44.2 16.4 %collective-permute-start.12 = (bf16[320,512]{1,0:T(8,128)(2,1)S(1)}, bf16[320,512]{1,0:T(8,128)(2,1)S(1)}, u32[]{:S(2)}, u32[]{:S(2)}) collective-permute-start(bf16[320,512]{1,0:T(8,128)(2,1)S(1)} %constant_dynamic-update-slice_fusion.3.refs_4_), channel_id=1, source_target_pairs={{0,24},{8,0},{16,8},{24,16},{1,25},{9,1},{17,9},{25,17},{2,26},{10... | collective-permute-start | bytes 983048 | tf_op jit(solution)/shard_map/ppermute | solution.py:35
  49.6 23.3 %copy-start.2 = (bf16[320,512]{1,0:T(8,128)(2,1)}, bf16[320,512]{1,0:T(8,128)(2,1)S(1)}, u32[]{:S(2)}) copy-start(bf16[320,512]{1,0:T(8,128)(2,1)S(1)} %constant_dynamic-update-slice_fusion.refs_0_) | copy-start | bytes 983044
  49.6 13.0 %collective-permute-start.5 = (bf16[320,512]{1,0:T(8,128)(2,1)S(1)}, bf16[320,512]{1,0:T(8,128)(2,1)S(1)}, u32[]{:S(2)}, u32[]{:S(2)}) collective-permute-start(bf16[320,512]{1,0:T(8,128)(2,1)S(1)} %constant_dynamic-update-slice_fusion.refs_0_), channel_id=1, source_target_pairs={{0,8},{8,16},{16,24},{24,0},{1,9},{9,17},{17,25},{25,1},{2,10},{10... | collective-permute-start | bytes 983048 | tf_op jit(solution)/shard_map/ppermute | solution.py:35
  53.5 18.3 %collective-permute-start.11 = (bf16[320,512]{1,0:T(8,128)(2,1)S(1)}, bf16[320,512]{1,0:T(8,128)(2,1)S(1)}, u32[]{:S(2)}, u32[]{:S(2)}) collective-permute-start(bf16[320,512]{1,0:T(8,128)(2,1)S(1)} %constant_dynamic-update-slice_fusion.3.refs_4_), channel_id=1, source_target_pairs={{0,8},{8,16},{16,24},{24,0},{1,9},{9,17},{17,25},{25,1},{2,10},{10... | collective-permute-start | bytes 983048 | tf_op jit(solution)/shard_map/ppermute | solution.py:35
  56.9 14.9 %collective-permute-start.6 = (bf16[320,512]{1,0:T(8,128)(2,1)S(1)}, bf16[320,512]{1,0:T(8,128)(2,1)S(1)}, u32[]{:S(2)}, u32[]{:S(2)}) collective-permute-start(bf16[320,512]{1,0:T(8,128)(2,1)S(1)} %constant_dynamic-update-slice_fusion.refs_0_), channel_id=1, source_target_pairs={{0,24},{8,0},{16,8},{24,16},{1,25},{9,1},{17,9},{25,17},{2,26},{10... | collective-permute-start | bytes 983048 | tf_op jit(solution)/shard_map/ppermute | solution.py:35
  60.6 12.3 %copy-start.4 = (bf16[320,512]{1,0:T(8,128)(2,1)}, bf16[320,512]{1,0:T(8,128)(2,1)S(1)}, u32[]{:S(2)}) copy-start(bf16[320,512]{1,0:T(8,128)(2,1)S(1)} %collective-permute-done.12.refs_6_) | copy-start | bytes 983044
  60.6 11.2 %collective-permute-start.13 = (bf16[320,512]{1,0:T(8,128)(2,1)S(1)}, bf16[320,512]{1,0:T(8,128)(2,1)}, u32[]{:S(2)}, u32[]{:S(2)}) collective-permute-start(bf16[320,512]{1,0:T(8,128)(2,1)S(1)} %collective-permute-done.12.refs_6_), channel_id=1, source_target_pairs={{0,24},{8,0},{16,8},{24,16},{1,25},{9,1},{17,9},{25,17},{2,26},{10... | collective-permute-start | bytes 983048 | tf_op jit(solution)/shard_map/ppermute | solution.py:35
  62.6 10.3 %copy-start.5 = (bf16[320,512]{1,0:T(8,128)(2,1)}, bf16[320,512]{1,0:T(8,128)(2,1)S(1)}, u32[]{:S(2)}) copy-start(bf16[320,512]{1,0:T(8,128)(2,1)S(1)} %collective-permute-done.5.refs_1_) | copy-start | bytes 983044
  62.6 10.3 %collective-permute-start.7 = (bf16[320,512]{1,0:T(8,128)(2,1)S(1)}, bf16[320,512]{1,0:T(8,128)(2,1)}, u32[]{:S(2)}, u32[]{:S(2)}) collective-permute-start(bf16[320,512]{1,0:T(8,128)(2,1)S(1)} %collective-permute-done.5.refs_1_), channel_id=1, source_target_pairs={{0,8},{8,16},{16,24},{24,0},{1,9},{9,17},{17,25},{25,1},{2,10},{10... | collective-permute-start | bytes 983048 | tf_op jit(solution)/shard_map/ppermute | solution.py:35
  66.5 1.1 copy-start
  71.8 1.1 copy-start.6
  71.9 1.1 copy-start.7
  85.9 4.4 %collective-permute-start.14 = (bf16[192,2048]{1,0:T(8,128)(2,1)}, bf16[192,2048]{1,0:T(8,128)(2,1)S(1)}, u32[]{:S(2)}, u32[]{:S(2)}) collective-permute-start(bf16[192,2048]{1,0:T(8,128)(2,1)} %get-tuple-element.12), channel_id=1, source_target_pairs={{0,1},{1,0},{2,3},{3,2},{4,5},{5,4},{6,7},{7,6},{8,9},{9,8},{10,11... | collective-permute-start | bytes 2359304 | tf_op jit(solution)/shard_map/ppermute | solution.py:40
  91.7 3.1 %copy-start.1 = (bf16[192,2048]{1,0:T(8,128)(2,1)}, bf16[192,2048]{1,0:T(8,128)(2,1)S(1)}, u32[]{:S(2)}) copy-start(bf16[192,2048]{1,0:T(8,128)(2,1)S(1)} %add_convert_fusion.2) | copy-start | bytes 2359300
  91.7 21.6 %collective-permute-start.15 = (bf16[192,2048]{1,0:T(8,128)(2,1)S(1)}, bf16[192,2048]{1,0:T(8,128)(2,1)}, u32[]{:S(2)}, u32[]{:S(2)}) collective-permute-start(bf16[192,2048]{1,0:T(8,128)(2,1)S(1)} %add_convert_fusion.2), channel_id=1, source_target_pairs={{0,2},{2,0},{4,6},{6,4},{1,3},{3,1},{5,7},{7,5},{8,10},{10,8},{12,... | collective-permute-start | bytes 2359304 | tf_op jit(solution)/shard_map/ppermute | solution.py:40
  94.9 30.2 %all-to-all-start.1 = ((bf16[4,4,2,64,512]{4,3,2,1,0:T(8,128)(2,1)}), bf16[4,4,2,64,512]{4,3,2,1,0:T(8,128)(2,1)S(1)}, u32[]{:S(2)}, u32[]{:S(2)}) async-start(bf16[4,4,2,64,512]{4,3,2,1,0:T(8,128)(2,1)} %get-tuple-element.13), calls=%async_computation.1 | async-start | bytes 4194304 | tf_op jit(solution)/shard_map/all_to_all | solution.py:24
  114.9 20.7 %collective-permute-start.16 = (bf16[192,2048]{1,0:T(8,128)(2,1)S(1)}, bf16[192,2048]{1,0:T(8,128)(2,1)}, u32[]{:S(2)}, u32[]{:S(2)}) collective-permute-start(bf16[192,2048]{1,0:T(8,128)(2,1)S(1)} %add_convert_fusion.1), channel_id=1, source_target_pairs={{0,6},{2,4},{4,2},{6,0},{1,7},{3,5},{5,3},{7,1},{8,14},{10,12},{12... | collective-permute-start | bytes 2359304 | tf_op jit(solution)/shard_map/ppermute | solution.py:40
  126.3 17.4 %all-to-all-start.2 = ((bf16[4,2,64,512]{3,2,1,0:T(8,128)(2,1)}), bf16[4,2,64,512]{3,2,1,0:T(8,128)(2,1)S(1)}, u32[]{:S(2)}, u32[]{:S(2)}) async-start(bf16[4,2,64,512]{3,2,1,0:T(8,128)(2,1)} %reduce_sum.33), calls=%async_computation.2 | async-start | bytes 1048576 | tf_op jit(solution)/shard_map/all_to_all | solution.py:24
  137.1 15.7 %collective-permute-start.17 = (bf16[192,2048]{1,0:T(8,128)(2,1)S(1)}, bf16[192,2048]{1,0:T(8,128)(2,1)S(1)}, u32[]{:S(2)}, u32[]{:S(2)}) collective-permute-start(bf16[192,2048]{1,0:T(8,128)(2,1)S(1)} %add_convert_fusion), channel_id=1, source_target_pairs={{0,1},{1,0},{2,3},{3,2},{4,5},{5,4},{6,7},{7,6},{8,9},{9,8},{10,11... | collective-permute-start | bytes 2359304 | tf_op jit(solution)/shard_map/ppermute | solution.py:40
  144.5 26.8 %all-to-all-start.3 = ((bf16[4,64,512]{2,1,0:T(8,128)(2,1)}), bf16[4,64,512]{2,1,0:T(8,128)(2,1)S(1)}, u32[]{:S(2)}, u32[]{:S(2)}) async-start(bf16[4,64,512]{2,1,0:T(8,128)(2,1)} %bitcast.4), calls=%async_computation.3 | async-start | bytes 524288 | tf_op jit(solution)/shard_map/all_to_all | solution.py:24

commit v3 on v2

--- a/solution.py
+++ b/solution.py
@@ -73,16 +73,14 @@
 
 def far_copies(plus, minus, dsts, sems):
     me = lax.axis_index("y")
-    rows = plus[0].shape[0] // 5
+    rows = minus[0].shape[0] // 4
     width = N_Y * rows
     copies = []
     for n in range(len(FAR)):
         group = []
+        refs = (plus, minus)[n % 2]
         for part, dst in enumerate(dsts):
-            if n < 4:
-                refs, piece = (plus, minus)[n % 2], n // 2 * 2 + part
-            else:
-                refs, piece = (plus, minus)[part], 4
+            piece = n // 2 * 2 + part
             for k, dist in enumerate((0, 1, -1, 2)):
                 y = lax.rem(me - dist + 2 * N_Y, N_Y)
                 at = pl.multiple_of(n * width + y * rows, rows)
@@ -91,7 +89,6 @@
                     dst.at[pl.ds(at, rows)],
                     sems.at[n, part, k],
                 )
-                copy.start()
                 group.append(copy)
         copies.append(group)
     return copies
@@ -99,45 +96,54 @@
 
 def weight_kernel(x_hbm, c_hbm, pre_hbm, hid_hbm, *refs):
     plus, minus = refs[0:4], refs[4:8]
-    grad_ref, dw_hbm, x, c, up, down, pre_acc, hid_acc, dw, sems, far_sems, out_sems = (
-        refs[8:]
-    )
+    grad_ref, dw_hbm, x, c, up, down, pre_near, hid_near, pre_acc, hid_acc = refs[8:18]
+    dw, x_sems, c_sems, sums_sems, far_sems, out_sems = refs[18:]
     width = dw.shape[1] * dw.shape[2]
-    first = [
-        pltpu.make_async_copy(src, dst, sems.at[k])
-        for k, (src, dst) in enumerate(
-            ((x_hbm, x), (pre_hbm, pre_acc), (hid_hbm, hid_acc))
-        )
+    blocks = far_copies(plus, minus, (up, down), far_sems)
+    sums = [
+        pltpu.make_async_copy(pre_hbm, pre_near, sums_sems.at[0]),
+        pltpu.make_async_copy(hid_hbm, hid_near, sums_sems.at[1]),
     ]
-    for copy in first:
-        copy.start()
-    places = []
-    c_copies = []
-    for n, (_, _, z) in enumerate(z_blocks((None, FAR))):
+    places = [z for _, _, z in z_blocks((None, FAR), (None, NEAR))]
+    x_copies = []
+    for n, z in enumerate(places):
         at = pl.ds(pl.multiple_of(z * width, width), width)
-        copy = pltpu.make_async_copy(c_hbm.at[:, at], c.at[n], sems.at[3 + n])
-        copy.start()
-        places.append(at)
-        c_copies.append(copy)
-    blocks = far_copies(plus, minus, (up, down), far_sems)
-    for copy in first:
-        copy.wait()
-    for n, at in enumerate(places):
-        for copy in (c_copies[n], *blocks[n]):
+        x_copies.append(pltpu.make_async_copy(x_hbm.at[:, at], x.at[n], x_sems.at[n]))
+        x_copies[n].start()
+        if n < len(FAR):
+            copy = pltpu.make_async_copy(c_hbm.at[:, at], c.at[n], c_sems.at[n])
+            blocks[n].append(copy)
+            for copy in blocks[n]:
+                copy.start()
+        if n == len(FAR) - 1:
+            for copy in sums:
+                copy.start()
+    for n in range(len(FAR)):
+        for copy in (x_copies[n], *blocks[n]):
             copy.wait()
         mine = slice(n * width, (n + 1) * width)
-        pre_acc[...] += jnp.dot(x[:, at], up[mine], preferred_element_type=F32)
-        hid_acc[...] += jnp.dot(c[n], down[mine], preferred_element_type=F32)
-    grad_ref[...] = (2.0 * jnp.maximum(pre_acc[...], 0.0) * hid_acc[...]).astype(BF)
+        pre = jnp.dot(x[n], up[mine], preferred_element_type=F32)
+        hid = jnp.dot(c[n], down[mine], preferred_element_type=F32)
+        if n == 0:
+            pre_acc[...] = pre
+            hid_acc[...] = hid
+        else:
+            pre_acc[...] += pre
+            hid_acc[...] += hid
+    for copy in sums:
+        copy.wait()
+    pre = pre_acc[...] + pre_near[...]
+    grad_ref[...] = (2.0 * jnp.maximum(pre, 0.0) * (hid_acc[...] + hid_near[...])).astype(BF)
     out = []
-    for z in range(N_Z):
+    for n, z in enumerate(places):
+        if n >= len(FAR):
+            x_copies[n].wait()
         product = lax.dot_general(
-            x[:, z * width : (z + 1) * width], grad_ref[...],
-            (((0,), (0,)), ((), ())), preferred_element_type=F32,
+            x[n], grad_ref[...], (((0,), (0,)), ((), ())), preferred_element_type=F32
         ).astype(BF)
-        dw[z] = product.reshape(dw.shape[1:])
+        dw[n] = product.reshape(dw.shape[1:])
         copy = pltpu.make_async_copy(
-            dw.at[z], dw_hbm.at[:, z % 4, z // 4], out_sems.at[z]
+            dw.at[n], dw_hbm.at[:, lax.rem(z, 4), lax.div(z, 4)], out_sems.at[n]
         )
         copy.start()
         out.append(copy)
@@ -152,6 +158,9 @@
     tokens = keep_ref.shape[0]
     width = N_Y * near_ref.shape[2] // 2
     copies = far_copies(plus, minus, (up,), sems)
+    for group in copies:
+        for copy in group:
+            copy.start()
     for group in copies:
         for copy in group:
             copy.wait()
@@ -197,11 +206,10 @@
     for _ in range(3):
         back.append(shifted(back[-1], Z, 1))
         ahead.append(shifted(ahead[-1], Z, -1))
-    plus_last = shifted(back[3][:rows], Z, 1)
-    minus_last = shifted(ahead[3][rows:], Z, -1)
+    last = shifted(back[3], Z, 1)
     near = copies_over(jnp.stack([own, back[1], ahead[1]]), "y")
-    plus = [jnp.concatenate([back[2], back[3], plus_last], axis=0)]
-    minus = [jnp.concatenate([ahead[2], ahead[3], minus_last], axis=0)]
+    plus = [jnp.concatenate([back[2], back[3], last], axis=0)]
+    minus = [jnp.concatenate([ahead[2], ahead[3]], axis=0)]
     plus.append(shifted(plus[0], "y", 1))
     minus_after = shifted(minus[0], "y", -1)
     minus.append(shifted(minus[0], "y", 1))
@@ -226,14 +234,15 @@
         9 * unit,
         range(12),
         [
-            pltpu.VMEM((tokens, width), BF),
+            pltpu.VMEM((N_Z, tokens, part), BF),
             pltpu.VMEM((len(FAR), tokens, part), BF),
             pltpu.VMEM((len(FAR) * part, h), BF),
             pltpu.VMEM((len(FAR) * part, h), BF),
-            pltpu.VMEM((tokens, h), F32),
-            pltpu.VMEM((tokens, h), F32),
+            *[pltpu.VMEM((tokens, h), F32)] * 4,
             pltpu.VMEM((N_Z, N_Y, rows, h), BF),
-            pltpu.SemaphoreType.DMA((3 + len(FAR),)),
+            pltpu.SemaphoreType.DMA((N_Z,)),
+            pltpu.SemaphoreType.DMA((len(FAR),)),
+            pltpu.SemaphoreType.DMA((2,)),
             pltpu.SemaphoreType.DMA((len(FAR), 2, N_Y)),
             pltpu.SemaphoreType.DMA((N_Z,)),
         ],

time: 173 us -> 179 us (1.035)
  waiting for transfers between devices: 55.3 us -> 75.7 us
  starting transfers between devices: 86.6 us -> 71.7 us
    ppermute x14 -> x13, waiting for transfers between devices: 2.58 us -> 23.3 us  [shifted(): return lax.ppermute(value, axes, [(i, (i + step) % n) for i in range(n)])]
    ppermute x14 -> x13, starting transfers between devices: 57.3 us -> 41.7 us  [shifted(): return lax.ppermute(value, axes, [(i, (i + step) % n) for i in range(n)])]
  transfers between devices with their start and end apart: 22 -> 21, of which waited for: 10 -> 11; matrix products, arithmetic and copies ran while one was open for 5% -> 4% of each run, Pallas kernels for 2% -> 2%
where the time goes in v3:
time: 179 us; the launch traced here: 178 us
  waiting for transfers between devices  75.7 us (42%)
  starting transfers between devices  71.7 us (40%)
  Pallas kernels  17 us (9%)
  other arithmetic  8.75 us (5%)
  local copies, waits for them, and re-layouts  4.1 us (2%)
    ppermute x13, starting transfers between devices, shifted(): return lax.ppermute(value, axes, [(i, (i + step) % n) for i in range(n)])  41.7 us
    all_to_all x4, waiting for transfers between devices, exchange(): return lax.all_to_all(parts, axes, split_axis=0, concat_axis=0, tiled=True)  29.4 us
    ppermute x13, waiting for transfers between devices, shifted(): return lax.ppermute(value, axes, [(i, (i + step) % n) for i in range(n)])  23.3 us
    ppermute x4, waiting for transfers between devices, swapped(): return lax.ppermute(value, axes, [(i, partner(i)) for i in range(n)])  23.1 us
    all_to_all x4, starting transfers between devices, exchange(): return lax.all_to_all(parts, axes, split_axis=0, concat_axis=0, tiled=True)  20.6 us
    pallas_call x3, Pallas kernels, call(): pl.pallas_call(kernel, out_shape=tuple((jax.ShapeDtypeStruct(s, dtype) fo...  17 us
    ppermute x4, starting transfers between devices, swapped(): return lax.ppermute(value, axes, [(i, partner(i)) for i in range(n)])  9.38 us
    convert_element_type x3, other arithmetic, total(): return (a.astype(F32) + b.astype(F32)).astype(BF)  4.42 us
  transfers between devices with their start and end apart: 21, of which 11 were waited for; matrix products, arithmetic and copies ran while one was open for 4% of the time, Pallas kernels for 2%

profile of v3, /device:TPU:4, one launch (start us, length us, event | category | flops | bytes accessed | tf_op | source)
XLA Modules:
  0.0 178.2 jit_solution(4377031918461718308)
XLA Ops:
  0.6 0.9 fusion
  1.5 3.8 %collective-permute-start = (bf16[128,512]{1,0:T(8,128)(2,1)S(1)}, bf16[128,512]{1,0:T(8,128)(2,1)S(1)}, u32[]{:S(2)}, u32[]{:S(2)}) collective-permute-start(bf16[128,512]{1,0:T(8,128)(2,1)S(1)} %get-tuple-element.17), channel_id=1, source_target_pairs={{0,32},{32,64},{64,96},{96,128},{128,160},{160,192},{192,224},{224... | collective-permute-start | bytes 393224 | tf_op jit(solution)/shard_map/ppermute | solution.py:35
  5.4 11.1 %collective-permute-done = bf16[128,512]{1,0:T(8,128)(2,1)S(1)} collective-permute-done((bf16[128,512]{1,0:T(8,128)(2,1)S(1)}, bf16[128,512]{1,0:T(8,128)(2,1)S(1)}, u32[]{:S(2)}, u32[]{:S(2)}) %collective-permute-start) | collective-permute-done | bytes 131104 | tf_op jit(solution)/shard_map/ppermute | solution.py:35
  16.4 1.9 %collective-permute-start.2 = (bf16[128,512]{1,0:T(8,128)(2,1)S(1)}, bf16[128,512]{1,0:T(8,128)(2,1)S(1)}, u32[]{:S(2)}, u32[]{:S(2)}) collective-permute-start(bf16[128,512]{1,0:T(8,128)(2,1)S(1)} %collective-permute-done), channel_id=1, source_target_pairs={{0,32},{32,64},{64,96},{96,128},{128,160},{160,192},{192,224},{224... | collective-permute-start | bytes 393224 | tf_op jit(solution)/shard_map/ppermute | solution.py:35
  18.3 5.1 %collective-permute-start.1 = (bf16[128,512]{1,0:T(8,128)(2,1)S(1)}, bf16[128,512]{1,0:T(8,128)(2,1)S(1)}, u32[]{:S(2)}, u32[]{:S(2)}) collective-permute-start(bf16[128,512]{1,0:T(8,128)(2,1)S(1)} %get-tuple-element.17), channel_id=1, source_target_pairs={{0,480},{32,0},{64,32},{96,64},{128,96},{160,128},{192,160},{224,1... | collective-permute-start | bytes 393224 | tf_op jit(solution)/shard_map/ppermute | solution.py:35
  23.5 1.0 collective-permute-done.2
  24.5 1.9 %collective-permute-start.3 = (bf16[128,512]{1,0:T(8,128)(2,1)S(1)}, bf16[128,512]{1,0:T(8,128)(2,1)S(1)}, u32[]{:S(2)}, u32[]{:S(2)}) collective-permute-start(bf16[128,512]{1,0:T(8,128)(2,1)S(1)} %collective-permute-done.2), channel_id=1, source_target_pairs={{0,32},{32,64},{64,96},{96,128},{128,160},{160,192},{192,224},{224... | collective-permute-start | bytes 393224 | tf_op jit(solution)/shard_map/ppermute | solution.py:35
  26.4 0.0 collective-permute-done.1
  26.5 1.3 broadcast_in_dim.6
  27.7 4.5 %all-to-all-start = ((bf16[4,3,128,512]{3,2,1,0:T(8,128)(2,1)}), bf16[4,3,128,512]{3,2,1,0:T(8,128)(2,1)S(1)}, u32[]{:S(2)}, u32[]{:S(2)}) async-start(bf16[4,3,128,512]{3,2,1,0:T(8,128)(2,1)} %broadcast_in_dim.6), calls=%async_computation | async-start | bytes 3145728 | tf_op jit(solution)/shard_map/all_to_all | solution.py:24
  32.2 5.1 %collective-permute-start.8 = (bf16[128,512]{1,0:T(8,128)(2,1)S(1)}, bf16[128,512]{1,0:T(8,128)(2,1)S(1)}, u32[]{:S(2)}, u32[]{:S(2)}) collective-permute-start(bf16[128,512]{1,0:T(8,128)(2,1)S(1)} %collective-permute-done.1), channel_id=1, source_target_pairs={{0,480},{32,0},{64,32},{96,64},{128,96},{160,128},{192,160},{224,1... | collective-permute-start | bytes 393224 | tf_op jit(solution)/shard_map/ppermute | solution.py:35
  37.3 0.0 collective-permute-done.3
  37.3 1.9 %collective-permute-start.4 = (bf16[128,512]{1,0:T(8,128)(2,1)S(1)}, bf16[128,512]{1,0:T(8,128)(2,1)S(1)}, u32[]{:S(2)}, u32[]{:S(2)}) collective-permute-start(bf16[128,512]{1,0:T(8,128)(2,1)S(1)} %collective-permute-done.3), channel_id=1, source_target_pairs={{0,32},{32,64},{64,96},{96,128},{128,160},{160,192},{192,224},{224... | collective-permute-start | bytes 393224 | tf_op jit(solution)/shard_map/ppermute | solution.py:35
  39.3 6.1 %collective-permute-done.4 = bf16[128,512]{1,0:T(8,128)(2,1)S(1)} collective-permute-done((bf16[128,512]{1,0:T(8,128)(2,1)S(1)}, bf16[128,512]{1,0:T(8,128)(2,1)S(1)}, u32[]{:S(2)}, u32[]{:S(2)}) %collective-permute-start.4) | collective-permute-done | bytes 131104 | tf_op jit(solution)/shard_map/ppermute | solution.py:35
  45.4 0.0 copy-start.2
  45.4 3.9 %collective-permute-start.5 = (bf16[384,512]{1,0:T(8,128)(2,1)S(1)}, bf16[384,512]{1,0:T(8,128)(2,1)S(1)}, u32[]{:S(2)}, u32[]{:S(2)}) collective-permute-start(bf16[384,512]{1,0:T(8,128)(2,1)S(1)} %constant_dynamic-update-slice_fusion.refs_0_), channel_id=1, source_target_pairs={{0,8},{8,16},{16,24},{24,0},{1,9},{9,17},{17,25},{25,1},{2,10},{10... | collective-permute-start | bytes 1179656 | tf_op jit(solution)/shard_map/ppermute | solution.py:35
  49.4 0.0 collective-permute-done.8
  49.4 1.9 %collective-permute-start.9 = (bf16[128,512]{1,0:T(8,128)(2,1)S(1)}, bf16[128,512]{1,0:T(8,128)(2,1)S(1)}, u32[]{:S(2)}, u32[]{:S(2)}) collective-permute-start(bf16[128,512]{1,0:T(8,128)(2,1)S(1)} %collective-permute-done.8), channel_id=1, source_target_pairs={{0,480},{32,0},{64,32},{96,64},{128,96},{160,128},{192,160},{224,1... | collective-permute-start | bytes 393224 | tf_op jit(solution)/shard_map/ppermute | solution.py:35
  51.3 4.9 %collective-permute-done.9 = bf16[128,512]{1,0:T(8,128)(2,1)S(1)} collective-permute-done((bf16[128,512]{1,0:T(8,128)(2,1)S(1)}, bf16[128,512]{1,0:T(8,128)(2,1)S(1)}, u32[]{:S(2)}, u32[]{:S(2)}) %collective-permute-start.9) | collective-permute-done | bytes 131104 | tf_op jit(solution)/shard_map/ppermute | solution.py:35
  56.3 0.0 copy-start.3
  56.3 3.1 %collective-permute-start.11 = (bf16[256,512]{1,0:T(8,128)(2,1)S(1)}, bf16[256,512]{1,0:T(8,128)(2,1)}, u32[]{:S(2)}, u32[]{:S(2)}) collective-permute-start(bf16[256,512]{1,0:T(8,128)(2,1)S(1)} %constant_dynamic-update-slice_fusion.3.refs_4_), channel_id=1, source_target_pairs={{0,24},{8,0},{16,8},{24,16},{1,25},{9,1},{17,9},{25,17},{2,26},{10... | collective-permute-start | bytes 786440 | tf_op jit(solution)/shard_map/ppermute | solution.py:35
  59.4 3.9 %collective-permute-start.6 = (bf16[384,512]{1,0:T(8,128)(2,1)S(1)}, bf16[384,512]{1,0:T(8,128)(2,1)S(1)}, u32[]{:S(2)}, u32[]{:S(2)}) collective-permute-start(bf16[384,512]{1,0:T(8,128)(2,1)S(1)} %constant_dynamic-update-slice_fusion.refs_0_), channel_id=1, source_target_pairs={{0,24},{8,0},{16,8},{24,16},{1,25},{9,1},{17,9},{25,17},{2,26},{10... | collective-permute-start | bytes 1179656 | tf_op jit(solution)/shard_map/ppermute | solution.py:35
  63.3 0.0 collective-permute-done.5.refs_1_
  63.4 0.0 copy-start.4
  63.4 1.9 %collective-permute-start.7 = (bf16[384,512]{1,0:T(8,128)(2,1)S(1)}, bf16[384,512]{1,0:T(8,128)(2,1)S(1)}, u32[]{:S(2)}, u32[]{:S(2)}) collective-permute-start(bf16[384,512]{1,0:T(8,128)(2,1)S(1)} %collective-permute-done.5.refs_1_), channel_id=1, source_target_pairs={{0,8},{8,16},{16,24},{24,0},{1,9},{9,17},{17,25},{25,1},{2,10},{10... | collective-permute-start | bytes 1179656 | tf_op jit(solution)/shard_map/ppermute | solution.py:35
  65.3 2.7 %collective-permute-start.10 = (bf16[256,512]{1,0:T(8,128)(2,1)S(1)}, bf16[256,512]{1,0:T(8,128)(2,1)}, u32[]{:S(2)}, u32[]{:S(2)}) collective-permute-start(bf16[256,512]{1,0:T(8,128)(2,1)S(1)} %constant_dynamic-update-slice_fusion.3.refs_4_), channel_id=1, source_target_pairs={{0,8},{8,16},{16,24},{24,0},{1,9},{9,17},{17,25},{25,1},{2,10},{10... | collective-permute-start | bytes 786440 | tf_op jit(solution)/shard_map/ppermute | solution.py:35
  68.0 0.0 collective-permute-done.11.refs_6_
  68.0 4.3 %collective-permute-start.12 = (bf16[256,512]{1,0:T(8,128)(2,1)}, bf16[256,512]{1,0:T(8,128)(2,1)}, u32[]{:S(2)}, u32[]{:S(2)}) collective-permute-start(bf16[256,512]{1,0:T(8,128)(2,1)} %collective-permute-done.11.refs_6_), channel_id=1, source_target_pairs={{0,24},{8,0},{16,8},{24,16},{1,25},{9,1},{17,9},{25,17},{2,26},{10... | collective-permute-start | bytes 786440 | tf_op jit(solution)/shard_map/ppermute | solution.py:35
  72.4 0.0 all-to-all-done.near_ref
  72.4 0.0 copy-start
  72.4 1.1 copy-done
  73.5 4.2 %shard_map.59 = (f32[384,512]{1,0:T(8,128)}, f32[384,512]{1,0:T(8,128)}) custom-call(bf16[384,2048]{1,0:T(8,128)(2,1)} %x_hbm.1, bf16[384,2048]{1,0:T(8,128)(2,1)} %c_hbm.1, bf16[4,3,128,512]{3,2,1,0:T(8,128)(2,1)} %copy-done), custom_call_target="tpu_custom_call" | custom-call | flops 603979776 | bytes 4718592 | tf_op jit(solution)/shard_map/pallas_call | solution.py:182
  77.7 0.2 collective-permute-done.10.refs_5_
  77.9 0.0 collective-permute-done.6.refs_2_
  77.9 0.0 collective-permute-done.12.refs_7_
  77.9 0.0 collective-permute-done.7.refs_3_
  77.9 0.7 copy-done.5
  78.6 0.2 copy-done.6
  78.8 7.3 %shard_map.60 = (bf16[384,512]{1,0:T(8,128)(2,1)}, bf16[4,4,2,64,512]{4,3,2,1,0:T(8,128)(2,1)}) custom-call(bf16[384,2048]{1,0:T(8,128)(2,1)} %x_hbm.1, bf16[384,2048]{1,0:T(8,128)(2,1)} %c_hbm.1, f32[384,512]{1,0:T(8,128)} %get-tuple-element.8.pre_hbm, f32[384,512]{1,0:T(8,128)} %get-tuple-element.9.hid_hbm, bf16[384,512]{1,0:T(8,128)(2,1)} %copy-done.2, ...), custom_call_target="tpu_custom_call" | custom-call | flops 1811939328 | bytes 6553600 | tf_op jit(solution)/shard_map/pallas_call | solution.py:182
  86.1 5.6 %shard_map.61 = (bf16[192,2048]{1,0:T(8,128)(2,1)}, bf16[192,2048]{1,0:T(8,128)(2,1)}) custom-call(bf16[384,512]{1,0:T(8,128)(2,1)} %get-tuple-element.10.grad_ref, bf16[4,3,128,512]{3,2,1,0:T(8,128)(2,1)} %copy-done, bf16[384,512]{1,0:T(8,128)(2,1)} %copy-done.2, bf16[384,512]{1,0:T(8,128)(2,1)} %copy-done.4, bf16[384,512]{1,0:T(8,128)(2,1)} %copy-done.5, ...), custom_call_target="tpu_custom_call" | custom-call | flops 805306368 | bytes 4587520 | tf_op jit(solution)/shard_map/pallas_call | solution.py:182
  91.7 1.9 %collective-permute-start.13 = (bf16[192,2048]{1,0:T(8,128)(2,1)}, bf16[192,2048]{1,0:T(8,128)(2,1)S(1)}, u32[]{:S(2)}, u32[]{:S(2)}) collective-permute-start(bf16[192,2048]{1,0:T(8,128)(2,1)} %get-tuple-element.12), channel_id=1, source_target_pairs={{0,1},{1,0},{2,3},{3,2},{4,5},{5,4},{6,7},{7,6},{8,9},{9,8},{10,11... | collective-permute-start | bytes 2359304 | tf_op jit(solution)/shard_map/ppermute | solution.py:40
  93.6 2.5 %collective-permute-done.13 = bf16[192,2048]{1,0:T(8,128)(2,1)S(1)} collective-permute-done((bf16[192,2048]{1,0:T(8,128)(2,1)}, bf16[192,2048]{1,0:T(8,128)(2,1)S(1)}, u32[]{:S(2)}, u32[]{:S(2)}) %collective-permute-start.13) | collective-permute-done | bytes 786464 | tf_op jit(solution)/shard_map/ppermute | solution.py:40
  96.1 1.4 add_convert_fusion.2
  97.5 0.0 copy-start.1
  97.5 3.1 %collective-permute-start.14 = (bf16[192,2048]{1,0:T(8,128)(2,1)S(1)}, bf16[192,2048]{1,0:T(8,128)(2,1)}, u32[]{:S(2)}, u32[]{:S(2)}) collective-permute-start(bf16[192,2048]{1,0:T(8,128)(2,1)S(1)} %add_convert_fusion.2), channel_id=1, source_target_pairs={{0,2},{2,0},{4,6},{6,4},{1,3},{3,1},{5,7},{7,5},{8,10},{10,8},{12,... | collective-permute-start | bytes 2359304 | tf_op jit(solution)/shard_map/ppermute | solution.py:40
  100.6 3.7 %all-to-all-start.1 = ((bf16[4,4,2,64,512]{4,3,2,1,0:T(8,128)(2,1)}), bf16[4,4,2,64,512]{4,3,2,1,0:T(8,128)(2,1)S(1)}, u32[]{:S(2)}, u32[]{:S(2)}) async-start(bf16[4,4,2,64,512]{4,3,2,1,0:T(8,128)(2,1)} %get-tuple-element.13), calls=%async_computation.1 | async-start | bytes 4194304 | tf_op jit(solution)/shard_map/all_to_all | solution.py:24
  104.3 14.7 %collective-permute-done.14 = bf16[192,2048]{1,0:T(8,128)(2,1)} collective-permute-done((bf16[192,2048]{1,0:T(8,128)(2,1)S(1)}, bf16[192,2048]{1,0:T(8,128)(2,1)}, u32[]{:S(2)}, u32[]{:S(2)}) %collective-permute-start.14) | collective-permute-done | bytes 786464 | tf_op jit(solution)/shard_map/ppermute | solution.py:40
  119.0 1.6 add_convert_fusion.1
  120.7 2.4 %collective-permute-start.15 = (bf16[192,2048]{1,0:T(8,128)(2,1)S(1)}, bf16[192,2048]{1,0:T(8,128)(2,1)}, u32[]{:S(2)}, u32[]{:S(2)}) collective-permute-start(bf16[192,2048]{1,0:T(8,128)(2,1)S(1)} %add_convert_fusion.1), channel_id=1, source_target_pairs={{0,6},{2,4},{4,2},{6,0},{1,7},{3,5},{5,3},{7,1},{8,14},{10,12},{12... | collective-permute-start | bytes 2359304 | tf_op jit(solution)/shard_map/ppermute | solution.py:40
  123.1 7.7 %all-to-all-done.1 = bf16[4,4,2,64,512]{4,3,2,1,0:T(8,128)(2,1)S(1)} async-done(((bf16[4,4,2,64,512]{4,3,2,1,0:T(8,128)(2,1)}), bf16[4,4,2,64,512]{4,3,2,1,0:T(8,128)(2,1)S(1)}, u32[]{:S(2)}, u32[]{:S(2)}) %all-to-all-start.1) | async-done | bytes 2097184 | tf_op jit(solution)/shard_map/all_to_all | solution.py:24
  130.8 1.3 reduce_sum.33
  132.1 3.5 %all-to-all-start.2 = ((bf16[4,2,64,512]{3,2,1,0:T(8,128)(2,1)}), bf16[4,2,64,512]{3,2,1,0:T(8,128)(2,1)S(1)}, u32[]{:S(2)}, u32[]{:S(2)}) async-start(bf16[4,2,64,512]{3,2,1,0:T(8,128)(2,1)} %reduce_sum.33), calls=%async_computation.2 | async-start | bytes 1048576 | tf_op jit(solution)/shard_map/all_to_all | solution.py:24
  135.6 5.9 %collective-permute-done.15 = bf16[192,2048]{1,0:T(8,128)(2,1)} collective-permute-done((bf16[192,2048]{1,0:T(8,128)(2,1)S(1)}, bf16[192,2048]{1,0:T(8,128)(2,1)}, u32[]{:S(2)}, u32[]{:S(2)}) %collective-permute-start.15) | collective-permute-done | bytes 786464 | tf_op jit(solution)/shard_map/ppermute | solution.py:40
  141.4 1.4 add_convert_fusion
  142.8 1.9 %collective-permute-start.16 = (bf16[192,2048]{1,0:T(8,128)(2,1)S(1)}, bf16[192,2048]{1,0:T(8,128)(2,1)S(1)}, u32[]{:S(2)}, u32[]{:S(2)}) collective-permute-start(bf16[192,2048]{1,0:T(8,128)(2,1)S(1)} %add_convert_fusion), channel_id=1, source_target_pairs={{0,1},{1,0},{2,3},{3,2},{4,5},{5,4},{6,7},{7,6},{8,9},{9,8},{10,11... | collective-permute-start | bytes 2359304 | tf_op jit(solution)/shard_map/ppermute | solution.py:40
  144.8 4.6 %all-to-all-done.2 = bf16[4,2,64,512]{3,2,1,0:T(8,128)(2,1)S(1)} async-done(((bf16[4,2,64,512]{3,2,1,0:T(8,128)(2,1)}), bf16[4,2,64,512]{3,2,1,0:T(8,128)(2,1)S(1)}, u32[]{:S(2)}, u32[]{:S(2)}) %all-to-all-start.2) | async-done | bytes 524320 | tf_op jit(solution)/shard_map/all_to_all | solution.py:24
  149.3 0.1 reduce_sum.34
  149.4 0.7 broadcast_in_dim.7
  150.1 8.9 %all-to-all-start.3 = ((bf16[4,64,512]{2,1,0:T(8,128)(2,1)}), bf16[4,64,512]{2,1,0:T(8,128)(2,1)S(1)}, u32[]{:S(2)}, u32[]{:S(2)}) async-start(bf16[4,64,512]{2,1,0:T(8,128)(2,1)} %bitcast.4), calls=%async_computation.3 | async-start | bytes 524288 | tf_op jit(solution)/shard_map/all_to_all | solution.py:24
  159.0 0.0 collective-permute-done.16
  159.0 0.1 broadcast_select_fusion.1
  159.2 1.2 pad_maximum_fusion
  160.4 17.1 %all-to-all-done.3 = bf16[4,64,512]{2,1,0:T(8,128)(2,1)S(1)} async-done(((bf16[4,64,512]{2,1,0:T(8,128)(2,1)}), bf16[4,64,512]{2,1,0:T(8,128)(2,1)S(1)}, u32[]{:S(2)}, u32[]{:S(2)}) %all-to-all-start.3) | async-done | bytes 262176 | tf_op jit(solution)/shard_map/all_to_all | solution.py:24
  177.5 0.7 convert_reduce_fusion
  (12 shorter events, 0.1 us)
Async XLA Ops:
  1.5 14.9 %collective-permute-start = (bf16[128,512]{1,0:T(8,128)(2,1)S(1)}, bf16[128,512]{1,0:T(8,128)(2,1)S(1)}, u32[]{:S(2)}, u32[]{:S(2)}) collective-permute-start(bf16[128,512]{1,0:T(8,128)(2,1)S(1)} %get-tuple-element.17), channel_id=1, source_target_pairs={{0,32},{32,64},{64,96},{96,128},{128,160},{160,192},{192,224},{224... | collective-permute-start | bytes 393224 | tf_op jit(solution)/shard_map/ppermute | solution.py:35
  16.4 8.1 %collective-permute-start.2 = (bf16[128,512]{1,0:T(8,128)(2,1)S(1)}, bf16[128,512]{1,0:T(8,128)(2,1)S(1)}, u32[]{:S(2)}, u32[]{:S(2)}) collective-permute-start(bf16[128,512]{1,0:T(8,128)(2,1)S(1)} %collective-permute-done), channel_id=1, source_target_pairs={{0,32},{32,64},{64,96},{96,128},{128,160},{160,192},{192,224},{224... | collective-permute-start | bytes 393224 | tf_op jit(solution)/shard_map/ppermute | solution.py:35
  18.3 8.1 %collective-permute-start.1 = (bf16[128,512]{1,0:T(8,128)(2,1)S(1)}, bf16[128,512]{1,0:T(8,128)(2,1)S(1)}, u32[]{:S(2)}, u32[]{:S(2)}) collective-permute-start(bf16[128,512]{1,0:T(8,128)(2,1)S(1)} %get-tuple-element.17), channel_id=1, source_target_pairs={{0,480},{32,0},{64,32},{96,64},{128,96},{160,128},{192,160},{224,1... | collective-permute-start | bytes 393224 | tf_op jit(solution)/shard_map/ppermute | solution.py:35
  24.5 12.9 %collective-permute-start.3 = (bf16[128,512]{1,0:T(8,128)(2,1)S(1)}, bf16[128,512]{1,0:T(8,128)(2,1)S(1)}, u32[]{:S(2)}, u32[]{:S(2)}) collective-permute-start(bf16[128,512]{1,0:T(8,128)(2,1)S(1)} %collective-permute-done.2), channel_id=1, source_target_pairs={{0,32},{32,64},{64,96},{96,128},{128,160},{160,192},{192,224},{224... | collective-permute-start | bytes 393224 | tf_op jit(solution)/shard_map/ppermute | solution.py:35
  27.7 44.6 %all-to-all-start = ((bf16[4,3,128,512]{3,2,1,0:T(8,128)(2,1)}), bf16[4,3,128,512]{3,2,1,0:T(8,128)(2,1)S(1)}, u32[]{:S(2)}, u32[]{:S(2)}) async-start(bf16[4,3,128,512]{3,2,1,0:T(8,128)(2,1)} %broadcast_in_dim.6), calls=%async_computation | async-start | bytes 3145728 | tf_op jit(solution)/shard_map/all_to_all | solution.py:24
  32.2 17.2 %collective-permute-start.8 = (bf16[128,512]{1,0:T(8,128)(2,1)S(1)}, bf16[128,512]{1,0:T(8,128)(2,1)S(1)}, u32[]{:S(2)}, u32[]{:S(2)}) collective-permute-start(bf16[128,512]{1,0:T(8,128)(2,1)S(1)} %collective-permute-done.1), channel_id=1, source_target_pairs={{0,480},{32,0},{64,32},{96,64},{128,96},{160,128},{192,160},{224,1... | collective-permute-start | bytes 393224 | tf_op jit(solution)/shard_map/ppermute | solution.py:35
  37.3 8.1 %collective-permute-start.4 = (bf16[128,512]{1,0:T(8,128)(2,1)S(1)}, bf16[128,512]{1,0:T(8,128)(2,1)S(1)}, u32[]{:S(2)}, u32[]{:S(2)}) collective-permute-start(bf16[128,512]{1,0:T(8,128)(2,1)S(1)} %collective-permute-done.3), channel_id=1, source_target_pairs={{0,32},{32,64},{64,96},{96,128},{128,160},{160,192},{192,224},{224... | collective-permute-start | bytes 393224 | tf_op jit(solution)/shard_map/ppermute | solution.py:35
  45.4 32.3 %copy-start.2 = (bf16[384,512]{1,0:T(8,128)(2,1)}, bf16[384,512]{1,0:T(8,128)(2,1)S(1)}, u32[]{:S(2)}) copy-start(bf16[384,512]{1,0:T(8,128)(2,1)S(1)} %constant_dynamic-update-slice_fusion.refs_0_) | copy-start | bytes 1179652
  45.4 17.9 %collective-permute-start.5 = (bf16[384,512]{1,0:T(8,128)(2,1)S(1)}, bf16[384,512]{1,0:T(8,128)(2,1)S(1)}, u32[]{:S(2)}, u32[]{:S(2)}) collective-permute-start(bf16[384,512]{1,0:T(8,128)(2,1)S(1)} %constant_dynamic-update-slice_fusion.refs_0_), channel_id=1, source_target_pairs={{0,8},{8,16},{16,24},{24,0},{1,9},{9,17},{17,25},{25,1},{2,10},{10... | collective-permute-start | bytes 1179656 | tf_op jit(solution)/shard_map/ppermute | solution.py:35
  49.4 6.9 %collective-permute-start.9 = (bf16[128,512]{1,0:T(8,128)(2,1)S(1)}, bf16[128,512]{1,0:T(8,128)(2,1)S(1)}, u32[]{:S(2)}, u32[]{:S(2)}) collective-permute-start(bf16[128,512]{1,0:T(8,128)(2,1)S(1)} %collective-permute-done.8), channel_id=1, source_target_pairs={{0,480},{32,0},{64,32},{96,64},{128,96},{160,128},{192,160},{224,1... | collective-permute-start | bytes 393224 | tf_op jit(solution)/shard_map/ppermute | solution.py:35
  56.3 21.6 %copy-start.3 = (bf16[256,512]{1,0:T(8,128)(2,1)}, bf16[256,512]{1,0:T(8,128)(2,1)S(1)}, u32[]{:S(2)}) copy-start(bf16[256,512]{1,0:T(8,128)(2,1)S(1)} %constant_dynamic-update-slice_fusion.3.refs_4_) | copy-start | bytes 786436
  56.3 11.7 %collective-permute-start.11 = (bf16[256,512]{1,0:T(8,128)(2,1)S(1)}, bf16[256,512]{1,0:T(8,128)(2,1)}, u32[]{:S(2)}, u32[]{:S(2)}) collective-permute-start(bf16[256,512]{1,0:T(8,128)(2,1)S(1)} %constant_dynamic-update-slice_fusion.3.refs_4_), channel_id=1, source_target_pairs={{0,24},{8,0},{16,8},{24,16},{1,25},{9,1},{17,9},{25,17},{2,26},{10... | collective-permute-start | bytes 786440 | tf_op jit(solution)/shard_map/ppermute | solution.py:35
  59.4 18.5 %collective-permute-start.6 = (bf16[384,512]{1,0:T(8,128)(2,1)S(1)}, bf16[384,512]{1,0:T(8,128)(2,1)S(1)}, u32[]{:S(2)}, u32[]{:S(2)}) collective-permute-start(bf16[384,512]{1,0:T(8,128)(2,1)S(1)} %constant_dynamic-update-slice_fusion.refs_0_), channel_id=1, source_target_pairs={{0,24},{8,0},{16,8},{24,16},{1,25},{9,1},{17,9},{25,17},{2,26},{10... | collective-permute-start | bytes 1179656 | tf_op jit(solution)/shard_map/ppermute | solution.py:35
  63.4 14.6 %copy-start.4 = (bf16[384,512]{1,0:T(8,128)(2,1)}, bf16[384,512]{1,0:T(8,128)(2,1)S(1)}, u32[]{:S(2)}) copy-start(bf16[384,512]{1,0:T(8,128)(2,1)S(1)} %collective-permute-done.5.refs_1_) | copy-start | bytes 1179652
  63.4 14.5 %collective-permute-start.7 = (bf16[384,512]{1,0:T(8,128)(2,1)S(1)}, bf16[384,512]{1,0:T(8,128)(2,1)S(1)}, u32[]{:S(2)}, u32[]{:S(2)}) collective-permute-start(bf16[384,512]{1,0:T(8,128)(2,1)S(1)} %collective-permute-done.5.refs_1_), channel_id=1, source_target_pairs={{0,8},{8,16},{16,24},{24,0},{1,9},{9,17},{17,25},{25,1},{2,10},{10... | collective-permute-start | bytes 1179656 | tf_op jit(solution)/shard_map/ppermute | solution.py:35
  65.3 12.6 %collective-permute-start.10 = (bf16[256,512]{1,0:T(8,128)(2,1)S(1)}, bf16[256,512]{1,0:T(8,128)(2,1)}, u32[]{:S(2)}, u32[]{:S(2)}) collective-permute-start(bf16[256,512]{1,0:T(8,128)(2,1)S(1)} %constant_dynamic-update-slice_fusion.3.refs_4_), channel_id=1, source_target_pairs={{0,8},{8,16},{16,24},{24,0},{1,9},{9,17},{17,25},{25,1},{2,10},{10... | collective-permute-start | bytes 786440 | tf_op jit(solution)/shard_map/ppermute | solution.py:35
  68.0 9.9 %collective-permute-start.12 = (bf16[256,512]{1,0:T(8,128)(2,1)}, bf16[256,512]{1,0:T(8,128)(2,1)}, u32[]{:S(2)}, u32[]{:S(2)}) collective-permute-start(bf16[256,512]{1,0:T(8,128)(2,1)} %collective-permute-done.11.refs_6_), channel_id=1, source_target_pairs={{0,24},{8,0},{16,8},{24,16},{1,25},{9,1},{17,9},{25,17},{2,26},{10... | collective-permute-start | bytes 786440 | tf_op jit(solution)/shard_map/ppermute | solution.py:35
  72.4 1.1 copy-start
  77.9 0.8 copy-start.5
  77.9 0.9 copy-start.6
  91.7 4.4 %collective-permute-start.13 = (bf16[192,2048]{1,0:T(8,128)(2,1)}, bf16[192,2048]{1,0:T(8,128)(2,1)S(1)}, u32[]{:S(2)}, u32[]{:S(2)}) collective-permute-start(bf16[192,2048]{1,0:T(8,128)(2,1)} %get-tuple-element.12), channel_id=1, source_target_pairs={{0,1},{1,0},{2,3},{3,2},{4,5},{5,4},{6,7},{7,6},{8,9},{9,8},{10,11... | collective-permute-start | bytes 2359304 | tf_op jit(solution)/shard_map/ppermute | solution.py:40
  97.5 3.1 %copy-start.1 = (bf16[192,2048]{1,0:T(8,128)(2,1)}, bf16[192,2048]{1,0:T(8,128)(2,1)S(1)}, u32[]{:S(2)}) copy-start(bf16[192,2048]{1,0:T(8,128)(2,1)S(1)} %add_convert_fusion.2) | copy-start | bytes 2359300
  97.5 21.6 %collective-permute-start.14 = (bf16[192,2048]{1,0:T(8,128)(2,1)S(1)}, bf16[192,2048]{1,0:T(8,128)(2,1)}, u32[]{:S(2)}, u32[]{:S(2)}) collective-permute-start(bf16[192,2048]{1,0:T(8,128)(2,1)S(1)} %add_convert_fusion.2), channel_id=1, source_target_pairs={{0,2},{2,0},{4,6},{6,4},{1,3},{3,1},{5,7},{7,5},{8,10},{10,8},{12,... | collective-permute-start | bytes 2359304 | tf_op jit(solution)/shard_map/ppermute | solution.py:40
  100.6 30.2 %all-to-all-start.1 = ((bf16[4,4,2,64,512]{4,3,2,1,0:T(8,128)(2,1)}), bf16[4,4,2,64,512]{4,3,2,1,0:T(8,128)(2,1)S(1)}, u32[]{:S(2)}, u32[]{:S(2)}) async-start(bf16[4,4,2,64,512]{4,3,2,1,0:T(8,128)(2,1)} %get-tuple-element.13), calls=%async_computation.1 | async-start | bytes 4194304 | tf_op jit(solution)/shard_map/all_to_all | solution.py:24
  120.7 20.7 %collective-permute-start.15 = (bf16[192,2048]{1,0:T(8,128)(2,1)S(1)}, bf16[192,2048]{1,0:T(8,128)(2,1)}, u32[]{:S(2)}, u32[]{:S(2)}) collective-permute-start(bf16[192,2048]{1,0:T(8,128)(2,1)S(1)} %add_convert_fusion.1), channel_id=1, source_target_pairs={{0,6},{2,4},{4,2},{6,0},{1,7},{3,5},{5,3},{7,1},{8,14},{10,12},{12... | collective-permute-start | bytes 2359304 | tf_op jit(solution)/shard_map/ppermute | solution.py:40
  132.1 17.2 %all-to-all-start.2 = ((bf16[4,2,64,512]{3,2,1,0:T(8,128)(2,1)}), bf16[4,2,64,512]{3,2,1,0:T(8,128)(2,1)S(1)}, u32[]{:S(2)}, u32[]{:S(2)}) async-start(bf16[4,2,64,512]{3,2,1,0:T(8,128)(2,1)} %reduce_sum.33), calls=%async_computation.2 | async-start | bytes 1048576 | tf_op jit(solution)/shard_map/all_to_all | solution.py:24
  142.8 16.2 %collective-permute-start.16 = (bf16[192,2048]{1,0:T(8,128)(2,1)S(1)}, bf16[192,2048]{1,0:T(8,128)(2,1)S(1)}, u32[]{:S(2)}, u32[]{:S(2)}) collective-permute-start(bf16[192,2048]{1,0:T(8,128)(2,1)S(1)} %add_convert_fusion), channel_id=1, source_target_pairs={{0,1},{1,0},{2,3},{3,2},{4,5},{5,4},{6,7},{7,6},{8,9},{9,8},{10,11... | collective-permute-start | bytes 2359304 | tf_op jit(solution)/shard_map/ppermute | solution.py:40
  150.1 27.4 %all-to-all-start.3 = ((bf16[4,64,512]{2,1,0:T(8,128)(2,1)}), bf16[4,64,512]{2,1,0:T(8,128)(2,1)S(1)}, u32[]{:S(2)}, u32[]{:S(2)}) async-start(bf16[4,64,512]{2,1,0:T(8,128)(2,1)} %bitcast.4), calls=%async_computation.3 | async-start | bytes 524288 | tf_op jit(solution)/shard_map/all_to_all | solution.py:24

commit v4 on v3

v4 whole, which is shorter than its diff:
```python
import jax
import jax.numpy as jnp
from jax import lax
from jax.experimental import pallas as pl
from jax.experimental.pallas import tpu as pltpu
from jax.sharding import Mesh
from jax.sharding import PartitionSpec as P


FS = ("zh", "zl", "y")
REP_FS = ("rep", "zh", "zl", "y")
Z = ("rep", "zh", "zl")
TP = ("x", "core")
N_Z = 8
N_Y = 4

BF = jnp.bfloat16
F32 = jnp.float32
NEAR = (0, 1, -1)
FAR = (2, -2, 3, -3, 4)


def exchange(parts, axes):
    return lax.all_to_all(parts, axes, split_axis=0, concat_axis=0, tiled=True)


def copies_over(value, axes):
    n = lax.axis_size(axes)
    copies = jnp.broadcast_to(value, (n, *value.shape))
    return exchange(copies, axes)


def shifted(value, axes, step):
    n = lax.axis_size(axes)
    return lax.ppermute(value, axes, [(i, (i + step) % n) for i in range(n)])


def swapped(value, axes, partner):
    n = lax.axis_size(axes)
    return lax.ppermute(value, axes, [(i, partner(i)) for i in range(n)])


def near_z(k):
    me = lax.axis_index("zh") * 4 + lax.axis_index("zl")
    step = jnp.where(k == 0, 0, jnp.where(k == 1, 1, -1))
    return lax.rem(me - step + 2 * N_Z, N_Z)


def far_z(n):
    me = lax.axis_index("zh") * 4 + lax.axis_index("zl")
    step = (2 + lax.div(n, 2)) * (1 - 2 * lax.rem(n, 2))
    return lax.rem(me - step + 2 * N_Z, N_Z)


def block(index, width):
    return pl.ds(pl.multiple_of(index * width, width), width)


def near_rows(ref, k, part):
    rows = ref.shape[2] // 2
    at = slice(part * rows, (part + 1) * rows)
    return jnp.concatenate([ref[y, k, at] for y in range(N_Y)], axis=0)


def near_kernel(x_ref, c_ref, near_ref, pre_ref, hid_ref):
    width = N_Y * near_ref.shape[2] // 2
    pre_ref[...] = jnp.zeros_like(pre_ref)
    hid_ref[...] = jnp.zeros_like(hid_ref)

    @pl.loop(0, len(NEAR))
    def _(k):
        at = block(near_z(k), width)
        up, down = near_rows(near_ref, k, 0), near_rows(near_ref, k, 1)
        pre_ref[...] += jnp.dot(x_ref[:, at], up, preferred_element_type=F32)
        hid_ref[...] += jnp.dot(c_ref[:, at], down, preferred_element_type=F32)


def far_copies(n, plus, minus, dsts, sems):
    me = lax.axis_index("y")
    rows = plus[0].shape[0] // 5
    copies = []
    for part, dst in enumerate(dsts):
        if n < 4:
            refs, piece = (plus, minus)[n % 2], n // 2 * 2 + part
        else:
            refs, piece = (plus, minus)[part], 4
        for k, dist in enumerate((0, 1, -1, 2)):
            y = lax.rem(me - dist + 2 * N_Y, N_Y)
            at = pl.multiple_of(n * N_Y * rows + y * rows, rows)
            src = refs[k].at[pl.ds(piece * rows, rows)]
            copies.append(
                pltpu.make_async_copy(src, dst.at[pl.ds(at, rows)], sems.at[n, part, k])
            )
    return copies


def wait_far(n, like, dsts, sems):
    rows = like.shape[0] // 5
    for part, dst in enumerate(dsts):
        for k in range(N_Y):
            at = block(n * N_Y + k, rows)
            pltpu.make_async_copy(
                like.at[pl.ds(0, rows)], dst.at[at], sems.at[n, part, k]
            ).wait()


def weight_kernel(x_hbm, c_hbm, pre_hbm, hid_hbm, *refs):
    plus, minus = refs[0:4], refs[4:8]
    grad_ref, dw_hbm, x, c, up, down, pre_near, hid_near, pre_acc, hid_acc = refs[8:18]
    dw, x_sems, c_sems, sums_sems, far_sems, out_sems = refs[18:]
    width = dw.shape[1] * dw.shape[2]

    def x_copy(z):
        at = block(z, width)
        return pltpu.make_async_copy(x_hbm.at[:, at], x.at[:, at], x_sems.at[z])

    def c_copy(n):
        at = block(far_z(n), width)
        return pltpu.make_async_copy(c_hbm.at[:, at], c.at[n], c_sems.at[n])

    def out_copy(z):
        to = dw_hbm.at[:, lax.rem(z, 4), lax.div(z, 4)]
        return pltpu.make_async_copy(dw.at[z], to, out_sems.at[z])

    for n in range(len(FAR)):
        x_copy(far_z(n)).start()
        c_copy(n).start()
        for copy in far_copies(n, plus, minus, (up, down), far_sems):
            copy.start()
    sums = [
        pltpu.make_async_copy(pre_hbm, pre_near, sums_sems.at[0]),
        pltpu.make_async_copy(hid_hbm, hid_near, sums_sems.at[1]),
    ]
    for copy in sums:
        copy.start()
    for k in range(len(NEAR)):
        x_copy(near_z(k)).start()
    pre_acc[...] = jnp.zeros_like(pre_acc)
    hid_acc[...] = jnp.zeros_like(hid_acc)

    @pl.loop(0, len(FAR))
    def _(n):
        z = far_z(n)
        x_copy(z).wait()
        c_copy(n).wait()
        wait_far(n, plus[0], (up, down), far_sems)
        mine = block(n, width)
        cols = x[:, block(z, width)]
        pre_acc[...] += jnp.dot(cols, up[mine, :], preferred_element_type=F32)
        hid_acc[...] += jnp.dot(c[n], down[mine, :], preferred_element_type=F32)

    for copy in sums:
        copy.wait()
    pre = pre_acc[...] + pre_near[...]
    hid = hid_acc[...] + hid_near[...]
    grad_ref[...] = (2.0 * jnp.maximum(pre, 0.0) * hid).astype(BF)
    for k in range(len(NEAR)):
        x_copy(near_z(k)).wait()

    @pl.loop(0, N_Z)
    def _(z):
        product = lax.dot_general(
            x[:, block(z, width)], grad_ref[...], (((0,), (0,)), ((), ())),
            preferred_element_type=F32,
        ).astype(BF)
        dw[z] = product.reshape(dw.shape[1:])
        out_copy(z).start()

    for z in range(N_Z):
        out_copy(z).wait()


def input_kernel(grad_ref, near_ref, *refs):
    plus, minus = refs[0:4], refs[4:8]
    keep_ref, give_ref, up, sems = refs[8:]
    core = lax.axis_index("core")
    tokens = keep_ref.shape[0]
    width = N_Y * near_ref.shape[2] // 2
    for n in range(len(FAR)):
        for copy in far_copies(n, plus, minus, (up,), sems):
            copy.start()

    def product(out, which, z, rows):
        mine = grad_ref[block(which, tokens), :]
        out[:, block(z, width)] = lax.dot_general(
            mine, rows, (((1,), (1,)), ((), ())), preferred_element_type=F32
        ).astype(BF)

    @pl.loop(0, len(NEAR))
    def _(k):
        rows = near_rows(near_ref, k, 0)
        product(give_ref, 1 - core, near_z(k), rows)
        product(keep_ref, core, near_z(k), rows)

    @pl.loop(0, len(FAR))
    def _(n):
        wait_far(n, plus[0], (up,), sems)
        rows = up[block(n, width), :]
        product(give_ref, 1 - core, far_z(n), rows)
        product(keep_ref, core, far_z(n), rows)


def call(kernel, outs, args, flops, in_hbm, scratch=(), dtype=BF, out_hbm=()):
    vm = pl.BlockSpec(memory_space=pltpu.VMEM)
    hbm = pl.BlockSpec(memory_space=pl.ANY)
    return pl.pallas_call(
        kernel,
        out_shape=tuple(jax.ShapeDtypeStruct(s, dtype) for s in outs),
        in_specs=[hbm if k in in_hbm else vm for k in range(len(args))],
        out_specs=tuple(hbm if k in out_hbm else vm for k in range(len(outs))),
        scratch_shapes=scratch,
        cost_estimate=pl.CostEstimate(
            flops=flops,
            bytes_accessed=2 * sum(a.size for a in args),
            transcendentals=0,
        ),
    )(*args)


def total(a, b):
    return (a.astype(F32) + b.astype(F32)).astype(BF)


def per_device(inputs, w_up, w_down, cotangent):
    rows, h = w_up.shape
    tokens, width = inputs.shape
    own = jnp.concatenate([w_up, w_down.T], axis=0)
    back = [own]
    ahead = [own]
    for _ in range(3):
        back.append(shifted(back[-1], Z, 1))
        ahead.append(shifted(ahead[-1], Z, -1))
    plus_last = shifted(back[3][:rows], Z, 1)
    minus_last = shifted(ahead[3][rows:], Z, -1)
    near = copies_over(jnp.stack([own, back[1], ahead[1]]), "y")
    plus = [jnp.concatenate([back[2], back[3], plus_last], axis=0)]
    minus = [jnp.concatenate([ahead[2], ahead[3], minus_last], axis=0)]
    plus.append(shifted(plus[0], "y", 1))
    minus_after = shifted(minus[0], "y", -1)
    minus.append(shifted(minus[0], "y", 1))
    plus.append(shifted(plus[0], "y", -1))
    minus.append(minus_after)
    plus.append(shifted(plus[1], "y", 1))
    minus.append(shifted(minus_after, "y", -1))
    unit = tokens * width * h // 2
    part = N_Y * rows
    pre, hid = call(
        near_kernel,
        [(tokens, h)] * 2,
        (inputs, cotangent, near),
        3 * unit,
        (),
        dtype=F32,
    )
    grad, dw = call(
        weight_kernel,
        [(tokens, h), (N_Y, 4, 2, rows, h)],
        (inputs, cotangent, pre, hid, *plus, *minus),
        9 * unit,
        range(12),
        [
            pltpu.VMEM((tokens, width), BF),
            pltpu.VMEM((len(FAR), tokens, part), BF),
            pltpu.VMEM((len(FAR) * part, h), BF),
            pltpu.VMEM((len(FAR) * part, h), BF),
            *[pltpu.VMEM((tokens, h), F32)] * 4,
            pltpu.VMEM((N_Z, N_Y, rows, h), BF),
            pltpu.SemaphoreType.DMA((N_Z,)),
            pltpu.SemaphoreType.DMA((len(FAR),)),
            pltpu.SemaphoreType.DMA((2,)),
            pltpu.SemaphoreType.DMA((len(FAR), 2, N_Y)),
            pltpu.SemaphoreType.DMA((N_Z,)),
        ],
        out_hbm=(1,),
    )
    keep, give = call(
        input_kernel,
        [(tokens // 2, width)] * 2,
        (grad, near, *plus, *minus),
        4 * unit,
        range(2, 10),
        [
            pltpu.VMEM((len(FAR) * part, h), BF),
            pltpu.SemaphoreType.DMA((len(FAR), 1, N_Y)),
        ],
    )

    over_core = total(keep, swapped(give, "core", lambda i: 1 - i))
    step = swapped(over_core, "x", lambda i: i ^ 1)
    over_pair = total(over_core, step)
    step = swapped(over_pair, "x", lambda i: 3 - i)
    mine = total(over_pair, step)
    other = swapped(mine, "core", lambda i: 1 - i)
    first = lax.axis_index("core") == 0
    d_inputs = jnp.concatenate(
        [jnp.where(first, mine, other), jnp.where(first, other, mine)], axis=0
    )

    by_y = exchange(dw, "y")
    over_y = by_y.astype(F32).sum(0).astype(BF)
    by_near = exchange(over_y, "zl")
    over_near = by_near.astype(F32).sum(0).astype(BF)
    to_far = jnp.broadcast_to(over_near, (2, *over_near.shape)).reshape(4, rows, h)
    by_far = exchange(to_far, ("rep", "zh"))
    return (d_inputs, by_far.astype(F32).sum(0))


def solution(mesh):
    split = Mesh(
        mesh.devices.reshape(2, 2, 4, N_Y, 4, 2),
        ("rep", "zh", "zl", "y", "x", "core"),
    )
    placed = (P(REP_FS, None), P(FS, TP), P(TP, FS), P(REP_FS, None))
    return jax.shard_map(
        per_device,
        mesh=split,
        in_specs=placed,
        out_specs=(P(REP_FS, None), P(FS, TP)),
        check_vma=False,
    )
```

time: 179 us -> 174 us (0.972)
  waiting for transfers between devices: 75.7 us -> 54.8 us
  starting transfers between devices: 71.7 us -> 86.4 us
  Pallas kernels: 17 us -> 18.9 us
    ppermute x13 -> x14, waiting for transfers between devices: 23.3 us -> 2.14 us  [shifted(): return lax.ppermute(value, axes, [(i, (i + step) % n) for i in range(n)])]
    ppermute x13 -> x14, starting transfers between devices: 41.7 us -> 57.3 us  [shifted(): return lax.ppermute(value, axes, [(i, (i + step) % n) for i in range(n)])]
    pallas_call x3, Pallas kernels: 17 us -> 18.9 us  [call(): pl.pallas_call(kernel, out_shape=tuple((jax.ShapeDtypeStruct(s, dtype) fo...]
  transfers between devices with their start and end apart: 21 -> 22, of which waited for: 11 -> 10; matrix products, arithmetic and copies ran while one was open for 4% -> 5% of each run, Pallas kernels for 2% -> 3%
where the time goes in v4:
time: 174 us; the launch traced here: 173 us
  starting transfers between devices  86.4 us (50%)
  waiting for transfers between devices  54.8 us (31%)
  Pallas kernels  18.9 us (11%)
  other arithmetic  8.75 us (5%)
  local copies, waits for them, and re-layouts  3.48 us (2%)
    ppermute x14, starting transfers between devices, shifted(): return lax.ppermute(value, axes, [(i, (i + step) % n) for i in range(n)])  57.3 us
    all_to_all x4, waiting for transfers between devices, exchange(): return lax.all_to_all(parts, axes, split_axis=0, concat_axis=0, tiled=True)  29.5 us
    ppermute x4, waiting for transfers between devices, swapped(): return lax.ppermute(value, axes, [(i, partner(i)) for i in range(n)])  23.1 us
    all_to_all x4, starting transfers between devices, exchange(): return lax.all_to_all(parts, axes, split_axis=0, concat_axis=0, tiled=True)  19.6 us
    pallas_call x3, Pallas kernels, call(): pl.pallas_call(kernel, out_shape=tuple((jax.ShapeDtypeStruct(s, dtype) fo...  18.9 us
    ppermute x4, starting transfers between devices, swapped(): return lax.ppermute(value, axes, [(i, partner(i)) for i in range(n)])  9.39 us
    convert_element_type x3, other arithmetic, total(): return (a.astype(F32) + b.astype(F32)).astype(BF)  4.42 us
  transfers between devices with their start and end apart: 22, of which 10 were waited for; matrix products, arithmetic and copies ran while one was open for 5% of the time, Pallas kernels for 3%

profile of v4, /device:TPU:4, one launch (start us, length us, event | category | flops | bytes accessed | tf_op | source)
XLA Modules:
  0.0 173.3 jit_solution(5942953131948915904)
XLA Ops:
  0.6 0.9 fusion
  1.5 11.4 %collective-permute-start.1 = (bf16[128,512]{1,0:T(8,128)(2,1)S(1)}, bf16[128,512]{1,0:T(8,128)(2,1)S(1)}, u32[]{:S(2)}, u32[]{:S(2)}) collective-permute-start(bf16[128,512]{1,0:T(8,128)(2,1)S(1)} %get-tuple-element.17), channel_id=1, source_target_pairs={{0,480},{32,0},{64,32},{96,64},{128,96},{160,128},{192,160},{224,1... | collective-permute-start | bytes 393224 | tf_op jit(solution)/shard_map/ppermute | solution.py:35
  12.9 1.9 %collective-permute-start = (bf16[128,512]{1,0:T(8,128)(2,1)S(1)}, bf16[128,512]{1,0:T(8,128)(2,1)S(1)}, u32[]{:S(2)}, u32[]{:S(2)}) collective-permute-start(bf16[128,512]{1,0:T(8,128)(2,1)S(1)} %get-tuple-element.17), channel_id=1, source_target_pairs={{0,32},{32,64},{64,96},{96,128},{128,160},{160,192},{192,224},{224... | collective-permute-start | bytes 393224 | tf_op jit(solution)/shard_map/ppermute | solution.py:35
  14.9 0.8 collective-permute-done.1
  15.7 5.6 %collective-permute-start.8 = (bf16[128,512]{1,0:T(8,128)(2,1)S(1)}, bf16[128,512]{1,0:T(8,128)(2,1)S(1)}, u32[]{:S(2)}, u32[]{:S(2)}) collective-permute-start(bf16[128,512]{1,0:T(8,128)(2,1)S(1)} %collective-permute-done.1), channel_id=1, source_target_pairs={{0,480},{32,0},{64,32},{96,64},{128,96},{160,128},{192,160},{224,1... | collective-permute-start | bytes 393224 | tf_op jit(solution)/shard_map/ppermute | solution.py:35
  21.3 0.0 collective-permute-done
  21.3 1.9 %collective-permute-start.2 = (bf16[128,512]{1,0:T(8,128)(2,1)S(1)}, bf16[128,512]{1,0:T(8,128)(2,1)S(1)}, u32[]{:S(2)}, u32[]{:S(2)}) collective-permute-start(bf16[128,512]{1,0:T(8,128)(2,1)S(1)} %collective-permute-done), channel_id=1, source_target_pairs={{0,32},{32,64},{64,96},{96,128},{128,160},{160,192},{192,224},{224... | collective-permute-start | bytes 393224 | tf_op jit(solution)/shard_map/ppermute | solution.py:35
  23.3 1.3 broadcast_in_dim.6
  24.5 4.5 %all-to-all-start = ((bf16[4,3,128,512]{3,2,1,0:T(8,128)(2,1)}), bf16[4,3,128,512]{3,2,1,0:T(8,128)(2,1)S(1)}, u32[]{:S(2)}, u32[]{:S(2)}) async-start(bf16[4,3,128,512]{3,2,1,0:T(8,128)(2,1)} %broadcast_in_dim.6), calls=%async_computation | async-start | bytes 3145728 | tf_op jit(solution)/shard_map/all_to_all | solution.py:24
  29.0 0.0 collective-permute-done.8
  29.0 5.1 %collective-permute-start.9 = (bf16[128,512]{1,0:T(8,128)(2,1)S(1)}, bf16[128,512]{1,0:T(8,128)(2,1)S(1)}, u32[]{:S(2)}, u32[]{:S(2)}) collective-permute-start(bf16[128,512]{1,0:T(8,128)(2,1)S(1)} %collective-permute-done.8), channel_id=1, source_target_pairs={{0,480},{32,0},{64,32},{96,64},{128,96},{160,128},{192,160},{224,1... | collective-permute-start | bytes 393224 | tf_op jit(solution)/shard_map/ppermute | solution.py:35
  34.1 0.0 collective-permute-done.2
  34.1 1.9 %collective-permute-start.3 = (bf16[128,512]{1,0:T(8,128)(2,1)S(1)}, bf16[128,512]{1,0:T(8,128)(2,1)S(1)}, u32[]{:S(2)}, u32[]{:S(2)}) collective-permute-start(bf16[128,512]{1,0:T(8,128)(2,1)S(1)} %collective-permute-done.2), channel_id=1, source_target_pairs={{0,32},{32,64},{64,96},{96,128},{128,160},{160,192},{192,224},{224... | collective-permute-start | bytes 393224 | tf_op jit(solution)/shard_map/ppermute | solution.py:35
  36.1 0.5 collective-permute-done.9
  36.6 5.6 %collective-permute-start.10 = (bf16[64,512]{1,0:T(8,128)(2,1)S(1)}, bf16[64,512]{1,0:T(8,128)(2,1)S(1)}, u32[]{:S(2)}, u32[]{:S(2)}) collective-permute-start(bf16[64,512]{1,0:T(8,128)(2,1)S(1)} %slice.9), channel_id=1, source_target_pairs={{0,480},{32,0},{64,32},{96,64},{128,96},{160,128},{192,160},{224,1... | collective-permute-start | bytes 196616 | tf_op jit(solution)/shard_map/ppermute | solution.py:35
  42.2 0.0 collective-permute-done.3
  42.2 1.9 %collective-permute-start.4 = (bf16[64,512]{1,0:T(8,128)(2,1)S(1)}, bf16[64,512]{1,0:T(8,128)(2,1)S(1)}, u32[]{:S(2)}, u32[]{:S(2)}) collective-permute-start(bf16[64,512]{1,0:T(8,128)(2,1)S(1)} %slice.8), channel_id=1, source_target_pairs={{0,32},{32,64},{64,96},{96,128},{128,160},{160,192},{192,224},{224... | collective-permute-start | bytes 196616 | tf_op jit(solution)/shard_map/ppermute | solution.py:35
  44.2 0.0 collective-permute-done.10
  44.2 0.0 copy-start.3
  44.2 5.1 %collective-permute-start.12 = (bf16[320,512]{1,0:T(8,128)(2,1)S(1)}, bf16[320,512]{1,0:T(8,128)(2,1)S(1)}, u32[]{:S(2)}, u32[]{:S(2)}) collective-permute-start(bf16[320,512]{1,0:T(8,128)(2,1)S(1)} %constant_dynamic-update-slice_fusion.3.refs_4_), channel_id=1, source_target_pairs={{0,24},{8,0},{16,8},{24,16},{1,25},{9,1},{17,9},{25,17},{2,26},{10... | collective-permute-start | bytes 983048 | tf_op jit(solution)/shard_map/ppermute | solution.py:35
  49.4 0.2 collective-permute-done.4
  49.6 3.9 %collective-permute-start.5 = (bf16[320,512]{1,0:T(8,128)(2,1)S(1)}, bf16[320,512]{1,0:T(8,128)(2,1)S(1)}, u32[]{:S(2)}, u32[]{:S(2)}) collective-permute-start(bf16[320,512]{1,0:T(8,128)(2,1)S(1)} %constant_dynamic-update-slice_fusion.refs_0_), channel_id=1, source_target_pairs={{0,8},{8,16},{16,24},{24,0},{1,9},{9,17},{17,25},{25,1},{2,10},{10... | collective-permute-start | bytes 983048 | tf_op jit(solution)/shard_map/ppermute | solution.py:35
  53.5 3.4 %collective-permute-start.11 = (bf16[320,512]{1,0:T(8,128)(2,1)S(1)}, bf16[320,512]{1,0:T(8,128)(2,1)S(1)}, u32[]{:S(2)}, u32[]{:S(2)}) collective-permute-start(bf16[320,512]{1,0:T(8,128)(2,1)S(1)} %constant_dynamic-update-slice_fusion.3.refs_4_), channel_id=1, source_target_pairs={{0,8},{8,16},{16,24},{24,0},{1,9},{9,17},{17,25},{25,1},{2,10},{10... | collective-permute-start | bytes 983048 | tf_op jit(solution)/shard_map/ppermute | solution.py:35
  56.9 3.7 %collective-permute-start.6 = (bf16[320,512]{1,0:T(8,128)(2,1)S(1)}, bf16[320,512]{1,0:T(8,128)(2,1)S(1)}, u32[]{:S(2)}, u32[]{:S(2)}) collective-permute-start(bf16[320,512]{1,0:T(8,128)(2,1)S(1)} %constant_dynamic-update-slice_fusion.refs_0_), channel_id=1, source_target_pairs={{0,24},{8,0},{16,8},{24,16},{1,25},{9,1},{17,9},{25,17},{2,26},{10... | collective-permute-start | bytes 983048 | tf_op jit(solution)/shard_map/ppermute | solution.py:35
  60.6 0.0 collective-permute-done.12.refs_6_
  60.6 1.9 %collective-permute-start.13 = (bf16[320,512]{1,0:T(8,128)(2,1)S(1)}, bf16[320,512]{1,0:T(8,128)(2,1)}, u32[]{:S(2)}, u32[]{:S(2)}) collective-permute-start(bf16[320,512]{1,0:T(8,128)(2,1)S(1)} %collective-permute-done.12.refs_6_), channel_id=1, source_target_pairs={{0,24},{8,0},{16,8},{24,16},{1,25},{9,1},{17,9},{25,17},{2,26},{10... | collective-permute-start | bytes 983048 | tf_op jit(solution)/shard_map/ppermute | solution.py:35
  62.6 0.0 collective-permute-done.5.refs_1_
  62.6 3.9 %collective-permute-start.7 = (bf16[320,512]{1,0:T(8,128)(2,1)S(1)}, bf16[320,512]{1,0:T(8,128)(2,1)}, u32[]{:S(2)}, u32[]{:S(2)}) collective-permute-start(bf16[320,512]{1,0:T(8,128)(2,1)S(1)} %collective-permute-done.5.refs_1_), channel_id=1, source_target_pairs={{0,8},{8,16},{16,24},{24,0},{1,9},{9,17},{17,25},{25,1},{2,10},{10... | collective-permute-start | bytes 983048 | tf_op jit(solution)/shard_map/ppermute | solution.py:35
  66.5 0.0 all-to-all-done.near_ref
  66.5 0.0 copy-start
  66.5 1.1 copy-done
  67.7 4.6 %shard_map.59 = (f32[384,512]{1,0:T(8,128)}, f32[384,512]{1,0:T(8,128)}) custom-call(bf16[384,2048]{1,0:T(8,128)(2,1)} %x_hbm.1, bf16[384,2048]{1,0:T(8,128)(2,1)} %c_hbm.1, bf16[4,3,128,512]{3,2,1,0:T(8,128)(2,1)} %copy-done), custom_call_target="tpu_custom_call" | custom-call | flops 603979776 | bytes 4718592 | tf_op jit(solution)/shard_map/pallas_call | solution.py:206
  72.3 0.0 collective-permute-done.11.refs_5_
  72.3 0.0 collective-permute-done.6.refs_2_
  72.3 0.0 collective-permute-done.13.refs_7_
  72.3 0.6 collective-permute-done.7.refs_3_
  72.9 0.1 copy-done.6
  73.0 0.1 copy-done.7
  73.1 8.8 %shard_map.60 = (bf16[384,512]{1,0:T(8,128)(2,1)}, bf16[4,4,2,64,512]{4,3,2,1,0:T(8,128)(2,1)}) custom-call(bf16[384,2048]{1,0:T(8,128)(2,1)} %x_hbm.1, bf16[384,2048]{1,0:T(8,128)(2,1)} %c_hbm.1, f32[384,512]{1,0:T(8,128)} %get-tuple-element.8.pre_hbm, f32[384,512]{1,0:T(8,128)} %get-tuple-element.9.hid_hbm, bf16[320,512]{1,0:T(8,128)(2,1)} %copy-done.2, ...), custom_call_target="tpu_custom_call" | custom-call | flops 1811939328 | bytes 6553600 | tf_op jit(solution)/shard_map/pallas_call | solution.py:206
  81.9 5.5 %shard_map.61 = (bf16[192,2048]{1,0:T(8,128)(2,1)}, bf16[192,2048]{1,0:T(8,128)(2,1)}) custom-call(bf16[384,512]{1,0:T(8,128)(2,1)} %get-tuple-element.10.grad_ref, bf16[4,3,128,512]{3,2,1,0:T(8,128)(2,1)} %copy-done, bf16[320,512]{1,0:T(8,128)(2,1)} %copy-done.2, bf16[320,512]{1,0:T(8,128)(2,1)} %copy-done.5, bf16[320,512]{1,0:T(8,128)(2,1)} %copy-done.7, ...), custom_call_target="tpu_custom_call" | custom-call | flops 805306368 | bytes 4587520 | tf_op jit(solution)/shard_map/pallas_call | solution.py:206
  87.4 1.9 %collective-permute-start.14 = (bf16[192,2048]{1,0:T(8,128)(2,1)}, bf16[192,2048]{1,0:T(8,128)(2,1)S(1)}, u32[]{:S(2)}, u32[]{:S(2)}) collective-permute-start(bf16[192,2048]{1,0:T(8,128)(2,1)} %get-tuple-element.12), channel_id=1, source_target_pairs={{0,1},{1,0},{2,3},{3,2},{4,5},{5,4},{6,7},{7,6},{8,9},{9,8},{10,11... | collective-permute-start | bytes 2359304 | tf_op jit(solution)/shard_map/ppermute | solution.py:40
  89.4 2.5 %collective-permute-done.14 = bf16[192,2048]{1,0:T(8,128)(2,1)S(1)} collective-permute-done((bf16[192,2048]{1,0:T(8,128)(2,1)}, bf16[192,2048]{1,0:T(8,128)(2,1)S(1)}, u32[]{:S(2)}, u32[]{:S(2)}) %collective-permute-start.14) | collective-permute-done | bytes 786464 | tf_op jit(solution)/shard_map/ppermute | solution.py:40
  91.8 1.4 add_convert_fusion.2
  93.2 0.0 copy-start.1
  93.3 3.1 %collective-permute-start.15 = (bf16[192,2048]{1,0:T(8,128)(2,1)S(1)}, bf16[192,2048]{1,0:T(8,128)(2,1)}, u32[]{:S(2)}, u32[]{:S(2)}) collective-permute-start(bf16[192,2048]{1,0:T(8,128)(2,1)S(1)} %add_convert_fusion.2), channel_id=1, source_target_pairs={{0,2},{2,0},{4,6},{6,4},{1,3},{3,1},{5,7},{7,5},{8,10},{10,8},{12,... | collective-permute-start | bytes 2359304 | tf_op jit(solution)/shard_map/ppermute | solution.py:40
  96.4 3.6 %all-to-all-start.1 = ((bf16[4,4,2,64,512]{4,3,2,1,0:T(8,128)(2,1)}), bf16[4,4,2,64,512]{4,3,2,1,0:T(8,128)(2,1)S(1)}, u32[]{:S(2)}, u32[]{:S(2)}) async-start(bf16[4,4,2,64,512]{4,3,2,1,0:T(8,128)(2,1)} %get-tuple-element.13), calls=%async_computation.1 | async-start | bytes 4194304 | tf_op jit(solution)/shard_map/all_to_all | solution.py:24
  100.0 14.8 %collective-permute-done.15 = bf16[192,2048]{1,0:T(8,128)(2,1)} collective-permute-done((bf16[192,2048]{1,0:T(8,128)(2,1)S(1)}, bf16[192,2048]{1,0:T(8,128)(2,1)}, u32[]{:S(2)}, u32[]{:S(2)}) %collective-permute-start.15) | collective-permute-done | bytes 786464 | tf_op jit(solution)/shard_map/ppermute | solution.py:40
  114.8 1.6 add_convert_fusion.1
  116.5 2.4 %collective-permute-start.16 = (bf16[192,2048]{1,0:T(8,128)(2,1)S(1)}, bf16[192,2048]{1,0:T(8,128)(2,1)}, u32[]{:S(2)}, u32[]{:S(2)}) collective-permute-start(bf16[192,2048]{1,0:T(8,128)(2,1)S(1)} %add_convert_fusion.1), channel_id=1, source_target_pairs={{0,6},{2,4},{4,2},{6,0},{1,7},{3,5},{5,3},{7,1},{8,14},{10,12},{12... | collective-permute-start | bytes 2359304 | tf_op jit(solution)/shard_map/ppermute | solution.py:40
  118.9 7.7 %all-to-all-done.1 = bf16[4,4,2,64,512]{4,3,2,1,0:T(8,128)(2,1)S(1)} async-done(((bf16[4,4,2,64,512]{4,3,2,1,0:T(8,128)(2,1)}), bf16[4,4,2,64,512]{4,3,2,1,0:T(8,128)(2,1)S(1)}, u32[]{:S(2)}, u32[]{:S(2)}) %all-to-all-start.1) | async-done | bytes 2097184 | tf_op jit(solution)/shard_map/all_to_all | solution.py:24
  126.6 1.3 reduce_sum.33
  127.9 3.5 %all-to-all-start.2 = ((bf16[4,2,64,512]{3,2,1,0:T(8,128)(2,1)}), bf16[4,2,64,512]{3,2,1,0:T(8,128)(2,1)S(1)}, u32[]{:S(2)}, u32[]{:S(2)}) async-start(bf16[4,2,64,512]{3,2,1,0:T(8,128)(2,1)} %reduce_sum.33), calls=%async_computation.2 | async-start | bytes 1048576 | tf_op jit(solution)/shard_map/all_to_all | solution.py:24
  131.3 5.9 %collective-permute-done.16 = bf16[192,2048]{1,0:T(8,128)(2,1)} collective-permute-done((bf16[192,2048]{1,0:T(8,128)(2,1)S(1)}, bf16[192,2048]{1,0:T(8,128)(2,1)}, u32[]{:S(2)}, u32[]{:S(2)}) %collective-permute-start.16) | collective-permute-done | bytes 786464 | tf_op jit(solution)/shard_map/ppermute | solution.py:40
  137.2 1.4 add_convert_fusion
  138.6 1.9 %collective-permute-start.17 = (bf16[192,2048]{1,0:T(8,128)(2,1)S(1)}, bf16[192,2048]{1,0:T(8,128)(2,1)S(1)}, u32[]{:S(2)}, u32[]{:S(2)}) collective-permute-start(bf16[192,2048]{1,0:T(8,128)(2,1)S(1)} %add_convert_fusion), channel_id=1, source_target_pairs={{0,1},{1,0},{2,3},{3,2},{4,5},{5,4},{6,7},{7,6},{8,9},{9,8},{10,11... | collective-permute-start | bytes 2359304 | tf_op jit(solution)/shard_map/ppermute | solution.py:40
  140.5 4.7 %all-to-all-done.2 = bf16[4,2,64,512]{3,2,1,0:T(8,128)(2,1)S(1)} async-done(((bf16[4,2,64,512]{3,2,1,0:T(8,128)(2,1)}), bf16[4,2,64,512]{3,2,1,0:T(8,128)(2,1)S(1)}, u32[]{:S(2)}, u32[]{:S(2)}) %all-to-all-start.2) | async-done | bytes 524320 | tf_op jit(solution)/shard_map/all_to_all | solution.py:24
  145.2 0.1 reduce_sum.34
  145.3 0.7 broadcast_in_dim.7
  146.1 8.1 %all-to-all-start.3 = ((bf16[4,64,512]{2,1,0:T(8,128)(2,1)}), bf16[4,64,512]{2,1,0:T(8,128)(2,1)S(1)}, u32[]{:S(2)}, u32[]{:S(2)}) async-start(bf16[4,64,512]{2,1,0:T(8,128)(2,1)} %bitcast.4), calls=%async_computation.3 | async-start | bytes 524288 | tf_op jit(solution)/shard_map/all_to_all | solution.py:24
  154.1 0.0 collective-permute-done.17
  154.1 0.1 broadcast_select_fusion.1
  154.3 1.2 pad_maximum_fusion
  155.5 17.1 %all-to-all-done.3 = bf16[4,64,512]{2,1,0:T(8,128)(2,1)S(1)} async-done(((bf16[4,64,512]{2,1,0:T(8,128)(2,1)}), bf16[4,64,512]{2,1,0:T(8,128)(2,1)S(1)}, u32[]{:S(2)}, u32[]{:S(2)}) %all-to-all-start.3) | async-done | bytes 262176 | tf_op jit(solution)/shard_map/all_to_all | solution.py:24
  172.6 0.7 convert_reduce_fusion
  (19 shorter events, 0.1 us)
Async XLA Ops:
  1.5 14.1 %collective-permute-start.1 = (bf16[128,512]{1,0:T(8,128)(2,1)S(1)}, bf16[128,512]{1,0:T(8,128)(2,1)S(1)}, u32[]{:S(2)}, u32[]{:S(2)}) collective-permute-start(bf16[128,512]{1,0:T(8,128)(2,1)S(1)} %get-tuple-element.17), channel_id=1, source_target_pairs={{0,480},{32,0},{64,32},{96,64},{128,96},{160,128},{192,160},{224,1... | collective-permute-start | bytes 393224 | tf_op jit(solution)/shard_map/ppermute | solution.py:35
  12.9 8.3 %collective-permute-start = (bf16[128,512]{1,0:T(8,128)(2,1)S(1)}, bf16[128,512]{1,0:T(8,128)(2,1)S(1)}, u32[]{:S(2)}, u32[]{:S(2)}) collective-permute-start(bf16[128,512]{1,0:T(8,128)(2,1)S(1)} %get-tuple-element.17), channel_id=1, source_target_pairs={{0,32},{32,64},{64,96},{96,128},{128,160},{160,192},{192,224},{224... | collective-permute-start | bytes 393224 | tf_op jit(solution)/shard_map/ppermute | solution.py:35
  15.7 13.3 %collective-permute-start.8 = (bf16[128,512]{1,0:T(8,128)(2,1)S(1)}, bf16[128,512]{1,0:T(8,128)(2,1)S(1)}, u32[]{:S(2)}, u32[]{:S(2)}) collective-permute-start(bf16[128,512]{1,0:T(8,128)(2,1)S(1)} %collective-permute-done.1), channel_id=1, source_target_pairs={{0,480},{32,0},{64,32},{96,64},{128,96},{160,128},{192,160},{224,1... | collective-permute-start | bytes 393224 | tf_op jit(solution)/shard_map/ppermute | solution.py:35
  21.3 12.9 %collective-permute-start.2 = (bf16[128,512]{1,0:T(8,128)(2,1)S(1)}, bf16[128,512]{1,0:T(8,128)(2,1)S(1)}, u32[]{:S(2)}, u32[]{:S(2)}) collective-permute-start(bf16[128,512]{1,0:T(8,128)(2,1)S(1)} %collective-permute-done), channel_id=1, source_target_pairs={{0,32},{32,64},{64,96},{96,128},{128,160},{160,192},{192,224},{224... | collective-permute-start | bytes 393224 | tf_op jit(solution)/shard_map/ppermute | solution.py:35
  24.5 42.0 %all-to-all-start = ((bf16[4,3,128,512]{3,2,1,0:T(8,128)(2,1)}), bf16[4,3,128,512]{3,2,1,0:T(8,128)(2,1)S(1)}, u32[]{:S(2)}, u32[]{:S(2)}) async-start(bf16[4,3,128,512]{3,2,1,0:T(8,128)(2,1)} %broadcast_in_dim.6), calls=%async_computation | async-start | bytes 3145728 | tf_op jit(solution)/shard_map/all_to_all | solution.py:24
  29.0 7.6 %collective-permute-start.9 = (bf16[128,512]{1,0:T(8,128)(2,1)S(1)}, bf16[128,512]{1,0:T(8,128)(2,1)S(1)}, u32[]{:S(2)}, u32[]{:S(2)}) collective-permute-start(bf16[128,512]{1,0:T(8,128)(2,1)S(1)} %collective-permute-done.8), channel_id=1, source_target_pairs={{0,480},{32,0},{64,32},{96,64},{128,96},{160,128},{192,160},{224,1... | collective-permute-start | bytes 393224 | tf_op jit(solution)/shard_map/ppermute | solution.py:35
  34.1 8.1 %collective-permute-start.3 = (bf16[128,512]{1,0:T(8,128)(2,1)S(1)}, bf16[128,512]{1,0:T(8,128)(2,1)S(1)}, u32[]{:S(2)}, u32[]{:S(2)}) collective-permute-start(bf16[128,512]{1,0:T(8,128)(2,1)S(1)} %collective-permute-done.2), channel_id=1, source_target_pairs={{0,32},{32,64},{64,96},{96,128},{128,160},{160,192},{192,224},{224... | collective-permute-start | bytes 393224 | tf_op jit(solution)/shard_map/ppermute | solution.py:35
  36.6 7.6 %collective-permute-start.10 = (bf16[64,512]{1,0:T(8,128)(2,1)S(1)}, bf16[64,512]{1,0:T(8,128)(2,1)S(1)}, u32[]{:S(2)}, u32[]{:S(2)}) collective-permute-start(bf16[64,512]{1,0:T(8,128)(2,1)S(1)} %slice.9), channel_id=1, source_target_pairs={{0,480},{32,0},{64,32},{96,64},{128,96},{160,128},{192,160},{224,1... | collective-permute-start | bytes 196616 | tf_op jit(solution)/shard_map/ppermute | solution.py:35
  42.2 7.4 %collective-permute-start.4 = (bf16[64,512]{1,0:T(8,128)(2,1)S(1)}, bf16[64,512]{1,0:T(8,128)(2,1)S(1)}, u32[]{:S(2)}, u32[]{:S(2)}) collective-permute-start(bf16[64,512]{1,0:T(8,128)(2,1)S(1)} %slice.8), channel_id=1, source_target_pairs={{0,32},{32,64},{64,96},{96,128},{128,160},{160,192},{192,224},{224... | collective-permute-start | bytes 196616 | tf_op jit(solution)/shard_map/ppermute | solution.py:35
  44.2 28.7 %copy-start.3 = (bf16[320,512]{1,0:T(8,128)(2,1)}, bf16[320,512]{1,0:T(8,128)(2,1)S(1)}, u32[]{:S(2)}) copy-start(bf16[320,512]{1,0:T(8,128)(2,1)S(1)} %constant_dynamic-update-slice_fusion.3.refs_4_) | copy-start | bytes 983044
  44.2 16.4 %collective-permute-start.12 = (bf16[320,512]{1,0:T(8,128)(2,1)S(1)}, bf16[320,512]{1,0:T(8,128)(2,1)S(1)}, u32[]{:S(2)}, u32[]{:S(2)}) collective-permute-start(bf16[320,512]{1,0:T(8,128)(2,1)S(1)} %constant_dynamic-update-slice_fusion.3.refs_4_), channel_id=1, source_target_pairs={{0,24},{8,0},{16,8},{24,16},{1,25},{9,1},{17,9},{25,17},{2,26},{10... | collective-permute-start | bytes 983048 | tf_op jit(solution)/shard_map/ppermute | solution.py:35
  49.6 23.3 %copy-start.2 = (bf16[320,512]{1,0:T(8,128)(2,1)}, bf16[320,512]{1,0:T(8,128)(2,1)S(1)}, u32[]{:S(2)}) copy-start(bf16[320,512]{1,0:T(8,128)(2,1)S(1)} %constant_dynamic-update-slice_fusion.refs_0_) | copy-start | bytes 983044
  49.6 13.0 %collective-permute-start.5 = (bf16[320,512]{1,0:T(8,128)(2,1)S(1)}, bf16[320,512]{1,0:T(8,128)(2,1)S(1)}, u32[]{:S(2)}, u32[]{:S(2)}) collective-permute-start(bf16[320,512]{1,0:T(8,128)(2,1)S(1)} %constant_dynamic-update-slice_fusion.refs_0_), channel_id=1, source_target_pairs={{0,8},{8,16},{16,24},{24,0},{1,9},{9,17},{17,25},{25,1},{2,10},{10... | collective-permute-start | bytes 983048 | tf_op jit(solution)/shard_map/ppermute | solution.py:35
  53.5 18.7 %collective-permute-start.11 = (bf16[320,512]{1,0:T(8,128)(2,1)S(1)}, bf16[320,512]{1,0:T(8,128)(2,1)S(1)}, u32[]{:S(2)}, u32[]{:S(2)}) collective-permute-start(bf16[320,512]{1,0:T(8,128)(2,1)S(1)} %constant_dynamic-update-slice_fusion.3.refs_4_), channel_id=1, source_target_pairs={{0,8},{8,16},{16,24},{24,0},{1,9},{9,17},{17,25},{25,1},{2,10},{10... | collective-permute-start | bytes 983048 | tf_op jit(solution)/shard_map/ppermute | solution.py:35
  56.9 15.4 %collective-permute-start.6 = (bf16[320,512]{1,0:T(8,128)(2,1)S(1)}, bf16[320,512]{1,0:T(8,128)(2,1)S(1)}, u32[]{:S(2)}, u32[]{:S(2)}) collective-permute-start(bf16[320,512]{1,0:T(8,128)(2,1)S(1)} %constant_dynamic-update-slice_fusion.refs_0_), channel_id=1, source_target_pairs={{0,24},{8,0},{16,8},{24,16},{1,25},{9,1},{17,9},{25,17},{2,26},{10... | collective-permute-start | bytes 983048 | tf_op jit(solution)/shard_map/ppermute | solution.py:35
  60.6 12.3 %copy-start.4 = (bf16[320,512]{1,0:T(8,128)(2,1)}, bf16[320,512]{1,0:T(8,128)(2,1)S(1)}, u32[]{:S(2)}) copy-start(bf16[320,512]{1,0:T(8,128)(2,1)S(1)} %collective-permute-done.12.refs_6_) | copy-start | bytes 983044
  60.6 11.7 %collective-permute-start.13 = (bf16[320,512]{1,0:T(8,128)(2,1)S(1)}, bf16[320,512]{1,0:T(8,128)(2,1)}, u32[]{:S(2)}, u32[]{:S(2)}) collective-permute-start(bf16[320,512]{1,0:T(8,128)(2,1)S(1)} %collective-permute-done.12.refs_6_), channel_id=1, source_target_pairs={{0,24},{8,0},{16,8},{24,16},{1,25},{9,1},{17,9},{25,17},{2,26},{10... | collective-permute-start | bytes 983048 | tf_op jit(solution)/shard_map/ppermute | solution.py:35
  62.6 10.3 %copy-start.5 = (bf16[320,512]{1,0:T(8,128)(2,1)}, bf16[320,512]{1,0:T(8,128)(2,1)S(1)}, u32[]{:S(2)}) copy-start(bf16[320,512]{1,0:T(8,128)(2,1)S(1)} %collective-permute-done.5.refs_1_) | copy-start | bytes 983044
  62.6 10.3 %collective-permute-start.7 = (bf16[320,512]{1,0:T(8,128)(2,1)S(1)}, bf16[320,512]{1,0:T(8,128)(2,1)}, u32[]{:S(2)}, u32[]{:S(2)}) collective-permute-start(bf16[320,512]{1,0:T(8,128)(2,1)S(1)} %collective-permute-done.5.refs_1_), channel_id=1, source_target_pairs={{0,8},{8,16},{16,24},{24,0},{1,9},{9,17},{17,25},{25,1},{2,10},{10... | collective-permute-start | bytes 983048 | tf_op jit(solution)/shard_map/ppermute | solution.py:35
  66.5 1.1 copy-start
  72.3 0.7 copy-start.6
  72.3 0.8 copy-start.7
  87.4 4.4 %collective-permute-start.14 = (bf16[192,2048]{1,0:T(8,128)(2,1)}, bf16[192,2048]{1,0:T(8,128)(2,1)S(1)}, u32[]{:S(2)}, u32[]{:S(2)}) collective-permute-start(bf16[192,2048]{1,0:T(8,128)(2,1)} %get-tuple-element.12), channel_id=1, source_target_pairs={{0,1},{1,0},{2,3},{3,2},{4,5},{5,4},{6,7},{7,6},{8,9},{9,8},{10,11... | collective-permute-start | bytes 2359304 | tf_op jit(solution)/shard_map/ppermute | solution.py:40
  93.2 3.1 %copy-start.1 = (bf16[192,2048]{1,0:T(8,128)(2,1)}, bf16[192,2048]{1,0:T(8,128)(2,1)S(1)}, u32[]{:S(2)}) copy-start(bf16[192,2048]{1,0:T(8,128)(2,1)S(1)} %add_convert_fusion.2) | copy-start | bytes 2359300
  93.3 21.6 %collective-permute-start.15 = (bf16[192,2048]{1,0:T(8,128)(2,1)S(1)}, bf16[192,2048]{1,0:T(8,128)(2,1)}, u32[]{:S(2)}, u32[]{:S(2)}) collective-permute-start(bf16[192,2048]{1,0:T(8,128)(2,1)S(1)} %add_convert_fusion.2), channel_id=1, source_target_pairs={{0,2},{2,0},{4,6},{6,4},{1,3},{3,1},{5,7},{7,5},{8,10},{10,8},{12,... | collective-permute-start | bytes 2359304 | tf_op jit(solution)/shard_map/ppermute | solution.py:40
  96.4 30.2 %all-to-all-start.1 = ((bf16[4,4,2,64,512]{4,3,2,1,0:T(8,128)(2,1)}), bf16[4,4,2,64,512]{4,3,2,1,0:T(8,128)(2,1)S(1)}, u32[]{:S(2)}, u32[]{:S(2)}) async-start(bf16[4,4,2,64,512]{4,3,2,1,0:T(8,128)(2,1)} %get-tuple-element.13), calls=%async_computation.1 | async-start | bytes 4194304 | tf_op jit(solution)/shard_map/all_to_all | solution.py:24
  116.5 20.7 %collective-permute-start.16 = (bf16[192,2048]{1,0:T(8,128)(2,1)S(1)}, bf16[192,2048]{1,0:T(8,128)(2,1)}, u32[]{:S(2)}, u32[]{:S(2)}) collective-permute-start(bf16[192,2048]{1,0:T(8,128)(2,1)S(1)} %add_convert_fusion.1), channel_id=1, source_target_pairs={{0,6},{2,4},{4,2},{6,0},{1,7},{3,5},{5,3},{7,1},{8,14},{10,12},{12... | collective-permute-start | bytes 2359304 | tf_op jit(solution)/shard_map/ppermute | solution.py:40
  127.9 17.4 %all-to-all-start.2 = ((bf16[4,2,64,512]{3,2,1,0:T(8,128)(2,1)}), bf16[4,2,64,512]{3,2,1,0:T(8,128)(2,1)S(1)}, u32[]{:S(2)}, u32[]{:S(2)}) async-start(bf16[4,2,64,512]{3,2,1,0:T(8,128)(2,1)} %reduce_sum.33), calls=%async_computation.2 | async-start | bytes 1048576 | tf_op jit(solution)/shard_map/all_to_all | solution.py:24
  138.6 15.5 %collective-permute-start.17 = (bf16[192,2048]{1,0:T(8,128)(2,1)S(1)}, bf16[192,2048]{1,0:T(8,128)(2,1)S(1)}, u32[]{:S(2)}, u32[]{:S(2)}) collective-permute-start(bf16[192,2048]{1,0:T(8,128)(2,1)S(1)} %add_convert_fusion), channel_id=1, source_target_pairs={{0,1},{1,0},{2,3},{3,2},{4,5},{5,4},{6,7},{7,6},{8,9},{9,8},{10,11... | collective-permute-start | bytes 2359304 | tf_op jit(solution)/shard_map/ppermute | solution.py:40
  146.1 26.6 %all-to-all-start.3 = ((bf16[4,64,512]{2,1,0:T(8,128)(2,1)}), bf16[4,64,512]{2,1,0:T(8,128)(2,1)S(1)}, u32[]{:S(2)}, u32[]{:S(2)}) async-start(bf16[4,64,512]{2,1,0:T(8,128)(2,1)} %bitcast.4), calls=%async_computation.3 | async-start | bytes 524288 | tf_op jit(solution)/shard_map/all_to_all | solution.py:24

commit v5 on v2

--- a/solution.py
+++ b/solution.py
@@ -97,42 +97,26 @@
     return copies
 
 
-def weight_kernel(x_hbm, c_hbm, pre_hbm, hid_hbm, *refs):
+def weight_kernel(x_ref, c_ref, pre_ref, hid_ref, *refs):
     plus, minus = refs[0:4], refs[4:8]
-    grad_ref, dw_hbm, x, c, up, down, pre_acc, hid_acc, dw, sems, far_sems, out_sems = (
-        refs[8:]
-    )
+    grad_hbm, dw_hbm, up, down, pre_acc, hid_acc, grad, dw, far_sems, out_sems = refs[8:]
     width = dw.shape[1] * dw.shape[2]
-    first = [
-        pltpu.make_async_copy(src, dst, sems.at[k])
-        for k, (src, dst) in enumerate(
-            ((x_hbm, x), (pre_hbm, pre_acc), (hid_hbm, hid_acc))
-        )
-    ]
-    for copy in first:
-        copy.start()
-    places = []
-    c_copies = []
+    blocks = far_copies(plus, minus, (up, down), far_sems)
     for n, (_, _, z) in enumerate(z_blocks((None, FAR))):
+        for copy in blocks[n]:
+            copy.wait()
         at = pl.ds(pl.multiple_of(z * width, width), width)
-        copy = pltpu.make_async_copy(c_hbm.at[:, at], c.at[n], sems.at[3 + n])
-        copy.start()
-        places.append(at)
-        c_copies.append(copy)
-    blocks = far_copies(plus, minus, (up, down), far_sems)
-    for copy in first:
-        copy.wait()
-    for n, at in enumerate(places):
-        for copy in (c_copies[n], *blocks[n]):
-            copy.wait()
         mine = slice(n * width, (n + 1) * width)
-        pre_acc[...] += jnp.dot(x[:, at], up[mine], preferred_element_type=F32)
-        hid_acc[...] += jnp.dot(c[n], down[mine], preferred_element_type=F32)
-    grad_ref[...] = (2.0 * jnp.maximum(pre_acc[...], 0.0) * hid_acc[...]).astype(BF)
-    out = []
+        pre = jnp.dot(x_ref[:, at], up[mine], preferred_element_type=F32)
+        hid = jnp.dot(c_ref[:, at], down[mine], preferred_element_type=F32)
+        pre_acc[...] = (pre_ref if n == 0 else pre_acc)[...] + pre
+        hid_acc[...] = (hid_ref if n == 0 else hid_acc)[...] + hid
+    grad[...] = (2.0 * jnp.maximum(pre_acc[...], 0.0) * hid_acc[...]).astype(BF)
+    out = [pltpu.make_async_copy(grad, grad_hbm, out_sems.at[N_Z])]
+    out[0].start()
     for z in range(N_Z):
         product = lax.dot_general(
-            x[:, z * width : (z + 1) * width], grad_ref[...],
+            x_ref[:, z * width : (z + 1) * width], grad[...],
             (((0,), (0,)), ((), ())), preferred_element_type=F32,
         ).astype(BF)
         dw[z] = product.reshape(dw.shape[1:])
@@ -167,15 +151,20 @@
             ).astype(BF)
 
 
-def call(kernel, outs, args, flops, in_hbm, scratch=(), dtype=BF, out_hbm=()):
+def call(kernel, outs, args, flops, in_any, scratch=(), dtype=BF, out_hbm=()):
     vm = pl.BlockSpec(memory_space=pltpu.VMEM)
-    hbm = pl.BlockSpec(memory_space=pl.ANY)
+    any_ = pl.BlockSpec(memory_space=pl.ANY)
+    hbm = pl.BlockSpec(memory_space=pltpu.HBM)
     return pl.pallas_call(
         kernel,
-        out_shape=tuple(jax.ShapeDtypeStruct(s, dtype) for s in outs),
-        in_specs=[hbm if k in in_hbm else vm for k in range(len(args))],
+        out_shape=tuple(
+            pltpu.HBM(s, dtype) if k in out_hbm else jax.ShapeDtypeStruct(s, dtype)
+            for k, s in enumerate(outs)
+        ),
+        in_specs=[any_ if k in in_any else vm for k in range(len(args))],
         out_specs=tuple(hbm if k in out_hbm else vm for k in range(len(outs))),
         scratch_shapes=scratch,
+        compiler_params=pltpu.CompilerParams(vmem_limit_bytes=24 * 2**20),
         cost_estimate=pl.CostEstimate(
             flops=flops,
             bytes_accessed=2 * sum(a.size for a in args),
@@ -224,20 +213,18 @@
         [(tokens, h), (N_Y, 4, 2, rows, h)],
         (inputs, cotangent, pre, hid, *plus, *minus),
         9 * unit,
-        range(12),
+        range(4, 12),
         [
-            pltpu.VMEM((tokens, width), BF),
-            pltpu.VMEM((len(FAR), tokens, part), BF),
             pltpu.VMEM((len(FAR) * part, h), BF),
             pltpu.VMEM((len(FAR) * part, h), BF),
             pltpu.VMEM((tokens, h), F32),
             pltpu.VMEM((tokens, h), F32),
+            pltpu.VMEM((tokens, h), BF),
             pltpu.VMEM((N_Z, N_Y, rows, h), BF),
-            pltpu.SemaphoreType.DMA((3 + len(FAR),)),
             pltpu.SemaphoreType.DMA((len(FAR), 2, N_Y)),
-            pltpu.SemaphoreType.DMA((N_Z,)),
+            pltpu.SemaphoreType.DMA((N_Z + 1,)),
         ],
-        out_hbm=(1,),
+        out_hbm=(0, 1),
     )
     keep, give = call(
         input_kernel,

time: 173 us -> 171 us (0.988)
  Pallas kernels: 17.1 us -> 8.86 us
  local copies, waits for them, and re-layouts: 3.24 us -> 8.22 us
  waiting for transfers between devices: 55.3 us -> 59 us
    pallas_call x3, Pallas kernels: 17.1 us -> 8.86 us  [call(): pl.pallas_call(kernel, out_shape=tuple((pltpu.HBM(s, dtype) if k in out_h...]
    unnamed x20 -> x12, local copies, waits for them, and re-layouts: 1.21 us -> 5.57 us
    ppermute x14, waiting for transfers between devices: 2.58 us -> 6.51 us  [shifted(): return lax.ppermute(value, axes, [(i, (i + step) % n) for i in range(n)])]
  transfers between devices with their start and end apart: 22 -> 22, of which waited for: 10 -> 11; matrix products, arithmetic and copies ran while one was open for 5% -> 7% of each run, Pallas kernels for 2% -> 0%
where the time goes in v5:
time: 171 us; the launch traced here: 170 us
  starting transfers between devices  84.9 us (50%)
  waiting for transfers between devices  59 us (35%)
  Pallas kernels  8.86 us (5%)
  local copies, waits for them, and re-layouts  8.22 us (5%)
  other arithmetic  7.62 us (4%)
    ppermute x14, starting transfers between devices, shifted(): return lax.ppermute(value, axes, [(i, (i + step) % n) for i in range(n)])  55.7 us
    all_to_all x4, waiting for transfers between devices, exchange(): return lax.all_to_all(parts, axes, split_axis=0, concat_axis=0, tiled=True)  29.5 us
    ppermute x4, waiting for transfers between devices, swapped(): return lax.ppermute(value, axes, [(i, partner(i)) for i in range(n)])  22.9 us
    all_to_all x4, starting transfers between devices, exchange(): return lax.all_to_all(parts, axes, split_axis=0, concat_axis=0, tiled=True)  19.8 us
    ppermute x4, starting transfers between devices, swapped(): return lax.ppermute(value, axes, [(i, partner(i)) for i in range(n)])  9.38 us
    pallas_call x3, Pallas kernels, call(): pl.pallas_call(kernel, out_shape=tuple((pltpu.HBM(s, dtype) if k in out_h...  8.86 us
    ppermute x14, waiting for transfers between devices, shifted(): return lax.ppermute(value, axes, [(i, (i + step) % n) for i in range(n)])  6.51 us
    unnamed x12, local copies, waits for them, and re-layouts  5.57 us
  transfers between devices with their start and end apart: 22, of which 11 were waited for; matrix products, arithmetic and copies ran while one was open for 7% of the time, Pallas kernels for 0%

profile of v5, /device:TPU:4, one launch (start us, length us, event | category | flops | bytes accessed | tf_op | source)
XLA Modules:
  0.0 169.6 jit_solution(14530792313763336335)
XLA Ops:
  0.6 0.9 fusion
  1.5 11.4 %collective-permute-start.1 = (bf16[128,512]{1,0:T(8,128)(2,1)S(1)}, bf16[128,512]{1,0:T(8,128)(2,1)S(1)}, u32[]{:S(2)}, u32[]{:S(2)}) collective-permute-start(bf16[128,512]{1,0:T(8,128)(2,1)S(1)} %get-tuple-element.17), channel_id=1, source_target_pairs={{0,480},{32,0},{64,32},{96,64},{128,96},{160,128},{192,160},{224,1... | collective-permute-start | bytes 393224 | tf_op jit(solution)/shard_map/ppermute | solution.py:35
  12.9 1.9 %collective-permute-start = (bf16[128,512]{1,0:T(8,128)(2,1)S(1)}, bf16[128,512]{1,0:T(8,128)(2,1)S(1)}, u32[]{:S(2)}, u32[]{:S(2)}) collective-permute-start(bf16[128,512]{1,0:T(8,128)(2,1)S(1)} %get-tuple-element.17), channel_id=1, source_target_pairs={{0,32},{32,64},{64,96},{96,128},{128,160},{160,192},{192,224},{224... | collective-permute-start | bytes 393224 | tf_op jit(solution)/shard_map/ppermute | solution.py:35
  14.9 0.8 collective-permute-done.1
  15.7 5.6 %collective-permute-start.8 = (bf16[128,512]{1,0:T(8,128)(2,1)S(1)}, bf16[128,512]{1,0:T(8,128)(2,1)}, u32[]{:S(2)}, u32[]{:S(2)}) collective-permute-start(bf16[128,512]{1,0:T(8,128)(2,1)S(1)} %collective-permute-done.1), channel_id=1, source_target_pairs={{0,480},{32,0},{64,32},{96,64},{128,96},{160,128},{192,160},{224,1... | collective-permute-start | bytes 393224 | tf_op jit(solution)/shard_map/ppermute | solution.py:35
  21.3 0.0 collective-permute-done
  21.3 1.9 %collective-permute-start.2 = (bf16[128,512]{1,0:T(8,128)(2,1)S(1)}, bf16[128,512]{1,0:T(8,128)(2,1)}, u32[]{:S(2)}, u32[]{:S(2)}) collective-permute-start(bf16[128,512]{1,0:T(8,128)(2,1)S(1)} %collective-permute-done), channel_id=1, source_target_pairs={{0,32},{32,64},{64,96},{96,128},{128,160},{160,192},{192,224},{224... | collective-permute-start | bytes 393224 | tf_op jit(solution)/shard_map/ppermute | solution.py:35
  23.3 1.3 broadcast_in_dim.6
  24.5 4.6 %all-to-all-start = ((bf16[4,3,128,512]{3,2,1,0:T(8,128)(2,1)}), bf16[4,3,128,512]{3,2,1,0:T(8,128)(2,1)S(1)}, u32[]{:S(2)}, u32[]{:S(2)}) async-start(bf16[4,3,128,512]{3,2,1,0:T(8,128)(2,1)} %broadcast_in_dim.6), calls=%async_computation | async-start | bytes 3145728 | tf_op jit(solution)/shard_map/all_to_all | solution.py:24
  29.1 0.0 collective-permute-done.8
  29.1 5.1 %collective-permute-start.9 = (bf16[128,512]{1,0:T(8,128)(2,1)}, bf16[128,512]{1,0:T(8,128)(2,1)S(1)}, u32[]{:S(2)}, u32[]{:S(2)}) collective-permute-start(bf16[128,512]{1,0:T(8,128)(2,1)} %collective-permute-done.8), channel_id=1, source_target_pairs={{0,480},{32,0},{64,32},{96,64},{128,96},{160,128},{192,160},{224,1... | collective-permute-start | bytes 393224 | tf_op jit(solution)/shard_map/ppermute | solution.py:35
  34.3 1.9 %collective-permute-start.3 = (bf16[128,512]{1,0:T(8,128)(2,1)}, bf16[128,512]{1,0:T(8,128)(2,1)S(1)}, u32[]{:S(2)}, u32[]{:S(2)}) collective-permute-start(bf16[128,512]{1,0:T(8,128)(2,1)} %collective-permute-done.2), channel_id=1, source_target_pairs={{0,32},{32,64},{64,96},{96,128},{128,160},{160,192},{192,224},{224... | collective-permute-start | bytes 393224 | tf_op jit(solution)/shard_map/ppermute | solution.py:35
  36.2 1.6 constant_dynamic-update-slice_fusion.5
  37.8 0.9 constant_dynamic-update-slice_fusion.2
  38.7 0.0 collective-permute-done.9
  38.7 5.1 %collective-permute-start.10 = (bf16[64,512]{1,0:T(8,128)(2,1)S(1)}, bf16[64,512]{1,0:T(8,128)(2,1)S(1)}, u32[]{:S(2)}, u32[]{:S(2)}) collective-permute-start(bf16[64,512]{1,0:T(8,128)(2,1)S(1)} %slice.9), channel_id=1, source_target_pairs={{0,480},{32,0},{64,32},{96,64},{128,96},{160,128},{192,160},{224,1... | collective-permute-start | bytes 196616 | tf_op jit(solution)/shard_map/ppermute | solution.py:35
  43.9 0.0 collective-permute-done.3
  43.9 1.9 %collective-permute-start.4 = (bf16[64,512]{1,0:T(8,128)(2,1)S(1)}, bf16[64,512]{1,0:T(8,128)(2,1)S(1)}, u32[]{:S(2)}, u32[]{:S(2)}) collective-permute-start(bf16[64,512]{1,0:T(8,128)(2,1)S(1)} %slice.8), channel_id=1, source_target_pairs={{0,32},{32,64},{64,96},{96,128},{128,160},{160,192},{192,224},{224... | collective-permute-start | bytes 196616 | tf_op jit(solution)/shard_map/ppermute | solution.py:35
  45.8 0.7 constant_dynamic-update-slice_fusion.4
  46.5 0.6 constant_dynamic-update-slice_fusion.3.refs_4_
  47.1 5.1 %collective-permute-start.12 = (bf16[320,512]{1,0:T(8,128)(2,1)}, bf16[320,512]{1,0:T(8,128)(2,1)}, u32[]{:S(2)}, u32[]{:S(2)}) collective-permute-start(bf16[320,512]{1,0:T(8,128)(2,1)} %constant_dynamic-update-slice_fusion.3.refs_4_), channel_id=1, source_target_pairs={{0,24},{8,0},{16,8},{24,16},{1,25},{9,1},{17,9},{25,17},{2,26},{10... | collective-permute-start | bytes 983048 | tf_op jit(solution)/shard_map/ppermute | solution.py:35
  52.3 0.0 collective-permute-done.4
  52.3 2.9 %collective-permute-start.5 = (bf16[320,512]{1,0:T(8,128)(2,1)S(1)}, bf16[320,512]{1,0:T(8,128)(2,1)}, u32[]{:S(2)}, u32[]{:S(2)}) collective-permute-start(bf16[320,512]{1,0:T(8,128)(2,1)S(1)} %constant_dynamic-update-slice_fusion.refs_0_), channel_id=1, source_target_pairs={{0,8},{8,16},{16,24},{24,0},{1,9},{9,17},{17,25},{25,1},{2,10},{10... | collective-permute-start | bytes 983048 | tf_op jit(solution)/shard_map/ppermute | solution.py:35
  55.2 3.4 %collective-permute-start.11 = (bf16[320,512]{1,0:T(8,128)(2,1)}, bf16[320,512]{1,0:T(8,128)(2,1)}, u32[]{:S(2)}, u32[]{:S(2)}) collective-permute-start(bf16[320,512]{1,0:T(8,128)(2,1)} %constant_dynamic-update-slice_fusion.3.refs_4_), channel_id=1, source_target_pairs={{0,8},{8,16},{16,24},{24,0},{1,9},{9,17},{17,25},{25,1},{2,10},{10... | collective-permute-start | bytes 983048 | tf_op jit(solution)/shard_map/ppermute | solution.py:35
  58.6 3.7 %collective-permute-start.6 = (bf16[320,512]{1,0:T(8,128)(2,1)S(1)}, bf16[320,512]{1,0:T(8,128)(2,1)}, u32[]{:S(2)}, u32[]{:S(2)}) collective-permute-start(bf16[320,512]{1,0:T(8,128)(2,1)S(1)} %constant_dynamic-update-slice_fusion.refs_0_), channel_id=1, source_target_pairs={{0,24},{8,0},{16,8},{24,16},{1,25},{9,1},{17,9},{25,17},{2,26},{10... | collective-permute-start | bytes 983048 | tf_op jit(solution)/shard_map/ppermute | solution.py:35
  62.3 0.0 collective-permute-done.12.refs_6_
  62.3 3.0 %collective-permute-start.13 = (bf16[320,512]{1,0:T(8,128)(2,1)}, bf16[320,512]{1,0:T(8,128)(2,1)}, u32[]{:S(2)}, u32[]{:S(2)}) collective-permute-start(bf16[320,512]{1,0:T(8,128)(2,1)} %collective-permute-done.12.refs_6_), channel_id=1, source_target_pairs={{0,24},{8,0},{16,8},{24,16},{1,25},{9,1},{17,9},{25,17},{2,26},{10... | collective-permute-start | bytes 983048 | tf_op jit(solution)/shard_map/ppermute | solution.py:35
  65.2 0.1 collective-permute-done.5.refs_1_
  65.4 2.8 %collective-permute-start.7 = (bf16[320,512]{1,0:T(8,128)(2,1)}, bf16[320,512]{1,0:T(8,128)(2,1)}, u32[]{:S(2)}, u32[]{:S(2)}) collective-permute-start(bf16[320,512]{1,0:T(8,128)(2,1)} %collective-permute-done.5.refs_1_), channel_id=1, source_target_pairs={{0,8},{8,16},{16,24},{24,0},{1,9},{9,17},{17,25},{25,1},{2,10},{10... | collective-permute-start | bytes 983048 | tf_op jit(solution)/shard_map/ppermute | solution.py:35
  68.1 0.0 all-to-all-done.near_ref
  68.2 0.0 copy-start.1
  68.2 1.4 copy-done.1
  69.6 0.8 shard_map.59
  70.4 0.5 collective-permute-done.11.refs_5_
  70.9 0.0 collective-permute-done.6.refs_2_
  70.9 1.9 %collective-permute-done.13.refs_7_ = bf16[320,512]{1,0:T(8,128)(2,1)} collective-permute-done((bf16[320,512]{1,0:T(8,128)(2,1)}, bf16[320,512]{1,0:T(8,128)(2,1)}, u32[]{:S(2)}, u32[]{:S(2)}) %collective-permute-start.13) | collective-permute-done | bytes 327712 | tf_op jit(solution)/shard_map/ppermute | solution.py:35
  72.8 3.1 %collective-permute-done.7.refs_3_ = bf16[320,512]{1,0:T(8,128)(2,1)} collective-permute-done((bf16[320,512]{1,0:T(8,128)(2,1)}, bf16[320,512]{1,0:T(8,128)(2,1)}, u32[]{:S(2)}, u32[]{:S(2)}) %collective-permute-start.7) | collective-permute-done | bytes 327712 | tf_op jit(solution)/shard_map/ppermute | solution.py:35
  75.9 5.0 %shard_map.60 = (bf16[384,512]{1,0:T(8,128)(2,1)}, bf16[4,4,2,64,512]{4,3,2,1,0:T(8,128)(2,1)}) custom-call(bf16[384,2048]{1,0:T(8,128)(2,1)S(1)} %copy-done, bf16[384,2048]{1,0:T(8,128)(2,1)S(1)} %copy-done.1, f32[384,512]{1,0:T(8,128)S(1)} %get-tuple-element.8.pre_ref, f32[384,512]{1,0:T(8,128)S(1)} %get-tuple-element.9.hid_ref, ...), custom_call_target="tpu_custom_call" | custom-call | flops 1811939328 | bytes 6553600 | tf_op jit(solution)/shard_map/pallas_call | solution.py:158
  80.9 0.0 copy-start.2
  80.9 1.0 copy-done.2
  81.9 3.1 %shard_map.61 = (bf16[192,2048]{1,0:T(8,128)(2,1)S(1)}, bf16[192,2048]{1,0:T(8,128)(2,1)S(1)}) custom-call(bf16[384,512]{1,0:T(8,128)(2,1)S(1)} %copy-done.2, bf16[4,3,128,512]{3,2,1,0:T(8,128)(2,1)S(1)} %all-to-all-done.near_ref, bf16[320,512]{1,0:T(8,128)(2,1)S(1)} %constant_dynamic-update-slice_fusion.refs_0_, ...), custom_call_target="tpu_custom_call" | custom-call | flops 805306368 | bytes 4587520 | tf_op jit(solution)/shard_map/pallas_call | solution.py:158
  85.0 1.9 %collective-permute-start.14 = (bf16[192,2048]{1,0:T(8,128)(2,1)S(1)}, bf16[192,2048]{1,0:T(8,128)(2,1)S(1)}, u32[]{:S(2)}, u32[]{:S(2)}) collective-permute-start(bf16[192,2048]{1,0:T(8,128)(2,1)S(1)} %get-tuple-element.12), channel_id=1, source_target_pairs={{0,1},{1,0},{2,3},{3,2},{4,5},{5,4},{6,7},{7,6},{8,9},{9,8},{10,11... | collective-permute-start | bytes 2359304 | tf_op jit(solution)/shard_map/ppermute | solution.py:40
  86.9 2.3 %collective-permute-done.14 = bf16[192,2048]{1,0:T(8,128)(2,1)S(1)} collective-permute-done((bf16[192,2048]{1,0:T(8,128)(2,1)S(1)}, bf16[192,2048]{1,0:T(8,128)(2,1)S(1)}, u32[]{:S(2)}, u32[]{:S(2)}) %collective-permute-start.14) | collective-permute-done | bytes 786464 | tf_op jit(solution)/shard_map/ppermute | solution.py:40
  89.2 0.3 add_convert_fusion.2
  89.5 0.0 copy-start.3
  89.5 3.1 %collective-permute-start.15 = (bf16[192,2048]{1,0:T(8,128)(2,1)S(1)}, bf16[192,2048]{1,0:T(8,128)(2,1)}, u32[]{:S(2)}, u32[]{:S(2)}) collective-permute-start(bf16[192,2048]{1,0:T(8,128)(2,1)S(1)} %add_convert_fusion.2), channel_id=1, source_target_pairs={{0,2},{2,0},{4,6},{6,4},{1,3},{3,1},{5,7},{7,5},{8,10},{10,8},{12,... | collective-permute-start | bytes 2359304 | tf_op jit(solution)/shard_map/ppermute | solution.py:40
  92.6 3.6 %all-to-all-start.1 = ((bf16[4,4,2,64,512]{4,3,2,1,0:T(8,128)(2,1)}), bf16[4,4,2,64,512]{4,3,2,1,0:T(8,128)(2,1)S(1)}, u32[]{:S(2)}, u32[]{:S(2)}) async-start(bf16[4,4,2,64,512]{4,3,2,1,0:T(8,128)(2,1)} %get-tuple-element.13), calls=%async_computation.1 | async-start | bytes 4194304 | tf_op jit(solution)/shard_map/all_to_all | solution.py:24
  96.2 14.8 %collective-permute-done.15 = bf16[192,2048]{1,0:T(8,128)(2,1)} collective-permute-done((bf16[192,2048]{1,0:T(8,128)(2,1)S(1)}, bf16[192,2048]{1,0:T(8,128)(2,1)}, u32[]{:S(2)}, u32[]{:S(2)}) %collective-permute-start.15) | collective-permute-done | bytes 786464 | tf_op jit(solution)/shard_map/ppermute | solution.py:40
  111.1 1.6 add_convert_fusion.1
  112.7 2.4 %collective-permute-start.16 = (bf16[192,2048]{1,0:T(8,128)(2,1)S(1)}, bf16[192,2048]{1,0:T(8,128)(2,1)}, u32[]{:S(2)}, u32[]{:S(2)}) collective-permute-start(bf16[192,2048]{1,0:T(8,128)(2,1)S(1)} %add_convert_fusion.1), channel_id=1, source_target_pairs={{0,6},{2,4},{4,2},{6,0},{1,7},{3,5},{5,3},{7,1},{8,14},{10,12},{12... | collective-permute-start | bytes 2359304 | tf_op jit(solution)/shard_map/ppermute | solution.py:40
  115.1 7.7 %all-to-all-done.1 = bf16[4,4,2,64,512]{4,3,2,1,0:T(8,128)(2,1)S(1)} async-done(((bf16[4,4,2,64,512]{4,3,2,1,0:T(8,128)(2,1)}), bf16[4,4,2,64,512]{4,3,2,1,0:T(8,128)(2,1)S(1)}, u32[]{:S(2)}, u32[]{:S(2)}) %all-to-all-start.1) | async-done | bytes 2097184 | tf_op jit(solution)/shard_map/all_to_all | solution.py:24
  122.8 1.3 reduce_sum.33
  124.1 3.5 %all-to-all-start.2 = ((bf16[4,2,64,512]{3,2,1,0:T(8,128)(2,1)}), bf16[4,2,64,512]{3,2,1,0:T(8,128)(2,1)S(1)}, u32[]{:S(2)}, u32[]{:S(2)}) async-start(bf16[4,2,64,512]{3,2,1,0:T(8,128)(2,1)} %reduce_sum.33), calls=%async_computation.2 | async-start | bytes 1048576 | tf_op jit(solution)/shard_map/all_to_all | solution.py:24
  127.6 5.9 %collective-permute-done.16 = bf16[192,2048]{1,0:T(8,128)(2,1)} collective-permute-done((bf16[192,2048]{1,0:T(8,128)(2,1)S(1)}, bf16[192,2048]{1,0:T(8,128)(2,1)}, u32[]{:S(2)}, u32[]{:S(2)}) %collective-permute-start.16) | collective-permute-done | bytes 786464 | tf_op jit(solution)/shard_map/ppermute | solution.py:40
  133.4 1.4 add_convert_fusion
  134.8 1.9 %collective-permute-start.17 = (bf16[192,2048]{1,0:T(8,128)(2,1)S(1)}, bf16[192,2048]{1,0:T(8,128)(2,1)S(1)}, u32[]{:S(2)}, u32[]{:S(2)}) collective-permute-start(bf16[192,2048]{1,0:T(8,128)(2,1)S(1)} %add_convert_fusion), channel_id=1, source_target_pairs={{0,1},{1,0},{2,3},{3,2},{4,5},{5,4},{6,7},{7,6},{8,9},{9,8},{10,11... | collective-permute-start | bytes 2359304 | tf_op jit(solution)/shard_map/ppermute | solution.py:40
  136.8 4.7 %all-to-all-done.2 = bf16[4,2,64,512]{3,2,1,0:T(8,128)(2,1)S(1)} async-done(((bf16[4,2,64,512]{3,2,1,0:T(8,128)(2,1)}), bf16[4,2,64,512]{3,2,1,0:T(8,128)(2,1)S(1)}, u32[]{:S(2)}, u32[]{:S(2)}) %all-to-all-start.2) | async-done | bytes 524320 | tf_op jit(solution)/shard_map/all_to_all | solution.py:24
  141.5 0.1 reduce_sum.34
  141.5 0.7 broadcast_in_dim.7
  142.3 8.1 %all-to-all-start.3 = ((bf16[4,64,512]{2,1,0:T(8,128)(2,1)}), bf16[4,64,512]{2,1,0:T(8,128)(2,1)S(1)}, u32[]{:S(2)}, u32[]{:S(2)}) async-start(bf16[4,64,512]{2,1,0:T(8,128)(2,1)} %bitcast.4), calls=%async_computation.3 | async-start | bytes 524288 | tf_op jit(solution)/shard_map/all_to_all | solution.py:24
  150.4 0.1 broadcast_select_fusion.1
  150.5 1.2 pad_maximum_fusion
  151.7 17.1 %all-to-all-done.3 = bf16[4,64,512]{2,1,0:T(8,128)(2,1)S(1)} async-done(((bf16[4,64,512]{2,1,0:T(8,128)(2,1)}), bf16[4,64,512]{2,1,0:T(8,128)(2,1)S(1)}, u32[]{:S(2)}, u32[]{:S(2)}) %all-to-all-start.3) | async-done | bytes 262176 | tf_op jit(solution)/shard_map/all_to_all | solution.py:24
  168.9 0.7 convert_reduce_fusion
  (11 shorter events, 0.1 us)
Async XLA Ops:
  1.5 14.1 %collective-permute-start.1 = (bf16[128,512]{1,0:T(8,128)(2,1)S(1)}, bf16[128,512]{1,0:T(8,128)(2,1)S(1)}, u32[]{:S(2)}, u32[]{:S(2)}) collective-permute-start(bf16[128,512]{1,0:T(8,128)(2,1)S(1)} %get-tuple-element.17), channel_id=1, source_target_pairs={{0,480},{32,0},{64,32},{96,64},{128,96},{160,128},{192,160},{224,1... | collective-permute-start | bytes 393224 | tf_op jit(solution)/shard_map/ppermute | solution.py:35
  12.9 8.3 %collective-permute-start = (bf16[128,512]{1,0:T(8,128)(2,1)S(1)}, bf16[128,512]{1,0:T(8,128)(2,1)S(1)}, u32[]{:S(2)}, u32[]{:S(2)}) collective-permute-start(bf16[128,512]{1,0:T(8,128)(2,1)S(1)} %get-tuple-element.17), channel_id=1, source_target_pairs={{0,32},{32,64},{64,96},{96,128},{128,160},{160,192},{192,224},{224... | collective-permute-start | bytes 393224 | tf_op jit(solution)/shard_map/ppermute | solution.py:35
  15.7 13.5 %collective-permute-start.8 = (bf16[128,512]{1,0:T(8,128)(2,1)S(1)}, bf16[128,512]{1,0:T(8,128)(2,1)}, u32[]{:S(2)}, u32[]{:S(2)}) collective-permute-start(bf16[128,512]{1,0:T(8,128)(2,1)S(1)} %collective-permute-done.1), channel_id=1, source_target_pairs={{0,480},{32,0},{64,32},{96,64},{128,96},{160,128},{192,160},{224,1... | collective-permute-start | bytes 393224 | tf_op jit(solution)/shard_map/ppermute | solution.py:35
  21.3 13.0 %collective-permute-start.2 = (bf16[128,512]{1,0:T(8,128)(2,1)S(1)}, bf16[128,512]{1,0:T(8,128)(2,1)}, u32[]{:S(2)}, u32[]{:S(2)}) collective-permute-start(bf16[128,512]{1,0:T(8,128)(2,1)S(1)} %collective-permute-done), channel_id=1, source_target_pairs={{0,32},{32,64},{64,96},{96,128},{128,160},{160,192},{192,224},{224... | collective-permute-start | bytes 393224 | tf_op jit(solution)/shard_map/ppermute | solution.py:35
  24.5 43.6 %copy-start = (bf16[384,2048]{1,0:T(8,128)(2,1)S(1)}, bf16[384,2048]{1,0:T(8,128)(2,1)}, u32[]{:S(2)}) copy-start(bf16[384,2048]{1,0:T(8,128)(2,1)} %x_ref.3) | copy-start | bytes 4718596
  24.5 43.6 %all-to-all-start = ((bf16[4,3,128,512]{3,2,1,0:T(8,128)(2,1)}), bf16[4,3,128,512]{3,2,1,0:T(8,128)(2,1)S(1)}, u32[]{:S(2)}, u32[]{:S(2)}) async-start(bf16[4,3,128,512]{3,2,1,0:T(8,128)(2,1)} %broadcast_in_dim.6), calls=%async_computation | async-start | bytes 3145728 | tf_op jit(solution)/shard_map/all_to_all | solution.py:24
  29.1 9.6 %collective-permute-start.9 = (bf16[128,512]{1,0:T(8,128)(2,1)}, bf16[128,512]{1,0:T(8,128)(2,1)S(1)}, u32[]{:S(2)}, u32[]{:S(2)}) collective-permute-start(bf16[128,512]{1,0:T(8,128)(2,1)} %collective-permute-done.8), channel_id=1, source_target_pairs={{0,480},{32,0},{64,32},{96,64},{128,96},{160,128},{192,160},{224,1... | collective-permute-start | bytes 393224 | tf_op jit(solution)/shard_map/ppermute | solution.py:35
  34.3 9.6 %collective-permute-start.3 = (bf16[128,512]{1,0:T(8,128)(2,1)}, bf16[128,512]{1,0:T(8,128)(2,1)S(1)}, u32[]{:S(2)}, u32[]{:S(2)}) collective-permute-start(bf16[128,512]{1,0:T(8,128)(2,1)} %collective-permute-done.2), channel_id=1, source_target_pairs={{0,32},{32,64},{64,96},{96,128},{128,160},{160,192},{192,224},{224... | collective-permute-start | bytes 393224 | tf_op jit(solution)/shard_map/ppermute | solution.py:35
  38.7 7.8 %collective-permute-start.10 = (bf16[64,512]{1,0:T(8,128)(2,1)S(1)}, bf16[64,512]{1,0:T(8,128)(2,1)S(1)}, u32[]{:S(2)}, u32[]{:S(2)}) collective-permute-start(bf16[64,512]{1,0:T(8,128)(2,1)S(1)} %slice.9), channel_id=1, source_target_pairs={{0,480},{32,0},{64,32},{96,64},{128,96},{160,128},{192,160},{224,1... | collective-permute-start | bytes 196616 | tf_op jit(solution)/shard_map/ppermute | solution.py:35
  43.9 8.4 %collective-permute-start.4 = (bf16[64,512]{1,0:T(8,128)(2,1)S(1)}, bf16[64,512]{1,0:T(8,128)(2,1)S(1)}, u32[]{:S(2)}, u32[]{:S(2)}) collective-permute-start(bf16[64,512]{1,0:T(8,128)(2,1)S(1)} %slice.8), channel_id=1, source_target_pairs={{0,32},{32,64},{64,96},{96,128},{128,160},{160,192},{192,224},{224... | collective-permute-start | bytes 196616 | tf_op jit(solution)/shard_map/ppermute | solution.py:35
  47.1 15.1 %collective-permute-start.12 = (bf16[320,512]{1,0:T(8,128)(2,1)}, bf16[320,512]{1,0:T(8,128)(2,1)}, u32[]{:S(2)}, u32[]{:S(2)}) collective-permute-start(bf16[320,512]{1,0:T(8,128)(2,1)} %constant_dynamic-update-slice_fusion.3.refs_4_), channel_id=1, source_target_pairs={{0,24},{8,0},{16,8},{24,16},{1,25},{9,1},{17,9},{25,17},{2,26},{10... | collective-permute-start | bytes 983048 | tf_op jit(solution)/shard_map/ppermute | solution.py:35
  52.3 13.1 %collective-permute-start.5 = (bf16[320,512]{1,0:T(8,128)(2,1)S(1)}, bf16[320,512]{1,0:T(8,128)(2,1)}, u32[]{:S(2)}, u32[]{:S(2)}) collective-permute-start(bf16[320,512]{1,0:T(8,128)(2,1)S(1)} %constant_dynamic-update-slice_fusion.refs_0_), channel_id=1, source_target_pairs={{0,8},{8,16},{16,24},{24,0},{1,9},{9,17},{17,25},{25,1},{2,10},{10... | collective-permute-start | bytes 983048 | tf_op jit(solution)/shard_map/ppermute | solution.py:35
  55.2 15.7 %collective-permute-start.11 = (bf16[320,512]{1,0:T(8,128)(2,1)}, bf16[320,512]{1,0:T(8,128)(2,1)}, u32[]{:S(2)}, u32[]{:S(2)}) collective-permute-start(bf16[320,512]{1,0:T(8,128)(2,1)} %constant_dynamic-update-slice_fusion.3.refs_4_), channel_id=1, source_target_pairs={{0,8},{8,16},{16,24},{24,0},{1,9},{9,17},{17,25},{25,1},{2,10},{10... | collective-permute-start | bytes 983048 | tf_op jit(solution)/shard_map/ppermute | solution.py:35
  58.6 12.3 %collective-permute-start.6 = (bf16[320,512]{1,0:T(8,128)(2,1)S(1)}, bf16[320,512]{1,0:T(8,128)(2,1)}, u32[]{:S(2)}, u32[]{:S(2)}) collective-permute-start(bf16[320,512]{1,0:T(8,128)(2,1)S(1)} %constant_dynamic-update-slice_fusion.refs_0_), channel_id=1, source_target_pairs={{0,24},{8,0},{16,8},{24,16},{1,25},{9,1},{17,9},{25,17},{2,26},{10... | collective-permute-start | bytes 983048 | tf_op jit(solution)/shard_map/ppermute | solution.py:35
  62.3 10.6 %collective-permute-start.13 = (bf16[320,512]{1,0:T(8,128)(2,1)}, bf16[320,512]{1,0:T(8,128)(2,1)}, u32[]{:S(2)}, u32[]{:S(2)}) collective-permute-start(bf16[320,512]{1,0:T(8,128)(2,1)} %collective-permute-done.12.refs_6_), channel_id=1, source_target_pairs={{0,24},{8,0},{16,8},{24,16},{1,25},{9,1},{17,9},{25,17},{2,26},{10... | collective-permute-start | bytes 983048 | tf_op jit(solution)/shard_map/ppermute | solution.py:35
  65.4 10.5 %collective-permute-start.7 = (bf16[320,512]{1,0:T(8,128)(2,1)}, bf16[320,512]{1,0:T(8,128)(2,1)}, u32[]{:S(2)}, u32[]{:S(2)}) collective-permute-start(bf16[320,512]{1,0:T(8,128)(2,1)} %collective-permute-done.5.refs_1_), channel_id=1, source_target_pairs={{0,8},{8,16},{16,24},{24,0},{1,9},{9,17},{17,25},{25,1},{2,10},{10... | collective-permute-start | bytes 983048 | tf_op jit(solution)/shard_map/ppermute | solution.py:35
  68.2 1.4 copy-start.1
  80.9 1.0 copy-start.2
  85.0 4.2 %collective-permute-start.14 = (bf16[192,2048]{1,0:T(8,128)(2,1)S(1)}, bf16[192,2048]{1,0:T(8,128)(2,1)S(1)}, u32[]{:S(2)}, u32[]{:S(2)}) collective-permute-start(bf16[192,2048]{1,0:T(8,128)(2,1)S(1)} %get-tuple-element.12), channel_id=1, source_target_pairs={{0,1},{1,0},{2,3},{3,2},{4,5},{5,4},{6,7},{7,6},{8,9},{9,8},{10,11... | collective-permute-start | bytes 2359304 | tf_op jit(solution)/shard_map/ppermute | solution.py:40
  89.5 3.1 %copy-start.3 = (bf16[192,2048]{1,0:T(8,128)(2,1)}, bf16[192,2048]{1,0:T(8,128)(2,1)S(1)}, u32[]{:S(2)}) copy-start(bf16[192,2048]{1,0:T(8,128)(2,1)S(1)} %add_convert_fusion.2) | copy-start | bytes 2359300
  89.5 21.6 %collective-permute-start.15 = (bf16[192,2048]{1,0:T(8,128)(2,1)S(1)}, bf16[192,2048]{1,0:T(8,128)(2,1)}, u32[]{:S(2)}, u32[]{:S(2)}) collective-permute-start(bf16[192,2048]{1,0:T(8,128)(2,1)S(1)} %add_convert_fusion.2), channel_id=1, source_target_pairs={{0,2},{2,0},{4,6},{6,4},{1,3},{3,1},{5,7},{7,5},{8,10},{10,8},{12,... | collective-permute-start | bytes 2359304 | tf_op jit(solution)/shard_map/ppermute | solution.py:40
  92.6 30.2 %all-to-all-start.1 = ((bf16[4,4,2,64,512]{4,3,2,1,0:T(8,128)(2,1)}), bf16[4,4,2,64,512]{4,3,2,1,0:T(8,128)(2,1)S(1)}, u32[]{:S(2)}, u32[]{:S(2)}) async-start(bf16[4,4,2,64,512]{4,3,2,1,0:T(8,128)(2,1)} %get-tuple-element.13), calls=%async_computation.1 | async-start | bytes 4194304 | tf_op jit(solution)/shard_map/all_to_all | solution.py:24
  112.7 20.7 %collective-permute-start.16 = (bf16[192,2048]{1,0:T(8,128)(2,1)S(1)}, bf16[192,2048]{1,0:T(8,128)(2,1)}, u32[]{:S(2)}, u32[]{:S(2)}) collective-permute-start(bf16[192,2048]{1,0:T(8,128)(2,1)S(1)} %add_convert_fusion.1), channel_id=1, source_target_pairs={{0,6},{2,4},{4,2},{6,0},{1,7},{3,5},{5,3},{7,1},{8,14},{10,12},{12... | collective-permute-start | bytes 2359304 | tf_op jit(solution)/shard_map/ppermute | solution.py:40
  124.1 17.4 %all-to-all-start.2 = ((bf16[4,2,64,512]{3,2,1,0:T(8,128)(2,1)}), bf16[4,2,64,512]{3,2,1,0:T(8,128)(2,1)S(1)}, u32[]{:S(2)}, u32[]{:S(2)}) async-start(bf16[4,2,64,512]{3,2,1,0:T(8,128)(2,1)} %reduce_sum.33), calls=%async_computation.2 | async-start | bytes 1048576 | tf_op jit(solution)/shard_map/all_to_all | solution.py:24
  134.8 15.6 %collective-permute-start.17 = (bf16[192,2048]{1,0:T(8,128)(2,1)S(1)}, bf16[192,2048]{1,0:T(8,128)(2,1)S(1)}, u32[]{:S(2)}, u32[]{:S(2)}) collective-permute-start(bf16[192,2048]{1,0:T(8,128)(2,1)S(1)} %add_convert_fusion), channel_id=1, source_target_pairs={{0,1},{1,0},{2,3},{3,2},{4,5},{5,4},{6,7},{7,6},{8,9},{9,8},{10,11... | collective-permute-start | bytes 2359304 | tf_op jit(solution)/shard_map/ppermute | solution.py:40
  142.3 26.6 %all-to-all-start.3 = ((bf16[4,64,512]{2,1,0:T(8,128)(2,1)}), bf16[4,64,512]{2,1,0:T(8,128)(2,1)S(1)}, u32[]{:S(2)}, u32[]{:S(2)}) async-start(bf16[4,64,512]{2,1,0:T(8,128)(2,1)} %bitcast.4), calls=%async_computation.3 | async-start | bytes 524288 | tf_op jit(solution)/shard_map/all_to_all | solution.py:24

commit v6 on v5

--- a/solution.py
+++ b/solution.py
@@ -53,22 +53,36 @@
     return jnp.concatenate([ref[y, k, at] for y in range(N_Y)], axis=0)
 
 
-def add_products(x_ref, c_ref, ref, shifts, pre_acc, hid_acc, fresh):
-    width = N_Y * ref.shape[2] // 2
-    for ref, k, z in z_blocks((ref, shifts)):
-        at = pl.ds(pl.multiple_of(z * width, width), width)
-        pre = jnp.dot(x_ref[:, at], rows_of(ref, k, 0), preferred_element_type=F32)
-        hid = jnp.dot(c_ref[:, at], rows_of(ref, k, 1), preferred_element_type=F32)
-        if fresh and k == 0:
-            pre_acc[...] = pre
-            hid_acc[...] = hid
+def near_kernel(x_hbm, c_hbm, near_ref, pre_ref, hid_ref, x_ref, c_ref, sems):
+    width = N_Y * near_ref.shape[2] // 2
+    groups = (near_ref, NEAR), (None, FAR)
+    places = [
+        pl.ds(pl.multiple_of(z * width, width), width) for _, _, z in z_blocks(*groups)
+    ]
+    copies = [
+        [
+            pltpu.make_async_copy(src.at[:, at], dst.at[:, at], sems.at[n, part])
+            for part, (src, dst) in enumerate(((x_hbm, x_ref), (c_hbm, c_ref)))
+        ]
+        for n, at in enumerate(places)
+    ]
+    for pair in copies:
+        for copy in pair:
+            copy.start()
+    for n, at in enumerate(places):
+        for copy in copies[n]:
+            copy.wait()
+        if n >= len(NEAR):
+            continue
+        up, down = rows_of(near_ref, n, 0), rows_of(near_ref, n, 1)
+        pre = jnp.dot(x_ref[:, at], up, preferred_element_type=F32)
+        hid = jnp.dot(c_ref[:, at], down, preferred_element_type=F32)
+        if n == 0:
+            pre_ref[...] = pre
+            hid_ref[...] = hid
         else:
-            pre_acc[...] += pre
-            hid_acc[...] += hid
-
-
-def near_kernel(x_ref, c_ref, near_ref, pre_ref, hid_ref):
-    add_products(x_ref, c_ref, near_ref, NEAR, pre_ref, hid_ref, True)
+            pre_ref[...] += pre
+            hid_ref[...] += hid
 
 
 def far_copies(plus, minus, dsts, sems):
@@ -151,20 +165,20 @@
             ).astype(BF)
 
 
-def call(kernel, outs, args, flops, in_any, scratch=(), dtype=BF, out_hbm=()):
+def call(kernel, outs, args, flops, in_any, scratch=(), out_hbm=(), limit=24 * 2**20):
     vm = pl.BlockSpec(memory_space=pltpu.VMEM)
     any_ = pl.BlockSpec(memory_space=pl.ANY)
     hbm = pl.BlockSpec(memory_space=pltpu.HBM)
     return pl.pallas_call(
         kernel,
         out_shape=tuple(
-            pltpu.HBM(s, dtype) if k in out_hbm else jax.ShapeDtypeStruct(s, dtype)
-            for k, s in enumerate(outs)
+            pltpu.HBM(s, t) if k in out_hbm else jax.ShapeDtypeStruct(s, t)
+            for k, (s, t) in enumerate(outs)
         ),
         in_specs=[any_ if k in in_any else vm for k in range(len(args))],
         out_specs=tuple(hbm if k in out_hbm else vm for k in range(len(outs))),
         scratch_shapes=scratch,
-        compiler_params=pltpu.CompilerParams(vmem_limit_bytes=24 * 2**20),
+        compiler_params=pltpu.CompilerParams(vmem_limit_bytes=limit),
         cost_estimate=pl.CostEstimate(
             flops=flops,
             bytes_accessed=2 * sum(a.size for a in args),
@@ -198,19 +212,21 @@
     minus.append(minus_after)
     plus.append(shifted(plus[1], "y", 1))
     minus.append(shifted(minus_after, "y", -1))
+    inputs = pltpu.with_memory_space_constraint(inputs, pltpu.HBM)
+    cotangent = pltpu.with_memory_space_constraint(cotangent, pltpu.HBM)
     unit = tokens * width * h // 2
     part = N_Y * rows
-    pre, hid = call(
+    pre, hid, inputs, cotangent = call(
         near_kernel,
-        [(tokens, h)] * 2,
+        [((tokens, h), F32)] * 2 + [((tokens, width), BF)] * 2,
         (inputs, cotangent, near),
         3 * unit,
-        (),
-        dtype=F32,
+        (0, 1),
+        [pltpu.SemaphoreType.DMA((N_Z, 2))],
     )
     grad, dw = call(
         weight_kernel,
-        [(tokens, h), (N_Y, 4, 2, rows, h)],
+        [((tokens, h), BF), ((N_Y, 4, 2, rows, h), BF)],
         (inputs, cotangent, pre, hid, *plus, *minus),
         9 * unit,
         range(4, 12),
@@ -228,7 +244,7 @@
     )
     keep, give = call(
         input_kernel,
-        [(tokens // 2, width)] * 2,
+        [((tokens // 2, width), BF)] * 2,
         (grad, near, *plus, *minus),
         4 * unit,
         range(2, 10),
@@ -236,6 +252,7 @@
             pltpu.VMEM((len(FAR) * part, h), BF),
             pltpu.SemaphoreType.DMA((len(FAR), 1, N_Y)),
         ],
+        limit=None,
     )
 
     over_core = total(keep, swapped(give, "core", lambda i: 1 - i))

time: 171 us -> 172 us (level)
  local copies, waits for them, and re-layouts: 8.22 us -> 2.11 us
  Pallas kernels: 8.86 us -> 14.8 us
    pallas_call x3, Pallas kernels: 8.86 us -> 14.8 us  [call(): pl.pallas_call(kernel, out_shape=tuple((pltpu.HBM(s, t) if k in out_hbm e...]
    unnamed x12 -> x20, local copies, waits for them, and re-layouts: 5.57 us -> 0.08 us
  transfers between devices with their start and end apart: 22 -> 22, of which waited for: 11 -> 11; matrix products, arithmetic and copies ran while one was open for 7% -> 5% of each run, Pallas kernels for 0% -> 2%
where the time goes in v6:
time: 172 us; the launch traced here: 171 us
  starting transfers between devices  86.6 us (50%)
  waiting for transfers between devices  57.8 us (34%)
  Pallas kernels  14.8 us (9%)
  other arithmetic  8.75 us (5%)
  local copies, waits for them, and re-layouts  2.11 us (1%)
    ppermute x14, starting transfers between devices, shifted(): return lax.ppermute(value, axes, [(i, (i + step) % n) for i in range(n)])  57.3 us
    all_to_all x4, waiting for transfers between devices, exchange(): return lax.all_to_all(parts, axes, split_axis=0, concat_axis=0, tiled=True)  29.5 us
    ppermute x4, waiting for transfers between devices, swapped(): return lax.ppermute(value, axes, [(i, partner(i)) for i in range(n)])  23.2 us
    all_to_all x4, starting transfers between devices, exchange(): return lax.all_to_all(parts, axes, split_axis=0, concat_axis=0, tiled=True)  19.8 us
    pallas_call x3, Pallas kernels, call(): pl.pallas_call(kernel, out_shape=tuple((pltpu.HBM(s, t) if k in out_hbm e...  14.8 us
    ppermute x4, starting transfers between devices, swapped(): return lax.ppermute(value, axes, [(i, partner(i)) for i in range(n)])  9.39 us
    ppermute x14, waiting for transfers between devices, shifted(): return lax.ppermute(value, axes, [(i, (i + step) % n) for i in range(n)])  5.17 us
    convert_element_type x3, other arithmetic, total(): return (a.astype(F32) + b.astype(F32)).astype(BF)  4.42 us
  transfers between devices with their start and end apart: 22, of which 11 were waited for; matrix products, arithmetic and copies ran while one was open for 5% of the time, Pallas kernels for 2%

profile of v6, /device:TPU:4, one launch (start us, length us, event | category | flops | bytes accessed | tf_op | source)
XLA Modules:
  0.0 171.1 jit_solution(11065937008867993597)
XLA Ops:
  0.6 0.9 fusion
  1.5 11.4 %collective-permute-start.1 = (bf16[128,512]{1,0:T(8,128)(2,1)S(1)}, bf16[128,512]{1,0:T(8,128)(2,1)S(1)}, u32[]{:S(2)}, u32[]{:S(2)}) collective-permute-start(bf16[128,512]{1,0:T(8,128)(2,1)S(1)} %get-tuple-element.21), channel_id=1, source_target_pairs={{0,480},{32,0},{64,32},{96,64},{128,96},{160,128},{192,160},{224,1... | collective-permute-start | bytes 393224 | tf_op jit(solution)/shard_map/ppermute | solution.py:35
  12.9 1.9 %collective-permute-start = (bf16[128,512]{1,0:T(8,128)(2,1)S(1)}, bf16[128,512]{1,0:T(8,128)(2,1)S(1)}, u32[]{:S(2)}, u32[]{:S(2)}) collective-permute-start(bf16[128,512]{1,0:T(8,128)(2,1)S(1)} %get-tuple-element.21), channel_id=1, source_target_pairs={{0,32},{32,64},{64,96},{96,128},{128,160},{160,192},{192,224},{224... | collective-permute-start | bytes 393224 | tf_op jit(solution)/shard_map/ppermute | solution.py:35
  14.9 0.8 collective-permute-done.1
  15.7 5.6 %collective-permute-start.8 = (bf16[128,512]{1,0:T(8,128)(2,1)S(1)}, bf16[128,512]{1,0:T(8,128)(2,1)S(1)}, u32[]{:S(2)}, u32[]{:S(2)}) collective-permute-start(bf16[128,512]{1,0:T(8,128)(2,1)S(1)} %collective-permute-done.1), channel_id=1, source_target_pairs={{0,480},{32,0},{64,32},{96,64},{128,96},{160,128},{192,160},{224,1... | collective-permute-start | bytes 393224 | tf_op jit(solution)/shard_map/ppermute | solution.py:35
  21.3 0.0 collective-permute-done
  21.3 1.9 %collective-permute-start.2 = (bf16[128,512]{1,0:T(8,128)(2,1)S(1)}, bf16[128,512]{1,0:T(8,128)(2,1)S(1)}, u32[]{:S(2)}, u32[]{:S(2)}) collective-permute-start(bf16[128,512]{1,0:T(8,128)(2,1)S(1)} %collective-permute-done), channel_id=1, source_target_pairs={{0,32},{32,64},{64,96},{96,128},{128,160},{160,192},{192,224},{224... | collective-permute-start | bytes 393224 | tf_op jit(solution)/shard_map/ppermute | solution.py:35
  23.3 1.3 broadcast_in_dim.6
  24.5 4.5 %all-to-all-start = ((bf16[4,3,128,512]{3,2,1,0:T(8,128)(2,1)}), bf16[4,3,128,512]{3,2,1,0:T(8,128)(2,1)S(1)}, u32[]{:S(2)}, u32[]{:S(2)}) async-start(bf16[4,3,128,512]{3,2,1,0:T(8,128)(2,1)} %broadcast_in_dim.6), calls=%async_computation | async-start | bytes 3145728 | tf_op jit(solution)/shard_map/all_to_all | solution.py:24
  29.0 0.0 collective-permute-done.8
  29.0 5.1 %collective-permute-start.9 = (bf16[128,512]{1,0:T(8,128)(2,1)S(1)}, bf16[128,512]{1,0:T(8,128)(2,1)S(1)}, u32[]{:S(2)}, u32[]{:S(2)}) collective-permute-start(bf16[128,512]{1,0:T(8,128)(2,1)S(1)} %collective-permute-done.8), channel_id=1, source_target_pairs={{0,480},{32,0},{64,32},{96,64},{128,96},{160,128},{192,160},{224,1... | collective-permute-start | bytes 393224 | tf_op jit(solution)/shard_map/ppermute | solution.py:35
  34.1 0.0 collective-permute-done.2
  34.1 1.9 %collective-permute-start.3 = (bf16[128,512]{1,0:T(8,128)(2,1)S(1)}, bf16[128,512]{1,0:T(8,128)(2,1)S(1)}, u32[]{:S(2)}, u32[]{:S(2)}) collective-permute-start(bf16[128,512]{1,0:T(8,128)(2,1)S(1)} %collective-permute-done.2), channel_id=1, source_target_pairs={{0,32},{32,64},{64,96},{96,128},{128,160},{160,192},{192,224},{224... | collective-permute-start | bytes 393224 | tf_op jit(solution)/shard_map/ppermute | solution.py:35
  36.1 0.5 collective-permute-done.9
  36.6 5.6 %collective-permute-start.10 = (bf16[64,512]{1,0:T(8,128)(2,1)S(1)}, bf16[64,512]{1,0:T(8,128)(2,1)S(1)}, u32[]{:S(2)}, u32[]{:S(2)}) collective-permute-start(bf16[64,512]{1,0:T(8,128)(2,1)S(1)} %slice.9), channel_id=1, source_target_pairs={{0,480},{32,0},{64,32},{96,64},{128,96},{160,128},{192,160},{224,1... | collective-permute-start | bytes 196616 | tf_op jit(solution)/shard_map/ppermute | solution.py:35
  42.2 0.0 collective-permute-done.3
  42.2 1.9 %collective-permute-start.4 = (bf16[64,512]{1,0:T(8,128)(2,1)S(1)}, bf16[64,512]{1,0:T(8,128)(2,1)S(1)}, u32[]{:S(2)}, u32[]{:S(2)}) collective-permute-start(bf16[64,512]{1,0:T(8,128)(2,1)S(1)} %slice.8), channel_id=1, source_target_pairs={{0,32},{32,64},{64,96},{96,128},{128,160},{160,192},{192,224},{224... | collective-permute-start | bytes 196616 | tf_op jit(solution)/shard_map/ppermute | solution.py:35
  44.2 0.0 collective-permute-done.10
  44.2 0.0 copy-start.2
  44.2 5.1 %collective-permute-start.12 = (bf16[320,512]{1,0:T(8,128)(2,1)S(1)}, bf16[320,512]{1,0:T(8,128)(2,1)S(1)}, u32[]{:S(2)}, u32[]{:S(2)}) collective-permute-start(bf16[320,512]{1,0:T(8,128)(2,1)S(1)} %constant_dynamic-update-slice_fusion.3.refs_4_), channel_id=1, source_target_pairs={{0,24},{8,0},{16,8},{24,16},{1,25},{9,1},{17,9},{25,17},{2,26},{10... | collective-permute-start | bytes 983048 | tf_op jit(solution)/shard_map/ppermute | solution.py:35
  49.4 0.2 collective-permute-done.4
  49.6 3.9 %collective-permute-start.5 = (bf16[320,512]{1,0:T(8,128)(2,1)S(1)}, bf16[320,512]{1,0:T(8,128)(2,1)S(1)}, u32[]{:S(2)}, u32[]{:S(2)}) collective-permute-start(bf16[320,512]{1,0:T(8,128)(2,1)S(1)} %constant_dynamic-update-slice_fusion.refs_0_), channel_id=1, source_target_pairs={{0,8},{8,16},{16,24},{24,0},{1,9},{9,17},{17,25},{25,1},{2,10},{10... | collective-permute-start | bytes 983048 | tf_op jit(solution)/shard_map/ppermute | solution.py:35
  53.5 3.4 %collective-permute-start.11 = (bf16[320,512]{1,0:T(8,128)(2,1)S(1)}, bf16[320,512]{1,0:T(8,128)(2,1)S(1)}, u32[]{:S(2)}, u32[]{:S(2)}) collective-permute-start(bf16[320,512]{1,0:T(8,128)(2,1)S(1)} %constant_dynamic-update-slice_fusion.3.refs_4_), channel_id=1, source_target_pairs={{0,8},{8,16},{16,24},{24,0},{1,9},{9,17},{17,25},{25,1},{2,10},{10... | collective-permute-start | bytes 983048 | tf_op jit(solution)/shard_map/ppermute | solution.py:35
  56.9 3.7 %collective-permute-start.6 = (bf16[320,512]{1,0:T(8,128)(2,1)S(1)}, bf16[320,512]{1,0:T(8,128)(2,1)S(1)}, u32[]{:S(2)}, u32[]{:S(2)}) collective-permute-start(bf16[320,512]{1,0:T(8,128)(2,1)S(1)} %constant_dynamic-update-slice_fusion.refs_0_), channel_id=1, source_target_pairs={{0,24},{8,0},{16,8},{24,16},{1,25},{9,1},{17,9},{25,17},{2,26},{10... | collective-permute-start | bytes 983048 | tf_op jit(solution)/shard_map/ppermute | solution.py:35
  60.6 0.0 collective-permute-done.12.refs_6_
  60.6 0.0 copy-start.3
  60.6 1.9 %collective-permute-start.13 = (bf16[320,512]{1,0:T(8,128)(2,1)S(1)}, bf16[320,512]{1,0:T(8,128)(2,1)}, u32[]{:S(2)}, u32[]{:S(2)}) collective-permute-start(bf16[320,512]{1,0:T(8,128)(2,1)S(1)} %collective-permute-done.12.refs_6_), channel_id=1, source_target_pairs={{0,24},{8,0},{16,8},{24,16},{1,25},{9,1},{17,9},{25,17},{2,26},{10... | collective-permute-start | bytes 983048 | tf_op jit(solution)/shard_map/ppermute | solution.py:35
  62.6 0.0 collective-permute-done.5.refs_1_
  62.6 3.9 %collective-permute-start.7 = (bf16[320,512]{1,0:T(8,128)(2,1)S(1)}, bf16[320,512]{1,0:T(8,128)(2,1)}, u32[]{:S(2)}, u32[]{:S(2)}) collective-permute-start(bf16[320,512]{1,0:T(8,128)(2,1)S(1)} %collective-permute-done.5.refs_1_), channel_id=1, source_target_pairs={{0,8},{8,16},{16,24},{24,0},{1,9},{9,17},{17,25},{25,1},{2,10},{10... | collective-permute-start | bytes 983048 | tf_op jit(solution)/shard_map/ppermute | solution.py:35
  66.5 0.0 all-to-all-done.near_ref
  66.5 0.0 copy-start
  66.5 2.7 %shard_map.59 = (f32[384,512]{1,0:T(8,128)S(1)}, f32[384,512]{1,0:T(8,128)S(1)}, bf16[384,2048]{1,0:T(8,128)(2,1)S(1)}, bf16[384,2048]{1,0:T(8,128)(2,1)S(1)}) custom-call(bf16[384,2048]{1,0:T(8,128)(2,1)} %x_hbm.1, bf16[384,2048]{1,0:T(8,128)(2,1)} %c_hbm.1, bf16[4,3,128,512]{3,2,1,0:T(8,128)(2,1)S(1)} %all-to-all-done.near_ref), custom_call_target="tpu_custom_call" | custom-call | flops 603979776 | bytes 4718592 | tf_op jit(solution)/shard_map/pallas_call | solution.py:172
  69.2 0.0 collective-permute-done.11.refs_5_
  69.3 0.0 collective-permute-done.6.refs_2_
  69.3 0.0 copy-start.6
  69.3 1.1 collective-permute-done.13.refs_7_
  70.4 2.4 %collective-permute-done.7.refs_3_ = bf16[320,512]{1,0:T(8,128)(2,1)} collective-permute-done((bf16[320,512]{1,0:T(8,128)(2,1)S(1)}, bf16[320,512]{1,0:T(8,128)(2,1)}, u32[]{:S(2)}, u32[]{:S(2)}) %collective-permute-start.7) | collective-permute-done | bytes 327712 | tf_op jit(solution)/shard_map/ppermute | solution.py:35
  72.9 0.0 copy-done.2
  72.9 6.6 %shard_map.60 = (bf16[384,512]{1,0:T(8,128)(2,1)}, bf16[4,4,2,64,512]{4,3,2,1,0:T(8,128)(2,1)}) custom-call(bf16[384,2048]{1,0:T(8,128)(2,1)S(1)} %get-tuple-element.10.x_ref, bf16[384,2048]{1,0:T(8,128)(2,1)S(1)} %get-tuple-element.11.c_ref, f32[384,512]{1,0:T(8,128)S(1)} %get-tuple-element.12.pre_ref, f32[384,512]{1,0:T(8,128)S(1)} %get-tuple-element.13.hid_ref, ...), custom_call_target="tpu_custom_call" | custom-call | flops 1811939328 | bytes 6553600 | tf_op jit(solution)/shard_map/pallas_call | solution.py:172
  79.5 5.5 %shard_map.61 = (bf16[192,2048]{1,0:T(8,128)(2,1)}, bf16[192,2048]{1,0:T(8,128)(2,1)}) custom-call(bf16[384,512]{1,0:T(8,128)(2,1)} %get-tuple-element.14.grad_ref, bf16[4,3,128,512]{3,2,1,0:T(8,128)(2,1)} %copy-done, bf16[320,512]{1,0:T(8,128)(2,1)} %copy-done.1, bf16[320,512]{1,0:T(8,128)(2,1)} %copy-done.4, bf16[320,512]{1,0:T(8,128)(2,1)} %copy-done.6, ...), custom_call_target="tpu_custom_call" | custom-call | flops 805306368 | bytes 4587520 | tf_op jit(solution)/shard_map/pallas_call | solution.py:172
  85.0 1.9 %collective-permute-start.14 = (bf16[192,2048]{1,0:T(8,128)(2,1)}, bf16[192,2048]{1,0:T(8,128)(2,1)S(1)}, u32[]{:S(2)}, u32[]{:S(2)}) collective-permute-start(bf16[192,2048]{1,0:T(8,128)(2,1)} %get-tuple-element.16), channel_id=1, source_target_pairs={{0,1},{1,0},{2,3},{3,2},{4,5},{5,4},{6,7},{7,6},{8,9},{9,8},{10,11... | collective-permute-start | bytes 2359304 | tf_op jit(solution)/shard_map/ppermute | solution.py:40
  87.0 2.5 %collective-permute-done.14 = bf16[192,2048]{1,0:T(8,128)(2,1)S(1)} collective-permute-done((bf16[192,2048]{1,0:T(8,128)(2,1)}, bf16[192,2048]{1,0:T(8,128)(2,1)S(1)}, u32[]{:S(2)}, u32[]{:S(2)}) %collective-permute-start.14) | collective-permute-done | bytes 786464 | tf_op jit(solution)/shard_map/ppermute | solution.py:40
  89.4 1.4 add_convert_fusion.2
  90.8 0.0 copy-start.7
  90.8 3.1 %collective-permute-start.15 = (bf16[192,2048]{1,0:T(8,128)(2,1)S(1)}, bf16[192,2048]{1,0:T(8,128)(2,1)}, u32[]{:S(2)}, u32[]{:S(2)}) collective-permute-start(bf16[192,2048]{1,0:T(8,128)(2,1)S(1)} %add_convert_fusion.2), channel_id=1, source_target_pairs={{0,2},{2,0},{4,6},{6,4},{1,3},{3,1},{5,7},{7,5},{8,10},{10,8},{12,... | collective-permute-start | bytes 2359304 | tf_op jit(solution)/shard_map/ppermute | solution.py:40
  94.0 3.6 %all-to-all-start.1 = ((bf16[4,4,2,64,512]{4,3,2,1,0:T(8,128)(2,1)}), bf16[4,4,2,64,512]{4,3,2,1,0:T(8,128)(2,1)S(1)}, u32[]{:S(2)}, u32[]{:S(2)}) async-start(bf16[4,4,2,64,512]{4,3,2,1,0:T(8,128)(2,1)} %get-tuple-element.17), calls=%async_computation.1 | async-start | bytes 4194304 | tf_op jit(solution)/shard_map/all_to_all | solution.py:24
  97.6 14.8 %collective-permute-done.15 = bf16[192,2048]{1,0:T(8,128)(2,1)} collective-permute-done((bf16[192,2048]{1,0:T(8,128)(2,1)S(1)}, bf16[192,2048]{1,0:T(8,128)(2,1)}, u32[]{:S(2)}, u32[]{:S(2)}) %collective-permute-start.15) | collective-permute-done | bytes 786464 | tf_op jit(solution)/shard_map/ppermute | solution.py:40
  112.4 1.6 add_convert_fusion.1
  114.1 2.4 %collective-permute-start.16 = (bf16[192,2048]{1,0:T(8,128)(2,1)S(1)}, bf16[192,2048]{1,0:T(8,128)(2,1)}, u32[]{:S(2)}, u32[]{:S(2)}) collective-permute-start(bf16[192,2048]{1,0:T(8,128)(2,1)S(1)} %add_convert_fusion.1), channel_id=1, source_target_pairs={{0,6},{2,4},{4,2},{6,0},{1,7},{3,5},{5,3},{7,1},{8,14},{10,12},{12... | collective-permute-start | bytes 2359304 | tf_op jit(solution)/shard_map/ppermute | solution.py:40
  116.5 7.7 %all-to-all-done.1 = bf16[4,4,2,64,512]{4,3,2,1,0:T(8,128)(2,1)S(1)} async-done(((bf16[4,4,2,64,512]{4,3,2,1,0:T(8,128)(2,1)}), bf16[4,4,2,64,512]{4,3,2,1,0:T(8,128)(2,1)S(1)}, u32[]{:S(2)}, u32[]{:S(2)}) %all-to-all-start.1) | async-done | bytes 2097184 | tf_op jit(solution)/shard_map/all_to_all | solution.py:24
  124.2 1.3 reduce_sum.33
  125.5 3.5 %all-to-all-start.2 = ((bf16[4,2,64,512]{3,2,1,0:T(8,128)(2,1)}), bf16[4,2,64,512]{3,2,1,0:T(8,128)(2,1)S(1)}, u32[]{:S(2)}, u32[]{:S(2)}) async-start(bf16[4,2,64,512]{3,2,1,0:T(8,128)(2,1)} %reduce_sum.33), calls=%async_computation.2 | async-start | bytes 1048576 | tf_op jit(solution)/shard_map/all_to_all | solution.py:24
  128.9 5.9 %collective-permute-done.16 = bf16[192,2048]{1,0:T(8,128)(2,1)} collective-permute-done((bf16[192,2048]{1,0:T(8,128)(2,1)S(1)}, bf16[192,2048]{1,0:T(8,128)(2,1)}, u32[]{:S(2)}, u32[]{:S(2)}) %collective-permute-start.16) | collective-permute-done | bytes 786464 | tf_op jit(solution)/shard_map/ppermute | solution.py:40
  134.8 1.4 add_convert_fusion
  136.2 1.9 %collective-permute-start.17 = (bf16[192,2048]{1,0:T(8,128)(2,1)S(1)}, bf16[192,2048]{1,0:T(8,128)(2,1)S(1)}, u32[]{:S(2)}, u32[]{:S(2)}) collective-permute-start(bf16[192,2048]{1,0:T(8,128)(2,1)S(1)} %add_convert_fusion), channel_id=1, source_target_pairs={{0,1},{1,0},{2,3},{3,2},{4,5},{5,4},{6,7},{7,6},{8,9},{9,8},{10,11... | collective-permute-start | bytes 2359304 | tf_op jit(solution)/shard_map/ppermute | solution.py:40
  138.1 4.7 %all-to-all-done.2 = bf16[4,2,64,512]{3,2,1,0:T(8,128)(2,1)S(1)} async-done(((bf16[4,2,64,512]{3,2,1,0:T(8,128)(2,1)}), bf16[4,2,64,512]{3,2,1,0:T(8,128)(2,1)S(1)}, u32[]{:S(2)}, u32[]{:S(2)}) %all-to-all-start.2) | async-done | bytes 524320 | tf_op jit(solution)/shard_map/all_to_all | solution.py:24
  142.8 0.1 reduce_sum.34
  142.9 0.7 broadcast_in_dim.7
  143.6 8.3 %all-to-all-start.3 = ((bf16[4,64,512]{2,1,0:T(8,128)(2,1)}), bf16[4,64,512]{2,1,0:T(8,128)(2,1)S(1)}, u32[]{:S(2)}, u32[]{:S(2)}) async-start(bf16[4,64,512]{2,1,0:T(8,128)(2,1)} %bitcast.4), calls=%async_computation.3 | async-start | bytes 524288 | tf_op jit(solution)/shard_map/all_to_all | solution.py:24
  151.9 0.0 collective-permute-done.17
  151.9 0.1 broadcast_select_fusion.1
  152.1 1.2 pad_maximum_fusion
  153.3 17.1 %all-to-all-done.3 = bf16[4,64,512]{2,1,0:T(8,128)(2,1)S(1)} async-done(((bf16[4,64,512]{2,1,0:T(8,128)(2,1)}), bf16[4,64,512]{2,1,0:T(8,128)(2,1)S(1)}, u32[]{:S(2)}, u32[]{:S(2)}) %all-to-all-start.3) | async-done | bytes 262176 | tf_op jit(solution)/shard_map/all_to_all | solution.py:24
  170.4 0.7 convert_reduce_fusion
  (19 shorter events, 0.1 us)
Async XLA Ops:
  1.5 14.1 %collective-permute-start.1 = (bf16[128,512]{1,0:T(8,128)(2,1)S(1)}, bf16[128,512]{1,0:T(8,128)(2,1)S(1)}, u32[]{:S(2)}, u32[]{:S(2)}) collective-permute-start(bf16[128,512]{1,0:T(8,128)(2,1)S(1)} %get-tuple-element.21), channel_id=1, source_target_pairs={{0,480},{32,0},{64,32},{96,64},{128,96},{160,128},{192,160},{224,1... | collective-permute-start | bytes 393224 | tf_op jit(solution)/shard_map/ppermute | solution.py:35
  12.9 8.3 %collective-permute-start = (bf16[128,512]{1,0:T(8,128)(2,1)S(1)}, bf16[128,512]{1,0:T(8,128)(2,1)S(1)}, u32[]{:S(2)}, u32[]{:S(2)}) collective-permute-start(bf16[128,512]{1,0:T(8,128)(2,1)S(1)} %get-tuple-element.21), channel_id=1, source_target_pairs={{0,32},{32,64},{64,96},{96,128},{128,160},{160,192},{192,224},{224... | collective-permute-start | bytes 393224 | tf_op jit(solution)/shard_map/ppermute | solution.py:35
  15.7 13.3 %collective-permute-start.8 = (bf16[128,512]{1,0:T(8,128)(2,1)S(1)}, bf16[128,512]{1,0:T(8,128)(2,1)S(1)}, u32[]{:S(2)}, u32[]{:S(2)}) collective-permute-start(bf16[128,512]{1,0:T(8,128)(2,1)S(1)} %collective-permute-done.1), channel_id=1, source_target_pairs={{0,480},{32,0},{64,32},{96,64},{128,96},{160,128},{192,160},{224,1... | collective-permute-start | bytes 393224 | tf_op jit(solution)/shard_map/ppermute | solution.py:35
  21.3 12.9 %collective-permute-start.2 = (bf16[128,512]{1,0:T(8,128)(2,1)S(1)}, bf16[128,512]{1,0:T(8,128)(2,1)S(1)}, u32[]{:S(2)}, u32[]{:S(2)}) collective-permute-start(bf16[128,512]{1,0:T(8,128)(2,1)S(1)} %collective-permute-done), channel_id=1, source_target_pairs={{0,32},{32,64},{64,96},{96,128},{128,160},{160,192},{192,224},{224... | collective-permute-start | bytes 393224 | tf_op jit(solution)/shard_map/ppermute | solution.py:35
  24.5 42.0 %all-to-all-start = ((bf16[4,3,128,512]{3,2,1,0:T(8,128)(2,1)}), bf16[4,3,128,512]{3,2,1,0:T(8,128)(2,1)S(1)}, u32[]{:S(2)}, u32[]{:S(2)}) async-start(bf16[4,3,128,512]{3,2,1,0:T(8,128)(2,1)} %broadcast_in_dim.6), calls=%async_computation | async-start | bytes 3145728 | tf_op jit(solution)/shard_map/all_to_all | solution.py:24
  29.0 7.6 %collective-permute-start.9 = (bf16[128,512]{1,0:T(8,128)(2,1)S(1)}, bf16[128,512]{1,0:T(8,128)(2,1)S(1)}, u32[]{:S(2)}, u32[]{:S(2)}) collective-permute-start(bf16[128,512]{1,0:T(8,128)(2,1)S(1)} %collective-permute-done.8), channel_id=1, source_target_pairs={{0,480},{32,0},{64,32},{96,64},{128,96},{160,128},{192,160},{224,1... | collective-permute-start | bytes 393224 | tf_op jit(solution)/shard_map/ppermute | solution.py:35
  34.1 8.1 %collective-permute-start.3 = (bf16[128,512]{1,0:T(8,128)(2,1)S(1)}, bf16[128,512]{1,0:T(8,128)(2,1)S(1)}, u32[]{:S(2)}, u32[]{:S(2)}) collective-permute-start(bf16[128,512]{1,0:T(8,128)(2,1)S(1)} %collective-permute-done.2), channel_id=1, source_target_pairs={{0,32},{32,64},{64,96},{96,128},{128,160},{160,192},{192,224},{224... | collective-permute-start | bytes 393224 | tf_op jit(solution)/shard_map/ppermute | solution.py:35
  36.6 7.6 %collective-permute-start.10 = (bf16[64,512]{1,0:T(8,128)(2,1)S(1)}, bf16[64,512]{1,0:T(8,128)(2,1)S(1)}, u32[]{:S(2)}, u32[]{:S(2)}) collective-permute-start(bf16[64,512]{1,0:T(8,128)(2,1)S(1)} %slice.9), channel_id=1, source_target_pairs={{0,480},{32,0},{64,32},{96,64},{128,96},{160,128},{192,160},{224,1... | collective-permute-start | bytes 196616 | tf_op jit(solution)/shard_map/ppermute | solution.py:35
  42.2 7.4 %collective-permute-start.4 = (bf16[64,512]{1,0:T(8,128)(2,1)S(1)}, bf16[64,512]{1,0:T(8,128)(2,1)S(1)}, u32[]{:S(2)}, u32[]{:S(2)}) collective-permute-start(bf16[64,512]{1,0:T(8,128)(2,1)S(1)} %slice.8), channel_id=1, source_target_pairs={{0,32},{32,64},{64,96},{96,128},{128,160},{160,192},{192,224},{224... | collective-permute-start | bytes 196616 | tf_op jit(solution)/shard_map/ppermute | solution.py:35
  44.2 28.7 %copy-start.2 = (bf16[320,512]{1,0:T(8,128)(2,1)}, bf16[320,512]{1,0:T(8,128)(2,1)S(1)}, u32[]{:S(2)}) copy-start(bf16[320,512]{1,0:T(8,128)(2,1)S(1)} %constant_dynamic-update-slice_fusion.3.refs_4_) | copy-start | bytes 983044
  44.2 16.4 %collective-permute-start.12 = (bf16[320,512]{1,0:T(8,128)(2,1)S(1)}, bf16[320,512]{1,0:T(8,128)(2,1)S(1)}, u32[]{:S(2)}, u32[]{:S(2)}) collective-permute-start(bf16[320,512]{1,0:T(8,128)(2,1)S(1)} %constant_dynamic-update-slice_fusion.3.refs_4_), channel_id=1, source_target_pairs={{0,24},{8,0},{16,8},{24,16},{1,25},{9,1},{17,9},{25,17},{2,26},{10... | collective-permute-start | bytes 983048 | tf_op jit(solution)/shard_map/ppermute | solution.py:35
  49.6 23.3 %copy-start.1 = (bf16[320,512]{1,0:T(8,128)(2,1)}, bf16[320,512]{1,0:T(8,128)(2,1)S(1)}, u32[]{:S(2)}) copy-start(bf16[320,512]{1,0:T(8,128)(2,1)S(1)} %constant_dynamic-update-slice_fusion.refs_0_) | copy-start | bytes 983044
  49.6 13.0 %collective-permute-start.5 = (bf16[320,512]{1,0:T(8,128)(2,1)S(1)}, bf16[320,512]{1,0:T(8,128)(2,1)S(1)}, u32[]{:S(2)}, u32[]{:S(2)}) collective-permute-start(bf16[320,512]{1,0:T(8,128)(2,1)S(1)} %constant_dynamic-update-slice_fusion.refs_0_), channel_id=1, source_target_pairs={{0,8},{8,16},{16,24},{24,0},{1,9},{9,17},{17,25},{25,1},{2,10},{10... | collective-permute-start | bytes 983048 | tf_op jit(solution)/shard_map/ppermute | solution.py:35
  53.5 15.7 %collective-permute-start.11 = (bf16[320,512]{1,0:T(8,128)(2,1)S(1)}, bf16[320,512]{1,0:T(8,128)(2,1)S(1)}, u32[]{:S(2)}, u32[]{:S(2)}) collective-permute-start(bf16[320,512]{1,0:T(8,128)(2,1)S(1)} %constant_dynamic-update-slice_fusion.3.refs_4_), channel_id=1, source_target_pairs={{0,8},{8,16},{16,24},{24,0},{1,9},{9,17},{17,25},{25,1},{2,10},{10... | collective-permute-start | bytes 983048 | tf_op jit(solution)/shard_map/ppermute | solution.py:35
  56.9 12.3 %collective-permute-start.6 = (bf16[320,512]{1,0:T(8,128)(2,1)S(1)}, bf16[320,512]{1,0:T(8,128)(2,1)S(1)}, u32[]{:S(2)}, u32[]{:S(2)}) collective-permute-start(bf16[320,512]{1,0:T(8,128)(2,1)S(1)} %constant_dynamic-update-slice_fusion.refs_0_), channel_id=1, source_target_pairs={{0,24},{8,0},{16,8},{24,16},{1,25},{9,1},{17,9},{25,17},{2,26},{10... | collective-permute-start | bytes 983048 | tf_op jit(solution)/shard_map/ppermute | solution.py:35
  60.6 12.3 %copy-start.3 = (bf16[320,512]{1,0:T(8,128)(2,1)}, bf16[320,512]{1,0:T(8,128)(2,1)S(1)}, u32[]{:S(2)}) copy-start(bf16[320,512]{1,0:T(8,128)(2,1)S(1)} %collective-permute-done.12.refs_6_) | copy-start | bytes 983044
  60.6 9.8 %collective-permute-start.13 = (bf16[320,512]{1,0:T(8,128)(2,1)S(1)}, bf16[320,512]{1,0:T(8,128)(2,1)}, u32[]{:S(2)}, u32[]{:S(2)}) collective-permute-start(bf16[320,512]{1,0:T(8,128)(2,1)S(1)} %collective-permute-done.12.refs_6_), channel_id=1, source_target_pairs={{0,24},{8,0},{16,8},{24,16},{1,25},{9,1},{17,9},{25,17},{2,26},{10... | collective-permute-start | bytes 983048 | tf_op jit(solution)/shard_map/ppermute | solution.py:35
  62.6 10.3 %copy-start.4 = (bf16[320,512]{1,0:T(8,128)(2,1)}, bf16[320,512]{1,0:T(8,128)(2,1)S(1)}, u32[]{:S(2)}) copy-start(bf16[320,512]{1,0:T(8,128)(2,1)S(1)} %collective-permute-done.5.refs_1_) | copy-start | bytes 983044
  62.6 10.3 %collective-permute-start.7 = (bf16[320,512]{1,0:T(8,128)(2,1)S(1)}, bf16[320,512]{1,0:T(8,128)(2,1)}, u32[]{:S(2)}, u32[]{:S(2)}) collective-permute-start(bf16[320,512]{1,0:T(8,128)(2,1)S(1)} %collective-permute-done.5.refs_1_), channel_id=1, source_target_pairs={{0,8},{8,16},{16,24},{24,0},{1,9},{9,17},{17,25},{25,1},{2,10},{10... | collective-permute-start | bytes 983048 | tf_op jit(solution)/shard_map/ppermute | solution.py:35
  66.5 2.7 %copy-start = (bf16[4,3,128,512]{3,2,1,0:T(8,128)(2,1)}, bf16[4,3,128,512]{3,2,1,0:T(8,128)(2,1)S(1)}, u32[]{:S(2)}) copy-start(bf16[4,3,128,512]{3,2,1,0:T(8,128)(2,1)S(1)} %all-to-all-done.near_ref) | copy-start | bytes 4718596
  69.3 10.2 %copy-start.5 = (bf16[320,512]{1,0:T(8,128)(2,1)}, bf16[320,512]{1,0:T(8,128)(2,1)S(1)}, u32[]{:S(2)}) copy-start(bf16[320,512]{1,0:T(8,128)(2,1)S(1)} %collective-permute-done.11.refs_5_) | copy-start | bytes 983044
  69.3 10.2 %copy-start.6 = (bf16[320,512]{1,0:T(8,128)(2,1)}, bf16[320,512]{1,0:T(8,128)(2,1)S(1)}, u32[]{:S(2)}) copy-start(bf16[320,512]{1,0:T(8,128)(2,1)S(1)} %collective-permute-done.6.refs_2_) | copy-start | bytes 983044
  85.0 4.4 %collective-permute-start.14 = (bf16[192,2048]{1,0:T(8,128)(2,1)}, bf16[192,2048]{1,0:T(8,128)(2,1)S(1)}, u32[]{:S(2)}, u32[]{:S(2)}) collective-permute-start(bf16[192,2048]{1,0:T(8,128)(2,1)} %get-tuple-element.16), channel_id=1, source_target_pairs={{0,1},{1,0},{2,3},{3,2},{4,5},{5,4},{6,7},{7,6},{8,9},{9,8},{10,11... | collective-permute-start | bytes 2359304 | tf_op jit(solution)/shard_map/ppermute | solution.py:40
  90.8 3.1 %copy-start.7 = (bf16[192,2048]{1,0:T(8,128)(2,1)}, bf16[192,2048]{1,0:T(8,128)(2,1)S(1)}, u32[]{:S(2)}) copy-start(bf16[192,2048]{1,0:T(8,128)(2,1)S(1)} %add_convert_fusion.2) | copy-start | bytes 2359300
  90.8 21.6 %collective-permute-start.15 = (bf16[192,2048]{1,0:T(8,128)(2,1)S(1)}, bf16[192,2048]{1,0:T(8,128)(2,1)}, u32[]{:S(2)}, u32[]{:S(2)}) collective-permute-start(bf16[192,2048]{1,0:T(8,128)(2,1)S(1)} %add_convert_fusion.2), channel_id=1, source_target_pairs={{0,2},{2,0},{4,6},{6,4},{1,3},{3,1},{5,7},{7,5},{8,10},{10,8},{12,... | collective-permute-start | bytes 2359304 | tf_op jit(solution)/shard_map/ppermute | solution.py:40
  94.0 30.2 %all-to-all-start.1 = ((bf16[4,4,2,64,512]{4,3,2,1,0:T(8,128)(2,1)}), bf16[4,4,2,64,512]{4,3,2,1,0:T(8,128)(2,1)S(1)}, u32[]{:S(2)}, u32[]{:S(2)}) async-start(bf16[4,4,2,64,512]{4,3,2,1,0:T(8,128)(2,1)} %get-tuple-element.17), calls=%async_computation.1 | async-start | bytes 4194304 | tf_op jit(solution)/shard_map/all_to_all | solution.py:24
  114.1 20.7 %collective-permute-start.16 = (bf16[192,2048]{1,0:T(8,128)(2,1)S(1)}, bf16[192,2048]{1,0:T(8,128)(2,1)}, u32[]{:S(2)}, u32[]{:S(2)}) collective-permute-start(bf16[192,2048]{1,0:T(8,128)(2,1)S(1)} %add_convert_fusion.1), channel_id=1, source_target_pairs={{0,6},{2,4},{4,2},{6,0},{1,7},{3,5},{5,3},{7,1},{8,14},{10,12},{12... | collective-permute-start | bytes 2359304 | tf_op jit(solution)/shard_map/ppermute | solution.py:40
  125.5 17.4 %all-to-all-start.2 = ((bf16[4,2,64,512]{3,2,1,0:T(8,128)(2,1)}), bf16[4,2,64,512]{3,2,1,0:T(8,128)(2,1)S(1)}, u32[]{:S(2)}, u32[]{:S(2)}) async-start(bf16[4,2,64,512]{3,2,1,0:T(8,128)(2,1)} %reduce_sum.33), calls=%async_computation.2 | async-start | bytes 1048576 | tf_op jit(solution)/shard_map/all_to_all | solution.py:24
  136.2 15.7 %collective-permute-start.17 = (bf16[192,2048]{1,0:T(8,128)(2,1)S(1)}, bf16[192,2048]{1,0:T(8,128)(2,1)S(1)}, u32[]{:S(2)}, u32[]{:S(2)}) collective-permute-start(bf16[192,2048]{1,0:T(8,128)(2,1)S(1)} %add_convert_fusion), channel_id=1, source_target_pairs={{0,1},{1,0},{2,3},{3,2},{4,5},{5,4},{6,7},{7,6},{8,9},{9,8},{10,11... | collective-permute-start | bytes 2359304 | tf_op jit(solution)/shard_map/ppermute | solution.py:40
  143.6 26.8 %all-to-all-start.3 = ((bf16[4,64,512]{2,1,0:T(8,128)(2,1)}), bf16[4,64,512]{2,1,0:T(8,128)(2,1)S(1)}, u32[]{:S(2)}, u32[]{:S(2)}) async-start(bf16[4,64,512]{2,1,0:T(8,128)(2,1)} %bitcast.4), calls=%async_computation.3 | async-start | bytes 524288 | tf_op jit(solution)/shard_map/all_to_all | solution.py:24

commit v7 on v6

--- a/solution.py
+++ b/solution.py
@@ -85,40 +85,29 @@
             hid_ref[...] += hid
 
 
-def far_copies(plus, minus, dsts, sems):
+def order_far(plus, minus, dsts):
     me = lax.axis_index("y")
     rows = plus[0].shape[0] // 5
-    width = N_Y * rows
-    copies = []
-    for n in range(len(FAR)):
-        group = []
-        for part, dst in enumerate(dsts):
-            if n < 4:
-                refs, piece = (plus, minus)[n % 2], n // 2 * 2 + part
-            else:
-                refs, piece = (plus, minus)[part], 4
-            for k, dist in enumerate((0, 1, -1, 2)):
-                y = lax.rem(me - dist + 2 * N_Y, N_Y)
-                at = pl.multiple_of(n * width + y * rows, rows)
-                copy = pltpu.make_async_copy(
-                    refs[k].at[pl.ds(piece * rows, rows)],
-                    dst.at[pl.ds(at, rows)],
-                    sems.at[n, part, k],
-                )
-                copy.start()
-                group.append(copy)
-        copies.append(group)
-    return copies
+    for k, dist in enumerate((0, 1, -1, 2)):
+        y = lax.rem(me - dist + 2 * N_Y, N_Y)
+        for n in range(len(FAR)):
+            for part, dst in enumerate(dsts):
+                if n < 4:
+                    ref, piece = (plus, minus)[n % 2][k], n // 2 * 2 + part
+                else:
+                    ref, piece = (plus, minus)[part][k], 4
+                at = pl.multiple_of(n * N_Y * rows + y * rows, rows)
+                dst[pl.ds(at, rows), :] = ref[piece * rows : (piece + 1) * rows, :]
 
 
 def weight_kernel(x_ref, c_ref, pre_ref, hid_ref, *refs):
     plus, minus = refs[0:4], refs[4:8]
-    grad_hbm, dw_hbm, up, down, pre_acc, hid_acc, grad, dw, far_sems, out_sems = refs[8:]
+    grad_hbm, dw_hbm, up_hbm, up, down, pre_acc, hid_acc, grad, dw, out_sems = refs[8:]
     width = dw.shape[1] * dw.shape[2]
-    blocks = far_copies(plus, minus, (up, down), far_sems)
+    order_far(plus, minus, (up, down))
+    out = [pltpu.make_async_copy(up, up_hbm, out_sems.at[N_Z + 1])]
+    out[0].start()
     for n, (_, _, z) in enumerate(z_blocks((None, FAR))):
-        for copy in blocks[n]:
-            copy.wait()
         at = pl.ds(pl.multiple_of(z * width, width), width)
         mine = slice(n * width, (n + 1) * width)
         pre = jnp.dot(x_ref[:, at], up[mine], preferred_element_type=F32)
@@ -126,8 +115,8 @@
         pre_acc[...] = (pre_ref if n == 0 else pre_acc)[...] + pre
         hid_acc[...] = (hid_ref if n == 0 else hid_acc)[...] + hid
     grad[...] = (2.0 * jnp.maximum(pre_acc[...], 0.0) * hid_acc[...]).astype(BF)
-    out = [pltpu.make_async_copy(grad, grad_hbm, out_sems.at[N_Z])]
-    out[0].start()
+    out.append(pltpu.make_async_copy(grad, grad_hbm, out_sems.at[N_Z]))
+    out[1].start()
     for z in range(N_Z):
         product = lax.dot_general(
             x_ref[:, z * width : (z + 1) * width], grad[...],
@@ -143,21 +132,15 @@
         copy.wait()
 
 
-def input_kernel(grad_ref, near_ref, *refs):
-    plus, minus = refs[0:4], refs[4:8]
-    keep_ref, give_ref, up, sems = refs[8:]
+def input_kernel(grad_ref, near_ref, up_ref, keep_ref, give_ref):
     core = lax.axis_index("core")
     tokens = keep_ref.shape[0]
     width = N_Y * near_ref.shape[2] // 2
-    copies = far_copies(plus, minus, (up,), sems)
-    for group in copies:
-        for copy in group:
-            copy.wait()
     for out, which in ((give_ref, 1 - core), (keep_ref, core)):
         mine = grad_ref[pl.ds(pl.multiple_of(which * tokens, tokens), tokens), :]
         for ref, k, z in z_blocks((near_ref, NEAR), (None, FAR)):
             if ref is None:
-                block = up[k * width : (k + 1) * width]
+                block = up_ref[k * width : (k + 1) * width]
             else:
                 block = rows_of(ref, k, 0)
             out[:, pl.ds(pl.multiple_of(z * width, width), width)] = lax.dot_general(
@@ -224,12 +207,16 @@
         (0, 1),
         [pltpu.SemaphoreType.DMA((N_Z, 2))],
     )
-    grad, dw = call(
+    grad, dw, up = call(
         weight_kernel,
-        [((tokens, h), BF), ((N_Y, 4, 2, rows, h), BF)],
+        [
+            ((tokens, h), BF),
+            ((N_Y, 4, 2, rows, h), BF),
+            ((len(FAR) * part, h), BF),
+        ],
         (inputs, cotangent, pre, hid, *plus, *minus),
         9 * unit,
-        range(4, 12),
+        (),
         [
             pltpu.VMEM((len(FAR) * part, h), BF),
             pltpu.VMEM((len(FAR) * part, h), BF),
@@ -237,21 +224,16 @@
             pltpu.VMEM((tokens, h), F32),
             pltpu.VMEM((tokens, h), BF),
             pltpu.VMEM((N_Z, N_Y, rows, h), BF),
-            pltpu.SemaphoreType.DMA((len(FAR), 2, N_Y)),
-            pltpu.SemaphoreType.DMA((N_Z + 1,)),
+            pltpu.SemaphoreType.DMA((N_Z + 2,)),
         ],
-        out_hbm=(0, 1),
+        out_hbm=(0, 1, 2),
     )
     keep, give = call(
         input_kernel,
         [((tokens // 2, width), BF)] * 2,
-        (grad, near, *plus, *minus),
+        (grad, near, up),
         4 * unit,
-        range(2, 10),
-        [
-            pltpu.VMEM((len(FAR) * part, h), BF),
-            pltpu.SemaphoreType.DMA((len(FAR), 1, N_Y)),
-        ],
+        (),
         limit=None,
     )
 

time: 172 us -> 169 us (0.983)
  Pallas kernels: 14.8 us -> 11.5 us
    pallas_call x3, Pallas kernels: 14.8 us -> 11.5 us  [call(): pl.pallas_call(kernel, out_shape=tuple((pltpu.HBM(s, t) if k in out_hbm e...]
where the time goes in v7:
time: 169 us; the launch traced here: 168 us
  starting transfers between devices  86.5 us (51%)
  waiting for transfers between devices  57.9 us (34%)
  Pallas kernels  11.5 us (7%)
  other arithmetic  8.75 us (5%)
  local copies, waits for them, and re-layouts  2.09 us (1%)
    ppermute x14, starting transfers between devices, shifted(): return lax.ppermute(value, axes, [(i, (i + step) % n) for i in range(n)])  57.3 us
    all_to_all x4, waiting for transfers between devices, exchange(): return lax.all_to_all(parts, axes, split_axis=0, concat_axis=0, tiled=True)  29.5 us
    ppermute x4, waiting for transfers between devices, swapped(): return lax.ppermute(value, axes, [(i, partner(i)) for i in range(n)])  23.2 us
    all_to_all x4, starting transfers between devices, exchange(): return lax.all_to_all(parts, axes, split_axis=0, concat_axis=0, tiled=True)  19.8 us
    pallas_call x3, Pallas kernels, call(): pl.pallas_call(kernel, out_shape=tuple((pltpu.HBM(s, t) if k in out_hbm e...  11.5 us
    ppermute x4, starting transfers between devices, swapped(): return lax.ppermute(value, axes, [(i, partner(i)) for i in range(n)])  9.37 us
    ppermute x14, waiting for transfers between devices, shifted(): return lax.ppermute(value, axes, [(i, (i + step) % n) for i in range(n)])  5.2 us
    convert_element_type x3, other arithmetic, total(): return (a.astype(F32) + b.astype(F32)).astype(BF)  4.42 us
  transfers between devices with their start and end apart: 22, of which 11 were waited for; matrix products, arithmetic and copies ran while one was open for 5% of the time, Pallas kernels for 2%

profile of v7, /device:TPU:4, one launch (start us, length us, event | category | flops | bytes accessed | tf_op | source)
XLA Modules:
  0.0 167.7 jit_solution(5385391722144860113)
XLA Ops:
  0.6 0.9 fusion
  1.5 11.4 %collective-permute-start.1 = (bf16[128,512]{1,0:T(8,128)(2,1)S(1)}, bf16[128,512]{1,0:T(8,128)(2,1)S(1)}, u32[]{:S(2)}, u32[]{:S(2)}) collective-permute-start(bf16[128,512]{1,0:T(8,128)(2,1)S(1)} %get-tuple-element.23), channel_id=1, source_target_pairs={{0,480},{32,0},{64,32},{96,64},{128,96},{160,128},{192,160},{224,1... | collective-permute-start | bytes 393224 | tf_op jit(solution)/shard_map/ppermute | solution.py:35
  12.9 1.9 %collective-permute-start = (bf16[128,512]{1,0:T(8,128)(2,1)S(1)}, bf16[128,512]{1,0:T(8,128)(2,1)S(1)}, u32[]{:S(2)}, u32[]{:S(2)}) collective-permute-start(bf16[128,512]{1,0:T(8,128)(2,1)S(1)} %get-tuple-element.23), channel_id=1, source_target_pairs={{0,32},{32,64},{64,96},{96,128},{128,160},{160,192},{192,224},{224... | collective-permute-start | bytes 393224 | tf_op jit(solution)/shard_map/ppermute | solution.py:35
  14.9 0.8 collective-permute-done.1
  15.7 5.6 %collective-permute-start.8 = (bf16[128,512]{1,0:T(8,128)(2,1)S(1)}, bf16[128,512]{1,0:T(8,128)(2,1)S(1)}, u32[]{:S(2)}, u32[]{:S(2)}) collective-permute-start(bf16[128,512]{1,0:T(8,128)(2,1)S(1)} %collective-permute-done.1), channel_id=1, source_target_pairs={{0,480},{32,0},{64,32},{96,64},{128,96},{160,128},{192,160},{224,1... | collective-permute-start | bytes 393224 | tf_op jit(solution)/shard_map/ppermute | solution.py:35
  21.3 0.0 collective-permute-done
  21.3 1.9 %collective-permute-start.2 = (bf16[128,512]{1,0:T(8,128)(2,1)S(1)}, bf16[128,512]{1,0:T(8,128)(2,1)S(1)}, u32[]{:S(2)}, u32[]{:S(2)}) collective-permute-start(bf16[128,512]{1,0:T(8,128)(2,1)S(1)} %collective-permute-done), channel_id=1, source_target_pairs={{0,32},{32,64},{64,96},{96,128},{128,160},{160,192},{192,224},{224... | collective-permute-start | bytes 393224 | tf_op jit(solution)/shard_map/ppermute | solution.py:35
  23.3 1.3 broadcast_in_dim.6
  24.5 4.5 %all-to-all-start = ((bf16[4,3,128,512]{3,2,1,0:T(8,128)(2,1)}), bf16[4,3,128,512]{3,2,1,0:T(8,128)(2,1)S(1)}, u32[]{:S(2)}, u32[]{:S(2)}) async-start(bf16[4,3,128,512]{3,2,1,0:T(8,128)(2,1)} %broadcast_in_dim.6), calls=%async_computation | async-start | bytes 3145728 | tf_op jit(solution)/shard_map/all_to_all | solution.py:24
  29.0 0.0 collective-permute-done.8
  29.0 5.1 %collective-permute-start.9 = (bf16[128,512]{1,0:T(8,128)(2,1)S(1)}, bf16[128,512]{1,0:T(8,128)(2,1)S(1)}, u32[]{:S(2)}, u32[]{:S(2)}) collective-permute-start(bf16[128,512]{1,0:T(8,128)(2,1)S(1)} %collective-permute-done.8), channel_id=1, source_target_pairs={{0,480},{32,0},{64,32},{96,64},{128,96},{160,128},{192,160},{224,1... | collective-permute-start | bytes 393224 | tf_op jit(solution)/shard_map/ppermute | solution.py:35
  34.1 0.0 collective-permute-done.2
  34.1 1.9 %collective-permute-start.3 = (bf16[128,512]{1,0:T(8,128)(2,1)S(1)}, bf16[128,512]{1,0:T(8,128)(2,1)S(1)}, u32[]{:S(2)}, u32[]{:S(2)}) collective-permute-start(bf16[128,512]{1,0:T(8,128)(2,1)S(1)} %collective-permute-done.2), channel_id=1, source_target_pairs={{0,32},{32,64},{64,96},{96,128},{128,160},{160,192},{192,224},{224... | collective-permute-start | bytes 393224 | tf_op jit(solution)/shard_map/ppermute | solution.py:35
  36.1 0.5 collective-permute-done.9
  36.6 5.6 %collective-permute-start.10 = (bf16[64,512]{1,0:T(8,128)(2,1)S(1)}, bf16[64,512]{1,0:T(8,128)(2,1)S(1)}, u32[]{:S(2)}, u32[]{:S(2)}) collective-permute-start(bf16[64,512]{1,0:T(8,128)(2,1)S(1)} %slice.9), channel_id=1, source_target_pairs={{0,480},{32,0},{64,32},{96,64},{128,96},{160,128},{192,160},{224,1... | collective-permute-start | bytes 196616 | tf_op jit(solution)/shard_map/ppermute | solution.py:35
  42.2 0.0 collective-permute-done.3
  42.2 1.9 %collective-permute-start.4 = (bf16[64,512]{1,0:T(8,128)(2,1)S(1)}, bf16[64,512]{1,0:T(8,128)(2,1)S(1)}, u32[]{:S(2)}, u32[]{:S(2)}) collective-permute-start(bf16[64,512]{1,0:T(8,128)(2,1)S(1)} %slice.8), channel_id=1, source_target_pairs={{0,32},{32,64},{64,96},{96,128},{128,160},{160,192},{192,224},{224... | collective-permute-start | bytes 196616 | tf_op jit(solution)/shard_map/ppermute | solution.py:35
  44.2 0.0 collective-permute-done.10
  44.2 5.1 %collective-permute-start.12 = (bf16[320,512]{1,0:T(8,128)(2,1)S(1)}, bf16[320,512]{1,0:T(8,128)(2,1)S(1)}, u32[]{:S(2)}, u32[]{:S(2)}) collective-permute-start(bf16[320,512]{1,0:T(8,128)(2,1)S(1)} %constant_dynamic-update-slice_fusion.3.refs_4_), channel_id=1, source_target_pairs={{0,24},{8,0},{16,8},{24,16},{1,25},{9,1},{17,9},{25,17},{2,26},{10... | collective-permute-start | bytes 983048 | tf_op jit(solution)/shard_map/ppermute | solution.py:35
  49.4 0.2 collective-permute-done.4
  49.6 3.9 %collective-permute-start.5 = (bf16[320,512]{1,0:T(8,128)(2,1)S(1)}, bf16[320,512]{1,0:T(8,128)(2,1)S(1)}, u32[]{:S(2)}, u32[]{:S(2)}) collective-permute-start(bf16[320,512]{1,0:T(8,128)(2,1)S(1)} %constant_dynamic-update-slice_fusion.refs_0_), channel_id=1, source_target_pairs={{0,8},{8,16},{16,24},{24,0},{1,9},{9,17},{17,25},{25,1},{2,10},{10... | collective-permute-start | bytes 983048 | tf_op jit(solution)/shard_map/ppermute | solution.py:35
  53.5 3.4 %collective-permute-start.11 = (bf16[320,512]{1,0:T(8,128)(2,1)S(1)}, bf16[320,512]{1,0:T(8,128)(2,1)S(1)}, u32[]{:S(2)}, u32[]{:S(2)}) collective-permute-start(bf16[320,512]{1,0:T(8,128)(2,1)S(1)} %constant_dynamic-update-slice_fusion.3.refs_4_), channel_id=1, source_target_pairs={{0,8},{8,16},{16,24},{24,0},{1,9},{9,17},{17,25},{25,1},{2,10},{10... | collective-permute-start | bytes 983048 | tf_op jit(solution)/shard_map/ppermute | solution.py:35
  56.9 3.7 %collective-permute-start.6 = (bf16[320,512]{1,0:T(8,128)(2,1)S(1)}, bf16[320,512]{1,0:T(8,128)(2,1)S(1)}, u32[]{:S(2)}, u32[]{:S(2)}) collective-permute-start(bf16[320,512]{1,0:T(8,128)(2,1)S(1)} %constant_dynamic-update-slice_fusion.refs_0_), channel_id=1, source_target_pairs={{0,24},{8,0},{16,8},{24,16},{1,25},{9,1},{17,9},{25,17},{2,26},{10... | collective-permute-start | bytes 983048 | tf_op jit(solution)/shard_map/ppermute | solution.py:35
  60.6 0.0 collective-permute-done.12.refs_6_
  60.6 1.9 %collective-permute-start.13 = (bf16[320,512]{1,0:T(8,128)(2,1)S(1)}, bf16[320,512]{1,0:T(8,128)(2,1)}, u32[]{:S(2)}, u32[]{:S(2)}) collective-permute-start(bf16[320,512]{1,0:T(8,128)(2,1)S(1)} %collective-permute-done.12.refs_6_), channel_id=1, source_target_pairs={{0,24},{8,0},{16,8},{24,16},{1,25},{9,1},{17,9},{25,17},{2,26},{10... | collective-permute-start | bytes 983048 | tf_op jit(solution)/shard_map/ppermute | solution.py:35
  62.5 0.0 collective-permute-done.5.refs_1_
  62.6 3.9 %collective-permute-start.7 = (bf16[320,512]{1,0:T(8,128)(2,1)S(1)}, bf16[320,512]{1,0:T(8,128)(2,1)}, u32[]{:S(2)}, u32[]{:S(2)}) collective-permute-start(bf16[320,512]{1,0:T(8,128)(2,1)S(1)} %collective-permute-done.5.refs_1_), channel_id=1, source_target_pairs={{0,8},{8,16},{16,24},{24,0},{1,9},{9,17},{17,25},{25,1},{2,10},{10... | collective-permute-start | bytes 983048 | tf_op jit(solution)/shard_map/ppermute | solution.py:35
  66.5 0.0 all-to-all-done.near_ref
  66.5 0.0 copy-start
  66.5 2.7 %shard_map.59 = (f32[384,512]{1,0:T(8,128)S(1)}, f32[384,512]{1,0:T(8,128)S(1)}, bf16[384,2048]{1,0:T(8,128)(2,1)S(1)}, bf16[384,2048]{1,0:T(8,128)(2,1)S(1)}) custom-call(bf16[384,2048]{1,0:T(8,128)(2,1)} %x_hbm.1, bf16[384,2048]{1,0:T(8,128)(2,1)} %c_hbm.1, bf16[4,3,128,512]{3,2,1,0:T(8,128)(2,1)S(1)} %all-to-all-done.near_ref), custom_call_target="tpu_custom_call" | custom-call | flops 603979776 | bytes 4718592 | tf_op jit(solution)/shard_map/pallas_call | solution.py:155
  69.2 0.0 copy-done
  69.2 0.0 collective-permute-done.11.refs_5_
  69.2 0.0 collective-permute-done.6.refs_2_
  69.2 1.2 collective-permute-done.13.refs_7_
  70.4 2.4 %collective-permute-done.7.refs_3_ = bf16[320,512]{1,0:T(8,128)(2,1)} collective-permute-done((bf16[320,512]{1,0:T(8,128)(2,1)S(1)}, bf16[320,512]{1,0:T(8,128)(2,1)}, u32[]{:S(2)}, u32[]{:S(2)}) %collective-permute-start.7) | collective-permute-done | bytes 327712 | tf_op jit(solution)/shard_map/ppermute | solution.py:35
  72.8 4.4 %shard_map.60 = (bf16[384,512]{1,0:T(8,128)(2,1)}, bf16[4,4,2,64,512]{4,3,2,1,0:T(8,128)(2,1)}, bf16[1280,512]{1,0:T(8,128)(2,1)}) custom-call(bf16[384,2048]{1,0:T(8,128)(2,1)S(1)} %get-tuple-element.11.x_ref, bf16[384,2048]{1,0:T(8,128)(2,1)S(1)} %get-tuple-element.12.c_ref, f32[384,512]{1,0:T(8,128)S(1)} %get-tuple-element.13.pre_ref, ...), custom_call_target="tpu_custom_call" | custom-call | flops 1811939328 | bytes 6553600 | tf_op jit(solution)/shard_map/pallas_call | solution.py:155
  77.2 4.4 %shard_map.61 = (bf16[192,2048]{1,0:T(8,128)(2,1)}, bf16[192,2048]{1,0:T(8,128)(2,1)}) custom-call(bf16[384,512]{1,0:T(8,128)(2,1)} %get-tuple-element.15.grad_ref, bf16[4,3,128,512]{3,2,1,0:T(8,128)(2,1)} %copy-done, bf16[1280,512]{1,0:T(8,128)(2,1)} %get-tuple-element.16.up_ref), custom_call_target="tpu_custom_call" | custom-call | flops 805306368 | bytes 3276800 | tf_op jit(solution)/shard_map/pallas_call | solution.py:155
  81.7 1.9 %collective-permute-start.14 = (bf16[192,2048]{1,0:T(8,128)(2,1)}, bf16[192,2048]{1,0:T(8,128)(2,1)S(1)}, u32[]{:S(2)}, u32[]{:S(2)}) collective-permute-start(bf16[192,2048]{1,0:T(8,128)(2,1)} %get-tuple-element.18), channel_id=1, source_target_pairs={{0,1},{1,0},{2,3},{3,2},{4,5},{5,4},{6,7},{7,6},{8,9},{9,8},{10,11... | collective-permute-start | bytes 2359304 | tf_op jit(solution)/shard_map/ppermute | solution.py:40
  83.6 2.5 %collective-permute-done.14 = bf16[192,2048]{1,0:T(8,128)(2,1)S(1)} collective-permute-done((bf16[192,2048]{1,0:T(8,128)(2,1)}, bf16[192,2048]{1,0:T(8,128)(2,1)S(1)}, u32[]{:S(2)}, u32[]{:S(2)}) %collective-permute-start.14) | collective-permute-done | bytes 786464 | tf_op jit(solution)/shard_map/ppermute | solution.py:40
  86.1 1.4 add_convert_fusion.2
  87.5 0.0 copy-start.1
  87.5 3.1 %collective-permute-start.15 = (bf16[192,2048]{1,0:T(8,128)(2,1)S(1)}, bf16[192,2048]{1,0:T(8,128)(2,1)}, u32[]{:S(2)}, u32[]{:S(2)}) collective-permute-start(bf16[192,2048]{1,0:T(8,128)(2,1)S(1)} %add_convert_fusion.2), channel_id=1, source_target_pairs={{0,2},{2,0},{4,6},{6,4},{1,3},{3,1},{5,7},{7,5},{8,10},{10,8},{12,... | collective-permute-start | bytes 2359304 | tf_op jit(solution)/shard_map/ppermute | solution.py:40
  90.6 0.0 copy-done.1
  90.6 3.6 %all-to-all-start.1 = ((bf16[4,4,2,64,512]{4,3,2,1,0:T(8,128)(2,1)}), bf16[4,4,2,64,512]{4,3,2,1,0:T(8,128)(2,1)S(1)}, u32[]{:S(2)}, u32[]{:S(2)}) async-start(bf16[4,4,2,64,512]{4,3,2,1,0:T(8,128)(2,1)} %get-tuple-element.19), calls=%async_computation.1 | async-start | bytes 4194304 | tf_op jit(solution)/shard_map/all_to_all | solution.py:24
  94.2 14.8 %collective-permute-done.15 = bf16[192,2048]{1,0:T(8,128)(2,1)} collective-permute-done((bf16[192,2048]{1,0:T(8,128)(2,1)S(1)}, bf16[192,2048]{1,0:T(8,128)(2,1)}, u32[]{:S(2)}, u32[]{:S(2)}) %collective-permute-start.15) | collective-permute-done | bytes 786464 | tf_op jit(solution)/shard_map/ppermute | solution.py:40
  109.1 1.6 add_convert_fusion.1
  110.7 2.4 %collective-permute-start.16 = (bf16[192,2048]{1,0:T(8,128)(2,1)S(1)}, bf16[192,2048]{1,0:T(8,128)(2,1)}, u32[]{:S(2)}, u32[]{:S(2)}) collective-permute-start(bf16[192,2048]{1,0:T(8,128)(2,1)S(1)} %add_convert_fusion.1), channel_id=1, source_target_pairs={{0,6},{2,4},{4,2},{6,0},{1,7},{3,5},{5,3},{7,1},{8,14},{10,12},{12... | collective-permute-start | bytes 2359304 | tf_op jit(solution)/shard_map/ppermute | solution.py:40
  113.1 7.7 %all-to-all-done.1 = bf16[4,4,2,64,512]{4,3,2,1,0:T(8,128)(2,1)S(1)} async-done(((bf16[4,4,2,64,512]{4,3,2,1,0:T(8,128)(2,1)}), bf16[4,4,2,64,512]{4,3,2,1,0:T(8,128)(2,1)S(1)}, u32[]{:S(2)}, u32[]{:S(2)}) %all-to-all-start.1) | async-done | bytes 2097184 | tf_op jit(solution)/shard_map/all_to_all | solution.py:24
  120.8 1.3 reduce_sum.33
  122.1 3.5 %all-to-all-start.2 = ((bf16[4,2,64,512]{3,2,1,0:T(8,128)(2,1)}), bf16[4,2,64,512]{3,2,1,0:T(8,128)(2,1)S(1)}, u32[]{:S(2)}, u32[]{:S(2)}) async-start(bf16[4,2,64,512]{3,2,1,0:T(8,128)(2,1)} %reduce_sum.33), calls=%async_computation.2 | async-start | bytes 1048576 | tf_op jit(solution)/shard_map/all_to_all | solution.py:24
  125.6 5.9 %collective-permute-done.16 = bf16[192,2048]{1,0:T(8,128)(2,1)} collective-permute-done((bf16[192,2048]{1,0:T(8,128)(2,1)S(1)}, bf16[192,2048]{1,0:T(8,128)(2,1)}, u32[]{:S(2)}, u32[]{:S(2)}) %collective-permute-start.16) | collective-permute-done | bytes 786464 | tf_op jit(solution)/shard_map/ppermute | solution.py:40
  131.4 1.4 add_convert_fusion
  132.8 1.9 %collective-permute-start.17 = (bf16[192,2048]{1,0:T(8,128)(2,1)S(1)}, bf16[192,2048]{1,0:T(8,128)(2,1)S(1)}, u32[]{:S(2)}, u32[]{:S(2)}) collective-permute-start(bf16[192,2048]{1,0:T(8,128)(2,1)S(1)} %add_convert_fusion), channel_id=1, source_target_pairs={{0,1},{1,0},{2,3},{3,2},{4,5},{5,4},{6,7},{7,6},{8,9},{9,8},{10,11... | collective-permute-start | bytes 2359304 | tf_op jit(solution)/shard_map/ppermute | solution.py:40
  134.8 4.7 %all-to-all-done.2 = bf16[4,2,64,512]{3,2,1,0:T(8,128)(2,1)S(1)} async-done(((bf16[4,2,64,512]{3,2,1,0:T(8,128)(2,1)}), bf16[4,2,64,512]{3,2,1,0:T(8,128)(2,1)S(1)}, u32[]{:S(2)}, u32[]{:S(2)}) %all-to-all-start.2) | async-done | bytes 524320 | tf_op jit(solution)/shard_map/all_to_all | solution.py:24
  139.5 0.1 reduce_sum.34
  139.5 0.7 broadcast_in_dim.7
  140.3 8.3 %all-to-all-start.3 = ((bf16[4,64,512]{2,1,0:T(8,128)(2,1)}), bf16[4,64,512]{2,1,0:T(8,128)(2,1)S(1)}, u32[]{:S(2)}, u32[]{:S(2)}) async-start(bf16[4,64,512]{2,1,0:T(8,128)(2,1)} %bitcast.4), calls=%async_computation.3 | async-start | bytes 524288 | tf_op jit(solution)/shard_map/all_to_all | solution.py:24
  148.6 0.0 collective-permute-done.17
  148.6 0.1 broadcast_select_fusion.1
  148.7 1.2 pad_maximum_fusion
  149.9 17.1 %all-to-all-done.3 = bf16[4,64,512]{2,1,0:T(8,128)(2,1)S(1)} async-done(((bf16[4,64,512]{2,1,0:T(8,128)(2,1)}), bf16[4,64,512]{2,1,0:T(8,128)(2,1)S(1)}, u32[]{:S(2)}, u32[]{:S(2)}) %all-to-all-start.3) | async-done | bytes 262176 | tf_op jit(solution)/shard_map/all_to_all | solution.py:24
  167.1 0.7 convert_reduce_fusion
  (9 shorter events, 0.1 us)
Async XLA Ops:
  1.5 14.1 %collective-permute-start.1 = (bf16[128,512]{1,0:T(8,128)(2,1)S(1)}, bf16[128,512]{1,0:T(8,128)(2,1)S(1)}, u32[]{:S(2)}, u32[]{:S(2)}) collective-permute-start(bf16[128,512]{1,0:T(8,128)(2,1)S(1)} %get-tuple-element.23), channel_id=1, source_target_pairs={{0,480},{32,0},{64,32},{96,64},{128,96},{160,128},{192,160},{224,1... | collective-permute-start | bytes 393224 | tf_op jit(solution)/shard_map/ppermute | solution.py:35
  12.9 8.3 %collective-permute-start = (bf16[128,512]{1,0:T(8,128)(2,1)S(1)}, bf16[128,512]{1,0:T(8,128)(2,1)S(1)}, u32[]{:S(2)}, u32[]{:S(2)}) collective-permute-start(bf16[128,512]{1,0:T(8,128)(2,1)S(1)} %get-tuple-element.23), channel_id=1, source_target_pairs={{0,32},{32,64},{64,96},{96,128},{128,160},{160,192},{192,224},{224... | collective-permute-start | bytes 393224 | tf_op jit(solution)/shard_map/ppermute | solution.py:35
  15.7 13.3 %collective-permute-start.8 = (bf16[128,512]{1,0:T(8,128)(2,1)S(1)}, bf16[128,512]{1,0:T(8,128)(2,1)S(1)}, u32[]{:S(2)}, u32[]{:S(2)}) collective-permute-start(bf16[128,512]{1,0:T(8,128)(2,1)S(1)} %collective-permute-done.1), channel_id=1, source_target_pairs={{0,480},{32,0},{64,32},{96,64},{128,96},{160,128},{192,160},{224,1... | collective-permute-start | bytes 393224 | tf_op jit(solution)/shard_map/ppermute | solution.py:35
  21.3 12.9 %collective-permute-start.2 = (bf16[128,512]{1,0:T(8,128)(2,1)S(1)}, bf16[128,512]{1,0:T(8,128)(2,1)S(1)}, u32[]{:S(2)}, u32[]{:S(2)}) collective-permute-start(bf16[128,512]{1,0:T(8,128)(2,1)S(1)} %collective-permute-done), channel_id=1, source_target_pairs={{0,32},{32,64},{64,96},{96,128},{128,160},{160,192},{192,224},{224... | collective-permute-start | bytes 393224 | tf_op jit(solution)/shard_map/ppermute | solution.py:35
  24.5 41.9 %all-to-all-start = ((bf16[4,3,128,512]{3,2,1,0:T(8,128)(2,1)}), bf16[4,3,128,512]{3,2,1,0:T(8,128)(2,1)S(1)}, u32[]{:S(2)}, u32[]{:S(2)}) async-start(bf16[4,3,128,512]{3,2,1,0:T(8,128)(2,1)} %broadcast_in_dim.6), calls=%async_computation | async-start | bytes 3145728 | tf_op jit(solution)/shard_map/all_to_all | solution.py:24
  29.0 7.6 %collective-permute-start.9 = (bf16[128,512]{1,0:T(8,128)(2,1)S(1)}, bf16[128,512]{1,0:T(8,128)(2,1)S(1)}, u32[]{:S(2)}, u32[]{:S(2)}) collective-permute-start(bf16[128,512]{1,0:T(8,128)(2,1)S(1)} %collective-permute-done.8), channel_id=1, source_target_pairs={{0,480},{32,0},{64,32},{96,64},{128,96},{160,128},{192,160},{224,1... | collective-permute-start | bytes 393224 | tf_op jit(solution)/shard_map/ppermute | solution.py:35
  34.1 8.1 %collective-permute-start.3 = (bf16[128,512]{1,0:T(8,128)(2,1)S(1)}, bf16[128,512]{1,0:T(8,128)(2,1)S(1)}, u32[]{:S(2)}, u32[]{:S(2)}) collective-permute-start(bf16[128,512]{1,0:T(8,128)(2,1)S(1)} %collective-permute-done.2), channel_id=1, source_target_pairs={{0,32},{32,64},{64,96},{96,128},{128,160},{160,192},{192,224},{224... | collective-permute-start | bytes 393224 | tf_op jit(solution)/shard_map/ppermute | solution.py:35
  36.6 7.6 %collective-permute-start.10 = (bf16[64,512]{1,0:T(8,128)(2,1)S(1)}, bf16[64,512]{1,0:T(8,128)(2,1)S(1)}, u32[]{:S(2)}, u32[]{:S(2)}) collective-permute-start(bf16[64,512]{1,0:T(8,128)(2,1)S(1)} %slice.9), channel_id=1, source_target_pairs={{0,480},{32,0},{64,32},{96,64},{128,96},{160,128},{192,160},{224,1... | collective-permute-start | bytes 196616 | tf_op jit(solution)/shard_map/ppermute | solution.py:35
  42.2 7.4 %collective-permute-start.4 = (bf16[64,512]{1,0:T(8,128)(2,1)S(1)}, bf16[64,512]{1,0:T(8,128)(2,1)S(1)}, u32[]{:S(2)}, u32[]{:S(2)}) collective-permute-start(bf16[64,512]{1,0:T(8,128)(2,1)S(1)} %slice.8), channel_id=1, source_target_pairs={{0,32},{32,64},{64,96},{96,128},{128,160},{160,192},{192,224},{224... | collective-permute-start | bytes 196616 | tf_op jit(solution)/shard_map/ppermute | solution.py:35
  44.2 16.4 %collective-permute-start.12 = (bf16[320,512]{1,0:T(8,128)(2,1)S(1)}, bf16[320,512]{1,0:T(8,128)(2,1)S(1)}, u32[]{:S(2)}, u32[]{:S(2)}) collective-permute-start(bf16[320,512]{1,0:T(8,128)(2,1)S(1)} %constant_dynamic-update-slice_fusion.3.refs_4_), channel_id=1, source_target_pairs={{0,24},{8,0},{16,8},{24,16},{1,25},{9,1},{17,9},{25,17},{2,26},{10... | collective-permute-start | bytes 983048 | tf_op jit(solution)/shard_map/ppermute | solution.py:35
  49.6 12.9 %collective-permute-start.5 = (bf16[320,512]{1,0:T(8,128)(2,1)S(1)}, bf16[320,512]{1,0:T(8,128)(2,1)S(1)}, u32[]{:S(2)}, u32[]{:S(2)}) collective-permute-start(bf16[320,512]{1,0:T(8,128)(2,1)S(1)} %constant_dynamic-update-slice_fusion.refs_0_), channel_id=1, source_target_pairs={{0,8},{8,16},{16,24},{24,0},{1,9},{9,17},{17,25},{25,1},{2,10},{10... | collective-permute-start | bytes 983048 | tf_op jit(solution)/shard_map/ppermute | solution.py:35
  53.5 15.7 %collective-permute-start.11 = (bf16[320,512]{1,0:T(8,128)(2,1)S(1)}, bf16[320,512]{1,0:T(8,128)(2,1)S(1)}, u32[]{:S(2)}, u32[]{:S(2)}) collective-permute-start(bf16[320,512]{1,0:T(8,128)(2,1)S(1)} %constant_dynamic-update-slice_fusion.3.refs_4_), channel_id=1, source_target_pairs={{0,8},{8,16},{16,24},{24,0},{1,9},{9,17},{17,25},{25,1},{2,10},{10... | collective-permute-start | bytes 983048 | tf_op jit(solution)/shard_map/ppermute | solution.py:35
  56.9 12.3 %collective-permute-start.6 = (bf16[320,512]{1,0:T(8,128)(2,1)S(1)}, bf16[320,512]{1,0:T(8,128)(2,1)S(1)}, u32[]{:S(2)}, u32[]{:S(2)}) collective-permute-start(bf16[320,512]{1,0:T(8,128)(2,1)S(1)} %constant_dynamic-update-slice_fusion.refs_0_), channel_id=1, source_target_pairs={{0,24},{8,0},{16,8},{24,16},{1,25},{9,1},{17,9},{25,17},{2,26},{10... | collective-permute-start | bytes 983048 | tf_op jit(solution)/shard_map/ppermute | solution.py:35
  60.6 9.8 %collective-permute-start.13 = (bf16[320,512]{1,0:T(8,128)(2,1)S(1)}, bf16[320,512]{1,0:T(8,128)(2,1)}, u32[]{:S(2)}, u32[]{:S(2)}) collective-permute-start(bf16[320,512]{1,0:T(8,128)(2,1)S(1)} %collective-permute-done.12.refs_6_), channel_id=1, source_target_pairs={{0,24},{8,0},{16,8},{24,16},{1,25},{9,1},{17,9},{25,17},{2,26},{10... | collective-permute-start | bytes 983048 | tf_op jit(solution)/shard_map/ppermute | solution.py:35
  62.6 10.3 %collective-permute-start.7 = (bf16[320,512]{1,0:T(8,128)(2,1)S(1)}, bf16[320,512]{1,0:T(8,128)(2,1)}, u32[]{:S(2)}, u32[]{:S(2)}) collective-permute-start(bf16[320,512]{1,0:T(8,128)(2,1)S(1)} %collective-permute-done.5.refs_1_), channel_id=1, source_target_pairs={{0,8},{8,16},{16,24},{24,0},{1,9},{9,17},{17,25},{25,1},{2,10},{10... | collective-permute-start | bytes 983048 | tf_op jit(solution)/shard_map/ppermute | solution.py:35
  66.5 2.7 %copy-start = (bf16[4,3,128,512]{3,2,1,0:T(8,128)(2,1)}, bf16[4,3,128,512]{3,2,1,0:T(8,128)(2,1)S(1)}, u32[]{:S(2)}) copy-start(bf16[4,3,128,512]{3,2,1,0:T(8,128)(2,1)S(1)} %all-to-all-done.near_ref) | copy-start | bytes 4718596
  81.7 4.4 %collective-permute-start.14 = (bf16[192,2048]{1,0:T(8,128)(2,1)}, bf16[192,2048]{1,0:T(8,128)(2,1)S(1)}, u32[]{:S(2)}, u32[]{:S(2)}) collective-permute-start(bf16[192,2048]{1,0:T(8,128)(2,1)} %get-tuple-element.18), channel_id=1, source_target_pairs={{0,1},{1,0},{2,3},{3,2},{4,5},{5,4},{6,7},{7,6},{8,9},{9,8},{10,11... | collective-permute-start | bytes 2359304 | tf_op jit(solution)/shard_map/ppermute | solution.py:40
  87.5 3.1 %copy-start.1 = (bf16[192,2048]{1,0:T(8,128)(2,1)}, bf16[192,2048]{1,0:T(8,128)(2,1)S(1)}, u32[]{:S(2)}) copy-start(bf16[192,2048]{1,0:T(8,128)(2,1)S(1)} %add_convert_fusion.2) | copy-start | bytes 2359300
  87.5 21.6 %collective-permute-start.15 = (bf16[192,2048]{1,0:T(8,128)(2,1)S(1)}, bf16[192,2048]{1,0:T(8,128)(2,1)}, u32[]{:S(2)}, u32[]{:S(2)}) collective-permute-start(bf16[192,2048]{1,0:T(8,128)(2,1)S(1)} %add_convert_fusion.2), channel_id=1, source_target_pairs={{0,2},{2,0},{4,6},{6,4},{1,3},{3,1},{5,7},{7,5},{8,10},{10,8},{12,... | collective-permute-start | bytes 2359304 | tf_op jit(solution)/shard_map/ppermute | solution.py:40
  90.6 30.2 %all-to-all-start.1 = ((bf16[4,4,2,64,512]{4,3,2,1,0:T(8,128)(2,1)}), bf16[4,4,2,64,512]{4,3,2,1,0:T(8,128)(2,1)S(1)}, u32[]{:S(2)}, u32[]{:S(2)}) async-start(bf16[4,4,2,64,512]{4,3,2,1,0:T(8,128)(2,1)} %get-tuple-element.19), calls=%async_computation.1 | async-start | bytes 4194304 | tf_op jit(solution)/shard_map/all_to_all | solution.py:24
  110.7 20.7 %collective-permute-start.16 = (bf16[192,2048]{1,0:T(8,128)(2,1)S(1)}, bf16[192,2048]{1,0:T(8,128)(2,1)}, u32[]{:S(2)}, u32[]{:S(2)}) collective-permute-start(bf16[192,2048]{1,0:T(8,128)(2,1)S(1)} %add_convert_fusion.1), channel_id=1, source_target_pairs={{0,6},{2,4},{4,2},{6,0},{1,7},{3,5},{5,3},{7,1},{8,14},{10,12},{12... | collective-permute-start | bytes 2359304 | tf_op jit(solution)/shard_map/ppermute | solution.py:40
  122.1 17.4 %all-to-all-start.2 = ((bf16[4,2,64,512]{3,2,1,0:T(8,128)(2,1)}), bf16[4,2,64,512]{3,2,1,0:T(8,128)(2,1)S(1)}, u32[]{:S(2)}, u32[]{:S(2)}) async-start(bf16[4,2,64,512]{3,2,1,0:T(8,128)(2,1)} %reduce_sum.33), calls=%async_computation.2 | async-start | bytes 1048576 | tf_op jit(solution)/shard_map/all_to_all | solution.py:24
  132.8 15.7 %collective-permute-start.17 = (bf16[192,2048]{1,0:T(8,128)(2,1)S(1)}, bf16[192,2048]{1,0:T(8,128)(2,1)S(1)}, u32[]{:S(2)}, u32[]{:S(2)}) collective-permute-start(bf16[192,2048]{1,0:T(8,128)(2,1)S(1)} %add_convert_fusion), channel_id=1, source_target_pairs={{0,1},{1,0},{2,3},{3,2},{4,5},{5,4},{6,7},{7,6},{8,9},{9,8},{10,11... | collective-permute-start | bytes 2359304 | tf_op jit(solution)/shard_map/ppermute | solution.py:40
  140.3 26.8 %all-to-all-start.3 = ((bf16[4,64,512]{2,1,0:T(8,128)(2,1)}), bf16[4,64,512]{2,1,0:T(8,128)(2,1)S(1)}, u32[]{:S(2)}, u32[]{:S(2)}) async-start(bf16[4,64,512]{2,1,0:T(8,128)(2,1)} %bitcast.4), calls=%async_computation.3 | async-start | bytes 524288 | tf_op jit(solution)/shard_map/all_to_all | solution.py:24

commit v8 on v7

--- a/solution.py
+++ b/solution.py
@@ -181,11 +181,12 @@
     back = [own]
     ahead = [own]
     for _ in range(3):
+        ahead.append(shifted(ahead[-1], Z, -1))
         back.append(shifted(back[-1], Z, 1))
-        ahead.append(shifted(ahead[-1], Z, -1))
-    plus_last = shifted(back[3][:rows], Z, 1)
-    minus_last = shifted(ahead[3][rows:], Z, -1)
-    near = copies_over(jnp.stack([own, back[1], ahead[1]]), "y")
+    last = shifted(back[3], Z, 1)
+    plus_last, minus_last = last[:rows], last[rows:]
+    near = jnp.stack([own, back[1], ahead[1]])
+    near = copies_over(near, "y")
     plus = [jnp.concatenate([back[2], back[3], plus_last], axis=0)]
     minus = [jnp.concatenate([ahead[2], ahead[3], minus_last], axis=0)]
     plus.append(shifted(plus[0], "y", 1))

time: 169 us -> 178 us (1.053)
  waiting for transfers between devices: 57.9 us -> 76.1 us
  starting transfers between devices: 86.5 us -> 77.6 us
    ppermute x14 -> x13, waiting for transfers between devices: 5.2 us -> 24 us  [shifted(): return lax.ppermute(value, axes, [(i, (i + step) % n) for i in range(n)])]
    ppermute x14 -> x13, starting transfers between devices: 57.3 us -> 45.4 us  [shifted(): return lax.ppermute(value, axes, [(i, (i + step) % n) for i in range(n)])]
    all_to_all x4, starting transfers between devices: 19.8 us -> 22.9 us  [exchange(): return lax.all_to_all(parts, axes, split_axis=0, concat_axis=0, tiled=True)]
    ppermute x4, waiting for transfers between devices: 23.2 us -> 20.5 us  [swapped(): return lax.ppermute(value, axes, [(i, partner(i)) for i in range(n)])]
    all_to_all x4, waiting for transfers between devices: 29.5 us -> 31.6 us  [exchange(): return lax.all_to_all(parts, axes, split_axis=0, concat_axis=0, tiled=True)]
  transfers between devices with their start and end apart: 22 -> 21, of which waited for: 11 -> 12; matrix products, arithmetic and copies ran while one was open for 5% -> 4% of each run, Pallas kernels for 2% -> 2%
where the time goes in v8:
time: 178 us; the launch traced here: 177 us
  starting transfers between devices  77.6 us (44%)
  waiting for transfers between devices  76.1 us (43%)
  Pallas kernels  11.5 us (6%)
  other arithmetic  8.79 us (5%)
  local copies, waits for them, and re-layouts  2.04 us (1%)
    ppermute x13, starting transfers between devices, shifted(): return lax.ppermute(value, axes, [(i, (i + step) % n) for i in range(n)])  45.4 us
    all_to_all x4, waiting for transfers between devices, exchange(): return lax.all_to_all(parts, axes, split_axis=0, concat_axis=0, tiled=True)  31.6 us
    ppermute x13, waiting for transfers between devices, shifted(): return lax.ppermute(value, axes, [(i, (i + step) % n) for i in range(n)])  24 us
    all_to_all x4, starting transfers between devices, exchange(): return lax.all_to_all(parts, axes, split_axis=0, concat_axis=0, tiled=True)  22.9 us
    ppermute x4, waiting for transfers between devices, swapped(): return lax.ppermute(value, axes, [(i, partner(i)) for i in range(n)])  20.5 us
    pallas_call x3, Pallas kernels, call(): pl.pallas_call(kernel, out_shape=tuple((pltpu.HBM(s, t) if k in out_hbm e...  11.5 us
    ppermute x4, starting transfers between devices, swapped(): return lax.ppermute(value, axes, [(i, partner(i)) for i in range(n)])  9.39 us
    convert_element_type x3, other arithmetic, total(): return (a.astype(F32) + b.astype(F32)).astype(BF)  4.42 us
  transfers between devices with their start and end apart: 21, of which 12 were waited for; matrix products, arithmetic and copies ran while one was open for 4% of the time, Pallas kernels for 2%

profile of v8, /device:TPU:4, one launch (start us, length us, event | category | flops | bytes accessed | tf_op | source)
XLA Modules:
  0.0 177.0 jit_solution(2894089135681351591)
XLA Ops:
  0.6 0.9 fusion
  1.5 3.8 %collective-permute-start = (bf16[128,512]{1,0:T(8,128)(2,1)S(1)}, bf16[128,512]{1,0:T(8,128)(2,1)S(1)}, u32[]{:S(2)}, u32[]{:S(2)}) collective-permute-start(bf16[128,512]{1,0:T(8,128)(2,1)S(1)} %get-tuple-element.25), channel_id=1, source_target_pairs={{0,32},{32,64},{64,96},{96,128},{128,160},{160,192},{192,224},{224... | collective-permute-start | bytes 393224 | tf_op jit(solution)/shard_map/ppermute | solution.py:35
  5.4 11.1 %collective-permute-done = bf16[128,512]{1,0:T(8,128)(2,1)S(1)} collective-permute-done((bf16[128,512]{1,0:T(8,128)(2,1)S(1)}, bf16[128,512]{1,0:T(8,128)(2,1)S(1)}, u32[]{:S(2)}, u32[]{:S(2)}) %collective-permute-start) | collective-permute-done | bytes 131104 | tf_op jit(solution)/shard_map/ppermute | solution.py:35
  16.4 1.9 %collective-permute-start.2 = (bf16[128,512]{1,0:T(8,128)(2,1)S(1)}, bf16[128,512]{1,0:T(8,128)(2,1)S(1)}, u32[]{:S(2)}, u32[]{:S(2)}) collective-permute-start(bf16[128,512]{1,0:T(8,128)(2,1)S(1)} %collective-permute-done), channel_id=1, source_target_pairs={{0,32},{32,64},{64,96},{96,128},{128,160},{160,192},{192,224},{224... | collective-permute-start | bytes 393224 | tf_op jit(solution)/shard_map/ppermute | solution.py:35
  18.3 5.1 %collective-permute-start.1 = (bf16[128,512]{1,0:T(8,128)(2,1)S(1)}, bf16[128,512]{1,0:T(8,128)(2,1)S(1)}, u32[]{:S(2)}, u32[]{:S(2)}) collective-permute-start(bf16[128,512]{1,0:T(8,128)(2,1)S(1)} %get-tuple-element.25), channel_id=1, source_target_pairs={{0,480},{32,0},{64,32},{96,64},{128,96},{160,128},{192,160},{224,1... | collective-permute-start | bytes 393224 | tf_op jit(solution)/shard_map/ppermute | solution.py:35
  23.5 1.0 collective-permute-done.2
  24.5 1.9 %collective-permute-start.3 = (bf16[128,512]{1,0:T(8,128)(2,1)S(1)}, bf16[128,512]{1,0:T(8,128)(2,1)S(1)}, u32[]{:S(2)}, u32[]{:S(2)}) collective-permute-start(bf16[128,512]{1,0:T(8,128)(2,1)S(1)} %collective-permute-done.2), channel_id=1, source_target_pairs={{0,32},{32,64},{64,96},{96,128},{128,160},{160,192},{192,224},{224... | collective-permute-start | bytes 393224 | tf_op jit(solution)/shard_map/ppermute | solution.py:35
  26.4 0.0 collective-permute-done.1
  26.4 5.1 %collective-permute-start.8 = (bf16[128,512]{1,0:T(8,128)(2,1)S(1)}, bf16[128,512]{1,0:T(8,128)(2,1)S(1)}, u32[]{:S(2)}, u32[]{:S(2)}) collective-permute-start(bf16[128,512]{1,0:T(8,128)(2,1)S(1)} %collective-permute-done.1), channel_id=1, source_target_pairs={{0,480},{32,0},{64,32},{96,64},{128,96},{160,128},{192,160},{224,1... | collective-permute-start | bytes 393224 | tf_op jit(solution)/shard_map/ppermute | solution.py:35
  31.5 1.0 collective-permute-done.3
  32.5 1.9 %collective-permute-start.4 = (bf16[128,512]{1,0:T(8,128)(2,1)S(1)}, bf16[128,512]{1,0:T(8,128)(2,1)S(1)}, u32[]{:S(2)}, u32[]{:S(2)}) collective-permute-start(bf16[128,512]{1,0:T(8,128)(2,1)S(1)} %collective-permute-done.3), channel_id=1, source_target_pairs={{0,32},{32,64},{64,96},{96,128},{128,160},{160,192},{192,224},{224... | collective-permute-start | bytes 393224 | tf_op jit(solution)/shard_map/ppermute | solution.py:35
  34.5 1.3 broadcast_in_dim.6
  35.8 4.5 %all-to-all-start = ((bf16[4,3,128,512]{3,2,1,0:T(8,128)(2,1)}), bf16[4,3,128,512]{3,2,1,0:T(8,128)(2,1)S(1)}, u32[]{:S(2)}, u32[]{:S(2)}) async-start(bf16[4,3,128,512]{3,2,1,0:T(8,128)(2,1)} %broadcast_in_dim.6), calls=%async_computation | async-start | bytes 3145728 | tf_op jit(solution)/shard_map/all_to_all | solution.py:24
  40.3 0.0 collective-permute-done.8
  40.3 5.1 %collective-permute-start.9 = (bf16[128,512]{1,0:T(8,128)(2,1)S(1)}, bf16[128,512]{1,0:T(8,128)(2,1)S(1)}, u32[]{:S(2)}, u32[]{:S(2)}) collective-permute-start(bf16[128,512]{1,0:T(8,128)(2,1)S(1)} %collective-permute-done.8), channel_id=1, source_target_pairs={{0,480},{32,0},{64,32},{96,64},{128,96},{160,128},{192,160},{224,1... | collective-permute-start | bytes 393224 | tf_op jit(solution)/shard_map/ppermute | solution.py:35
  45.4 0.0 collective-permute-done.4
  45.4 3.9 %collective-permute-start.5 = (bf16[320,512]{1,0:T(8,128)(2,1)S(1)}, bf16[320,512]{1,0:T(8,128)(2,1)S(1)}, u32[]{:S(2)}, u32[]{:S(2)}) collective-permute-start(bf16[320,512]{1,0:T(8,128)(2,1)S(1)} %pad_maximum_fusion.2.refs_0_), channel_id=1, source_target_pairs={{0,8},{8,16},{16,24},{24,0},{1,9},{9,17},{17,25},{25,1},{2,10},{10... | collective-permute-start | bytes 983048 | tf_op jit(solution)/shard_map/ppermute | solution.py:35
  49.4 0.0 collective-permute-done.9
  49.4 3.6 %collective-permute-start.11 = (bf16[320,512]{1,0:T(8,128)(2,1)S(1)}, bf16[320,512]{1,0:T(8,128)(2,1)S(1)}, u32[]{:S(2)}, u32[]{:S(2)}) collective-permute-start(bf16[320,512]{1,0:T(8,128)(2,1)S(1)} %pad_maximum_fusion.3.refs_4_), channel_id=1, source_target_pairs={{0,24},{8,0},{16,8},{24,16},{1,25},{9,1},{17,9},{25,17},{2,26},{10... | collective-permute-start | bytes 983048 | tf_op jit(solution)/shard_map/ppermute | solution.py:35
  53.1 3.4 %collective-permute-start.6 = (bf16[320,512]{1,0:T(8,128)(2,1)S(1)}, bf16[320,512]{1,0:T(8,128)(2,1)S(1)}, u32[]{:S(2)}, u32[]{:S(2)}) collective-permute-start(bf16[320,512]{1,0:T(8,128)(2,1)S(1)} %pad_maximum_fusion.2.refs_0_), channel_id=1, source_target_pairs={{0,24},{8,0},{16,8},{24,16},{1,25},{9,1},{17,9},{25,17},{2,26},{10... | collective-permute-start | bytes 983048 | tf_op jit(solution)/shard_map/ppermute | solution.py:35
  56.5 2.4 %collective-permute-start.10 = (bf16[320,512]{1,0:T(8,128)(2,1)S(1)}, bf16[320,512]{1,0:T(8,128)(2,1)S(1)}, u32[]{:S(2)}, u32[]{:S(2)}) collective-permute-start(bf16[320,512]{1,0:T(8,128)(2,1)S(1)} %pad_maximum_fusion.3.refs_4_), channel_id=1, source_target_pairs={{0,8},{8,16},{16,24},{24,0},{1,9},{9,17},{17,25},{25,1},{2,10},{10... | collective-permute-start | bytes 983048 | tf_op jit(solution)/shard_map/ppermute | solution.py:35
  58.9 9.1 %collective-permute-done.5.refs_1_ = bf16[320,512]{1,0:T(8,128)(2,1)S(1)} collective-permute-done((bf16[320,512]{1,0:T(8,128)(2,1)S(1)}, bf16[320,512]{1,0:T(8,128)(2,1)S(1)}, u32[]{:S(2)}, u32[]{:S(2)}) %collective-permute-start.5) | collective-permute-done | bytes 327712 | tf_op jit(solution)/shard_map/ppermute | solution.py:35
  68.0 1.9 %collective-permute-start.7 = (bf16[320,512]{1,0:T(8,128)(2,1)S(1)}, bf16[320,512]{1,0:T(8,128)(2,1)}, u32[]{:S(2)}, u32[]{:S(2)}) collective-permute-start(bf16[320,512]{1,0:T(8,128)(2,1)S(1)} %collective-permute-done.5.refs_1_), channel_id=1, source_target_pairs={{0,8},{8,16},{16,24},{24,0},{1,9},{9,17},{17,25},{25,1},{2,10},{10... | collective-permute-start | bytes 983048 | tf_op jit(solution)/shard_map/ppermute | solution.py:35
  69.9 0.0 collective-permute-done.11.refs_6_
  69.9 5.1 %collective-permute-start.12 = (bf16[320,512]{1,0:T(8,128)(2,1)S(1)}, bf16[320,512]{1,0:T(8,128)(2,1)}, u32[]{:S(2)}, u32[]{:S(2)}) collective-permute-start(bf16[320,512]{1,0:T(8,128)(2,1)S(1)} %collective-permute-done.11.refs_6_), channel_id=1, source_target_pairs={{0,24},{8,0},{16,8},{24,16},{1,25},{9,1},{17,9},{25,17},{2,26},{10... | collective-permute-start | bytes 983048 | tf_op jit(solution)/shard_map/ppermute | solution.py:35
  75.1 0.0 all-to-all-done.near_ref
  75.1 0.0 copy-start
  75.1 2.7 %shard_map.59 = (f32[384,512]{1,0:T(8,128)S(1)}, f32[384,512]{1,0:T(8,128)S(1)}, bf16[384,2048]{1,0:T(8,128)(2,1)S(1)}, bf16[384,2048]{1,0:T(8,128)(2,1)S(1)}) custom-call(bf16[384,2048]{1,0:T(8,128)(2,1)} %x_hbm.1, bf16[384,2048]{1,0:T(8,128)(2,1)} %c_hbm.1, bf16[4,3,128,512]{3,2,1,0:T(8,128)(2,1)S(1)} %all-to-all-done.near_ref), custom_call_target="tpu_custom_call" | custom-call | flops 603979776 | bytes 4718592 | tf_op jit(solution)/shard_map/pallas_call | solution.py:155
  77.8 0.0 copy-done
  77.8 0.0 collective-permute-done.6.refs_2_
  77.8 0.0 collective-permute-done.10.refs_5_
  77.8 1.2 collective-permute-done.7.refs_3_
  79.0 0.6 collective-permute-done.12.refs_7_
  79.7 4.4 %shard_map.60 = (bf16[384,512]{1,0:T(8,128)(2,1)}, bf16[4,4,2,64,512]{4,3,2,1,0:T(8,128)(2,1)}, bf16[1280,512]{1,0:T(8,128)(2,1)}) custom-call(bf16[384,2048]{1,0:T(8,128)(2,1)S(1)} %get-tuple-element.11.x_ref, bf16[384,2048]{1,0:T(8,128)(2,1)S(1)} %get-tuple-element.12.c_ref, f32[384,512]{1,0:T(8,128)S(1)} %get-tuple-element.13.pre_ref, ...), custom_call_target="tpu_custom_call" | custom-call | flops 1811939328 | bytes 6553600 | tf_op jit(solution)/shard_map/pallas_call | solution.py:155
  84.1 4.4 %shard_map.61 = (bf16[192,2048]{1,0:T(8,128)(2,1)}, bf16[192,2048]{1,0:T(8,128)(2,1)}) custom-call(bf16[384,512]{1,0:T(8,128)(2,1)} %get-tuple-element.15.grad_ref, bf16[4,3,128,512]{3,2,1,0:T(8,128)(2,1)} %copy-done, bf16[1280,512]{1,0:T(8,128)(2,1)} %get-tuple-element.16.up_ref), custom_call_target="tpu_custom_call" | custom-call | flops 805306368 | bytes 3276800 | tf_op jit(solution)/shard_map/pallas_call | solution.py:155
  88.5 1.9 %collective-permute-start.13 = (bf16[192,2048]{1,0:T(8,128)(2,1)}, bf16[192,2048]{1,0:T(8,128)(2,1)S(1)}, u32[]{:S(2)}, u32[]{:S(2)}) collective-permute-start(bf16[192,2048]{1,0:T(8,128)(2,1)} %get-tuple-element.18), channel_id=1, source_target_pairs={{0,1},{1,0},{2,3},{3,2},{4,5},{5,4},{6,7},{7,6},{8,9},{9,8},{10,11... | collective-permute-start | bytes 2359304 | tf_op jit(solution)/shard_map/ppermute | solution.py:40
  90.4 2.5 %collective-permute-done.13 = bf16[192,2048]{1,0:T(8,128)(2,1)S(1)} collective-permute-done((bf16[192,2048]{1,0:T(8,128)(2,1)}, bf16[192,2048]{1,0:T(8,128)(2,1)S(1)}, u32[]{:S(2)}, u32[]{:S(2)}) %collective-permute-start.13) | collective-permute-done | bytes 786464 | tf_op jit(solution)/shard_map/ppermute | solution.py:40
  92.9 1.4 add_convert_fusion.2
  94.3 0.0 copy-start.1
  94.3 3.1 %collective-permute-start.14 = (bf16[192,2048]{1,0:T(8,128)(2,1)S(1)}, bf16[192,2048]{1,0:T(8,128)(2,1)}, u32[]{:S(2)}, u32[]{:S(2)}) collective-permute-start(bf16[192,2048]{1,0:T(8,128)(2,1)S(1)} %add_convert_fusion.2), channel_id=1, source_target_pairs={{0,2},{2,0},{4,6},{6,4},{1,3},{3,1},{5,7},{7,5},{8,10},{10,8},{12,... | collective-permute-start | bytes 2359304 | tf_op jit(solution)/shard_map/ppermute | solution.py:40
  97.4 0.0 copy-done.1
  97.4 5.1 %all-to-all-start.1 = ((bf16[4,4,2,64,512]{4,3,2,1,0:T(8,128)(2,1)}), bf16[4,4,2,64,512]{4,3,2,1,0:T(8,128)(2,1)S(1)}, u32[]{:S(2)}, u32[]{:S(2)}) async-start(bf16[4,4,2,64,512]{4,3,2,1,0:T(8,128)(2,1)} %get-tuple-element.19), calls=%async_computation.1 | async-start | bytes 4194304 | tf_op jit(solution)/shard_map/all_to_all | solution.py:24
  102.5 13.4 %collective-permute-done.14 = bf16[192,2048]{1,0:T(8,128)(2,1)} collective-permute-done((bf16[192,2048]{1,0:T(8,128)(2,1)S(1)}, bf16[192,2048]{1,0:T(8,128)(2,1)}, u32[]{:S(2)}, u32[]{:S(2)}) %collective-permute-start.14) | collective-permute-done | bytes 786464 | tf_op jit(solution)/shard_map/ppermute | solution.py:40
  115.9 1.6 add_convert_fusion.1
  117.5 2.4 %collective-permute-start.15 = (bf16[192,2048]{1,0:T(8,128)(2,1)S(1)}, bf16[192,2048]{1,0:T(8,128)(2,1)}, u32[]{:S(2)}, u32[]{:S(2)}) collective-permute-start(bf16[192,2048]{1,0:T(8,128)(2,1)S(1)} %add_convert_fusion.1), channel_id=1, source_target_pairs={{0,6},{2,4},{4,2},{6,0},{1,7},{3,5},{5,3},{7,1},{8,14},{10,12},{12... | collective-permute-start | bytes 2359304 | tf_op jit(solution)/shard_map/ppermute | solution.py:40
  120.0 8.9 %all-to-all-done.1 = bf16[4,4,2,64,512]{4,3,2,1,0:T(8,128)(2,1)S(1)} async-done(((bf16[4,4,2,64,512]{4,3,2,1,0:T(8,128)(2,1)}), bf16[4,4,2,64,512]{4,3,2,1,0:T(8,128)(2,1)S(1)}, u32[]{:S(2)}, u32[]{:S(2)}) %all-to-all-start.1) | async-done | bytes 2097184 | tf_op jit(solution)/shard_map/all_to_all | solution.py:24
  128.8 1.3 reduce_sum.33
  130.1 3.5 %all-to-all-start.2 = ((bf16[4,2,64,512]{3,2,1,0:T(8,128)(2,1)}), bf16[4,2,64,512]{3,2,1,0:T(8,128)(2,1)S(1)}, u32[]{:S(2)}, u32[]{:S(2)}) async-start(bf16[4,2,64,512]{3,2,1,0:T(8,128)(2,1)} %reduce_sum.33), calls=%async_computation.2 | async-start | bytes 1048576 | tf_op jit(solution)/shard_map/all_to_all | solution.py:24
  133.6 4.7 %collective-permute-done.15 = bf16[192,2048]{1,0:T(8,128)(2,1)} collective-permute-done((bf16[192,2048]{1,0:T(8,128)(2,1)S(1)}, bf16[192,2048]{1,0:T(8,128)(2,1)}, u32[]{:S(2)}, u32[]{:S(2)}) %collective-permute-start.15) | collective-permute-done | bytes 786464 | tf_op jit(solution)/shard_map/ppermute | solution.py:40
  138.2 1.4 add_convert_fusion
  139.6 1.9 %collective-permute-start.16 = (bf16[192,2048]{1,0:T(8,128)(2,1)S(1)}, bf16[192,2048]{1,0:T(8,128)(2,1)S(1)}, u32[]{:S(2)}, u32[]{:S(2)}) collective-permute-start(bf16[192,2048]{1,0:T(8,128)(2,1)S(1)} %add_convert_fusion), channel_id=1, source_target_pairs={{0,1},{1,0},{2,3},{3,2},{4,5},{5,4},{6,7},{7,6},{8,9},{9,8},{10,11... | collective-permute-start | bytes 2359304 | tf_op jit(solution)/shard_map/ppermute | solution.py:40
  141.6 5.6 %all-to-all-done.2 = bf16[4,2,64,512]{3,2,1,0:T(8,128)(2,1)S(1)} async-done(((bf16[4,2,64,512]{3,2,1,0:T(8,128)(2,1)}), bf16[4,2,64,512]{3,2,1,0:T(8,128)(2,1)S(1)}, u32[]{:S(2)}, u32[]{:S(2)}) %all-to-all-start.2) | async-done | bytes 524320 | tf_op jit(solution)/shard_map/all_to_all | solution.py:24
  147.2 0.1 reduce_sum.34
  147.3 0.7 broadcast_in_dim.7
  148.0 9.8 %all-to-all-start.3 = ((bf16[4,64,512]{2,1,0:T(8,128)(2,1)}), bf16[4,64,512]{2,1,0:T(8,128)(2,1)S(1)}, u32[]{:S(2)}, u32[]{:S(2)}) async-start(bf16[4,64,512]{2,1,0:T(8,128)(2,1)} %bitcast.4), calls=%async_computation.3 | async-start | bytes 524288 | tf_op jit(solution)/shard_map/all_to_all | solution.py:24
  157.9 0.0 collective-permute-done.16
  157.9 0.1 broadcast_select_fusion.1
  158.0 1.2 pad_maximum_fusion
  159.2 17.1 %all-to-all-done.3 = bf16[4,64,512]{2,1,0:T(8,128)(2,1)S(1)} async-done(((bf16[4,64,512]{2,1,0:T(8,128)(2,1)}), bf16[4,64,512]{2,1,0:T(8,128)(2,1)S(1)}, u32[]{:S(2)}, u32[]{:S(2)}) %all-to-all-start.3) | async-done | bytes 262176 | tf_op jit(solution)/shard_map/all_to_all | solution.py:24
  176.4 0.7 convert_reduce_fusion
  (4 shorter events, 0.1 us)
Async XLA Ops:
  1.5 14.9 %collective-permute-start = (bf16[128,512]{1,0:T(8,128)(2,1)S(1)}, bf16[128,512]{1,0:T(8,128)(2,1)S(1)}, u32[]{:S(2)}, u32[]{:S(2)}) collective-permute-start(bf16[128,512]{1,0:T(8,128)(2,1)S(1)} %get-tuple-element.25), channel_id=1, source_target_pairs={{0,32},{32,64},{64,96},{96,128},{128,160},{160,192},{192,224},{224... | collective-permute-start | bytes 393224 | tf_op jit(solution)/shard_map/ppermute | solution.py:35
  16.4 8.1 %collective-permute-start.2 = (bf16[128,512]{1,0:T(8,128)(2,1)S(1)}, bf16[128,512]{1,0:T(8,128)(2,1)S(1)}, u32[]{:S(2)}, u32[]{:S(2)}) collective-permute-start(bf16[128,512]{1,0:T(8,128)(2,1)S(1)} %collective-permute-done), channel_id=1, source_target_pairs={{0,32},{32,64},{64,96},{96,128},{128,160},{160,192},{192,224},{224... | collective-permute-start | bytes 393224 | tf_op jit(solution)/shard_map/ppermute | solution.py:35
  18.3 8.1 %collective-permute-start.1 = (bf16[128,512]{1,0:T(8,128)(2,1)S(1)}, bf16[128,512]{1,0:T(8,128)(2,1)S(1)}, u32[]{:S(2)}, u32[]{:S(2)}) collective-permute-start(bf16[128,512]{1,0:T(8,128)(2,1)S(1)} %get-tuple-element.25), channel_id=1, source_target_pairs={{0,480},{32,0},{64,32},{96,64},{128,96},{160,128},{192,160},{224,1... | collective-permute-start | bytes 393224 | tf_op jit(solution)/shard_map/ppermute | solution.py:35
  24.5 8.1 %collective-permute-start.3 = (bf16[128,512]{1,0:T(8,128)(2,1)S(1)}, bf16[128,512]{1,0:T(8,128)(2,1)S(1)}, u32[]{:S(2)}, u32[]{:S(2)}) collective-permute-start(bf16[128,512]{1,0:T(8,128)(2,1)S(1)} %collective-permute-done.2), channel_id=1, source_target_pairs={{0,32},{32,64},{64,96},{96,128},{128,160},{160,192},{192,224},{224... | collective-permute-start | bytes 393224 | tf_op jit(solution)/shard_map/ppermute | solution.py:35
  26.4 13.9 %collective-permute-start.8 = (bf16[128,512]{1,0:T(8,128)(2,1)S(1)}, bf16[128,512]{1,0:T(8,128)(2,1)S(1)}, u32[]{:S(2)}, u32[]{:S(2)}) collective-permute-start(bf16[128,512]{1,0:T(8,128)(2,1)S(1)} %collective-permute-done.1), channel_id=1, source_target_pairs={{0,480},{32,0},{64,32},{96,64},{128,96},{160,128},{192,160},{224,1... | collective-permute-start | bytes 393224 | tf_op jit(solution)/shard_map/ppermute | solution.py:35
  32.5 12.9 %collective-permute-start.4 = (bf16[128,512]{1,0:T(8,128)(2,1)S(1)}, bf16[128,512]{1,0:T(8,128)(2,1)S(1)}, u32[]{:S(2)}, u32[]{:S(2)}) collective-permute-start(bf16[128,512]{1,0:T(8,128)(2,1)S(1)} %collective-permute-done.3), channel_id=1, source_target_pairs={{0,32},{32,64},{64,96},{96,128},{128,160},{160,192},{192,224},{224... | collective-permute-start | bytes 393224 | tf_op jit(solution)/shard_map/ppermute | solution.py:35
  35.8 39.3 %all-to-all-start = ((bf16[4,3,128,512]{3,2,1,0:T(8,128)(2,1)}), bf16[4,3,128,512]{3,2,1,0:T(8,128)(2,1)S(1)}, u32[]{:S(2)}, u32[]{:S(2)}) async-start(bf16[4,3,128,512]{3,2,1,0:T(8,128)(2,1)} %broadcast_in_dim.6), calls=%async_computation | async-start | bytes 3145728 | tf_op jit(solution)/shard_map/all_to_all | solution.py:24
  40.3 9.1 %collective-permute-start.9 = (bf16[128,512]{1,0:T(8,128)(2,1)S(1)}, bf16[128,512]{1,0:T(8,128)(2,1)S(1)}, u32[]{:S(2)}, u32[]{:S(2)}) collective-permute-start(bf16[128,512]{1,0:T(8,128)(2,1)S(1)} %collective-permute-done.8), channel_id=1, source_target_pairs={{0,480},{32,0},{64,32},{96,64},{128,96},{160,128},{192,160},{224,1... | collective-permute-start | bytes 393224 | tf_op jit(solution)/shard_map/ppermute | solution.py:35
  45.4 22.6 %collective-permute-start.5 = (bf16[320,512]{1,0:T(8,128)(2,1)S(1)}, bf16[320,512]{1,0:T(8,128)(2,1)S(1)}, u32[]{:S(2)}, u32[]{:S(2)}) collective-permute-start(bf16[320,512]{1,0:T(8,128)(2,1)S(1)} %pad_maximum_fusion.2.refs_0_), channel_id=1, source_target_pairs={{0,8},{8,16},{16,24},{24,0},{1,9},{9,17},{17,25},{25,1},{2,10},{10... | collective-permute-start | bytes 983048 | tf_op jit(solution)/shard_map/ppermute | solution.py:35
  49.4 20.5 %collective-permute-start.11 = (bf16[320,512]{1,0:T(8,128)(2,1)S(1)}, bf16[320,512]{1,0:T(8,128)(2,1)S(1)}, u32[]{:S(2)}, u32[]{:S(2)}) collective-permute-start(bf16[320,512]{1,0:T(8,128)(2,1)S(1)} %pad_maximum_fusion.3.refs_4_), channel_id=1, source_target_pairs={{0,24},{8,0},{16,8},{24,16},{1,25},{9,1},{17,9},{25,17},{2,26},{10... | collective-permute-start | bytes 983048 | tf_op jit(solution)/shard_map/ppermute | solution.py:35
  53.1 24.7 %collective-permute-start.6 = (bf16[320,512]{1,0:T(8,128)(2,1)S(1)}, bf16[320,512]{1,0:T(8,128)(2,1)S(1)}, u32[]{:S(2)}, u32[]{:S(2)}) collective-permute-start(bf16[320,512]{1,0:T(8,128)(2,1)S(1)} %pad_maximum_fusion.2.refs_0_), channel_id=1, source_target_pairs={{0,24},{8,0},{16,8},{24,16},{1,25},{9,1},{17,9},{25,17},{2,26},{10... | collective-permute-start | bytes 983048 | tf_op jit(solution)/shard_map/ppermute | solution.py:35
  56.5 21.3 %collective-permute-start.10 = (bf16[320,512]{1,0:T(8,128)(2,1)S(1)}, bf16[320,512]{1,0:T(8,128)(2,1)S(1)}, u32[]{:S(2)}, u32[]{:S(2)}) collective-permute-start(bf16[320,512]{1,0:T(8,128)(2,1)S(1)} %pad_maximum_fusion.3.refs_4_), channel_id=1, source_target_pairs={{0,8},{8,16},{16,24},{24,0},{1,9},{9,17},{17,25},{25,1},{2,10},{10... | collective-permute-start | bytes 983048 | tf_op jit(solution)/shard_map/ppermute | solution.py:35
  68.0 11.0 %collective-permute-start.7 = (bf16[320,512]{1,0:T(8,128)(2,1)S(1)}, bf16[320,512]{1,0:T(8,128)(2,1)}, u32[]{:S(2)}, u32[]{:S(2)}) collective-permute-start(bf16[320,512]{1,0:T(8,128)(2,1)S(1)} %collective-permute-done.5.refs_1_), channel_id=1, source_target_pairs={{0,8},{8,16},{16,24},{24,0},{1,9},{9,17},{17,25},{25,1},{2,10},{10... | collective-permute-start | bytes 983048 | tf_op jit(solution)/shard_map/ppermute | solution.py:35
  69.9 9.7 %collective-permute-start.12 = (bf16[320,512]{1,0:T(8,128)(2,1)S(1)}, bf16[320,512]{1,0:T(8,128)(2,1)}, u32[]{:S(2)}, u32[]{:S(2)}) collective-permute-start(bf16[320,512]{1,0:T(8,128)(2,1)S(1)} %collective-permute-done.11.refs_6_), channel_id=1, source_target_pairs={{0,24},{8,0},{16,8},{24,16},{1,25},{9,1},{17,9},{25,17},{2,26},{10... | collective-permute-start | bytes 983048 | tf_op jit(solution)/shard_map/ppermute | solution.py:35
  75.1 2.7 %copy-start = (bf16[4,3,128,512]{3,2,1,0:T(8,128)(2,1)}, bf16[4,3,128,512]{3,2,1,0:T(8,128)(2,1)S(1)}, u32[]{:S(2)}) copy-start(bf16[4,3,128,512]{3,2,1,0:T(8,128)(2,1)S(1)} %all-to-all-done.near_ref) | copy-start | bytes 4718596
  88.5 4.4 %collective-permute-start.13 = (bf16[192,2048]{1,0:T(8,128)(2,1)}, bf16[192,2048]{1,0:T(8,128)(2,1)S(1)}, u32[]{:S(2)}, u32[]{:S(2)}) collective-permute-start(bf16[192,2048]{1,0:T(8,128)(2,1)} %get-tuple-element.18), channel_id=1, source_target_pairs={{0,1},{1,0},{2,3},{3,2},{4,5},{5,4},{6,7},{7,6},{8,9},{9,8},{10,11... | collective-permute-start | bytes 2359304 | tf_op jit(solution)/shard_map/ppermute | solution.py:40
  94.3 3.1 %copy-start.1 = (bf16[192,2048]{1,0:T(8,128)(2,1)}, bf16[192,2048]{1,0:T(8,128)(2,1)S(1)}, u32[]{:S(2)}) copy-start(bf16[192,2048]{1,0:T(8,128)(2,1)S(1)} %add_convert_fusion.2) | copy-start | bytes 2359300
  94.3 21.6 %collective-permute-start.14 = (bf16[192,2048]{1,0:T(8,128)(2,1)S(1)}, bf16[192,2048]{1,0:T(8,128)(2,1)}, u32[]{:S(2)}, u32[]{:S(2)}) collective-permute-start(bf16[192,2048]{1,0:T(8,128)(2,1)S(1)} %add_convert_fusion.2), channel_id=1, source_target_pairs={{0,2},{2,0},{4,6},{6,4},{1,3},{3,1},{5,7},{7,5},{8,10},{10,8},{12,... | collective-permute-start | bytes 2359304 | tf_op jit(solution)/shard_map/ppermute | solution.py:40
  97.4 31.4 %all-to-all-start.1 = ((bf16[4,4,2,64,512]{4,3,2,1,0:T(8,128)(2,1)}), bf16[4,4,2,64,512]{4,3,2,1,0:T(8,128)(2,1)S(1)}, u32[]{:S(2)}, u32[]{:S(2)}) async-start(bf16[4,4,2,64,512]{4,3,2,1,0:T(8,128)(2,1)} %get-tuple-element.19), calls=%async_computation.1 | async-start | bytes 4194304 | tf_op jit(solution)/shard_map/all_to_all | solution.py:24
  117.5 20.7 %collective-permute-start.15 = (bf16[192,2048]{1,0:T(8,128)(2,1)S(1)}, bf16[192,2048]{1,0:T(8,128)(2,1)}, u32[]{:S(2)}, u32[]{:S(2)}) collective-permute-start(bf16[192,2048]{1,0:T(8,128)(2,1)S(1)} %add_convert_fusion.1), channel_id=1, source_target_pairs={{0,6},{2,4},{4,2},{6,0},{1,7},{3,5},{5,3},{7,1},{8,14},{10,12},{12... | collective-permute-start | bytes 2359304 | tf_op jit(solution)/shard_map/ppermute | solution.py:40
  130.1 17.1 %all-to-all-start.2 = ((bf16[4,2,64,512]{3,2,1,0:T(8,128)(2,1)}), bf16[4,2,64,512]{3,2,1,0:T(8,128)(2,1)S(1)}, u32[]{:S(2)}, u32[]{:S(2)}) async-start(bf16[4,2,64,512]{3,2,1,0:T(8,128)(2,1)} %reduce_sum.33), calls=%async_computation.2 | async-start | bytes 1048576 | tf_op jit(solution)/shard_map/all_to_all | solution.py:24
  139.6 18.2 %collective-permute-start.16 = (bf16[192,2048]{1,0:T(8,128)(2,1)S(1)}, bf16[192,2048]{1,0:T(8,128)(2,1)S(1)}, u32[]{:S(2)}, u32[]{:S(2)}) collective-permute-start(bf16[192,2048]{1,0:T(8,128)(2,1)S(1)} %add_convert_fusion), channel_id=1, source_target_pairs={{0,1},{1,0},{2,3},{3,2},{4,5},{5,4},{6,7},{7,6},{8,9},{9,8},{10,11... | collective-permute-start | bytes 2359304 | tf_op jit(solution)/shard_map/ppermute | solution.py:40
  148.0 28.3 %all-to-all-start.3 = ((bf16[4,64,512]{2,1,0:T(8,128)(2,1)}), bf16[4,64,512]{2,1,0:T(8,128)(2,1)S(1)}, u32[]{:S(2)}, u32[]{:S(2)}) async-start(bf16[4,64,512]{2,1,0:T(8,128)(2,1)} %bitcast.4), calls=%async_computation.3 | async-start | bytes 524288 | tf_op jit(solution)/shard_map/all_to_all | solution.py:24

commit v9 on v8

--- a/solution.py
+++ b/solution.py
@@ -87,15 +87,12 @@
 
 def order_far(plus, minus, dsts):
     me = lax.axis_index("y")
-    rows = plus[0].shape[0] // 5
+    rows = minus[0].shape[0] // 4
     for k, dist in enumerate((0, 1, -1, 2)):
         y = lax.rem(me - dist + 2 * N_Y, N_Y)
         for n in range(len(FAR)):
             for part, dst in enumerate(dsts):
-                if n < 4:
-                    ref, piece = (plus, minus)[n % 2][k], n // 2 * 2 + part
-                else:
-                    ref, piece = (plus, minus)[part][k], 4
+                ref, piece = (plus, minus)[n % 2][k], n // 2 * 2 + part
                 at = pl.multiple_of(n * N_Y * rows + y * rows, rows)
                 dst[pl.ds(at, rows), :] = ref[piece * rows : (piece + 1) * rows, :]
 
@@ -184,18 +181,15 @@
         ahead.append(shifted(ahead[-1], Z, -1))
         back.append(shifted(back[-1], Z, 1))
     last = shifted(back[3], Z, 1)
-    plus_last, minus_last = last[:rows], last[rows:]
     near = jnp.stack([own, back[1], ahead[1]])
     near = copies_over(near, "y")
-    plus = [jnp.concatenate([back[2], back[3], plus_last], axis=0)]
-    minus = [jnp.concatenate([ahead[2], ahead[3], minus_last], axis=0)]
-    plus.append(shifted(plus[0], "y", 1))
-    minus_after = shifted(minus[0], "y", -1)
-    minus.append(shifted(minus[0], "y", 1))
-    plus.append(shifted(plus[0], "y", -1))
-    minus.append(minus_after)
+    minus = [jnp.concatenate([ahead[2], ahead[3]], axis=0)]
+    plus = [jnp.concatenate([back[2], back[3], last], axis=0)]
+    for stack in (minus, plus):
+        stack.append(shifted(stack[0], "y", 1))
+        stack.append(shifted(stack[0], "y", -1))
     plus.append(shifted(plus[1], "y", 1))
-    minus.append(shifted(minus_after, "y", -1))
+    minus.append(shifted(minus[2], "y", -1))
     inputs = pltpu.with_memory_space_constraint(inputs, pltpu.HBM)
     cotangent = pltpu.with_memory_space_constraint(cotangent, pltpu.HBM)
     unit = tokens * width * h // 2

time: 178 us -> 174 us (0.978)
  starting transfers between devices: 77.6 us -> 71.9 us
  waiting for transfers between devices: 76.1 us -> 78.1 us
    ppermute x13, starting transfers between devices: 45.4 us -> 41.7 us  [shifted(): return lax.ppermute(value, axes, [(i, (i + step) % n) for i in range(n)])]
    ppermute x4, waiting for transfers between devices: 20.5 us -> 22.9 us  [swapped(): return lax.ppermute(value, axes, [(i, partner(i)) for i in range(n)])]
    all_to_all x4, waiting for transfers between devices: 31.6 us -> 29.3 us  [exchange(): return lax.all_to_all(parts, axes, split_axis=0, concat_axis=0, tiled=True)]
    all_to_all x4, starting transfers between devices: 22.9 us -> 20.8 us  [exchange(): return lax.all_to_all(parts, axes, split_axis=0, concat_axis=0, tiled=True)]
    ppermute x13, waiting for transfers between devices: 24 us -> 25.9 us  [shifted(): return lax.ppermute(value, axes, [(i, (i + step) % n) for i in range(n)])]
  transfers between devices with their start and end apart: 21 -> 21, of which waited for: 12 -> 11; matrix products, arithmetic and copies ran while one was open for 4% -> 5% of each run, Pallas kernels for 2% -> 2%
where the time goes in v9:
time: 174 us; the launch traced here: 173 us
  waiting for transfers between devices  78.1 us (45%)
  starting transfers between devices  71.9 us (41%)
  Pallas kernels  11.5 us (7%)
  other arithmetic  8.75 us (5%)
  local copies, waits for them, and re-layouts  2.06 us (1%)
    ppermute x13, starting transfers between devices, shifted(): return lax.ppermute(value, axes, [(i, (i + step) % n) for i in range(n)])  41.7 us
    all_to_all x4, waiting for transfers between devices, exchange(): return lax.all_to_all(parts, axes, split_axis=0, concat_axis=0, tiled=True)  29.3 us
    ppermute x13, waiting for transfers between devices, shifted(): return lax.ppermute(value, axes, [(i, (i + step) % n) for i in range(n)])  25.9 us
    ppermute x4, waiting for transfers between devices, swapped(): return lax.ppermute(value, axes, [(i, partner(i)) for i in range(n)])  22.9 us
    all_to_all x4, starting transfers between devices, exchange(): return lax.all_to_all(parts, axes, split_axis=0, concat_axis=0, tiled=True)  20.8 us
    pallas_call x3, Pallas kernels, call(): pl.pallas_call(kernel, out_shape=tuple((pltpu.HBM(s, t) if k in out_hbm e...  11.5 us
    ppermute x4, starting transfers between devices, swapped(): return lax.ppermute(value, axes, [(i, partner(i)) for i in range(n)])  9.37 us
    convert_element_type x3, other arithmetic, total(): return (a.astype(F32) + b.astype(F32)).astype(BF)  4.42 us
  transfers between devices with their start and end apart: 21, of which 11 were waited for; matrix products, arithmetic and copies ran while one was open for 5% of the time, Pallas kernels for 2%

profile of v9, /device:TPU:4, one launch (start us, length us, event | category | flops | bytes accessed | tf_op | source)
XLA Modules:
  0.0 173.3 jit_solution(1738834423437105035)
XLA Ops:
  0.6 0.9 fusion
  1.5 3.8 %collective-permute-start = (bf16[128,512]{1,0:T(8,128)(2,1)S(1)}, bf16[128,512]{1,0:T(8,128)(2,1)S(1)}, u32[]{:S(2)}, u32[]{:S(2)}) collective-permute-start(bf16[128,512]{1,0:T(8,128)(2,1)S(1)} %get-tuple-element.23), channel_id=1, source_target_pairs={{0,32},{32,64},{64,96},{96,128},{128,160},{160,192},{192,224},{224... | collective-permute-start | bytes 393224 | tf_op jit(solution)/shard_map/ppermute | solution.py:35
  5.4 11.1 %collective-permute-done = bf16[128,512]{1,0:T(8,128)(2,1)S(1)} collective-permute-done((bf16[128,512]{1,0:T(8,128)(2,1)S(1)}, bf16[128,512]{1,0:T(8,128)(2,1)S(1)}, u32[]{:S(2)}, u32[]{:S(2)}) %collective-permute-start) | collective-permute-done | bytes 131104 | tf_op jit(solution)/shard_map/ppermute | solution.py:35
  16.4 1.9 %collective-permute-start.2 = (bf16[128,512]{1,0:T(8,128)(2,1)S(1)}, bf16[128,512]{1,0:T(8,128)(2,1)S(1)}, u32[]{:S(2)}, u32[]{:S(2)}) collective-permute-start(bf16[128,512]{1,0:T(8,128)(2,1)S(1)} %collective-permute-done), channel_id=1, source_target_pairs={{0,32},{32,64},{64,96},{96,128},{128,160},{160,192},{192,224},{224... | collective-permute-start | bytes 393224 | tf_op jit(solution)/shard_map/ppermute | solution.py:35
  18.3 5.1 %collective-permute-start.1 = (bf16[128,512]{1,0:T(8,128)(2,1)S(1)}, bf16[128,512]{1,0:T(8,128)(2,1)S(1)}, u32[]{:S(2)}, u32[]{:S(2)}) collective-permute-start(bf16[128,512]{1,0:T(8,128)(2,1)S(1)} %get-tuple-element.23), channel_id=1, source_target_pairs={{0,480},{32,0},{64,32},{96,64},{128,96},{160,128},{192,160},{224,1... | collective-permute-start | bytes 393224 | tf_op jit(solution)/shard_map/ppermute | solution.py:35
  23.5 1.0 collective-permute-done.2
  24.5 1.9 %collective-permute-start.3 = (bf16[128,512]{1,0:T(8,128)(2,1)S(1)}, bf16[128,512]{1,0:T(8,128)(2,1)S(1)}, u32[]{:S(2)}, u32[]{:S(2)}) collective-permute-start(bf16[128,512]{1,0:T(8,128)(2,1)S(1)} %collective-permute-done.2), channel_id=1, source_target_pairs={{0,32},{32,64},{64,96},{96,128},{128,160},{160,192},{192,224},{224... | collective-permute-start | bytes 393224 | tf_op jit(solution)/shard_map/ppermute | solution.py:35
  26.4 0.0 collective-permute-done.1
  26.5 1.3 broadcast_in_dim.6
  27.7 4.5 %all-to-all-start = ((bf16[4,3,128,512]{3,2,1,0:T(8,128)(2,1)}), bf16[4,3,128,512]{3,2,1,0:T(8,128)(2,1)S(1)}, u32[]{:S(2)}, u32[]{:S(2)}) async-start(bf16[4,3,128,512]{3,2,1,0:T(8,128)(2,1)} %broadcast_in_dim.6), calls=%async_computation | async-start | bytes 3145728 | tf_op jit(solution)/shard_map/all_to_all | solution.py:24
  32.2 5.1 %collective-permute-start.8 = (bf16[128,512]{1,0:T(8,128)(2,1)S(1)}, bf16[128,512]{1,0:T(8,128)(2,1)S(1)}, u32[]{:S(2)}, u32[]{:S(2)}) collective-permute-start(bf16[128,512]{1,0:T(8,128)(2,1)S(1)} %collective-permute-done.1), channel_id=1, source_target_pairs={{0,480},{32,0},{64,32},{96,64},{128,96},{160,128},{192,160},{224,1... | collective-permute-start | bytes 393224 | tf_op jit(solution)/shard_map/ppermute | solution.py:35
  37.3 0.0 collective-permute-done.3
  37.3 1.9 %collective-permute-start.4 = (bf16[128,512]{1,0:T(8,128)(2,1)S(1)}, bf16[128,512]{1,0:T(8,128)(2,1)S(1)}, u32[]{:S(2)}, u32[]{:S(2)}) collective-permute-start(bf16[128,512]{1,0:T(8,128)(2,1)S(1)} %collective-permute-done.3), channel_id=1, source_target_pairs={{0,32},{32,64},{64,96},{96,128},{128,160},{160,192},{192,224},{224... | collective-permute-start | bytes 393224 | tf_op jit(solution)/shard_map/ppermute | solution.py:35
  39.3 6.1 %collective-permute-done.4 = bf16[128,512]{1,0:T(8,128)(2,1)S(1)} collective-permute-done((bf16[128,512]{1,0:T(8,128)(2,1)S(1)}, bf16[128,512]{1,0:T(8,128)(2,1)S(1)}, u32[]{:S(2)}, u32[]{:S(2)}) %collective-permute-start.4) | collective-permute-done | bytes 131104 | tf_op jit(solution)/shard_map/ppermute | solution.py:35
  45.4 3.9 %collective-permute-start.5 = (bf16[384,512]{1,0:T(8,128)(2,1)S(1)}, bf16[384,512]{1,0:T(8,128)(2,1)S(1)}, u32[]{:S(2)}, u32[]{:S(2)}) collective-permute-start(bf16[384,512]{1,0:T(8,128)(2,1)S(1)} %constant_dynamic-update-slice_fusion.refs_0_), channel_id=1, source_target_pairs={{0,8},{8,16},{16,24},{24,0},{1,9},{9,17},{17,25},{25,1},{2,10},{10... | collective-permute-start | bytes 1179656 | tf_op jit(solution)/shard_map/ppermute | solution.py:35
  49.4 0.0 collective-permute-done.8
  49.4 1.9 %collective-permute-start.9 = (bf16[128,512]{1,0:T(8,128)(2,1)S(1)}, bf16[128,512]{1,0:T(8,128)(2,1)S(1)}, u32[]{:S(2)}, u32[]{:S(2)}) collective-permute-start(bf16[128,512]{1,0:T(8,128)(2,1)S(1)} %collective-permute-done.8), channel_id=1, source_target_pairs={{0,480},{32,0},{64,32},{96,64},{128,96},{160,128},{192,160},{224,1... | collective-permute-start | bytes 393224 | tf_op jit(solution)/shard_map/ppermute | solution.py:35
  51.3 4.9 %collective-permute-done.9 = bf16[128,512]{1,0:T(8,128)(2,1)S(1)} collective-permute-done((bf16[128,512]{1,0:T(8,128)(2,1)S(1)}, bf16[128,512]{1,0:T(8,128)(2,1)S(1)}, u32[]{:S(2)}, u32[]{:S(2)}) %collective-permute-start.9) | collective-permute-done | bytes 131104 | tf_op jit(solution)/shard_map/ppermute | solution.py:35
  56.3 3.1 %collective-permute-start.11 = (bf16[256,512]{1,0:T(8,128)(2,1)S(1)}, bf16[256,512]{1,0:T(8,128)(2,1)}, u32[]{:S(2)}, u32[]{:S(2)}) collective-permute-start(bf16[256,512]{1,0:T(8,128)(2,1)S(1)} %constant_dynamic-update-slice_fusion.3.refs_4_), channel_id=1, source_target_pairs={{0,24},{8,0},{16,8},{24,16},{1,25},{9,1},{17,9},{25,17},{2,26},{10... | collective-permute-start | bytes 786440 | tf_op jit(solution)/shard_map/ppermute | solution.py:35
  59.4 3.9 %collective-permute-start.6 = (bf16[384,512]{1,0:T(8,128)(2,1)S(1)}, bf16[384,512]{1,0:T(8,128)(2,1)S(1)}, u32[]{:S(2)}, u32[]{:S(2)}) collective-permute-start(bf16[384,512]{1,0:T(8,128)(2,1)S(1)} %constant_dynamic-update-slice_fusion.refs_0_), channel_id=1, source_target_pairs={{0,24},{8,0},{16,8},{24,16},{1,25},{9,1},{17,9},{25,17},{2,26},{10... | collective-permute-start | bytes 1179656 | tf_op jit(solution)/shard_map/ppermute | solution.py:35
  63.3 0.0 collective-permute-done.5.refs_1_
  63.3 1.9 %collective-permute-start.7 = (bf16[384,512]{1,0:T(8,128)(2,1)S(1)}, bf16[384,512]{1,0:T(8,128)(2,1)S(1)}, u32[]{:S(2)}, u32[]{:S(2)}) collective-permute-start(bf16[384,512]{1,0:T(8,128)(2,1)S(1)} %collective-permute-done.5.refs_1_), channel_id=1, source_target_pairs={{0,8},{8,16},{16,24},{24,0},{1,9},{9,17},{17,25},{25,1},{2,10},{10... | collective-permute-start | bytes 1179656 | tf_op jit(solution)/shard_map/ppermute | solution.py:35
  65.3 2.7 %collective-permute-start.10 = (bf16[256,512]{1,0:T(8,128)(2,1)S(1)}, bf16[256,512]{1,0:T(8,128)(2,1)}, u32[]{:S(2)}, u32[]{:S(2)}) collective-permute-start(bf16[256,512]{1,0:T(8,128)(2,1)S(1)} %constant_dynamic-update-slice_fusion.3.refs_4_), channel_id=1, source_target_pairs={{0,8},{8,16},{16,24},{24,0},{1,9},{9,17},{17,25},{25,1},{2,10},{10... | collective-permute-start | bytes 786440 | tf_op jit(solution)/shard_map/ppermute | solution.py:35
  68.0 0.0 collective-permute-done.11.refs_6_
  68.0 4.3 %collective-permute-start.12 = (bf16[256,512]{1,0:T(8,128)(2,1)}, bf16[256,512]{1,0:T(8,128)(2,1)}, u32[]{:S(2)}, u32[]{:S(2)}) collective-permute-start(bf16[256,512]{1,0:T(8,128)(2,1)} %collective-permute-done.11.refs_6_), channel_id=1, source_target_pairs={{0,24},{8,0},{16,8},{24,16},{1,25},{9,1},{17,9},{25,17},{2,26},{10... | collective-permute-start | bytes 786440 | tf_op jit(solution)/shard_map/ppermute | solution.py:35
  72.3 0.0 all-to-all-done.near_ref
  72.4 0.0 copy-start
  72.4 2.7 %shard_map.59 = (f32[384,512]{1,0:T(8,128)S(1)}, f32[384,512]{1,0:T(8,128)S(1)}, bf16[384,2048]{1,0:T(8,128)(2,1)S(1)}, bf16[384,2048]{1,0:T(8,128)(2,1)S(1)}) custom-call(bf16[384,2048]{1,0:T(8,128)(2,1)} %x_hbm.1, bf16[384,2048]{1,0:T(8,128)(2,1)} %c_hbm.1, bf16[4,3,128,512]{3,2,1,0:T(8,128)(2,1)S(1)} %all-to-all-done.near_ref), custom_call_target="tpu_custom_call" | custom-call | flops 603979776 | bytes 4718592 | tf_op jit(solution)/shard_map/pallas_call | solution.py:152
  75.1 0.0 copy-done
  75.1 2.8 %collective-permute-done.10.refs_5_ = bf16[256,512]{1,0:T(8,128)(2,1)} collective-permute-done((bf16[256,512]{1,0:T(8,128)(2,1)S(1)}, bf16[256,512]{1,0:T(8,128)(2,1)}, u32[]{:S(2)}, u32[]{:S(2)}) %collective-permute-start.10) | collective-permute-done | bytes 262176 | tf_op jit(solution)/shard_map/ppermute | solution.py:35
  77.9 0.0 collective-permute-done.6.refs_2_
  77.9 0.0 collective-permute-done.12.refs_7_
  77.9 0.0 collective-permute-done.7.refs_3_
  77.9 4.4 %shard_map.60 = (bf16[384,512]{1,0:T(8,128)(2,1)}, bf16[4,4,2,64,512]{4,3,2,1,0:T(8,128)(2,1)}, bf16[1280,512]{1,0:T(8,128)(2,1)}) custom-call(bf16[384,2048]{1,0:T(8,128)(2,1)S(1)} %get-tuple-element.11.x_ref, bf16[384,2048]{1,0:T(8,128)(2,1)S(1)} %get-tuple-element.12.c_ref, f32[384,512]{1,0:T(8,128)S(1)} %get-tuple-element.13.pre_ref, ...), custom_call_target="tpu_custom_call" | custom-call | flops 1811939328 | bytes 6553600 | tf_op jit(solution)/shard_map/pallas_call | solution.py:152
  82.3 4.4 %shard_map.61 = (bf16[192,2048]{1,0:T(8,128)(2,1)}, bf16[192,2048]{1,0:T(8,128)(2,1)}) custom-call(bf16[384,512]{1,0:T(8,128)(2,1)} %get-tuple-element.15.grad_ref, bf16[4,3,128,512]{3,2,1,0:T(8,128)(2,1)} %copy-done, bf16[1280,512]{1,0:T(8,128)(2,1)} %get-tuple-element.16.up_ref), custom_call_target="tpu_custom_call" | custom-call | flops 805306368 | bytes 3276800 | tf_op jit(solution)/shard_map/pallas_call | solution.py:152
  86.8 1.9 %collective-permute-start.13 = (bf16[192,2048]{1,0:T(8,128)(2,1)}, bf16[192,2048]{1,0:T(8,128)(2,1)S(1)}, u32[]{:S(2)}, u32[]{:S(2)}) collective-permute-start(bf16[192,2048]{1,0:T(8,128)(2,1)} %get-tuple-element.18), channel_id=1, source_target_pairs={{0,1},{1,0},{2,3},{3,2},{4,5},{5,4},{6,7},{7,6},{8,9},{9,8},{10,11... | collective-permute-start | bytes 2359304 | tf_op jit(solution)/shard_map/ppermute | solution.py:40
  88.7 2.5 %collective-permute-done.13 = bf16[192,2048]{1,0:T(8,128)(2,1)S(1)} collective-permute-done((bf16[192,2048]{1,0:T(8,128)(2,1)}, bf16[192,2048]{1,0:T(8,128)(2,1)S(1)}, u32[]{:S(2)}, u32[]{:S(2)}) %collective-permute-start.13) | collective-permute-done | bytes 786464 | tf_op jit(solution)/shard_map/ppermute | solution.py:40
  91.1 1.4 add_convert_fusion.2
  92.5 0.0 copy-start.1
  92.5 3.1 %collective-permute-start.14 = (bf16[192,2048]{1,0:T(8,128)(2,1)S(1)}, bf16[192,2048]{1,0:T(8,128)(2,1)}, u32[]{:S(2)}, u32[]{:S(2)}) collective-permute-start(bf16[192,2048]{1,0:T(8,128)(2,1)S(1)} %add_convert_fusion.2), channel_id=1, source_target_pairs={{0,2},{2,0},{4,6},{6,4},{1,3},{3,1},{5,7},{7,5},{8,10},{10,8},{12,... | collective-permute-start | bytes 2359304 | tf_op jit(solution)/shard_map/ppermute | solution.py:40
  95.7 0.0 copy-done.1
  95.7 3.8 %all-to-all-start.1 = ((bf16[4,4,2,64,512]{4,3,2,1,0:T(8,128)(2,1)}), bf16[4,4,2,64,512]{4,3,2,1,0:T(8,128)(2,1)S(1)}, u32[]{:S(2)}, u32[]{:S(2)}) async-start(bf16[4,4,2,64,512]{4,3,2,1,0:T(8,128)(2,1)} %get-tuple-element.19), calls=%async_computation.1 | async-start | bytes 4194304 | tf_op jit(solution)/shard_map/all_to_all | solution.py:24
  99.5 14.6 %collective-permute-done.14 = bf16[192,2048]{1,0:T(8,128)(2,1)} collective-permute-done((bf16[192,2048]{1,0:T(8,128)(2,1)S(1)}, bf16[192,2048]{1,0:T(8,128)(2,1)}, u32[]{:S(2)}, u32[]{:S(2)}) %collective-permute-start.14) | collective-permute-done | bytes 786464 | tf_op jit(solution)/shard_map/ppermute | solution.py:40
  114.1 1.6 add_convert_fusion.1
  115.8 2.4 %collective-permute-start.15 = (bf16[192,2048]{1,0:T(8,128)(2,1)S(1)}, bf16[192,2048]{1,0:T(8,128)(2,1)}, u32[]{:S(2)}, u32[]{:S(2)}) collective-permute-start(bf16[192,2048]{1,0:T(8,128)(2,1)S(1)} %add_convert_fusion.1), channel_id=1, source_target_pairs={{0,6},{2,4},{4,2},{6,0},{1,7},{3,5},{5,3},{7,1},{8,14},{10,12},{12... | collective-permute-start | bytes 2359304 | tf_op jit(solution)/shard_map/ppermute | solution.py:40
  118.2 7.7 %all-to-all-done.1 = bf16[4,4,2,64,512]{4,3,2,1,0:T(8,128)(2,1)S(1)} async-done(((bf16[4,4,2,64,512]{4,3,2,1,0:T(8,128)(2,1)}), bf16[4,4,2,64,512]{4,3,2,1,0:T(8,128)(2,1)S(1)}, u32[]{:S(2)}, u32[]{:S(2)}) %all-to-all-start.1) | async-done | bytes 2097184 | tf_op jit(solution)/shard_map/all_to_all | solution.py:24
  125.9 1.3 reduce_sum.33
  127.2 3.5 %all-to-all-start.2 = ((bf16[4,2,64,512]{3,2,1,0:T(8,128)(2,1)}), bf16[4,2,64,512]{3,2,1,0:T(8,128)(2,1)S(1)}, u32[]{:S(2)}, u32[]{:S(2)}) async-start(bf16[4,2,64,512]{3,2,1,0:T(8,128)(2,1)} %reduce_sum.33), calls=%async_computation.2 | async-start | bytes 1048576 | tf_op jit(solution)/shard_map/all_to_all | solution.py:24
  130.6 5.9 %collective-permute-done.15 = bf16[192,2048]{1,0:T(8,128)(2,1)} collective-permute-done((bf16[192,2048]{1,0:T(8,128)(2,1)S(1)}, bf16[192,2048]{1,0:T(8,128)(2,1)}, u32[]{:S(2)}, u32[]{:S(2)}) %collective-permute-start.15) | collective-permute-done | bytes 786464 | tf_op jit(solution)/shard_map/ppermute | solution.py:40
  136.5 1.4 add_convert_fusion
  137.9 1.9 %collective-permute-start.16 = (bf16[192,2048]{1,0:T(8,128)(2,1)S(1)}, bf16[192,2048]{1,0:T(8,128)(2,1)S(1)}, u32[]{:S(2)}, u32[]{:S(2)}) collective-permute-start(bf16[192,2048]{1,0:T(8,128)(2,1)S(1)} %add_convert_fusion), channel_id=1, source_target_pairs={{0,1},{1,0},{2,3},{3,2},{4,5},{5,4},{6,7},{7,6},{8,9},{9,8},{10,11... | collective-permute-start | bytes 2359304 | tf_op jit(solution)/shard_map/ppermute | solution.py:40
  139.8 4.4 %all-to-all-done.2 = bf16[4,2,64,512]{3,2,1,0:T(8,128)(2,1)S(1)} async-done(((bf16[4,2,64,512]{3,2,1,0:T(8,128)(2,1)}), bf16[4,2,64,512]{3,2,1,0:T(8,128)(2,1)S(1)}, u32[]{:S(2)}, u32[]{:S(2)}) %all-to-all-start.2) | async-done | bytes 524320 | tf_op jit(solution)/shard_map/all_to_all | solution.py:24
  144.3 0.1 reduce_sum.34
  144.4 0.7 broadcast_in_dim.7
  145.1 9.0 %all-to-all-start.3 = ((bf16[4,64,512]{2,1,0:T(8,128)(2,1)}), bf16[4,64,512]{2,1,0:T(8,128)(2,1)S(1)}, u32[]{:S(2)}, u32[]{:S(2)}) async-start(bf16[4,64,512]{2,1,0:T(8,128)(2,1)} %bitcast.4), calls=%async_computation.3 | async-start | bytes 524288 | tf_op jit(solution)/shard_map/all_to_all | solution.py:24
  154.1 0.0 collective-permute-done.16
  154.1 0.1 broadcast_select_fusion.1
  154.2 1.2 pad_maximum_fusion
  155.5 17.1 %all-to-all-done.3 = bf16[4,64,512]{2,1,0:T(8,128)(2,1)S(1)} async-done(((bf16[4,64,512]{2,1,0:T(8,128)(2,1)}), bf16[4,64,512]{2,1,0:T(8,128)(2,1)S(1)}, u32[]{:S(2)}, u32[]{:S(2)}) %all-to-all-start.3) | async-done | bytes 262176 | tf_op jit(solution)/shard_map/all_to_all | solution.py:24
  172.6 0.7 convert_reduce_fusion
  (6 shorter events, 0.1 us)
Async XLA Ops:
  1.5 14.9 %collective-permute-start = (bf16[128,512]{1,0:T(8,128)(2,1)S(1)}, bf16[128,512]{1,0:T(8,128)(2,1)S(1)}, u32[]{:S(2)}, u32[]{:S(2)}) collective-permute-start(bf16[128,512]{1,0:T(8,128)(2,1)S(1)} %get-tuple-element.23), channel_id=1, source_target_pairs={{0,32},{32,64},{64,96},{96,128},{128,160},{160,192},{192,224},{224... | collective-permute-start | bytes 393224 | tf_op jit(solution)/shard_map/ppermute | solution.py:35
  16.4 8.1 %collective-permute-start.2 = (bf16[128,512]{1,0:T(8,128)(2,1)S(1)}, bf16[128,512]{1,0:T(8,128)(2,1)S(1)}, u32[]{:S(2)}, u32[]{:S(2)}) collective-permute-start(bf16[128,512]{1,0:T(8,128)(2,1)S(1)} %collective-permute-done), channel_id=1, source_target_pairs={{0,32},{32,64},{64,96},{96,128},{128,160},{160,192},{192,224},{224... | collective-permute-start | bytes 393224 | tf_op jit(solution)/shard_map/ppermute | solution.py:35
  18.3 8.1 %collective-permute-start.1 = (bf16[128,512]{1,0:T(8,128)(2,1)S(1)}, bf16[128,512]{1,0:T(8,128)(2,1)S(1)}, u32[]{:S(2)}, u32[]{:S(2)}) collective-permute-start(bf16[128,512]{1,0:T(8,128)(2,1)S(1)} %get-tuple-element.23), channel_id=1, source_target_pairs={{0,480},{32,0},{64,32},{96,64},{128,96},{160,128},{192,160},{224,1... | collective-permute-start | bytes 393224 | tf_op jit(solution)/shard_map/ppermute | solution.py:35
  24.5 12.9 %collective-permute-start.3 = (bf16[128,512]{1,0:T(8,128)(2,1)S(1)}, bf16[128,512]{1,0:T(8,128)(2,1)S(1)}, u32[]{:S(2)}, u32[]{:S(2)}) collective-permute-start(bf16[128,512]{1,0:T(8,128)(2,1)S(1)} %collective-permute-done.2), channel_id=1, source_target_pairs={{0,32},{32,64},{64,96},{96,128},{128,160},{160,192},{192,224},{224... | collective-permute-start | bytes 393224 | tf_op jit(solution)/shard_map/ppermute | solution.py:35
  27.7 44.6 %all-to-all-start = ((bf16[4,3,128,512]{3,2,1,0:T(8,128)(2,1)}), bf16[4,3,128,512]{3,2,1,0:T(8,128)(2,1)S(1)}, u32[]{:S(2)}, u32[]{:S(2)}) async-start(bf16[4,3,128,512]{3,2,1,0:T(8,128)(2,1)} %broadcast_in_dim.6), calls=%async_computation | async-start | bytes 3145728 | tf_op jit(solution)/shard_map/all_to_all | solution.py:24
  32.2 17.2 %collective-permute-start.8 = (bf16[128,512]{1,0:T(8,128)(2,1)S(1)}, bf16[128,512]{1,0:T(8,128)(2,1)S(1)}, u32[]{:S(2)}, u32[]{:S(2)}) collective-permute-start(bf16[128,512]{1,0:T(8,128)(2,1)S(1)} %collective-permute-done.1), channel_id=1, source_target_pairs={{0,480},{32,0},{64,32},{96,64},{128,96},{160,128},{192,160},{224,1... | collective-permute-start | bytes 393224 | tf_op jit(solution)/shard_map/ppermute | solution.py:35
  37.3 8.1 %collective-permute-start.4 = (bf16[128,512]{1,0:T(8,128)(2,1)S(1)}, bf16[128,512]{1,0:T(8,128)(2,1)S(1)}, u32[]{:S(2)}, u32[]{:S(2)}) collective-permute-start(bf16[128,512]{1,0:T(8,128)(2,1)S(1)} %collective-permute-done.3), channel_id=1, source_target_pairs={{0,32},{32,64},{64,96},{96,128},{128,160},{160,192},{192,224},{224... | collective-permute-start | bytes 393224 | tf_op jit(solution)/shard_map/ppermute | solution.py:35
  45.4 17.9 %collective-permute-start.5 = (bf16[384,512]{1,0:T(8,128)(2,1)S(1)}, bf16[384,512]{1,0:T(8,128)(2,1)S(1)}, u32[]{:S(2)}, u32[]{:S(2)}) collective-permute-start(bf16[384,512]{1,0:T(8,128)(2,1)S(1)} %constant_dynamic-update-slice_fusion.refs_0_), channel_id=1, source_target_pairs={{0,8},{8,16},{16,24},{24,0},{1,9},{9,17},{17,25},{25,1},{2,10},{10... | collective-permute-start | bytes 1179656 | tf_op jit(solution)/shard_map/ppermute | solution.py:35
  49.4 6.9 %collective-permute-start.9 = (bf16[128,512]{1,0:T(8,128)(2,1)S(1)}, bf16[128,512]{1,0:T(8,128)(2,1)S(1)}, u32[]{:S(2)}, u32[]{:S(2)}) collective-permute-start(bf16[128,512]{1,0:T(8,128)(2,1)S(1)} %collective-permute-done.8), channel_id=1, source_target_pairs={{0,480},{32,0},{64,32},{96,64},{128,96},{160,128},{192,160},{224,1... | collective-permute-start | bytes 393224 | tf_op jit(solution)/shard_map/ppermute | solution.py:35
  56.3 11.7 %collective-permute-start.11 = (bf16[256,512]{1,0:T(8,128)(2,1)S(1)}, bf16[256,512]{1,0:T(8,128)(2,1)}, u32[]{:S(2)}, u32[]{:S(2)}) collective-permute-start(bf16[256,512]{1,0:T(8,128)(2,1)S(1)} %constant_dynamic-update-slice_fusion.3.refs_4_), channel_id=1, source_target_pairs={{0,24},{8,0},{16,8},{24,16},{1,25},{9,1},{17,9},{25,17},{2,26},{10... | collective-permute-start | bytes 786440 | tf_op jit(solution)/shard_map/ppermute | solution.py:35
  59.4 18.5 %collective-permute-start.6 = (bf16[384,512]{1,0:T(8,128)(2,1)S(1)}, bf16[384,512]{1,0:T(8,128)(2,1)S(1)}, u32[]{:S(2)}, u32[]{:S(2)}) collective-permute-start(bf16[384,512]{1,0:T(8,128)(2,1)S(1)} %constant_dynamic-update-slice_fusion.refs_0_), channel_id=1, source_target_pairs={{0,24},{8,0},{16,8},{24,16},{1,25},{9,1},{17,9},{25,17},{2,26},{10... | collective-permute-start | bytes 1179656 | tf_op jit(solution)/shard_map/ppermute | solution.py:35
  63.3 14.5 %collective-permute-start.7 = (bf16[384,512]{1,0:T(8,128)(2,1)S(1)}, bf16[384,512]{1,0:T(8,128)(2,1)S(1)}, u32[]{:S(2)}, u32[]{:S(2)}) collective-permute-start(bf16[384,512]{1,0:T(8,128)(2,1)S(1)} %collective-permute-done.5.refs_1_), channel_id=1, source_target_pairs={{0,8},{8,16},{16,24},{24,0},{1,9},{9,17},{17,25},{25,1},{2,10},{10... | collective-permute-start | bytes 1179656 | tf_op jit(solution)/shard_map/ppermute | solution.py:35
  65.3 12.6 %collective-permute-start.10 = (bf16[256,512]{1,0:T(8,128)(2,1)S(1)}, bf16[256,512]{1,0:T(8,128)(2,1)}, u32[]{:S(2)}, u32[]{:S(2)}) collective-permute-start(bf16[256,512]{1,0:T(8,128)(2,1)S(1)} %constant_dynamic-update-slice_fusion.3.refs_4_), channel_id=1, source_target_pairs={{0,8},{8,16},{16,24},{24,0},{1,9},{9,17},{17,25},{25,1},{2,10},{10... | collective-permute-start | bytes 786440 | tf_op jit(solution)/shard_map/ppermute | solution.py:35
  68.0 9.9 %collective-permute-start.12 = (bf16[256,512]{1,0:T(8,128)(2,1)}, bf16[256,512]{1,0:T(8,128)(2,1)}, u32[]{:S(2)}, u32[]{:S(2)}) collective-permute-start(bf16[256,512]{1,0:T(8,128)(2,1)} %collective-permute-done.11.refs_6_), channel_id=1, source_target_pairs={{0,24},{8,0},{16,8},{24,16},{1,25},{9,1},{17,9},{25,17},{2,26},{10... | collective-permute-start | bytes 786440 | tf_op jit(solution)/shard_map/ppermute | solution.py:35
  72.4 2.7 %copy-start = (bf16[4,3,128,512]{3,2,1,0:T(8,128)(2,1)}, bf16[4,3,128,512]{3,2,1,0:T(8,128)(2,1)S(1)}, u32[]{:S(2)}) copy-start(bf16[4,3,128,512]{3,2,1,0:T(8,128)(2,1)S(1)} %all-to-all-done.near_ref) | copy-start | bytes 4718596
  86.8 4.4 %collective-permute-start.13 = (bf16[192,2048]{1,0:T(8,128)(2,1)}, bf16[192,2048]{1,0:T(8,128)(2,1)S(1)}, u32[]{:S(2)}, u32[]{:S(2)}) collective-permute-start(bf16[192,2048]{1,0:T(8,128)(2,1)} %get-tuple-element.18), channel_id=1, source_target_pairs={{0,1},{1,0},{2,3},{3,2},{4,5},{5,4},{6,7},{7,6},{8,9},{9,8},{10,11... | collective-permute-start | bytes 2359304 | tf_op jit(solution)/shard_map/ppermute | solution.py:40
  92.5 3.1 %copy-start.1 = (bf16[192,2048]{1,0:T(8,128)(2,1)}, bf16[192,2048]{1,0:T(8,128)(2,1)S(1)}, u32[]{:S(2)}) copy-start(bf16[192,2048]{1,0:T(8,128)(2,1)S(1)} %add_convert_fusion.2) | copy-start | bytes 2359300
  92.5 21.6 %collective-permute-start.14 = (bf16[192,2048]{1,0:T(8,128)(2,1)S(1)}, bf16[192,2048]{1,0:T(8,128)(2,1)}, u32[]{:S(2)}, u32[]{:S(2)}) collective-permute-start(bf16[192,2048]{1,0:T(8,128)(2,1)S(1)} %add_convert_fusion.2), channel_id=1, source_target_pairs={{0,2},{2,0},{4,6},{6,4},{1,3},{3,1},{5,7},{7,5},{8,10},{10,8},{12,... | collective-permute-start | bytes 2359304 | tf_op jit(solution)/shard_map/ppermute | solution.py:40
  95.7 30.2 %all-to-all-start.1 = ((bf16[4,4,2,64,512]{4,3,2,1,0:T(8,128)(2,1)}), bf16[4,4,2,64,512]{4,3,2,1,0:T(8,128)(2,1)S(1)}, u32[]{:S(2)}, u32[]{:S(2)}) async-start(bf16[4,4,2,64,512]{4,3,2,1,0:T(8,128)(2,1)} %get-tuple-element.19), calls=%async_computation.1 | async-start | bytes 4194304 | tf_op jit(solution)/shard_map/all_to_all | solution.py:24
  115.8 20.7 %collective-permute-start.15 = (bf16[192,2048]{1,0:T(8,128)(2,1)S(1)}, bf16[192,2048]{1,0:T(8,128)(2,1)}, u32[]{:S(2)}, u32[]{:S(2)}) collective-permute-start(bf16[192,2048]{1,0:T(8,128)(2,1)S(1)} %add_convert_fusion.1), channel_id=1, source_target_pairs={{0,6},{2,4},{4,2},{6,0},{1,7},{3,5},{5,3},{7,1},{8,14},{10,12},{12... | collective-permute-start | bytes 2359304 | tf_op jit(solution)/shard_map/ppermute | solution.py:40
  127.2 17.1 %all-to-all-start.2 = ((bf16[4,2,64,512]{3,2,1,0:T(8,128)(2,1)}), bf16[4,2,64,512]{3,2,1,0:T(8,128)(2,1)S(1)}, u32[]{:S(2)}, u32[]{:S(2)}) async-start(bf16[4,2,64,512]{3,2,1,0:T(8,128)(2,1)} %reduce_sum.33), calls=%async_computation.2 | async-start | bytes 1048576 | tf_op jit(solution)/shard_map/all_to_all | solution.py:24
  137.9 16.2 %collective-permute-start.16 = (bf16[192,2048]{1,0:T(8,128)(2,1)S(1)}, bf16[192,2048]{1,0:T(8,128)(2,1)S(1)}, u32[]{:S(2)}, u32[]{:S(2)}) collective-permute-start(bf16[192,2048]{1,0:T(8,128)(2,1)S(1)} %add_convert_fusion), channel_id=1, source_target_pairs={{0,1},{1,0},{2,3},{3,2},{4,5},{5,4},{6,7},{7,6},{8,9},{9,8},{10,11... | collective-permute-start | bytes 2359304 | tf_op jit(solution)/shard_map/ppermute | solution.py:40
  145.1 27.5 %all-to-all-start.3 = ((bf16[4,64,512]{2,1,0:T(8,128)(2,1)}), bf16[4,64,512]{2,1,0:T(8,128)(2,1)S(1)}, u32[]{:S(2)}, u32[]{:S(2)}) async-start(bf16[4,64,512]{2,1,0:T(8,128)(2,1)} %bitcast.4), calls=%async_computation.3 | async-start | bytes 524288 | tf_op jit(solution)/shard_map/all_to_all | solution.py:24

commit v10 on v9

--- a/solution.py
+++ b/solution.py
@@ -185,9 +185,16 @@
     near = copies_over(near, "y")
     minus = [jnp.concatenate([ahead[2], ahead[3]], axis=0)]
     plus = [jnp.concatenate([back[2], back[3], last], axis=0)]
-    for stack in (minus, plus):
-        stack.append(shifted(stack[0], "y", 1))
-        stack.append(shifted(stack[0], "y", -1))
+    sends = {}
+    for name, stack, step in (
+        ("minus_after", minus, -1),
+        ("plus_before", plus, 1),
+        ("plus_after", plus, -1),
+        ("minus_before", minus, 1),
+    ):
+        sends[name] = shifted(stack[0], "y", step)
+    minus += [sends["minus_before"], sends["minus_after"]]
+    plus += [sends["plus_before"], sends["plus_after"]]
     plus.append(shifted(plus[1], "y", 1))
     minus.append(shifted(minus[2], "y", -1))
     inputs = pltpu.with_memory_space_constraint(inputs, pltpu.HBM)

time: 174 us -> 174 us (level)
  no operation moved by 1% of the time
where the time goes in v10:
time: 174 us; the launch traced here: 173 us
  waiting for transfers between devices  78.1 us (45%)
  starting transfers between devices  71.9 us (41%)
  Pallas kernels  11.5 us (7%)
  other arithmetic  8.75 us (5%)
  local copies, waits for them, and re-layouts  2.06 us (1%)
    ppermute x13, starting transfers between devices, shifted(): return lax.ppermute(value, axes, [(i, (i + step) % n) for i in range(n)])  41.7 us
    all_to_all x4, waiting for transfers between devices, exchange(): return lax.all_to_all(parts, axes, split_axis=0, concat_axis=0, tiled=True)  29.3 us
    ppermute x13, waiting for transfers between devices, shifted(): return lax.ppermute(value, axes, [(i, (i + step) % n) for i in range(n)])  25.9 us
    ppermute x4, waiting for transfers between devices, swapped(): return lax.ppermute(value, axes, [(i, partner(i)) for i in range(n)])  22.9 us
    all_to_all x4, starting transfers between devices, exchange(): return lax.all_to_all(parts, axes, split_axis=0, concat_axis=0, tiled=True)  20.8 us
    pallas_call x3, Pallas kernels, call(): pl.pallas_call(kernel, out_shape=tuple((pltpu.HBM(s, t) if k in out_hbm e...  11.5 us
    ppermute x4, starting transfers between devices, swapped(): return lax.ppermute(value, axes, [(i, partner(i)) for i in range(n)])  9.37 us
    convert_element_type x3, other arithmetic, total(): return (a.astype(F32) + b.astype(F32)).astype(BF)  4.42 us
  transfers between devices with their start and end apart: 21, of which 11 were waited for; matrix products, arithmetic and copies ran while one was open for 5% of the time, Pallas kernels for 2%

profile of v10, /device:TPU:4, one launch (start us, length us, event | category | flops | bytes accessed | tf_op | source)
XLA Modules:
  0.0 173.3 jit_solution(1738834423437105035)
XLA Ops:
  0.6 0.9 fusion
  1.5 3.8 %collective-permute-start = (bf16[128,512]{1,0:T(8,128)(2,1)S(1)}, bf16[128,512]{1,0:T(8,128)(2,1)S(1)}, u32[]{:S(2)}, u32[]{:S(2)}) collective-permute-start(bf16[128,512]{1,0:T(8,128)(2,1)S(1)} %get-tuple-element.23), channel_id=1, source_target_pairs={{0,32},{32,64},{64,96},{96,128},{128,160},{160,192},{192,224},{224... | collective-permute-start | bytes 393224 | tf_op jit(solution)/shard_map/ppermute | solution.py:35
  5.4 11.1 %collective-permute-done = bf16[128,512]{1,0:T(8,128)(2,1)S(1)} collective-permute-done((bf16[128,512]{1,0:T(8,128)(2,1)S(1)}, bf16[128,512]{1,0:T(8,128)(2,1)S(1)}, u32[]{:S(2)}, u32[]{:S(2)}) %collective-permute-start) | collective-permute-done | bytes 131104 | tf_op jit(solution)/shard_map/ppermute | solution.py:35
  16.4 1.9 %collective-permute-start.2 = (bf16[128,512]{1,0:T(8,128)(2,1)S(1)}, bf16[128,512]{1,0:T(8,128)(2,1)S(1)}, u32[]{:S(2)}, u32[]{:S(2)}) collective-permute-start(bf16[128,512]{1,0:T(8,128)(2,1)S(1)} %collective-permute-done), channel_id=1, source_target_pairs={{0,32},{32,64},{64,96},{96,128},{128,160},{160,192},{192,224},{224... | collective-permute-start | bytes 393224 | tf_op jit(solution)/shard_map/ppermute | solution.py:35
  18.3 5.1 %collective-permute-start.1 = (bf16[128,512]{1,0:T(8,128)(2,1)S(1)}, bf16[128,512]{1,0:T(8,128)(2,1)S(1)}, u32[]{:S(2)}, u32[]{:S(2)}) collective-permute-start(bf16[128,512]{1,0:T(8,128)(2,1)S(1)} %get-tuple-element.23), channel_id=1, source_target_pairs={{0,480},{32,0},{64,32},{96,64},{128,96},{160,128},{192,160},{224,1... | collective-permute-start | bytes 393224 | tf_op jit(solution)/shard_map/ppermute | solution.py:35
  23.5 1.0 collective-permute-done.2
  24.5 1.9 %collective-permute-start.3 = (bf16[128,512]{1,0:T(8,128)(2,1)S(1)}, bf16[128,512]{1,0:T(8,128)(2,1)S(1)}, u32[]{:S(2)}, u32[]{:S(2)}) collective-permute-start(bf16[128,512]{1,0:T(8,128)(2,1)S(1)} %collective-permute-done.2), channel_id=1, source_target_pairs={{0,32},{32,64},{64,96},{96,128},{128,160},{160,192},{192,224},{224... | collective-permute-start | bytes 393224 | tf_op jit(solution)/shard_map/ppermute | solution.py:35
  26.4 0.0 collective-permute-done.1
  26.5 1.3 broadcast_in_dim.6
  27.7 4.5 %all-to-all-start = ((bf16[4,3,128,512]{3,2,1,0:T(8,128)(2,1)}), bf16[4,3,128,512]{3,2,1,0:T(8,128)(2,1)S(1)}, u32[]{:S(2)}, u32[]{:S(2)}) async-start(bf16[4,3,128,512]{3,2,1,0:T(8,128)(2,1)} %broadcast_in_dim.6), calls=%async_computation | async-start | bytes 3145728 | tf_op jit(solution)/shard_map/all_to_all | solution.py:24
  32.2 5.1 %collective-permute-start.8 = (bf16[128,512]{1,0:T(8,128)(2,1)S(1)}, bf16[128,512]{1,0:T(8,128)(2,1)S(1)}, u32[]{:S(2)}, u32[]{:S(2)}) collective-permute-start(bf16[128,512]{1,0:T(8,128)(2,1)S(1)} %collective-permute-done.1), channel_id=1, source_target_pairs={{0,480},{32,0},{64,32},{96,64},{128,96},{160,128},{192,160},{224,1... | collective-permute-start | bytes 393224 | tf_op jit(solution)/shard_map/ppermute | solution.py:35
  37.3 0.0 collective-permute-done.3
  37.3 1.9 %collective-permute-start.4 = (bf16[128,512]{1,0:T(8,128)(2,1)S(1)}, bf16[128,512]{1,0:T(8,128)(2,1)S(1)}, u32[]{:S(2)}, u32[]{:S(2)}) collective-permute-start(bf16[128,512]{1,0:T(8,128)(2,1)S(1)} %collective-permute-done.3), channel_id=1, source_target_pairs={{0,32},{32,64},{64,96},{96,128},{128,160},{160,192},{192,224},{224... | collective-permute-start | bytes 393224 | tf_op jit(solution)/shard_map/ppermute | solution.py:35
  39.3 6.1 %collective-permute-done.4 = bf16[128,512]{1,0:T(8,128)(2,1)S(1)} collective-permute-done((bf16[128,512]{1,0:T(8,128)(2,1)S(1)}, bf16[128,512]{1,0:T(8,128)(2,1)S(1)}, u32[]{:S(2)}, u32[]{:S(2)}) %collective-permute-start.4) | collective-permute-done | bytes 131104 | tf_op jit(solution)/shard_map/ppermute | solution.py:35
  45.4 3.9 %collective-permute-start.5 = (bf16[384,512]{1,0:T(8,128)(2,1)S(1)}, bf16[384,512]{1,0:T(8,128)(2,1)S(1)}, u32[]{:S(2)}, u32[]{:S(2)}) collective-permute-start(bf16[384,512]{1,0:T(8,128)(2,1)S(1)} %constant_dynamic-update-slice_fusion.refs_0_), channel_id=1, source_target_pairs={{0,8},{8,16},{16,24},{24,0},{1,9},{9,17},{17,25},{25,1},{2,10},{10... | collective-permute-start | bytes 1179656 | tf_op jit(solution)/shard_map/ppermute | solution.py:35
  49.4 0.0 collective-permute-done.8
  49.4 1.9 %collective-permute-start.9 = (bf16[128,512]{1,0:T(8,128)(2,1)S(1)}, bf16[128,512]{1,0:T(8,128)(2,1)S(1)}, u32[]{:S(2)}, u32[]{:S(2)}) collective-permute-start(bf16[128,512]{1,0:T(8,128)(2,1)S(1)} %collective-permute-done.8), channel_id=1, source_target_pairs={{0,480},{32,0},{64,32},{96,64},{128,96},{160,128},{192,160},{224,1... | collective-permute-start | bytes 393224 | tf_op jit(solution)/shard_map/ppermute | solution.py:35
  51.3 4.9 %collective-permute-done.9 = bf16[128,512]{1,0:T(8,128)(2,1)S(1)} collective-permute-done((bf16[128,512]{1,0:T(8,128)(2,1)S(1)}, bf16[128,512]{1,0:T(8,128)(2,1)S(1)}, u32[]{:S(2)}, u32[]{:S(2)}) %collective-permute-start.9) | collective-permute-done | bytes 131104 | tf_op jit(solution)/shard_map/ppermute | solution.py:35
  56.3 3.1 %collective-permute-start.11 = (bf16[256,512]{1,0:T(8,128)(2,1)S(1)}, bf16[256,512]{1,0:T(8,128)(2,1)}, u32[]{:S(2)}, u32[]{:S(2)}) collective-permute-start(bf16[256,512]{1,0:T(8,128)(2,1)S(1)} %constant_dynamic-update-slice_fusion.3.refs_4_), channel_id=1, source_target_pairs={{0,24},{8,0},{16,8},{24,16},{1,25},{9,1},{17,9},{25,17},{2,26},{10... | collective-permute-start | bytes 786440 | tf_op jit(solution)/shard_map/ppermute | solution.py:35
  59.4 3.9 %collective-permute-start.6 = (bf16[384,512]{1,0:T(8,128)(2,1)S(1)}, bf16[384,512]{1,0:T(8,128)(2,1)S(1)}, u32[]{:S(2)}, u32[]{:S(2)}) collective-permute-start(bf16[384,512]{1,0:T(8,128)(2,1)S(1)} %constant_dynamic-update-slice_fusion.refs_0_), channel_id=1, source_target_pairs={{0,24},{8,0},{16,8},{24,16},{1,25},{9,1},{17,9},{25,17},{2,26},{10... | collective-permute-start | bytes 1179656 | tf_op jit(solution)/shard_map/ppermute | solution.py:35
  63.3 0.0 collective-permute-done.5.refs_1_
  63.3 1.9 %collective-permute-start.7 = (bf16[384,512]{1,0:T(8,128)(2,1)S(1)}, bf16[384,512]{1,0:T(8,128)(2,1)S(1)}, u32[]{:S(2)}, u32[]{:S(2)}) collective-permute-start(bf16[384,512]{1,0:T(8,128)(2,1)S(1)} %collective-permute-done.5.refs_1_), channel_id=1, source_target_pairs={{0,8},{8,16},{16,24},{24,0},{1,9},{9,17},{17,25},{25,1},{2,10},{10... | collective-permute-start | bytes 1179656 | tf_op jit(solution)/shard_map/ppermute | solution.py:35
  65.3 2.7 %collective-permute-start.10 = (bf16[256,512]{1,0:T(8,128)(2,1)S(1)}, bf16[256,512]{1,0:T(8,128)(2,1)}, u32[]{:S(2)}, u32[]{:S(2)}) collective-permute-start(bf16[256,512]{1,0:T(8,128)(2,1)S(1)} %constant_dynamic-update-slice_fusion.3.refs_4_), channel_id=1, source_target_pairs={{0,8},{8,16},{16,24},{24,0},{1,9},{9,17},{17,25},{25,1},{2,10},{10... | collective-permute-start | bytes 786440 | tf_op jit(solution)/shard_map/ppermute | solution.py:35
  68.0 0.0 collective-permute-done.11.refs_6_
  68.0 4.3 %collective-permute-start.12 = (bf16[256,512]{1,0:T(8,128)(2,1)}, bf16[256,512]{1,0:T(8,128)(2,1)}, u32[]{:S(2)}, u32[]{:S(2)}) collective-permute-start(bf16[256,512]{1,0:T(8,128)(2,1)} %collective-permute-done.11.refs_6_), channel_id=1, source_target_pairs={{0,24},{8,0},{16,8},{24,16},{1,25},{9,1},{17,9},{25,17},{2,26},{10... | collective-permute-start | bytes 786440 | tf_op jit(solution)/shard_map/ppermute | solution.py:35
  72.3 0.0 all-to-all-done.near_ref
  72.4 0.0 copy-start
  72.4 2.7 %shard_map.59 = (f32[384,512]{1,0:T(8,128)S(1)}, f32[384,512]{1,0:T(8,128)S(1)}, bf16[384,2048]{1,0:T(8,128)(2,1)S(1)}, bf16[384,2048]{1,0:T(8,128)(2,1)S(1)}) custom-call(bf16[384,2048]{1,0:T(8,128)(2,1)} %x_hbm.1, bf16[384,2048]{1,0:T(8,128)(2,1)} %c_hbm.1, bf16[4,3,128,512]{3,2,1,0:T(8,128)(2,1)S(1)} %all-to-all-done.near_ref), custom_call_target="tpu_custom_call" | custom-call | flops 603979776 | bytes 4718592 | tf_op jit(solution)/shard_map/pallas_call | solution.py:152
  75.1 0.0 copy-done
  75.1 2.8 %collective-permute-done.10.refs_5_ = bf16[256,512]{1,0:T(8,128)(2,1)} collective-permute-done((bf16[256,512]{1,0:T(8,128)(2,1)S(1)}, bf16[256,512]{1,0:T(8,128)(2,1)}, u32[]{:S(2)}, u32[]{:S(2)}) %collective-permute-start.10) | collective-permute-done | bytes 262176 | tf_op jit(solution)/shard_map/ppermute | solution.py:35
  77.9 0.0 collective-permute-done.6.refs_2_
  77.9 0.0 collective-permute-done.12.refs_7_
  77.9 0.0 collective-permute-done.7.refs_3_
  77.9 4.4 %shard_map.60 = (bf16[384,512]{1,0:T(8,128)(2,1)}, bf16[4,4,2,64,512]{4,3,2,1,0:T(8,128)(2,1)}, bf16[1280,512]{1,0:T(8,128)(2,1)}) custom-call(bf16[384,2048]{1,0:T(8,128)(2,1)S(1)} %get-tuple-element.11.x_ref, bf16[384,2048]{1,0:T(8,128)(2,1)S(1)} %get-tuple-element.12.c_ref, f32[384,512]{1,0:T(8,128)S(1)} %get-tuple-element.13.pre_ref, ...), custom_call_target="tpu_custom_call" | custom-call | flops 1811939328 | bytes 6553600 | tf_op jit(solution)/shard_map/pallas_call | solution.py:152
  82.3 4.4 %shard_map.61 = (bf16[192,2048]{1,0:T(8,128)(2,1)}, bf16[192,2048]{1,0:T(8,128)(2,1)}) custom-call(bf16[384,512]{1,0:T(8,128)(2,1)} %get-tuple-element.15.grad_ref, bf16[4,3,128,512]{3,2,1,0:T(8,128)(2,1)} %copy-done, bf16[1280,512]{1,0:T(8,128)(2,1)} %get-tuple-element.16.up_ref), custom_call_target="tpu_custom_call" | custom-call | flops 805306368 | bytes 3276800 | tf_op jit(solution)/shard_map/pallas_call | solution.py:152
  86.8 1.9 %collective-permute-start.13 = (bf16[192,2048]{1,0:T(8,128)(2,1)}, bf16[192,2048]{1,0:T(8,128)(2,1)S(1)}, u32[]{:S(2)}, u32[]{:S(2)}) collective-permute-start(bf16[192,2048]{1,0:T(8,128)(2,1)} %get-tuple-element.18), channel_id=1, source_target_pairs={{0,1},{1,0},{2,3},{3,2},{4,5},{5,4},{6,7},{7,6},{8,9},{9,8},{10,11... | collective-permute-start | bytes 2359304 | tf_op jit(solution)/shard_map/ppermute | solution.py:40
  88.7 2.5 %collective-permute-done.13 = bf16[192,2048]{1,0:T(8,128)(2,1)S(1)} collective-permute-done((bf16[192,2048]{1,0:T(8,128)(2,1)}, bf16[192,2048]{1,0:T(8,128)(2,1)S(1)}, u32[]{:S(2)}, u32[]{:S(2)}) %collective-permute-start.13) | collective-permute-done | bytes 786464 | tf_op jit(solution)/shard_map/ppermute | solution.py:40
  91.1 1.4 add_convert_fusion.2
  92.5 0.0 copy-start.1
  92.5 3.1 %collective-permute-start.14 = (bf16[192,2048]{1,0:T(8,128)(2,1)S(1)}, bf16[192,2048]{1,0:T(8,128)(2,1)}, u32[]{:S(2)}, u32[]{:S(2)}) collective-permute-start(bf16[192,2048]{1,0:T(8,128)(2,1)S(1)} %add_convert_fusion.2), channel_id=1, source_target_pairs={{0,2},{2,0},{4,6},{6,4},{1,3},{3,1},{5,7},{7,5},{8,10},{10,8},{12,... | collective-permute-start | bytes 2359304 | tf_op jit(solution)/shard_map/ppermute | solution.py:40
  95.7 0.0 copy-done.1
  95.7 3.8 %all-to-all-start.1 = ((bf16[4,4,2,64,512]{4,3,2,1,0:T(8,128)(2,1)}), bf16[4,4,2,64,512]{4,3,2,1,0:T(8,128)(2,1)S(1)}, u32[]{:S(2)}, u32[]{:S(2)}) async-start(bf16[4,4,2,64,512]{4,3,2,1,0:T(8,128)(2,1)} %get-tuple-element.19), calls=%async_computation.1 | async-start | bytes 4194304 | tf_op jit(solution)/shard_map/all_to_all | solution.py:24
  99.5 14.6 %collective-permute-done.14 = bf16[192,2048]{1,0:T(8,128)(2,1)} collective-permute-done((bf16[192,2048]{1,0:T(8,128)(2,1)S(1)}, bf16[192,2048]{1,0:T(8,128)(2,1)}, u32[]{:S(2)}, u32[]{:S(2)}) %collective-permute-start.14) | collective-permute-done | bytes 786464 | tf_op jit(solution)/shard_map/ppermute | solution.py:40
  114.1 1.6 add_convert_fusion.1
  115.8 2.4 %collective-permute-start.15 = (bf16[192,2048]{1,0:T(8,128)(2,1)S(1)}, bf16[192,2048]{1,0:T(8,128)(2,1)}, u32[]{:S(2)}, u32[]{:S(2)}) collective-permute-start(bf16[192,2048]{1,0:T(8,128)(2,1)S(1)} %add_convert_fusion.1), channel_id=1, source_target_pairs={{0,6},{2,4},{4,2},{6,0},{1,7},{3,5},{5,3},{7,1},{8,14},{10,12},{12... | collective-permute-start | bytes 2359304 | tf_op jit(solution)/shard_map/ppermute | solution.py:40
  118.2 7.7 %all-to-all-done.1 = bf16[4,4,2,64,512]{4,3,2,1,0:T(8,128)(2,1)S(1)} async-done(((bf16[4,4,2,64,512]{4,3,2,1,0:T(8,128)(2,1)}), bf16[4,4,2,64,512]{4,3,2,1,0:T(8,128)(2,1)S(1)}, u32[]{:S(2)}, u32[]{:S(2)}) %all-to-all-start.1) | async-done | bytes 2097184 | tf_op jit(solution)/shard_map/all_to_all | solution.py:24
  125.9 1.3 reduce_sum.33
  127.2 3.5 %all-to-all-start.2 = ((bf16[4,2,64,512]{3,2,1,0:T(8,128)(2,1)}), bf16[4,2,64,512]{3,2,1,0:T(8,128)(2,1)S(1)}, u32[]{:S(2)}, u32[]{:S(2)}) async-start(bf16[4,2,64,512]{3,2,1,0:T(8,128)(2,1)} %reduce_sum.33), calls=%async_computation.2 | async-start | bytes 1048576 | tf_op jit(solution)/shard_map/all_to_all | solution.py:24
  130.6 5.9 %collective-permute-done.15 = bf16[192,2048]{1,0:T(8,128)(2,1)} collective-permute-done((bf16[192,2048]{1,0:T(8,128)(2,1)S(1)}, bf16[192,2048]{1,0:T(8,128)(2,1)}, u32[]{:S(2)}, u32[]{:S(2)}) %collective-permute-start.15) | collective-permute-done | bytes 786464 | tf_op jit(solution)/shard_map/ppermute | solution.py:40
  136.5 1.4 add_convert_fusion
  137.9 1.9 %collective-permute-start.16 = (bf16[192,2048]{1,0:T(8,128)(2,1)S(1)}, bf16[192,2048]{1,0:T(8,128)(2,1)S(1)}, u32[]{:S(2)}, u32[]{:S(2)}) collective-permute-start(bf16[192,2048]{1,0:T(8,128)(2,1)S(1)} %add_convert_fusion), channel_id=1, source_target_pairs={{0,1},{1,0},{2,3},{3,2},{4,5},{5,4},{6,7},{7,6},{8,9},{9,8},{10,11... | collective-permute-start | bytes 2359304 | tf_op jit(solution)/shard_map/ppermute | solution.py:40
  139.8 4.4 %all-to-all-done.2 = bf16[4,2,64,512]{3,2,1,0:T(8,128)(2,1)S(1)} async-done(((bf16[4,2,64,512]{3,2,1,0:T(8,128)(2,1)}), bf16[4,2,64,512]{3,2,1,0:T(8,128)(2,1)S(1)}, u32[]{:S(2)}, u32[]{:S(2)}) %all-to-all-start.2) | async-done | bytes 524320 | tf_op jit(solution)/shard_map/all_to_all | solution.py:24
  144.3 0.1 reduce_sum.34
  144.4 0.7 broadcast_in_dim.7
  145.1 9.0 %all-to-all-start.3 = ((bf16[4,64,512]{2,1,0:T(8,128)(2,1)}), bf16[4,64,512]{2,1,0:T(8,128)(2,1)S(1)}, u32[]{:S(2)}, u32[]{:S(2)}) async-start(bf16[4,64,512]{2,1,0:T(8,128)(2,1)} %bitcast.4), calls=%async_computation.3 | async-start | bytes 524288 | tf_op jit(solution)/shard_map/all_to_all | solution.py:24
  154.1 0.0 collective-permute-done.16
  154.1 0.1 broadcast_select_fusion.1
  154.2 1.2 pad_maximum_fusion
  155.5 17.1 %all-to-all-done.3 = bf16[4,64,512]{2,1,0:T(8,128)(2,1)S(1)} async-done(((bf16[4,64,512]{2,1,0:T(8,128)(2,1)}), bf16[4,64,512]{2,1,0:T(8,128)(2,1)S(1)}, u32[]{:S(2)}, u32[]{:S(2)}) %all-to-all-start.3) | async-done | bytes 262176 | tf_op jit(solution)/shard_map/all_to_all | solution.py:24
  172.6 0.7 convert_reduce_fusion
  (6 shorter events, 0.1 us)
Async XLA Ops:
  1.5 14.9 %collective-permute-start = (bf16[128,512]{1,0:T(8,128)(2,1)S(1)}, bf16[128,512]{1,0:T(8,128)(2,1)S(1)}, u32[]{:S(2)}, u32[]{:S(2)}) collective-permute-start(bf16[128,512]{1,0:T(8,128)(2,1)S(1)} %get-tuple-element.23), channel_id=1, source_target_pairs={{0,32},{32,64},{64,96},{96,128},{128,160},{160,192},{192,224},{224... | collective-permute-start | bytes 393224 | tf_op jit(solution)/shard_map/ppermute | solution.py:35
  16.4 8.1 %collective-permute-start.2 = (bf16[128,512]{1,0:T(8,128)(2,1)S(1)}, bf16[128,512]{1,0:T(8,128)(2,1)S(1)}, u32[]{:S(2)}, u32[]{:S(2)}) collective-permute-start(bf16[128,512]{1,0:T(8,128)(2,1)S(1)} %collective-permute-done), channel_id=1, source_target_pairs={{0,32},{32,64},{64,96},{96,128},{128,160},{160,192},{192,224},{224... | collective-permute-start | bytes 393224 | tf_op jit(solution)/shard_map/ppermute | solution.py:35
  18.3 8.1 %collective-permute-start.1 = (bf16[128,512]{1,0:T(8,128)(2,1)S(1)}, bf16[128,512]{1,0:T(8,128)(2,1)S(1)}, u32[]{:S(2)}, u32[]{:S(2)}) collective-permute-start(bf16[128,512]{1,0:T(8,128)(2,1)S(1)} %get-tuple-element.23), channel_id=1, source_target_pairs={{0,480},{32,0},{64,32},{96,64},{128,96},{160,128},{192,160},{224,1... | collective-permute-start | bytes 393224 | tf_op jit(solution)/shard_map/ppermute | solution.py:35
  24.5 12.9 %collective-permute-start.3 = (bf16[128,512]{1,0:T(8,128)(2,1)S(1)}, bf16[128,512]{1,0:T(8,128)(2,1)S(1)}, u32[]{:S(2)}, u32[]{:S(2)}) collective-permute-start(bf16[128,512]{1,0:T(8,128)(2,1)S(1)} %collective-permute-done.2), channel_id=1, source_target_pairs={{0,32},{32,64},{64,96},{96,128},{128,160},{160,192},{192,224},{224... | collective-permute-start | bytes 393224 | tf_op jit(solution)/shard_map/ppermute | solution.py:35
  27.7 44.6 %all-to-all-start = ((bf16[4,3,128,512]{3,2,1,0:T(8,128)(2,1)}), bf16[4,3,128,512]{3,2,1,0:T(8,128)(2,1)S(1)}, u32[]{:S(2)}, u32[]{:S(2)}) async-start(bf16[4,3,128,512]{3,2,1,0:T(8,128)(2,1)} %broadcast_in_dim.6), calls=%async_computation | async-start | bytes 3145728 | tf_op jit(solution)/shard_map/all_to_all | solution.py:24
  32.2 17.2 %collective-permute-start.8 = (bf16[128,512]{1,0:T(8,128)(2,1)S(1)}, bf16[128,512]{1,0:T(8,128)(2,1)S(1)}, u32[]{:S(2)}, u32[]{:S(2)}) collective-permute-start(bf16[128,512]{1,0:T(8,128)(2,1)S(1)} %collective-permute-done.1), channel_id=1, source_target_pairs={{0,480},{32,0},{64,32},{96,64},{128,96},{160,128},{192,160},{224,1... | collective-permute-start | bytes 393224 | tf_op jit(solution)/shard_map/ppermute | solution.py:35
  37.3 8.1 %collective-permute-start.4 = (bf16[128,512]{1,0:T(8,128)(2,1)S(1)}, bf16[128,512]{1,0:T(8,128)(2,1)S(1)}, u32[]{:S(2)}, u32[]{:S(2)}) collective-permute-start(bf16[128,512]{1,0:T(8,128)(2,1)S(1)} %collective-permute-done.3), channel_id=1, source_target_pairs={{0,32},{32,64},{64,96},{96,128},{128,160},{160,192},{192,224},{224... | collective-permute-start | bytes 393224 | tf_op jit(solution)/shard_map/ppermute | solution.py:35
  45.4 17.9 %collective-permute-start.5 = (bf16[384,512]{1,0:T(8,128)(2,1)S(1)}, bf16[384,512]{1,0:T(8,128)(2,1)S(1)}, u32[]{:S(2)}, u32[]{:S(2)}) collective-permute-start(bf16[384,512]{1,0:T(8,128)(2,1)S(1)} %constant_dynamic-update-slice_fusion.refs_0_), channel_id=1, source_target_pairs={{0,8},{8,16},{16,24},{24,0},{1,9},{9,17},{17,25},{25,1},{2,10},{10... | collective-permute-start | bytes 1179656 | tf_op jit(solution)/shard_map/ppermute | solution.py:35
  49.4 6.9 %collective-permute-start.9 = (bf16[128,512]{1,0:T(8,128)(2,1)S(1)}, bf16[128,512]{1,0:T(8,128)(2,1)S(1)}, u32[]{:S(2)}, u32[]{:S(2)}) collective-permute-start(bf16[128,512]{1,0:T(8,128)(2,1)S(1)} %collective-permute-done.8), channel_id=1, source_target_pairs={{0,480},{32,0},{64,32},{96,64},{128,96},{160,128},{192,160},{224,1... | collective-permute-start | bytes 393224 | tf_op jit(solution)/shard_map/ppermute | solution.py:35
  56.3 11.7 %collective-permute-start.11 = (bf16[256,512]{1,0:T(8,128)(2,1)S(1)}, bf16[256,512]{1,0:T(8,128)(2,1)}, u32[]{:S(2)}, u32[]{:S(2)}) collective-permute-start(bf16[256,512]{1,0:T(8,128)(2,1)S(1)} %constant_dynamic-update-slice_fusion.3.refs_4_), channel_id=1, source_target_pairs={{0,24},{8,0},{16,8},{24,16},{1,25},{9,1},{17,9},{25,17},{2,26},{10... | collective-permute-start | bytes 786440 | tf_op jit(solution)/shard_map/ppermute | solution.py:35
  59.4 18.5 %collective-permute-start.6 = (bf16[384,512]{1,0:T(8,128)(2,1)S(1)}, bf16[384,512]{1,0:T(8,128)(2,1)S(1)}, u32[]{:S(2)}, u32[]{:S(2)}) collective-permute-start(bf16[384,512]{1,0:T(8,128)(2,1)S(1)} %constant_dynamic-update-slice_fusion.refs_0_), channel_id=1, source_target_pairs={{0,24},{8,0},{16,8},{24,16},{1,25},{9,1},{17,9},{25,17},{2,26},{10... | collective-permute-start | bytes 1179656 | tf_op jit(solution)/shard_map/ppermute | solution.py:35
  63.3 14.5 %collective-permute-start.7 = (bf16[384,512]{1,0:T(8,128)(2,1)S(1)}, bf16[384,512]{1,0:T(8,128)(2,1)S(1)}, u32[]{:S(2)}, u32[]{:S(2)}) collective-permute-start(bf16[384,512]{1,0:T(8,128)(2,1)S(1)} %collective-permute-done.5.refs_1_), channel_id=1, source_target_pairs={{0,8},{8,16},{16,24},{24,0},{1,9},{9,17},{17,25},{25,1},{2,10},{10... | collective-permute-start | bytes 1179656 | tf_op jit(solution)/shard_map/ppermute | solution.py:35
  65.3 12.6 %collective-permute-start.10 = (bf16[256,512]{1,0:T(8,128)(2,1)S(1)}, bf16[256,512]{1,0:T(8,128)(2,1)}, u32[]{:S(2)}, u32[]{:S(2)}) collective-permute-start(bf16[256,512]{1,0:T(8,128)(2,1)S(1)} %constant_dynamic-update-slice_fusion.3.refs_4_), channel_id=1, source_target_pairs={{0,8},{8,16},{16,24},{24,0},{1,9},{9,17},{17,25},{25,1},{2,10},{10... | collective-permute-start | bytes 786440 | tf_op jit(solution)/shard_map/ppermute | solution.py:35
  68.0 9.9 %collective-permute-start.12 = (bf16[256,512]{1,0:T(8,128)(2,1)}, bf16[256,512]{1,0:T(8,128)(2,1)}, u32[]{:S(2)}, u32[]{:S(2)}) collective-permute-start(bf16[256,512]{1,0:T(8,128)(2,1)} %collective-permute-done.11.refs_6_), channel_id=1, source_target_pairs={{0,24},{8,0},{16,8},{24,16},{1,25},{9,1},{17,9},{25,17},{2,26},{10... | collective-permute-start | bytes 786440 | tf_op jit(solution)/shard_map/ppermute | solution.py:35
  72.4 2.7 %copy-start = (bf16[4,3,128,512]{3,2,1,0:T(8,128)(2,1)}, bf16[4,3,128,512]{3,2,1,0:T(8,128)(2,1)S(1)}, u32[]{:S(2)}) copy-start(bf16[4,3,128,512]{3,2,1,0:T(8,128)(2,1)S(1)} %all-to-all-done.near_ref) | copy-start | bytes 4718596
  86.8 4.4 %collective-permute-start.13 = (bf16[192,2048]{1,0:T(8,128)(2,1)}, bf16[192,2048]{1,0:T(8,128)(2,1)S(1)}, u32[]{:S(2)}, u32[]{:S(2)}) collective-permute-start(bf16[192,2048]{1,0:T(8,128)(2,1)} %get-tuple-element.18), channel_id=1, source_target_pairs={{0,1},{1,0},{2,3},{3,2},{4,5},{5,4},{6,7},{7,6},{8,9},{9,8},{10,11... | collective-permute-start | bytes 2359304 | tf_op jit(solution)/shard_map/ppermute | solution.py:40
  92.5 3.1 %copy-start.1 = (bf16[192,2048]{1,0:T(8,128)(2,1)}, bf16[192,2048]{1,0:T(8,128)(2,1)S(1)}, u32[]{:S(2)}) copy-start(bf16[192,2048]{1,0:T(8,128)(2,1)S(1)} %add_convert_fusion.2) | copy-start | bytes 2359300
  92.5 21.6 %collective-permute-start.14 = (bf16[192,2048]{1,0:T(8,128)(2,1)S(1)}, bf16[192,2048]{1,0:T(8,128)(2,1)}, u32[]{:S(2)}, u32[]{:S(2)}) collective-permute-start(bf16[192,2048]{1,0:T(8,128)(2,1)S(1)} %add_convert_fusion.2), channel_id=1, source_target_pairs={{0,2},{2,0},{4,6},{6,4},{1,3},{3,1},{5,7},{7,5},{8,10},{10,8},{12,... | collective-permute-start | bytes 2359304 | tf_op jit(solution)/shard_map/ppermute | solution.py:40
  95.7 30.2 %all-to-all-start.1 = ((bf16[4,4,2,64,512]{4,3,2,1,0:T(8,128)(2,1)}), bf16[4,4,2,64,512]{4,3,2,1,0:T(8,128)(2,1)S(1)}, u32[]{:S(2)}, u32[]{:S(2)}) async-start(bf16[4,4,2,64,512]{4,3,2,1,0:T(8,128)(2,1)} %get-tuple-element.19), calls=%async_computation.1 | async-start | bytes 4194304 | tf_op jit(solution)/shard_map/all_to_all | solution.py:24
  115.8 20.7 %collective-permute-start.15 = (bf16[192,2048]{1,0:T(8,128)(2,1)S(1)}, bf16[192,2048]{1,0:T(8,128)(2,1)}, u32[]{:S(2)}, u32[]{:S(2)}) collective-permute-start(bf16[192,2048]{1,0:T(8,128)(2,1)S(1)} %add_convert_fusion.1), channel_id=1, source_target_pairs={{0,6},{2,4},{4,2},{6,0},{1,7},{3,5},{5,3},{7,1},{8,14},{10,12},{12... | collective-permute-start | bytes 2359304 | tf_op jit(solution)/shard_map/ppermute | solution.py:40
  127.2 17.1 %all-to-all-start.2 = ((bf16[4,2,64,512]{3,2,1,0:T(8,128)(2,1)}), bf16[4,2,64,512]{3,2,1,0:T(8,128)(2,1)S(1)}, u32[]{:S(2)}, u32[]{:S(2)}) async-start(bf16[4,2,64,512]{3,2,1,0:T(8,128)(2,1)} %reduce_sum.33), calls=%async_computation.2 | async-start | bytes 1048576 | tf_op jit(solution)/shard_map/all_to_all | solution.py:24
  137.9 16.2 %collective-permute-start.16 = (bf16[192,2048]{1,0:T(8,128)(2,1)S(1)}, bf16[192,2048]{1,0:T(8,128)(2,1)S(1)}, u32[]{:S(2)}, u32[]{:S(2)}) collective-permute-start(bf16[192,2048]{1,0:T(8,128)(2,1)S(1)} %add_convert_fusion), channel_id=1, source_target_pairs={{0,1},{1,0},{2,3},{3,2},{4,5},{5,4},{6,7},{7,6},{8,9},{9,8},{10,11... | collective-permute-start | bytes 2359304 | tf_op jit(solution)/shard_map/ppermute | solution.py:40
  145.1 27.5 %all-to-all-start.3 = ((bf16[4,64,512]{2,1,0:T(8,128)(2,1)}), bf16[4,64,512]{2,1,0:T(8,128)(2,1)S(1)}, u32[]{:S(2)}, u32[]{:S(2)}) async-start(bf16[4,64,512]{2,1,0:T(8,128)(2,1)} %bitcast.4), calls=%async_computation.3 | async-start | bytes 524288 | tf_op jit(solution)/shard_map/all_to_all | solution.py:24
